TPU v7x, 512 devices: a whole 4x8x8 slice. The times are simulated.
512 devices in a mesh: sp: 32 (over z, x), tp: 16 (over y, core).
Axes of the slice: x: 4, y: 8, z: 8, core: 2. Of those that a mesh axis runs over, the one named last changes fastest.
Arguments:
- moe_in: bfloat16 [6144, 2048], P('sp', 'tp'), may hold values from -6 to 6
- cotangent: bfloat16 [6144, 2048], P('sp', 'tp'), may hold values from -6 to 6
- routes: int32 [6144, 2], P('sp'), may hold values from 0 to 31, all different within a row; in each aligned block of 192 rows (0 to 191, 192 to 383, ...) at most 15 rows name the same one
- route_weight: float32 [6144, 2], P('sp'), may hold values from 0.2 to 1
- w_gate: bfloat16 [32, 3584, 2048], P('sp', 'tp'), may hold values from -0.125 to 0.125
- w_up: bfloat16 [32, 3584, 2048], P('sp', 'tp'), may hold values from -0.125 to 0.125
- w_down: bfloat16 [32, 3584, 2048], P('sp', 'tp'), may hold values from -0.09375 to 0.09375
- conv_pre: bfloat16 [6144, 2048], P('sp', 'tp'), may hold values from -6 to 6
- norm_mean: float32 [6144], P('sp'), may hold values from -3 to 3
- norm_rstd: float32 [6144], P('sp'), may hold values from 0.5 to 2
- ln_gain: float32 [2048], P('tp'), may hold values from 0.1 to 1.9
- ln_shift: float32 [2048], P('tp'), may hold values from -3 to 3
- taps: float32 [31, 2048], P(None, 'tp'), may hold values from -1 to 1
- w_proj: bfloat16 [2048, 2048], P('sp', 'tp'), may hold values from -0.125 to 0.125
Outputs:
- grad_up: bfloat16 [32, 3584, 2048], P('sp', 'tp')
- grad_down: bfloat16 [32, 3584, 2048], P('sp', 'tp')
- grad_stream: bfloat16 [6144, 2048], P('sp', 'tp')
- grad_proj: float32 [2048, 2048], P('sp', 'tp')
- grad_conv: bfloat16 [6144, 2048], P('sp', 'tp')
Inputs may be any that keep to these rules, and one draw needn't show every extreme that they name: `routes`: each token names 2 different experts. Among the tokens of one index of sp no expert is named more than 15 times, a bound that some block reaches.
All inputs are finite; a program needn't handle non-finite values.
Results may differ from a plain program's by a relative error of at most 0.02.
Values may be sent and summed in bfloat16 or wider, within the bound.
No kernel may reach another device: no remote copies, remote signals or barrier semaphores. Data moves between devices by JAX's collectives and lax.ppermute only.
A program may use at most 64 MiB of HBM per device.

v0:
```python
import functools
import jax
import jax.numpy as jnp
from jax import lax
from jax.experimental import pallas as pl
from jax.experimental.pallas import tpu as pltpu
from jax.sharding import PartitionSpec as P


BF16 = jnp.bfloat16
F32 = jnp.float32


def dot(a, b, a_dim, b_dim):
    return lax.dot_general(a, b, (((a_dim,), (b_dim,)), ((), ())), preferred_element_type=F32)


def silu_slope(pre_value, sigmoid_value):
    return sigmoid_value * (1.0 + pre_value * (1.0 - sigmoid_value))


def whole(count, space=pltpu.VMEM):
    return [pl.BlockSpec(memory_space=space)] * count


def send_body(routes, weights, rows, cotangent, sent, place_out, *, experts, slots):
    top, tokens = routes.shape
    expert = lax.broadcasted_iota(jnp.int32, (experts, tokens), 0)
    named = [(expert == routes[k : k + 1, :]).astype(F32) for k in range(top)]
    before = lax.broadcasted_iota(jnp.int32, (tokens, tokens), 0) < lax.broadcasted_iota(
        jnp.int32, (tokens, tokens), 1
    )
    both = functools.reduce(jnp.add, named)
    earlier = dot(both.astype(BF16), before.astype(F32).astype(BF16), 1, 0)
    position = lax.broadcasted_iota(jnp.int32, (experts * slots, tokens), 0)
    place = jnp.zeros((experts * slots, tokens), F32)
    weight = jnp.zeros((experts * slots, 1), F32)
    for k in range(top):
        slot = jnp.sum(earlier * named[k], axis=0, keepdims=True).astype(jnp.int32)
        hit = (position == routes[k : k + 1, :] * slots + slot).astype(F32)
        place = place + hit
        weight = weight + jnp.sum(hit * weights[k : k + 1, :], axis=1, keepdims=True)
    place = place.astype(BF16)
    place_out[...] = place
    channels = rows.shape[1]
    sent[:, :slots, :] = dot(place, rows[...], 1, 0).astype(BF16).reshape(experts, slots, channels)
    routed = (weight * dot(place, cotangent[...], 1, 0)).astype(BF16)
    sent[:, slots:, :] = routed.reshape(experts, slots, channels)


def send_rows(routes, weights, rows, cotangent, experts, slots):
    tokens, channels = rows.shape
    return pl.pallas_call(
        functools.partial(send_body, experts=experts, slots=slots),
        in_specs=whole(4),
        out_specs=whole(2),
        out_shape=(
            jax.ShapeDtypeStruct((experts, 2 * slots, channels), BF16),
            jax.ShapeDtypeStruct((experts * slots, tokens), BF16),
        ),
        name="send_rows",
    )(routes, weights, rows, cotangent)


def block_of(me, steps, core, blocks):
    chips = blocks // 2
    mine = lax.rem(me, 2)
    sign = 1 - 2 * mine
    chip = lax.rem(me // 2 + sign * steps + chips, chips)
    return 2 * chip + (mine if core == 0 else 1 - mine)


def places(blocks):
    chips = blocks // 2
    ahead = [(k, core) for k in range(1, chips // 2) for core in (1, 0)]
    behind = [(-k, core) for k in range(1, chips // 2) for core in (0, 1)]
    kept = [(0, 0), (chips // 2, 0), *ahead]
    given = [(0, 1), (chips // 2, 1), *behind]
    return kept, given


def expert_body(me, *refs, blocks, slots):
    chips = blocks // 2
    middle = chips // 2
    parts = refs[: 2 * middle + 2]
    gate_weight, up_weight, down_weight = refs[len(parts) : len(parts) + 3]
    rows, routed, hidden_out, up_out, kept, given = refs[len(parts) + 3 :]
    width = parts[0].shape[-1]
    count = parts[0].shape[-3] * slots

    def columns(place):
        at = block_of(me[0], *place, blocks) * width
        return pl.ds(pl.multiple_of(at, width), width)

    def put(place, part):
        cols = columns(place)
        rows[:, cols] = part[:, :slots, :].reshape(count, width)
        routed[:, cols] = part[:, slots:, :].reshape(count, width)

    for core in (0, 1):
        put((0, core), parts[core])
        put((middle, core), parts[2 + core])
        for k in range(1, middle):
            pair = parts[2 + 2 * k + core]
            for i in (0, 1):
                put((k if core else -k, i ^ core), pair[i])
    gate_pre = dot(rows[...], gate_weight[0], 1, 1)
    up_pre = dot(rows[...], up_weight[0], 1, 1)
    hidden_grad = dot(routed[...], down_weight[0], 1, 1)
    gate_sigmoid = jax.nn.sigmoid(gate_pre)
    gate_active = gate_pre * gate_sigmoid
    hidden_out[...] = (gate_active * up_pre).astype(BF16)
    gate_grad = (hidden_grad * up_pre * silu_slope(gate_pre, gate_sigmoid)).astype(BF16)
    up_grad = (hidden_grad * gate_active).astype(BF16)
    up_out[...] = up_grad
    for out, order in zip((kept, given), places(blocks)):
        for j in range(0, chips, 2):
            gate_cols, up_cols = (
                jnp.concatenate([weight[0, :, columns(order[j + i])] for i in (0, 1)], axis=1)
                for weight in (gate_weight, up_weight)
            )
            both = dot(gate_grad, gate_cols, 1, 0) + dot(up_grad, up_cols, 1, 0)
            for i in (0, 1):
                out[j + i] = both[:, i * width : (i + 1) * width].astype(BF16)


def expert_backward(me, parts, gate_weight, up_weight, down_weight, slots, blocks):
    experts, _, width = parts[0].shape
    count = experts * slots
    _, hidden, channels = gate_weight.shape
    work = 2 * count * hidden * channels
    return pl.pallas_call(
        functools.partial(expert_body, blocks=blocks, slots=slots),
        in_specs=whole(1, pltpu.SMEM) + whole(len(parts) + 3),
        out_specs=whole(6),
        out_shape=(
            jax.ShapeDtypeStruct((count, channels), BF16),
            jax.ShapeDtypeStruct((count, channels), BF16),
            jax.ShapeDtypeStruct((count, hidden), BF16),
            jax.ShapeDtypeStruct((count, hidden), BF16),
            jax.ShapeDtypeStruct((blocks // 2, count, width), BF16),
            jax.ShapeDtypeStruct((blocks // 2, count, width), BF16),
        ),
        cost_estimate=pl.CostEstimate(
            flops=5 * work, transcendentals=count * hidden, bytes_accessed=12 * 1024 * 1024
        ),
        name="expert_backward",
    )(me, *parts, gate_weight, up_weight, down_weight)


def passed_on(value):
    count = lax.axis_size("tp")
    return lax.ppermute(
        value, "tp", [(t, (t + (2 if t % 2 == 0 else count - 2)) % count) for t in range(count)]
    )


def swapped(value, hop):
    count = lax.axis_size("tp")
    return lax.ppermute(value, "tp", [(t, t ^ hop) for t in range(count)])


def to_other_core(value):
    return swapped(value, 1)


def all_blocks(own):
    middle = lax.axis_size("tp") // 4
    other = to_other_core(own)
    pair = jnp.stack([own, other])
    pairs = []
    for _ in range(1, middle):
        pair = passed_on(pair)
        pairs.append((pair, to_other_core(pair)))
    last = passed_on(pair[0])
    shared = to_other_core(last)
    return [own, other, last, shared, *[p for both in pairs for p in both]]


def added_up(kept, given):
    middle = kept.shape[0] // 2
    other = to_other_core(given)

    def pair(k):
        at = slice(2 * k, 2 * k + 2)
        return kept[at].astype(F32) + other[at].astype(F32)

    ends = pair(0)
    arrived = passed_on(ends[1].astype(BF16)).astype(F32)
    for k in range(middle - 1, 0, -1):
        value = pair(k)
        if k == middle - 1:
            value = value + jnp.stack([jnp.zeros_like(arrived), arrived])
        else:
            value = value + arrived
        arrived = passed_on(value.astype(BF16)).astype(F32)
    mine = ends[0] + arrived[1]
    return (mine + to_other_core(arrived[0].astype(BF16)).astype(F32)).astype(BF16)


def sent_to_all(value, axis):
    copies = jnp.broadcast_to(value, (lax.axis_size(axis), *value.shape))
    return lax.all_to_all(copies, axis, split_axis=0, concat_axis=0, tiled=True)


def steps(
    moe_in,
    cotangent,
    routes,
    route_weight,
    w_gate,
    w_up,
    w_down,
    conv_pre,
    norm_mean,
    norm_rstd,
    ln_gain,
    ln_shift,
    taps,
    w_proj,
):
    devices = lax.axis_size("sp")
    blocks = lax.axis_size("tp")
    local_tokens = routes.shape[0]
    channels = moe_in.shape[1]
    capacity = 5 * local_tokens // (2 * devices)
    slots = capacity + 1
    me = lax.axis_index("tp").astype(jnp.int32).reshape(1)
    sent, place = send_rows(routes.T, route_weight.T, moe_in, cotangent, devices, slots)
    own = lax.all_to_all(sent, "sp", split_axis=0, concat_axis=0, tiled=True)
    proj = sent_to_all(w_proj, "sp").reshape(-1, channels)
    parts = all_blocks(own)
    rows, routed, hidden, up_grad, kept, given = expert_backward(
        me, parts, w_gate, w_up, w_down, slots, blocks
    )
    shared = added_up(kept, given)
    shared = shared.reshape(devices, slots, channels)
    returned = lax.all_to_all(shared, "sp", split_axis=0, concat_axis=0, tiled=True)
    grad_up = dot(up_grad, rows, 0, 0).astype(BF16)[None]
    grad_down = dot(hidden, routed, 0, 0).astype(BF16)[None]
    grad_stream = (
        cotangent.astype(F32) + dot(place, returned.reshape(devices * slots, channels), 0, 0)
    ).astype(BF16)
    columns = lax.all_gather(grad_stream, "tp", axis=1, tiled=True)
    normed = (conv_pre.astype(F32) - norm_mean[:, None]) * norm_rstd[:, None]
    pre_act = normed * ln_gain[None, :] + ln_shift[None, :]
    act_sigmoid = jax.nn.sigmoid(pre_act)
    activated = (pre_act * act_sigmoid).astype(BF16)
    proj_part = dot(columns, activated, 0, 0).astype(BF16).reshape(devices, -1, channels)
    proj_parts = lax.all_to_all(proj_part, "sp", split_axis=0, concat_axis=0, tiled=True)
    act_grad = dot(columns, proj, 1, 0)
    normed_grad = act_grad * silu_slope(pre_act, act_sigmoid) * ln_gain[None, :]
    sums = jnp.concatenate([jnp.sum(normed_grad, axis=1), jnp.sum(normed_grad * normed, axis=1)])
    hop = 1
    while hop < blocks:
        sums = sums + swapped(sums, hop)
        hop *= 2
    first_sum, second_sum = (sums[:local_tokens], sums[local_tokens:])
    width = channels * blocks
    conv_grad = norm_rstd[:, None] * (
        normed_grad - first_sum[:, None] / width - normed * (second_sum[:, None] / width)
    )
    lag_count = taps.shape[0]
    rim_rows = lax.ppermute(
        conv_grad[: lag_count - 1], "sp", [(source, source - 1) for source in range(1, devices)]
    )
    extended = jnp.concatenate([conv_grad, rim_rows], axis=0)
    grad_conv = jnp.zeros((local_tokens, channels), F32)
    for lag in range(lag_count):
        grad_conv = grad_conv + taps[lag][None, :] * extended[lag : lag + local_tokens]
    grad_proj = jnp.sum(proj_parts.astype(F32), axis=0)
    return (grad_up, grad_down, grad_stream, grad_proj, grad_conv.astype(BF16))


def solution(mesh):
    placed = (
        P("sp", "tp"),
        P("sp", "tp"),
        P("sp", None),
        P("sp", None),
        P("sp", "tp", None),
        P("sp", "tp", None),
        P("sp", "tp", None),
        P("sp", "tp"),
        P("sp"),
        P("sp"),
        P("tp"),
        P("tp"),
        P(None, "tp"),
        P("sp", "tp"),
    )
    return jax.shard_map(
        steps,
        mesh=mesh,
        in_specs=placed,
        out_specs=(
            P("sp", "tp", None),
            P("sp", "tp", None),
            P("sp", "tp"),
            P("sp", "tp"),
            P("sp", "tp"),
        ),
        check_vma=False,
    )
```

profile of v0, /device:TPU:14, one launch (start us, length us, event | category | flops | bytes accessed | tf_op | source)
XLA Modules:
  0.0 220.8 jit_solution(5916301699835086750)
XLA Ops:
  0.6 2.1 send_rows.1
  2.7 24.6 %all_to_all.20.refs_0_ = bf16[32,32,128]{2,1,0:T(8,128)(2,1)S(1)} all-to-all(bf16[32,32,128]{2,1,0:T(8,128)(2,1)} %get-tuple-element.13), channel_id=1, replica_groups=mesh['sp'=32,'tp'=16] {'sp'}, dimensions={0} | all-to-all | bytes 524288 | tf_op jit(solution)/shard_map/all_to_all | solution.py:230
  27.4 1.9 collective-permute-start
  29.3 1.5 collective-permute-done.refs_1_
  30.8 3.5 %collective-permute-start.1 = (bf16[2,32,32,128]{3,2,1,0:T(8,128)(2,1)S(1)}, bf16[2,32,32,128]{3,2,1,0:T(8,128)(2,1)S(1)}, u32[]{:S(2)}, u32[]{:S(2)}) collective-permute-start(bf16[2,32,32,128]{3,2,1,0:T(8,128)(2,1)S(1)} %pad_maximum_fusion), channel_id=1, source_target_pairs={{0,2},{1,15},{2,4},{3,1},{4,6},{5,3},{6,8},{7,5},{8,10},{9,7},{10,... | collective-permute-start | bytes 1572872 | tf_op jit(solution)/shard_map/ppermute | solution.py:153
  34.3 7.6 %collective-permute-done.1.refs_4_ = bf16[2,32,32,128]{3,2,1,0:T(8,128)(2,1)S(1)} collective-permute-done((bf16[2,32,32,128]{3,2,1,0:T(8,128)(2,1)S(1)}, bf16[2,32,32,128]{3,2,1,0:T(8,128)(2,1)S(1)}, u32[]{:S(2)}, u32[]{:S(2)}) %collective-permute-start.1) | collective-permute-done | bytes 524320 | tf_op jit(solution)/shard_map/ppermute | solution.py:153
  41.9 3.5 %collective-permute-start.2 = (bf16[2,32,32,128]{3,2,1,0:T(8,128)(2,1)S(1)}, bf16[2,32,32,128]{3,2,1,0:T(8,128)(2,1)S(1)}, u32[]{:S(2)}, u32[]{:S(2)}) collective-permute-start(bf16[2,32,32,128]{3,2,1,0:T(8,128)(2,1)S(1)} %collective-permute-done.1.refs_4_), channel_id=1, source_target_pairs={{0,2},{1,15},{2,4},{3,1},{4,6},{5,3},{6,8},{7,5},{8,10},{9,7},{10,... | collective-permute-start | bytes 1572872 | tf_op jit(solution)/shard_map/ppermute | solution.py:153
  45.4 7.6 %collective-permute-done.2.refs_6_ = bf16[2,32,32,128]{3,2,1,0:T(8,128)(2,1)S(1)} collective-permute-done((bf16[2,32,32,128]{3,2,1,0:T(8,128)(2,1)S(1)}, bf16[2,32,32,128]{3,2,1,0:T(8,128)(2,1)S(1)}, u32[]{:S(2)}, u32[]{:S(2)}) %collective-permute-start.2) | collective-permute-done | bytes 524320 | tf_op jit(solution)/shard_map/ppermute | solution.py:153
  53.0 3.5 %collective-permute-start.3 = (bf16[2,32,32,128]{3,2,1,0:T(8,128)(2,1)S(1)}, bf16[2,32,32,128]{3,2,1,0:T(8,128)(2,1)S(1)}, u32[]{:S(2)}, u32[]{:S(2)}) collective-permute-start(bf16[2,32,32,128]{3,2,1,0:T(8,128)(2,1)S(1)} %collective-permute-done.2.refs_6_), channel_id=1, source_target_pairs={{0,2},{1,15},{2,4},{3,1},{4,6},{5,3},{6,8},{7,5},{8,10},{9,7},{10,... | collective-permute-start | bytes 1572872 | tf_op jit(solution)/shard_map/ppermute | solution.py:153
  56.5 1.9 collective-permute-start.6
  58.4 2.4 %collective-permute-start.7 = (bf16[2,32,32,128]{3,2,1,0:T(8,128)(2,1)S(1)}, bf16[2,32,32,128]{3,2,1,0:T(8,128)(2,1)S(1)}, u32[]{:S(2)}, u32[]{:S(2)}) collective-permute-start(bf16[2,32,32,128]{3,2,1,0:T(8,128)(2,1)S(1)} %collective-permute-done.2.refs_6_), channel_id=1, source_target_pairs={{0,1},{1,0},{2,3},{3,2},{4,5},{5,4},{6,7},{7,6},{8,9},{9,8},{10,11... | collective-permute-start | bytes 1572872 | tf_op jit(solution)/shard_map/ppermute | solution.py:160
  60.8 4.3 %collective-permute-done.3.refs_8_ = bf16[2,32,32,128]{3,2,1,0:T(8,128)(2,1)S(1)} collective-permute-done((bf16[2,32,32,128]{3,2,1,0:T(8,128)(2,1)S(1)}, bf16[2,32,32,128]{3,2,1,0:T(8,128)(2,1)S(1)}, u32[]{:S(2)}, u32[]{:S(2)}) %collective-permute-start.3) | collective-permute-done | bytes 524320 | tf_op jit(solution)/shard_map/ppermute | solution.py:153
  65.2 3.0 %collective-permute-start.4 = (bf16[32,32,128]{2,1,0:T(8,128)(2,1)S(1)}, bf16[32,32,128]{2,1,0:T(8,128)(2,1)S(1)}, u32[]{:S(2)}, u32[]{:S(2)}) collective-permute-start(bf16[32,32,128]{2,1,0:T(8,128)(2,1)S(1)} %slice_bitcast_fusion), channel_id=1, source_target_pairs={{0,2},{1,15},{2,4},{3,1},{4,6},{5,3},{6,8},{7,5},{8,10},{9,7},{10,... | collective-permute-start | bytes 786440 | tf_op jit(solution)/shard_map/ppermute | solution.py:153
  68.2 1.9 collective-permute-start.8
  70.1 4.5 %collective-permute-done.4.refs_2_ = bf16[32,32,128]{2,1,0:T(8,128)(2,1)S(1)} collective-permute-done((bf16[32,32,128]{2,1,0:T(8,128)(2,1)S(1)}, bf16[32,32,128]{2,1,0:T(8,128)(2,1)S(1)}, u32[]{:S(2)}, u32[]{:S(2)}) %collective-permute-start.4) | collective-permute-done | bytes 262176 | tf_op jit(solution)/shard_map/ppermute | solution.py:153
  74.7 1.9 collective-permute-start.5
  76.6 1.6 collective-permute-done.5.refs_3_
  78.3 9.4 %expert_backward.1 = (bf16[512,2048]{1,0:T(8,128)(2,1)}, bf16[512,2048]{1,0:T(8,128)(2,1)}, bf16[512,224]{1,0:T(8,128)(2,1)}, bf16[512,224]{1,0:T(8,128)(2,1)}, ...) custom-call(s32[1]{0:T(128)} %bitcast.me, bf16[32,32,128]{2,1,0:T(8,128)(2,1)} %copy-done.2, ...), custom_call_target="tpu_custom_call" | custom-call | flops 2348810240 | bytes 12582912 | tf_op jit(solution)/shard_map/expert_backward/pallas_call | solution.py:132
  87.7 2.1 collective-permute-start.9
  89.8 2.7 %collective-permute-done.9 = bf16[8,512,128]{2,1,0:T(8,128)(2,1)S(1)} collective-permute-done((bf16[8,512,128]{2,1,0:T(8,128)(2,1)}, bf16[8,512,128]{2,1,0:T(8,128)(2,1)S(1)}, u32[]{:S(2)}, u32[]{:S(2)}) %collective-permute-start.9) | collective-permute-done | bytes 1048608 | tf_op jit(solution)/shard_map/ppermute | solution.py:160
  92.6 1.0 convert_add_fusion
  93.6 3.0 %collective-permute-start.10 = (bf16[512,128]{1,0:T(8,128)(2,1)S(1)}, bf16[512,128]{1,0:T(8,128)(2,1)S(1)}, u32[]{:S(2)}, u32[]{:S(2)}) collective-permute-start(bf16[512,128]{1,0:T(8,128)(2,1)S(1)} %fusion.7), channel_id=1, source_target_pairs={{0,2},{1,15},{2,4},{3,1},{4,6},{5,3},{6,8},{7,5},{8,10},{9,7},{10,... | collective-permute-start | bytes 393224 | tf_op jit(solution)/shard_map/ppermute | solution.py:153
  96.6 5.1 %collective-permute-done.10 = bf16[512,128]{1,0:T(8,128)(2,1)S(1)} collective-permute-done((bf16[512,128]{1,0:T(8,128)(2,1)S(1)}, bf16[512,128]{1,0:T(8,128)(2,1)S(1)}, u32[]{:S(2)}, u32[]{:S(2)}) %collective-permute-start.10) | collective-permute-done | bytes 131104 | tf_op jit(solution)/shard_map/ppermute | solution.py:153
  101.7 1.1 add_convert_fusion.2
  102.7 3.0 %collective-permute-start.11 = (bf16[2,512,128]{2,1,0:T(8,128)(2,1)S(1)}, bf16[2,512,128]{2,1,0:T(8,128)(2,1)S(1)}, u32[]{:S(2)}, u32[]{:S(2)}) collective-permute-start(bf16[2,512,128]{2,1,0:T(8,128)(2,1)S(1)} %add_convert_fusion.2), channel_id=1, source_target_pairs={{0,2},{1,15},{2,4},{3,1},{4,6},{5,3},{6,8},{7,5},{8,10},{9,7},{10,... | collective-permute-start | bytes 786440 | tf_op jit(solution)/shard_map/ppermute | solution.py:153
  105.8 6.4 %collective-permute-done.11 = bf16[2,512,128]{2,1,0:T(8,128)(2,1)S(1)} collective-permute-done((bf16[2,512,128]{2,1,0:T(8,128)(2,1)S(1)}, bf16[2,512,128]{2,1,0:T(8,128)(2,1)S(1)}, u32[]{:S(2)}, u32[]{:S(2)}) %collective-permute-start.11) | collective-permute-done | bytes 262176 | tf_op jit(solution)/shard_map/ppermute | solution.py:153
  112.3 3.2 %collective-permute-start.12 = (bf16[2,512,128]{2,1,0:T(8,128)(2,1)S(1)}, bf16[2,512,128]{2,1,0:T(8,128)(2,1)S(1)}, u32[]{:S(2)}, u32[]{:S(2)}) collective-permute-start(bf16[2,512,128]{2,1,0:T(8,128)(2,1)S(1)} %add_convert_fusion.1), channel_id=1, source_target_pairs={{0,2},{1,15},{2,4},{3,1},{4,6},{5,3},{6,8},{7,5},{8,10},{9,7},{10,... | collective-permute-start | bytes 786440 | tf_op jit(solution)/shard_map/ppermute | solution.py:153
  115.5 6.4 %collective-permute-done.12 = bf16[2,512,128]{2,1,0:T(8,128)(2,1)S(1)} collective-permute-done((bf16[2,512,128]{2,1,0:T(8,128)(2,1)S(1)}, bf16[2,512,128]{2,1,0:T(8,128)(2,1)S(1)}, u32[]{:S(2)}, u32[]{:S(2)}) %collective-permute-start.12) | collective-permute-done | bytes 262176 | tf_op jit(solution)/shard_map/ppermute | solution.py:153
  122.1 3.1 %collective-permute-start.13 = (bf16[2,512,128]{2,1,0:T(8,128)(2,1)S(1)}, bf16[2,512,128]{2,1,0:T(8,128)(2,1)S(1)}, u32[]{:S(2)}, u32[]{:S(2)}) collective-permute-start(bf16[2,512,128]{2,1,0:T(8,128)(2,1)S(1)} %add_convert_fusion), channel_id=1, source_target_pairs={{0,2},{1,15},{2,4},{3,1},{4,6},{5,3},{6,8},{7,5},{8,10},{9,7},{10,... | collective-permute-start | bytes 786440 | tf_op jit(solution)/shard_map/ppermute | solution.py:153
  125.3 6.5 %collective-permute-done.13 = bf16[2,512,128]{2,1,0:T(8,128)(2,1)S(1)} collective-permute-done((bf16[2,512,128]{2,1,0:T(8,128)(2,1)S(1)}, bf16[2,512,128]{2,1,0:T(8,128)(2,1)S(1)}, u32[]{:S(2)}, u32[]{:S(2)}) %collective-permute-start.13) | collective-permute-done | bytes 262176 | tf_op jit(solution)/shard_map/ppermute | solution.py:153
  131.7 1.9 collective-permute-start.14
  133.7 1.3 collective-permute-done.14
  135.0 14.4 %all_to_all.21 = bf16[32,16,128]{2,1,0:T(8,128)(2,1)S(1)} all-to-all(bf16[32,16,128]{2,1,0:T(8,128)(2,1)S(1)} %bitcast.98), channel_id=1, replica_groups=mesh['sp'=32,'tp'=16] {'sp'}, dimensions={0} | all-to-all | bytes 262144 | tf_op jit(solution)/shard_map/all_to_all | solution.py:238
  149.4 0.9 broadcast_in_dim.8
  150.4 5.7 %all-to-all-start.3 = ((bf16[32,64,128]{2,1,0:T(8,128)(2,1)}), bf16[32,64,128]{2,1,0:T(8,128)(2,1)S(1)}, u32[]{:S(2)}, u32[]{:S(2)}) async-start(bf16[32,64,128]{2,1,0:T(8,128)(2,1)} %broadcast_in_dim.8), calls=%async_computation.3 | async-start | bytes 1048576 | tf_op jit(solution)/shard_map/all_to_all | solution.py:203
  156.3 20.3 %all_gather.3 = bf16[192,2048]{1,0:T(8,128)(2,1)S(1)} all-gather(bf16[192,128]{1,0:T(8,128)(2,1)S(1)} %fusion.3), channel_id=1, replica_groups=mesh['sp'=32,'tp'=16] {'tp'}, dimensions={1}, use_global_device_ids=true | all-gather | bytes 835584 | tf_op jit(solution)/shard_map/all_gather | solution.py:244
  177.2 2.3 %collective-permute-start.15 = (f32[384]{0:T(512)S(1)}, f32[384]{0:T(512)S(1)}, u32[]{:S(2)}, u32[]{:S(2)}) collective-permute-start(f32[384]{0:T(512)S(1)} %pad_maximum_fusion.2), channel_id=1, source_target_pairs={{0,1},{1,0},{2,3},{3,2},{4,5},{5,4},{6,7},{7,6},{8,9},{9,8},{10,11... | collective-permute-start | bytes 4616 | tf_op jit(solution)/shard_map/ppermute | solution.py:160
  180.4 2.2 %collective-permute-start.16 = (f32[384]{0:T(512)S(1)}, f32[384]{0:T(512)S(1)}, u32[]{:S(2)}, u32[]{:S(2)}) collective-permute-start(f32[384]{0:T(512)S(1)} %fusion.104), channel_id=1, source_target_pairs={{0,2},{1,3},{2,0},{3,1},{4,6},{5,7},{6,4},{7,5},{8,10},{9,11},{10,... | collective-permute-start | bytes 4616 | tf_op jit(solution)/shard_map/ppermute | solution.py:160
  182.6 3.2 %collective-permute-done.16 = f32[384]{0:T(512)S(1)} collective-permute-done((f32[384]{0:T(512)S(1)}, f32[384]{0:T(512)S(1)}, u32[]{:S(2)}, u32[]{:S(2)}) %collective-permute-start.16) | collective-permute-done | bytes 1568 | tf_op jit(solution)/shard_map/ppermute | solution.py:160
  185.9 4.6 %collective-permute-start.17 = (f32[384]{0:T(512)S(1)}, f32[384]{0:T(512)S(1)}, u32[]{:S(2)}, u32[]{:S(2)}) collective-permute-start(f32[384]{0:T(512)S(1)} %add.167), channel_id=1, source_target_pairs={{0,4},{1,5},{2,6},{3,7},{4,0},{5,1},{6,2},{7,3},{8,12},{9,13},{10,... | collective-permute-start | bytes 4616 | tf_op jit(solution)/shard_map/ppermute | solution.py:160
  190.4 1.4 convolution_convert_fusion.2
  191.8 10.0 %all-to-all-start.2 = ((bf16[32,64,128]{2,1,0:T(8,128)(2,1)}), bf16[32,64,128]{2,1,0:T(8,128)(2,1)S(1)}, u32[]{:S(2)}, u32[]{:S(2)}) async-start(bf16[32,64,128]{2,1,0:T(8,128)(2,1)} %bitcast.14), calls=%async_computation.2 | async-start | bytes 1048576 | tf_op jit(solution)/shard_map/all_to_all | solution.py:250
  201.8 4.3 %collective-permute-start.18 = (f32[384]{0:T(512)S(1)}, f32[384]{0:T(512)S(1)}, u32[]{:S(2)}, u32[]{:S(2)}) collective-permute-start(f32[384]{0:T(512)S(1)} %add.168), channel_id=1, source_target_pairs={{0,8},{1,9},{2,10},{3,11},{4,12},{5,13},{6,14},{7,15},{8,0},{9,1},... | collective-permute-start | bytes 4616 | tf_op jit(solution)/shard_map/ppermute | solution.py:160
  206.1 3.2 %fusion.1 = bf16[1,224,2048]{2,1,0:T(8,128)(2,1)} fusion(bf16[512,224]{1,0:T(8,128)(2,1)S(1)} %copy-done.4, bf16[512,2048]{1,0:T(8,128)(2,1)} %get-tuple-element.17), kind=kOutput, calls=%fused_computation.3 | convolution fusion | flops 470220800 | bytes 3244032 | tf_op jit(solution)/shard_map/dot_general | solution.py:15
  209.3 1.9 collective-permute-done.18
  211.5 2.8 %collective-permute-start.19 = (f32[30,128]{1,0:T(8,128)S(1)}, f32[30,128]{1,0:T(8,128)S(1)}, u32[]{:S(2)}, u32[]{:S(2)}) collective-permute-start(f32[30,128]{1,0:T(8,128)S(1)} %slice.323), channel_id=1, source_target_pairs={{16,0},{32,16},{48,32},{64,48},{80,64},{96,80},{112,96},{128,112},... | collective-permute-start | bytes 46088 | tf_op jit(solution)/shard_map/ppermute | solution.py:264
  214.3 1.6 fusion
  215.9 3.4 %collective-permute-done.19 = f32[30,128]{1,0:T(8,128)S(1)} collective-permute-done((f32[30,128]{1,0:T(8,128)S(1)}, f32[30,128]{1,0:T(8,128)S(1)}, u32[]{:S(2)}, u32[]{:S(2)}) %collective-permute-start.19) | collective-permute-done | bytes 15392 | tf_op jit(solution)/shard_map/ppermute | solution.py:264
  (72 shorter events, 4.0 us)
Async XLA Ops:
  27.4 50.8 %copy-start.2 = (bf16[32,32,128]{2,1,0:T(8,128)(2,1)}, bf16[32,32,128]{2,1,0:T(8,128)(2,1)S(1)}, u32[]{:S(2)}) copy-start(bf16[32,32,128]{2,1,0:T(8,128)(2,1)S(1)} %all_to_all.20.refs_0_) | copy-start | bytes 786436
  27.4 3.4 %collective-permute-start = (bf16[32,32,128]{2,1,0:T(8,128)(2,1)S(1)}, bf16[32,32,128]{2,1,0:T(8,128)(2,1)S(1)}, u32[]{:S(2)}, u32[]{:S(2)}) collective-permute-start(bf16[32,32,128]{2,1,0:T(8,128)(2,1)S(1)} %all_to_all.20.refs_0_), channel_id=1, source_target_pairs={{0,1},{1,0},{2,3},{3,2},{4,5},{5,4},{6,7},{7,6},{8,9},{9,8},{10,11... | collective-permute-start | bytes 786440 | tf_op jit(solution)/shard_map/ppermute | solution.py:160
  30.8 47.4 %copy-start.6 = (bf16[32,32,128]{2,1,0:T(8,128)(2,1)}, bf16[32,32,128]{2,1,0:T(8,128)(2,1)S(1)}, u32[]{:S(2)}) copy-start(bf16[32,32,128]{2,1,0:T(8,128)(2,1)S(1)} %collective-permute-done.refs_1_) | copy-start | bytes 786436
  30.8 11.1 %collective-permute-start.1 = (bf16[2,32,32,128]{3,2,1,0:T(8,128)(2,1)S(1)}, bf16[2,32,32,128]{3,2,1,0:T(8,128)(2,1)S(1)}, u32[]{:S(2)}, u32[]{:S(2)}) collective-permute-start(bf16[2,32,32,128]{3,2,1,0:T(8,128)(2,1)S(1)} %pad_maximum_fusion), channel_id=1, source_target_pairs={{0,2},{1,15},{2,4},{3,1},{4,6},{5,3},{6,8},{7,5},{8,10},{9,7},{10,... | collective-permute-start | bytes 1572872 | tf_op jit(solution)/shard_map/ppermute | solution.py:153
  41.9 36.3 %copy-start.15 = (bf16[2,32,32,128]{3,2,1,0:T(8,128)(2,1)}, bf16[2,32,32,128]{3,2,1,0:T(8,128)(2,1)S(1)}, u32[]{:S(2)}) copy-start(bf16[2,32,32,128]{3,2,1,0:T(8,128)(2,1)S(1)} %collective-permute-done.1.refs_4_) | copy-start | bytes 1572868
  41.9 11.1 %collective-permute-start.2 = (bf16[2,32,32,128]{3,2,1,0:T(8,128)(2,1)S(1)}, bf16[2,32,32,128]{3,2,1,0:T(8,128)(2,1)S(1)}, u32[]{:S(2)}, u32[]{:S(2)}) collective-permute-start(bf16[2,32,32,128]{3,2,1,0:T(8,128)(2,1)S(1)} %collective-permute-done.1.refs_4_), channel_id=1, source_target_pairs={{0,2},{1,15},{2,4},{3,1},{4,6},{5,3},{6,8},{7,5},{8,10},{9,7},{10,... | collective-permute-start | bytes 1572872 | tf_op jit(solution)/shard_map/ppermute | solution.py:153
  53.0 25.2 %copy-start.16 = (bf16[2,32,32,128]{3,2,1,0:T(8,128)(2,1)}, bf16[2,32,32,128]{3,2,1,0:T(8,128)(2,1)S(1)}, u32[]{:S(2)}) copy-start(bf16[2,32,32,128]{3,2,1,0:T(8,128)(2,1)S(1)} %collective-permute-done.2.refs_6_) | copy-start | bytes 1572868
  53.0 12.2 %collective-permute-start.3 = (bf16[2,32,32,128]{3,2,1,0:T(8,128)(2,1)S(1)}, bf16[2,32,32,128]{3,2,1,0:T(8,128)(2,1)S(1)}, u32[]{:S(2)}, u32[]{:S(2)}) collective-permute-start(bf16[2,32,32,128]{3,2,1,0:T(8,128)(2,1)S(1)} %collective-permute-done.2.refs_6_), channel_id=1, source_target_pairs={{0,2},{1,15},{2,4},{3,1},{4,6},{5,3},{6,8},{7,5},{8,10},{9,7},{10,... | collective-permute-start | bytes 1572872 | tf_op jit(solution)/shard_map/ppermute | solution.py:153
  56.5 20.1 %collective-permute-start.6 = (bf16[2,32,32,128]{3,2,1,0:T(8,128)(2,1)S(1)}, bf16[2,32,32,128]{3,2,1,0:T(8,128)(2,1)S(1)}, u32[]{:S(2)}, u32[]{:S(2)}) collective-permute-start(bf16[2,32,32,128]{3,2,1,0:T(8,128)(2,1)S(1)} %collective-permute-done.1.refs_4_), channel_id=1, source_target_pairs={{0,1},{1,0},{2,3},{3,2},{4,5},{5,4},{6,7},{7,6},{8,9},{9,8},{10,11... | collective-permute-start | bytes 1572872 | tf_op jit(solution)/shard_map/ppermute | solution.py:160
  58.4 18.2 %collective-permute-start.7 = (bf16[2,32,32,128]{3,2,1,0:T(8,128)(2,1)S(1)}, bf16[2,32,32,128]{3,2,1,0:T(8,128)(2,1)S(1)}, u32[]{:S(2)}, u32[]{:S(2)}) collective-permute-start(bf16[2,32,32,128]{3,2,1,0:T(8,128)(2,1)S(1)} %collective-permute-done.2.refs_6_), channel_id=1, source_target_pairs={{0,1},{1,0},{2,3},{3,2},{4,5},{5,4},{6,7},{7,6},{8,9},{9,8},{10,11... | collective-permute-start | bytes 1572872 | tf_op jit(solution)/shard_map/ppermute | solution.py:160
  65.2 13.1 %copy-start.9 = (bf16[2,32,32,128]{3,2,1,0:T(8,128)(2,1)}, bf16[2,32,32,128]{3,2,1,0:T(8,128)(2,1)S(1)}, u32[]{:S(2)}) copy-start(bf16[2,32,32,128]{3,2,1,0:T(8,128)(2,1)S(1)} %collective-permute-done.3.refs_8_) | copy-start | bytes 1572868
  65.2 9.5 %collective-permute-start.4 = (bf16[32,32,128]{2,1,0:T(8,128)(2,1)S(1)}, bf16[32,32,128]{2,1,0:T(8,128)(2,1)S(1)}, u32[]{:S(2)}, u32[]{:S(2)}) collective-permute-start(bf16[32,32,128]{2,1,0:T(8,128)(2,1)S(1)} %slice_bitcast_fusion), channel_id=1, source_target_pairs={{0,2},{1,15},{2,4},{3,1},{4,6},{5,3},{6,8},{7,5},{8,10},{9,7},{10,... | collective-permute-start | bytes 786440 | tf_op jit(solution)/shard_map/ppermute | solution.py:153
  68.2 10.0 %collective-permute-start.8 = (bf16[2,32,32,128]{3,2,1,0:T(8,128)(2,1)S(1)}, bf16[2,32,32,128]{3,2,1,0:T(8,128)(2,1)}, u32[]{:S(2)}, u32[]{:S(2)}) collective-permute-start(bf16[2,32,32,128]{3,2,1,0:T(8,128)(2,1)S(1)} %collective-permute-done.3.refs_8_), channel_id=1, source_target_pairs={{0,1},{1,0},{2,3},{3,2},{4,5},{5,4},{6,7},{7,6},{8,9},{9,8},{10,11... | collective-permute-start | bytes 1572872 | tf_op jit(solution)/shard_map/ppermute | solution.py:160
  74.7 3.6 %copy-start.19 = (bf16[32,32,128]{2,1,0:T(8,128)(2,1)}, bf16[32,32,128]{2,1,0:T(8,128)(2,1)S(1)}, u32[]{:S(2)}) copy-start(bf16[32,32,128]{2,1,0:T(8,128)(2,1)S(1)} %collective-permute-done.4.refs_2_) | copy-start | bytes 786436
  74.7 3.6 %collective-permute-start.5 = (bf16[32,32,128]{2,1,0:T(8,128)(2,1)S(1)}, bf16[32,32,128]{2,1,0:T(8,128)(2,1)}, u32[]{:S(2)}, u32[]{:S(2)}) collective-permute-start(bf16[32,32,128]{2,1,0:T(8,128)(2,1)S(1)} %collective-permute-done.4.refs_2_), channel_id=1, source_target_pairs={{0,1},{1,0},{2,3},{3,2},{4,5},{5,4},{6,7},{7,6},{8,9},{9,8},{10,11... | collective-permute-start | bytes 786440 | tf_op jit(solution)/shard_map/ppermute | solution.py:160
  76.6 1.7 copy-start.17
  76.6 1.7 copy-start.18
  87.7 24.5 %copy-start.1 = (bf16[8,512,128]{2,1,0:T(8,128)(2,1)S(1)}, bf16[8,512,128]{2,1,0:T(8,128)(2,1)}, u32[]{:S(2)}) copy-start(bf16[8,512,128]{2,1,0:T(8,128)(2,1)} %get-tuple-element.19) | copy-start | bytes 3145732
  87.7 4.9 %collective-permute-start.9 = (bf16[8,512,128]{2,1,0:T(8,128)(2,1)}, bf16[8,512,128]{2,1,0:T(8,128)(2,1)S(1)}, u32[]{:S(2)}, u32[]{:S(2)}) collective-permute-start(bf16[8,512,128]{2,1,0:T(8,128)(2,1)} %get-tuple-element.20), channel_id=1, source_target_pairs={{0,1},{1,0},{2,3},{3,2},{4,5},{5,4},{6,7},{7,6},{8,9},{9,8},{10,11... | collective-permute-start | bytes 3145736 | tf_op jit(solution)/shard_map/ppermute | solution.py:160
  93.6 8.1 %collective-permute-start.10 = (bf16[512,128]{1,0:T(8,128)(2,1)S(1)}, bf16[512,128]{1,0:T(8,128)(2,1)S(1)}, u32[]{:S(2)}, u32[]{:S(2)}) collective-permute-start(bf16[512,128]{1,0:T(8,128)(2,1)S(1)} %fusion.7), channel_id=1, source_target_pairs={{0,2},{1,15},{2,4},{3,1},{4,6},{5,3},{6,8},{7,5},{8,10},{9,7},{10,... | collective-permute-start | bytes 393224 | tf_op jit(solution)/shard_map/ppermute | solution.py:153
  101.7 47.8 %copy-start.11 = (bf16[64,128]{1,0:T(8,128)(2,1)S(1)}, bf16[64,128]{1,0:T(8,128)(2,1)}, u32[]{:S(2)}) copy-start(bf16[64,128]{1,0:T(8,128)(2,1)} %param.27) | copy-start | bytes 49156
  102.7 9.5 %collective-permute-start.11 = (bf16[2,512,128]{2,1,0:T(8,128)(2,1)S(1)}, bf16[2,512,128]{2,1,0:T(8,128)(2,1)S(1)}, u32[]{:S(2)}, u32[]{:S(2)}) collective-permute-start(bf16[2,512,128]{2,1,0:T(8,128)(2,1)S(1)} %add_convert_fusion.2), channel_id=1, source_target_pairs={{0,2},{1,15},{2,4},{3,1},{4,6},{5,3},{6,8},{7,5},{8,10},{9,7},{10,... | collective-permute-start | bytes 786440 | tf_op jit(solution)/shard_map/ppermute | solution.py:153
  112.3 43.7 %copy-start.5 = (bf16[512,192]{1,0:T(8,128)(2,1)S(1)}, bf16[512,192]{1,0:T(8,128)(2,1)}, u32[]{:S(2)}) copy-start(bf16[512,192]{1,0:T(8,128)(2,1)} %get-tuple-element.18) | copy-start | bytes 589828
  112.3 43.7 %copy-start.8 = (bf16[192,128]{1,0:T(8,128)(2,1)S(1)}, bf16[192,128]{1,0:T(8,128)(2,1)}, u32[]{:S(2)}) copy-start(bf16[192,128]{1,0:T(8,128)(2,1)} %cotangent.1) | copy-start | bytes 147460
  112.3 9.6 %collective-permute-start.12 = (bf16[2,512,128]{2,1,0:T(8,128)(2,1)S(1)}, bf16[2,512,128]{2,1,0:T(8,128)(2,1)S(1)}, u32[]{:S(2)}, u32[]{:S(2)}) collective-permute-start(bf16[2,512,128]{2,1,0:T(8,128)(2,1)S(1)} %add_convert_fusion.1), channel_id=1, source_target_pairs={{0,2},{1,15},{2,4},{3,1},{4,6},{5,3},{6,8},{7,5},{8,10},{9,7},{10,... | collective-permute-start | bytes 786440 | tf_op jit(solution)/shard_map/ppermute | solution.py:153
  122.1 54.6 %copy-start.10 = (bf16[192,128]{1,0:T(8,128)(2,1)S(1)}, bf16[192,128]{1,0:T(8,128)(2,1)}, u32[]{:S(2)}) copy-start(bf16[192,128]{1,0:T(8,128)(2,1)} %param.21) | copy-start | bytes 147460
  122.1 54.5 %copy-start.13 = (f32[192]{0:T(256)S(1)}, f32[192]{0:T(256)}, u32[]{:S(2)}) copy-start(f32[192]{0:T(256)} %param.23) | copy-start | bytes 2308
  122.1 54.5 %copy-start.14 = (f32[192]{0:T(256)S(1)}, f32[192]{0:T(256)}, u32[]{:S(2)}) copy-start(f32[192]{0:T(256)} %param.22) | copy-start | bytes 2308
  122.1 54.5 %copy-start.20 = (f32[128]{0:T(128)S(1)}, f32[128]{0:T(128)}, u32[]{:S(2)}) copy-start(f32[128]{0:T(128)} %param.25) | copy-start | bytes 1540
  122.1 54.5 %copy-start.21 = (f32[128]{0:T(128)S(1)}, f32[128]{0:T(128)}, u32[]{:S(2)}) copy-start(f32[128]{0:T(128)} %param.24) | copy-start | bytes 1540
  122.1 9.6 %collective-permute-start.13 = (bf16[2,512,128]{2,1,0:T(8,128)(2,1)S(1)}, bf16[2,512,128]{2,1,0:T(8,128)(2,1)S(1)}, u32[]{:S(2)}, u32[]{:S(2)}) collective-permute-start(bf16[2,512,128]{2,1,0:T(8,128)(2,1)S(1)} %add_convert_fusion), channel_id=1, source_target_pairs={{0,2},{1,15},{2,4},{3,1},{4,6},{5,3},{6,8},{7,5},{8,10},{9,7},{10,... | collective-permute-start | bytes 786440 | tf_op jit(solution)/shard_map/ppermute | solution.py:153
  131.7 3.2 %collective-permute-start.14 = (bf16[512,128]{1,0:T(8,128)(2,1)S(1)}, bf16[512,128]{1,0:T(8,128)(2,1)S(1)}, u32[]{:S(2)}, u32[]{:S(2)}) collective-permute-start(bf16[512,128]{1,0:T(8,128)(2,1)S(1)} %slice_bitcast_fusion.1), channel_id=1, source_target_pairs={{0,1},{1,0},{2,3},{3,2},{4,5},{5,4},{6,7},{7,6},{8,9},{9,8},{10,11... | collective-permute-start | bytes 393224 | tf_op jit(solution)/shard_map/ppermute | solution.py:160
  150.4 29.2 %copy-start.12 = (f32[31,128]{1,0:T(8,128)S(1)}, f32[31,128]{1,0:T(8,128)}, u32[]{:S(2)}) copy-start(f32[31,128]{1,0:T(8,128)} %param.26) | copy-start | bytes 47620
  150.4 26.3 %all-to-all-start.3 = ((bf16[32,64,128]{2,1,0:T(8,128)(2,1)}), bf16[32,64,128]{2,1,0:T(8,128)(2,1)S(1)}, u32[]{:S(2)}, u32[]{:S(2)}) async-start(bf16[32,64,128]{2,1,0:T(8,128)(2,1)} %broadcast_in_dim.8), calls=%async_computation.3 | async-start | bytes 1048576 | tf_op jit(solution)/shard_map/all_to_all | solution.py:203
  156.3 35.5 %copy-start.7 = (bf16[192,128]{1,0:T(8,128)(2,1)}, bf16[192,128]{1,0:T(8,128)(2,1)S(1)}, u32[]{:S(2)}) copy-start(bf16[192,128]{1,0:T(8,128)(2,1)S(1)} %fusion.3) | copy-start | bytes 147460
  176.7 29.4 %copy-start.4 = (bf16[512,224]{1,0:T(8,128)(2,1)S(1)}, bf16[512,224]{1,0:T(8,128)(2,1)}, u32[]{:S(2)}) copy-start(bf16[512,224]{1,0:T(8,128)(2,1)} %get-tuple-element.16) | copy-start | bytes 688132
  177.2 3.1 %collective-permute-start.15 = (f32[384]{0:T(512)S(1)}, f32[384]{0:T(512)S(1)}, u32[]{:S(2)}, u32[]{:S(2)}) collective-permute-start(f32[384]{0:T(512)S(1)} %pad_maximum_fusion.2), channel_id=1, source_target_pairs={{0,1},{1,0},{2,3},{3,2},{4,5},{5,4},{6,7},{7,6},{8,9},{9,8},{10,11... | collective-permute-start | bytes 4616 | tf_op jit(solution)/shard_map/ppermute | solution.py:160
  180.4 5.5 %collective-permute-start.16 = (f32[384]{0:T(512)S(1)}, f32[384]{0:T(512)S(1)}, u32[]{:S(2)}, u32[]{:S(2)}) collective-permute-start(f32[384]{0:T(512)S(1)} %fusion.104), channel_id=1, source_target_pairs={{0,2},{1,3},{2,0},{3,1},{4,6},{5,7},{6,4},{7,5},{8,10},{9,11},{10,... | collective-permute-start | bytes 4616 | tf_op jit(solution)/shard_map/ppermute | solution.py:160
  185.9 15.9 %collective-permute-start.17 = (f32[384]{0:T(512)S(1)}, f32[384]{0:T(512)S(1)}, u32[]{:S(2)}, u32[]{:S(2)}) collective-permute-start(f32[384]{0:T(512)S(1)} %add.167), channel_id=1, source_target_pairs={{0,4},{1,5},{2,6},{3,7},{4,0},{5,1},{6,2},{7,3},{8,12},{9,13},{10,... | collective-permute-start | bytes 4616 | tf_op jit(solution)/shard_map/ppermute | solution.py:160
  191.8 22.5 %copy-start = (bf16[512,2048]{1,0:T(8,128)(2,1)S(1)}, bf16[512,2048]{1,0:T(8,128)(2,1)}, u32[]{:S(2)}) copy-start(bf16[512,2048]{1,0:T(8,128)(2,1)} %get-tuple-element.15) | copy-start | bytes 6291460
  191.8 22.5 %copy-start.3 = (bf16[512,224]{1,0:T(8,128)(2,1)S(1)}, bf16[512,224]{1,0:T(8,128)(2,1)}, u32[]{:S(2)}) copy-start(bf16[512,224]{1,0:T(8,128)(2,1)} %get-tuple-element.14) | copy-start | bytes 688132
  191.8 28.3 %all-to-all-start.2 = ((bf16[32,64,128]{2,1,0:T(8,128)(2,1)}), bf16[32,64,128]{2,1,0:T(8,128)(2,1)S(1)}, u32[]{:S(2)}, u32[]{:S(2)}) async-start(bf16[32,64,128]{2,1,0:T(8,128)(2,1)} %bitcast.14), calls=%async_computation.2 | async-start | bytes 1048576 | tf_op jit(solution)/shard_map/all_to_all | solution.py:250
  201.8 9.4 %collective-permute-start.18 = (f32[384]{0:T(512)S(1)}, f32[384]{0:T(512)S(1)}, u32[]{:S(2)}, u32[]{:S(2)}) collective-permute-start(f32[384]{0:T(512)S(1)} %add.168), channel_id=1, source_target_pairs={{0,8},{1,9},{2,10},{3,11},{4,12},{5,13},{6,14},{7,15},{8,0},{9,1},... | collective-permute-start | bytes 4616 | tf_op jit(solution)/shard_map/ppermute | solution.py:160
  211.5 7.7 %collective-permute-start.19 = (f32[30,128]{1,0:T(8,128)S(1)}, f32[30,128]{1,0:T(8,128)S(1)}, u32[]{:S(2)}, u32[]{:S(2)}) collective-permute-start(f32[30,128]{1,0:T(8,128)S(1)} %slice.323), channel_id=1, source_target_pairs={{16,0},{32,16},{48,32},{64,48},{80,64},{96,80},{112,96},{128,112},... | collective-permute-start | bytes 46088 | tf_op jit(solution)/shard_map/ppermute | solution.py:264
where the time goes:
time: 222 us; the launch traced here: 221 us
  starting transfers between devices  71.6 us (32%)
  waiting for transfers between devices  64.9 us (29%)
  blocking collectives  59.3 us (27%)
  Pallas kernels  11.5 us (5%)
  matrix products  6.87 us (3%)
  other arithmetic  4.37 us (2%)
    ppermute x8, waiting for transfers between devices, passed_on(): lax.ppermute(value, 'tp', [(t, (t + (2 if t % 2 == 0 else count - 2)) % c...  48.5 us
    ppermute x11, starting transfers between devices, swapped(): return lax.ppermute(value, 'tp', [(t, t ^ hop) for t in range(count)])  27.5 us
    ppermute x8, starting transfers between devices, passed_on(): lax.ppermute(value, 'tp', [(t, (t + (2 if t % 2 == 0 else count - 2)) % c...  25.7 us
    all_to_all x1, blocking collectives, steps(): own = lax.all_to_all(sent, 'sp', split_axis=0, concat_axis=0, tiled=True)  24.6 us
    all_gather x1, blocking collectives, steps(): columns = lax.all_gather(grad_stream, 'tp', axis=1, tiled=True)  20.3 us
    all_to_all x1, blocking collectives, steps(): lax.all_to_all(shared, 'sp', split_axis=0, concat_axis=0, tiled=True)  14.4 us
    ppermute x11, waiting for transfers between devices, swapped(): return lax.ppermute(value, 'tp', [(t, t ^ hop) for t in range(count)])  13 us
    all_to_all x1, starting transfers between devices, steps(): lax.all_to_all(proj_part, 'sp', split_axis=0, concat_axis=0, tiled=True)  10 us
  transfers between devices with their start and end apart: 22, of which 16 were waited for; matrix products, arithmetic and copies ran while one was open for 3% of the time, Pallas kernels for 0%

commit v1 on v0

--- a/solution.py
+++ b/solution.py
@@ -7,6 +7,8 @@
 from jax.sharding import PartitionSpec as P
 
 
+TP = ("chip", "core")
+EARLY = 1
 BF16 = jnp.bfloat16
 F32 = jnp.float32
 
@@ -62,48 +64,28 @@
     )(routes, weights, rows, cotangent)
 
 
-def block_of(me, steps, core, blocks):
-    chips = blocks // 2
-    mine = lax.rem(me, 2)
-    sign = 1 - 2 * mine
-    chip = lax.rem(me // 2 + sign * steps + chips, chips)
-    return 2 * chip + (mine if core == 0 else 1 - mine)
-
-
-def places(blocks):
-    chips = blocks // 2
-    ahead = [(k, core) for k in range(1, chips // 2) for core in (1, 0)]
-    behind = [(-k, core) for k in range(1, chips // 2) for core in (0, 1)]
-    kept = [(0, 0), (chips // 2, 0), *ahead]
-    given = [(0, 1), (chips // 2, 1), *behind]
-    return kept, given
-
-
 def expert_body(me, *refs, blocks, slots):
     chips = blocks // 2
-    middle = chips // 2
-    parts = refs[: 2 * middle + 2]
-    gate_weight, up_weight, down_weight = refs[len(parts) : len(parts) + 3]
-    rows, routed, hidden_out, up_out, kept, given = refs[len(parts) + 3 :]
-    width = parts[0].shape[-1]
-    count = parts[0].shape[-3] * slots
-
-    def columns(place):
-        at = block_of(me[0], *place, blocks) * width
-        return pl.ds(pl.multiple_of(at, width), width)
-
-    def put(place, part):
-        cols = columns(place)
+    mine, shared = (refs[:chips], refs[chips : chips + 2])
+    gate_weight, up_weight, down_weight = refs[chips + 2 : chips + 5]
+    rows, routed, hidden_out, up_out, kept, given = refs[chips + 5 :]
+    width = mine[0].shape[-1]
+    count = mine[0].shape[-3] * slots
+    my_chip, my_core = (me[0] // 2, lax.rem(me[0], 2))
+
+    def columns(chip, core):
+        return pl.ds(pl.multiple_of((2 * chip + core) * width, width), width)
+
+    def put(cols, part):
         rows[:, cols] = part[:, :slots, :].reshape(count, width)
         routed[:, cols] = part[:, slots:, :].reshape(count, width)
 
-    for core in (0, 1):
-        put((0, core), parts[core])
-        put((middle, core), parts[2 + core])
-        for k in range(1, middle):
-            pair = parts[2 + 2 * k + core]
-            for i in (0, 1):
-                put((k if core else -k, i ^ core), pair[i])
+    early = 2 * EARLY + 1
+    for n, steps in enumerate(ring_order(chips)):
+        chip = lax.rem(my_chip + steps + chips, chips)
+        put(columns(chip, my_core), mine[n])
+        batch, at = (shared[0], n) if n < early else (shared[1], n - early)
+        put(columns(chip, 1 - my_core), batch[at])
     gate_pre = dot(rows[...], gate_weight[0], 1, 1)
     up_pre = dot(rows[...], up_weight[0], 1, 1)
     hidden_grad = dot(routed[...], down_weight[0], 1, 1)
@@ -113,10 +95,10 @@
     gate_grad = (hidden_grad * up_pre * silu_slope(gate_pre, gate_sigmoid)).astype(BF16)
     up_grad = (hidden_grad * gate_active).astype(BF16)
     up_out[...] = up_grad
-    for out, order in zip((kept, given), places(blocks)):
+    for out, core in ((given, 1 - my_core), (kept, my_core)):
         for j in range(0, chips, 2):
             gate_cols, up_cols = (
-                jnp.concatenate([weight[0, :, columns(order[j + i])] for i in (0, 1)], axis=1)
+                jnp.concatenate([weight[0, :, columns(j + i, core)] for i in (0, 1)], axis=1)
                 for weight in (gate_weight, up_weight)
             )
             both = dot(gate_grad, gate_cols, 1, 0) + dot(up_grad, up_cols, 1, 0)
@@ -148,54 +130,34 @@
     )(me, *parts, gate_weight, up_weight, down_weight)
 
 
-def passed_on(value):
-    count = lax.axis_size("tp")
-    return lax.ppermute(
-        value, "tp", [(t, (t + (2 if t % 2 == 0 else count - 2)) % count) for t in range(count)]
-    )
-
-
-def swapped(value, hop):
-    count = lax.axis_size("tp")
-    return lax.ppermute(value, "tp", [(t, t ^ hop) for t in range(count)])
+def along_chips(value, steps):
+    count = lax.axis_size("chip")
+    return lax.ppermute(value, "chip", [(y, (y + steps) % count) for y in range(count)])
 
 
 def to_other_core(value):
-    return swapped(value, 1)
+    return lax.ppermute(value, "core", [(0, 1), (1, 0)])
+
+
+def ring_order(chips):
+    return [0, *[k for step in range(1, chips // 2) for k in (-step, step)], -(chips // 2)]
 
 
 def all_blocks(own):
-    middle = lax.axis_size("tp") // 4
-    other = to_other_core(own)
-    pair = jnp.stack([own, other])
-    pairs = []
-    for _ in range(1, middle):
-        pair = passed_on(pair)
-        pairs.append((pair, to_other_core(pair)))
-    last = passed_on(pair[0])
-    shared = to_other_core(last)
-    return [own, other, last, shared, *[p for both in pairs for p in both]]
+    chips = lax.axis_size("chip")
+    arrived = [own]
+    for n, steps in enumerate(ring_order(chips)[1:]):
+        arrived.append(along_chips(arrived[max(0, n - 1)], 1 if steps < 0 else -1))
+    early = 2 * EARLY + 1
+    first = to_other_core(jnp.stack(arrived[:early]))
+    second = to_other_core(jnp.stack(arrived[early:]))
+    return [*arrived, first, second]
 
 
 def added_up(kept, given):
-    middle = kept.shape[0] // 2
-    other = to_other_core(given)
-
-    def pair(k):
-        at = slice(2 * k, 2 * k + 2)
-        return kept[at].astype(F32) + other[at].astype(F32)
-
-    ends = pair(0)
-    arrived = passed_on(ends[1].astype(BF16)).astype(F32)
-    for k in range(middle - 1, 0, -1):
-        value = pair(k)
-        if k == middle - 1:
-            value = value + jnp.stack([jnp.zeros_like(arrived), arrived])
-        else:
-            value = value + arrived
-        arrived = passed_on(value.astype(BF16)).astype(F32)
-    mine = ends[0] + arrived[1]
-    return (mine + to_other_core(arrived[0].astype(BF16)).astype(F32)).astype(BF16)
+    both = kept.astype(F32) + to_other_core(given).astype(F32)
+    arrived = lax.all_to_all(both.astype(BF16), "chip", split_axis=0, concat_axis=0, tiled=True)
+    return jnp.sum(arrived.astype(F32), axis=0).astype(BF16)
 
 
 def sent_to_all(value, axis):
@@ -220,12 +182,12 @@
     w_proj,
 ):
     devices = lax.axis_size("sp")
-    blocks = lax.axis_size("tp")
+    blocks = lax.axis_size(TP)
     local_tokens = routes.shape[0]
     channels = moe_in.shape[1]
     capacity = 5 * local_tokens // (2 * devices)
     slots = capacity + 1
-    me = lax.axis_index("tp").astype(jnp.int32).reshape(1)
+    me = lax.axis_index(TP).astype(jnp.int32).reshape(1)
     sent, place = send_rows(routes.T, route_weight.T, moe_in, cotangent, devices, slots)
     own = lax.all_to_all(sent, "sp", split_axis=0, concat_axis=0, tiled=True)
     proj = sent_to_all(w_proj, "sp").reshape(-1, channels)
@@ -241,7 +203,7 @@
     grad_stream = (
         cotangent.astype(F32) + dot(place, returned.reshape(devices * slots, channels), 0, 0)
     ).astype(BF16)
-    columns = lax.all_gather(grad_stream, "tp", axis=1, tiled=True)
+    columns = lax.all_gather(grad_stream, TP, axis=1, tiled=True)
     normed = (conv_pre.astype(F32) - norm_mean[:, None]) * norm_rstd[:, None]
     pre_act = normed * ln_gain[None, :] + ln_shift[None, :]
     act_sigmoid = jax.nn.sigmoid(pre_act)
@@ -251,10 +213,8 @@
     act_grad = dot(columns, proj, 1, 0)
     normed_grad = act_grad * silu_slope(pre_act, act_sigmoid) * ln_gain[None, :]
     sums = jnp.concatenate([jnp.sum(normed_grad, axis=1), jnp.sum(normed_grad * normed, axis=1)])
-    hop = 1
-    while hop < blocks:
-        sums = sums + swapped(sums, hop)
-        hop *= 2
+    sums = sent_to_all(sums[None], TP)
+    sums = jnp.sum(sums, axis=(0, 1))
     first_sum, second_sum = (sums[:local_tokens], sums[local_tokens:])
     width = channels * blocks
     conv_grad = norm_rstd[:, None] * (
@@ -274,31 +234,34 @@
 
 def solution(mesh):
     placed = (
-        P("sp", "tp"),
-        P("sp", "tp"),
+        P("sp", TP),
+        P("sp", TP),
         P("sp", None),
         P("sp", None),
-        P("sp", "tp", None),
-        P("sp", "tp", None),
-        P("sp", "tp", None),
-        P("sp", "tp"),
+        P("sp", TP, None),
+        P("sp", TP, None),
+        P("sp", TP, None),
+        P("sp", TP),
         P("sp"),
         P("sp"),
-        P("tp"),
-        P("tp"),
-        P(None, "tp"),
-        P("sp", "tp"),
+        P(TP),
+        P(TP),
+        P(None, TP),
+        P("sp", TP),
+    )
+    lines = jax.sharding.Mesh(
+        mesh.devices.reshape(mesh.devices.shape[0], -1, 2), ("sp", "chip", "core")
     )
     return jax.shard_map(
         steps,
-        mesh=mesh,
+        mesh=lines,
         in_specs=placed,
         out_specs=(
-            P("sp", "tp", None),
-            P("sp", "tp", None),
-            P("sp", "tp"),
-            P("sp", "tp"),
-            P("sp", "tp"),
+            P("sp", TP, None),
+            P("sp", TP, None),
+            P("sp", TP),
+            P("sp", TP),
+            P("sp", TP),
         ),
         check_vma=False,
     )

time: 222 us -> 207 us (0.932)
  the two profiles are of different devices: /device:TPU:14 before, /device:TPU:1 now
where the time goes in v1:
time: 207 us; the launch traced here: 206 us
  blocking collectives  93.4 us (45%)
  starting transfers between devices  52.8 us (26%)
  waiting for transfers between devices  29.4 us (14%)
  Pallas kernels  12.2 us (6%)
  matrix products  7.04 us (3%)
  local copies, waits for them, and re-layouts  6.25 us (3%)
  other arithmetic  3.67 us (2%)
    all_to_all x1, blocking collectives, added_up(): lax.all_to_all(both.astype(BF16), 'chip', split_axis=0, concat_axis=0, ti...  35.3 us
    all_to_all x1, blocking collectives, steps(): own = lax.all_to_all(sent, 'sp', split_axis=0, concat_axis=0, tiled=True)  25 us
    ppermute x7, starting transfers between devices, along_chips(): lax.ppermute(value, 'chip', [(y, (y + steps) % count) for y in range(coun...  21.9 us
    all_gather x1, blocking collectives, steps(): columns = lax.all_gather(grad_stream, TP, axis=1, tiled=True)  18.7 us
    all_to_all x1, blocking collectives, steps(): lax.all_to_all(shared, 'sp', split_axis=0, concat_axis=0, tiled=True)  14.4 us
    ppermute x3, starting transfers between devices, to_other_core(): return lax.ppermute(value, 'core', [(0, 1), (1, 0)])  12.3 us
    pallas_call x1, Pallas kernels, expert_backward(): pl.pallas_call(functools.partial(expert_body, blocks=blocks, slots=slots)...  10.1 us
    all_to_all x1, starting transfers between devices, steps(): lax.all_to_all(proj_part, 'sp', split_axis=0, concat_axis=0, tiled=True)  9.49 us
  transfers between devices with their start and end apart: 14, of which 9 were waited for; matrix products, arithmetic and copies ran while one was open for 5% of the time, Pallas kernels for 0%

profile of v1, /device:TPU:1, one launch (start us, length us, event | category | flops | bytes accessed | tf_op | source)
XLA Modules:
  0.0 205.8 jit_solution(14638946619574431968)
XLA Ops:
  0.6 2.1 %send_rows.1 = (bf16[32,32,128]{2,1,0:T(8,128)(2,1)}, bf16[512,192]{1,0:T(8,128)(2,1)}) custom-call(s32[2,192]{1,0:T(2,128)} %bitcast.101, f32[2,192]{1,0:T(2,128)} %bitcast.102, bf16[192,128]{1,0:T(8,128)(2,1)} %rows.1, bf16[192,128]{1,0:T(8,128)(2,1)} %cotangent.1), custom_call_target="tpu_custom_call" | custom-call | tf_op jit(solution)/shard_map/send_rows/pallas_call | solution.py:55
  2.7 25.0 %all_to_all.30.refs_0_ = bf16[32,32,128]{2,1,0:T(8,128)(2,1)S(1)} all-to-all(bf16[32,32,128]{2,1,0:T(8,128)(2,1)} %get-tuple-element.13), channel_id=1, replica_groups=mesh['sp'=32,'chip'=8,'core'=2] {'sp'}, dimensions={0} | all-to-all | bytes 524288 | tf_op jit(solution)/shard_map/all_to_all | solution.py:192
  27.7 3.2 %collective-permute-start = (bf16[32,32,128]{2,1,0:T(8,128)(2,1)S(1)}, bf16[32,32,128]{2,1,0:T(8,128)(2,1)S(1)}, u32[]{:S(2)}, u32[]{:S(2)}) collective-permute-start(bf16[32,32,128]{2,1,0:T(8,128)(2,1)S(1)} %all_to_all.30.refs_0_), channel_id=1, source_target_pairs={{0,2},{2,4},{4,6},{6,8},{8,10},{10,12},{12,14},{14,0},{1,3},{3,5},... | collective-permute-start | bytes 786440 | tf_op jit(solution)/shard_map/ppermute | solution.py:135
  30.9 3.8 %collective-permute-start.1 = (bf16[32,32,128]{2,1,0:T(8,128)(2,1)S(1)}, bf16[32,32,128]{2,1,0:T(8,128)(2,1)S(1)}, u32[]{:S(2)}, u32[]{:S(2)}) collective-permute-start(bf16[32,32,128]{2,1,0:T(8,128)(2,1)S(1)} %all_to_all.30.refs_0_), channel_id=1, source_target_pairs={{0,14},{2,0},{4,2},{6,4},{8,6},{10,8},{12,10},{14,12},{1,15},{3,1}... | collective-permute-start | bytes 786440 | tf_op jit(solution)/shard_map/ppermute | solution.py:135
  34.8 2.3 %collective-permute-done.refs_1_ = bf16[32,32,128]{2,1,0:T(8,128)(2,1)S(1)} collective-permute-done((bf16[32,32,128]{2,1,0:T(8,128)(2,1)S(1)}, bf16[32,32,128]{2,1,0:T(8,128)(2,1)S(1)}, u32[]{:S(2)}, u32[]{:S(2)}) %collective-permute-start) | collective-permute-done | bytes 262176 | tf_op jit(solution)/shard_map/ppermute | solution.py:135
  37.1 1.9 collective-permute-start.2
  39.0 4.6 %collective-permute-start.3 = (bf16[32,32,128]{2,1,0:T(8,128)(2,1)S(1)}, bf16[32,32,128]{2,1,0:T(8,128)(2,1)S(1)}, u32[]{:S(2)}, u32[]{:S(2)}) collective-permute-start(bf16[32,32,128]{2,1,0:T(8,128)(2,1)S(1)} %collective-permute-done.1.refs_2_), channel_id=1, source_target_pairs={{0,14},{2,0},{4,2},{6,4},{8,6},{10,8},{12,10},{14,12},{1,15},{3,1}... | collective-permute-start | bytes 786440 | tf_op jit(solution)/shard_map/ppermute | solution.py:135
  43.6 1.8 collective-permute-done.2.refs_3_
  45.4 1.9 collective-permute-start.4
  47.3 0.7 bitcast_dynamic-update-slice_fusion.4
  48.0 4.6 %collective-permute-start.5 = (bf16[32,32,128]{2,1,0:T(8,128)(2,1)S(1)}, bf16[32,32,128]{2,1,0:T(8,128)(2,1)S(1)}, u32[]{:S(2)}, u32[]{:S(2)}) collective-permute-start(bf16[32,32,128]{2,1,0:T(8,128)(2,1)S(1)} %collective-permute-done.3.refs_4_), channel_id=1, source_target_pairs={{0,14},{2,0},{4,2},{6,4},{8,6},{10,8},{12,10},{14,12},{1,15},{3,1}... | collective-permute-start | bytes 786440 | tf_op jit(solution)/shard_map/ppermute | solution.py:135
  52.6 0.7 bitcast_dynamic-update-slice_fusion.3
  53.3 0.4 collective-permute-done.4.refs_5_
  53.7 1.9 collective-permute-start.6
  55.6 0.7 bitcast_dynamic-update-slice_fusion.2
  56.4 0.8 bitcast_dynamic-update-slice_fusion.1
  57.1 4.9 %collective-permute-done.6.refs_7_ = bf16[32,32,128]{2,1,0:T(8,128)(2,1)S(1)} collective-permute-done((bf16[32,32,128]{2,1,0:T(8,128)(2,1)S(1)}, bf16[32,32,128]{2,1,0:T(8,128)(2,1)S(1)}, u32[]{:S(2)}, u32[]{:S(2)}) %collective-permute-start.6) | collective-permute-done | bytes 262176 | tf_op jit(solution)/shard_map/ppermute | solution.py:135
  62.0 0.8 bitcast_dynamic-update-slice_fusion
  62.8 8.4 %collective-permute-start.8 = (bf16[5,32,32,128]{3,2,1,0:T(8,128)(2,1)}, bf16[5,32,32,128]{3,2,1,0:T(8,128)(2,1)}, u32[]{:S(2)}, u32[]{:S(2)}) collective-permute-start(bf16[5,32,32,128]{3,2,1,0:T(8,128)(2,1)} %bitcast_dynamic-update-slice_fusion), channel_id=1, source_target_pairs={{0,1},{1,0},{2,3},{3,2},{4,5},{5,4},{6,7},{7,6},{8,9},{9,8},{10,11... | collective-permute-start | bytes 3932168 | tf_op jit(solution)/shard_map/ppermute | solution.py:139
  71.2 0.1 pad_maximum_fusion
  71.3 1.9 collective-permute-start.7
  73.2 2.2 %collective-permute-done.7.refs_8_ = bf16[3,32,32,128]{3,2,1,0:T(8,128)(2,1)S(1)} collective-permute-done((bf16[3,32,32,128]{3,2,1,0:T(8,128)(2,1)S(1)}, bf16[3,32,32,128]{3,2,1,0:T(8,128)(2,1)S(1)}, u32[]{:S(2)}, u32[]{:S(2)}) %collective-permute-start.7) | collective-permute-done | bytes 786464 | tf_op jit(solution)/shard_map/ppermute | solution.py:139
  75.5 0.9 copy-done.19
  76.4 10.1 %expert_backward.1 = (bf16[512,2048]{1,0:T(8,128)(2,1)}, bf16[512,2048]{1,0:T(8,128)(2,1)}, bf16[512,224]{1,0:T(8,128)(2,1)}, bf16[512,224]{1,0:T(8,128)(2,1)}, ...) custom-call(s32[1]{0:T(128)} %bitcast.me, bf16[32,32,128]{2,1,0:T(8,128)(2,1)} %copy-done.1, ...), custom_call_target="tpu_custom_call" | custom-call | flops 2348810240 | bytes 12582912 | tf_op jit(solution)/shard_map/expert_backward/pallas_call | solution.py:114
  86.4 2.0 collective-permute-start.9
  88.5 2.7 %collective-permute-done.9 = bf16[8,512,128]{2,1,0:T(8,128)(2,1)S(1)} collective-permute-done((bf16[8,512,128]{2,1,0:T(8,128)(2,1)}, bf16[8,512,128]{2,1,0:T(8,128)(2,1)S(1)}, u32[]{:S(2)}, u32[]{:S(2)}) %collective-permute-start.9) | collective-permute-done | bytes 1048608 | tf_op jit(solution)/shard_map/ppermute | solution.py:139
  91.2 1.5 add_convert_fusion
  92.7 35.3 %all_to_all.31 = bf16[8,512,128]{2,1,0:T(8,128)(2,1)S(1)} all-to-all(bf16[8,512,128]{2,1,0:T(8,128)(2,1)S(1)} %add_convert_fusion), channel_id=1, replica_groups=mesh['sp'=32,'chip'=8,'core'=2] {'chip'}, dimensions={0} | all-to-all | bytes 2097152 | tf_op jit(solution)/shard_map/all_to_all | solution.py:159
  128.0 0.1 reduce_sum.48
  128.1 14.4 %all_to_all.32 = bf16[32,16,128]{2,1,0:T(8,128)(2,1)S(1)} all-to-all(bf16[32,16,128]{2,1,0:T(8,128)(2,1)S(1)} %bitcast.96), channel_id=1, replica_groups=mesh['sp'=32,'chip'=8,'core'=2] {'sp'}, dimensions={0} | all-to-all | bytes 262144 | tf_op jit(solution)/shard_map/all_to_all | solution.py:200
  142.6 0.9 broadcast_in_dim.10
  143.5 4.0 %all-to-all-start.4 = ((bf16[32,64,128]{2,1,0:T(8,128)(2,1)}), bf16[32,64,128]{2,1,0:T(8,128)(2,1)S(1)}, u32[]{:S(2)}, u32[]{:S(2)}) async-start(bf16[32,64,128]{2,1,0:T(8,128)(2,1)} %broadcast_in_dim.10), calls=%async_computation.4 | async-start | bytes 1048576 | tf_op jit(solution)/shard_map/all_to_all | solution.py:165
  147.6 0.3 fusion.3
  147.9 18.7 %all_gather.3 = bf16[192,2048]{1,0:T(8,128)(2,1)S(1)} all-gather(bf16[192,128]{1,0:T(8,128)(2,1)S(1)} %fusion.3), channel_id=1, replica_groups=mesh['sp'=32,'chip'=8,'core'=2] {'chip','core'}, dimensions={1}, use_global_device_ids=true | all-gather | bytes 835584 | tf_op jit(solution)/shard_map/all_gather | solution.py:206
  166.6 0.5 fusion.100
  167.2 0.6 broadcast_in_dim.11
  167.8 3.8 %all-to-all-start.5 = ((f32[16,1,384]{2,1,0:T(1,128)}), f32[16,1,384]{2,1,0:T(1,128)S(1)}, u32[]{:S(2)}, u32[]{:S(2)}) async-start(f32[16,1,384]{2,1,0:T(1,128)} %broadcast_in_dim.11), calls=%async_computation.5 | async-start | bytes 49152 | tf_op jit(solution)/shard_map/all_to_all | solution.py:165
  171.6 1.4 convolution_convert_fusion.2
  173.0 6.0 %all-to-all-done.5 = f32[16,1,384]{2,1,0:T(1,128)S(1)} async-done(((f32[16,1,384]{2,1,0:T(1,128)}), f32[16,1,384]{2,1,0:T(1,128)S(1)}, u32[]{:S(2)}, u32[]{:S(2)}) %all-to-all-start.5) | async-done | bytes 24608 | tf_op jit(solution)/shard_map/all_to_all | solution.py:165
  179.0 9.5 %all-to-all-start.3 = ((bf16[32,64,128]{2,1,0:T(8,128)(2,1)}), bf16[32,64,128]{2,1,0:T(8,128)(2,1)S(1)}, u32[]{:S(2)}, u32[]{:S(2)}) async-start(bf16[32,64,128]{2,1,0:T(8,128)(2,1)} %bitcast.15), calls=%async_computation.3 | async-start | bytes 1048576 | tf_op jit(solution)/shard_map/all_to_all | solution.py:212
  188.5 3.3 %fusion.1 = bf16[1,224,2048]{2,1,0:T(8,128)(2,1)} fusion(bf16[512,224]{1,0:T(8,128)(2,1)S(1)} %copy-done.3, bf16[512,2048]{1,0:T(8,128)(2,1)} %get-tuple-element.17), kind=kOutput, calls=%fused_computation.3 | convolution fusion | flops 470220800 | bytes 3244032 | tf_op jit(solution)/shard_map/dot_general | solution.py:17
  192.0 0.2 subtract_multiply_fusion
  192.2 1.3 collective-permute-start.10
  193.5 1.6 fusion
  195.1 2.4 %collective-permute-done.10 = f32[30,128]{1,0:T(8,128)S(1)} collective-permute-done((f32[30,128]{1,0:T(8,128)S(1)}, f32[30,128]{1,0:T(8,128)S(1)}, u32[]{:S(2)}, u32[]{:S(2)}) %collective-permute-start.10) | collective-permute-done | bytes 15392 | tf_op jit(solution)/shard_map/ppermute | solution.py:224
  197.5 0.9 fusion.8
  198.4 6.7 %all-to-all-done.3 = bf16[32,64,128]{2,1,0:T(8,128)(2,1)S(1)} async-done(((bf16[32,64,128]{2,1,0:T(8,128)(2,1)}), bf16[32,64,128]{2,1,0:T(8,128)(2,1)S(1)}, u32[]{:S(2)}, u32[]{:S(2)}) %all-to-all-start.3) | async-done | bytes 524320 | tf_op jit(solution)/shard_map/all_to_all | solution.py:212
  205.1 0.7 convert_reduce_fusion
  (54 shorter events, 0.3 us)
Async XLA Ops:
  27.7 43.4 %copy-start.1 = (bf16[32,32,128]{2,1,0:T(8,128)(2,1)}, bf16[32,32,128]{2,1,0:T(8,128)(2,1)S(1)}, u32[]{:S(2)}) copy-start(bf16[32,32,128]{2,1,0:T(8,128)(2,1)S(1)} %all_to_all.30.refs_0_) | copy-start | bytes 786436
  27.7 9.3 %collective-permute-start = (bf16[32,32,128]{2,1,0:T(8,128)(2,1)S(1)}, bf16[32,32,128]{2,1,0:T(8,128)(2,1)S(1)}, u32[]{:S(2)}, u32[]{:S(2)}) collective-permute-start(bf16[32,32,128]{2,1,0:T(8,128)(2,1)S(1)} %all_to_all.30.refs_0_), channel_id=1, source_target_pairs={{0,2},{2,4},{4,6},{6,8},{8,10},{10,12},{12,14},{14,0},{1,3},{3,5},... | collective-permute-start | bytes 786440 | tf_op jit(solution)/shard_map/ppermute | solution.py:135
  30.9 8.0 %collective-permute-start.1 = (bf16[32,32,128]{2,1,0:T(8,128)(2,1)S(1)}, bf16[32,32,128]{2,1,0:T(8,128)(2,1)S(1)}, u32[]{:S(2)}, u32[]{:S(2)}) collective-permute-start(bf16[32,32,128]{2,1,0:T(8,128)(2,1)S(1)} %all_to_all.30.refs_0_), channel_id=1, source_target_pairs={{0,14},{2,0},{4,2},{6,4},{8,6},{10,8},{12,10},{14,12},{1,15},{3,1}... | collective-permute-start | bytes 786440 | tf_op jit(solution)/shard_map/ppermute | solution.py:135
  37.1 34.1 %copy-start.10 = (bf16[32,32,128]{2,1,0:T(8,128)(2,1)}, bf16[32,32,128]{2,1,0:T(8,128)(2,1)S(1)}, u32[]{:S(2)}) copy-start(bf16[32,32,128]{2,1,0:T(8,128)(2,1)S(1)} %collective-permute-done.refs_1_) | copy-start | bytes 786436
  37.1 8.3 %collective-permute-start.2 = (bf16[32,32,128]{2,1,0:T(8,128)(2,1)S(1)}, bf16[32,32,128]{2,1,0:T(8,128)(2,1)S(1)}, u32[]{:S(2)}, u32[]{:S(2)}) collective-permute-start(bf16[32,32,128]{2,1,0:T(8,128)(2,1)S(1)} %collective-permute-done.refs_1_), channel_id=1, source_target_pairs={{0,2},{2,4},{4,6},{6,8},{8,10},{10,12},{12,14},{14,0},{1,3},{3,5},... | collective-permute-start | bytes 786440 | tf_op jit(solution)/shard_map/ppermute | solution.py:135
  39.0 32.2 %copy-start.11 = (bf16[32,32,128]{2,1,0:T(8,128)(2,1)}, bf16[32,32,128]{2,1,0:T(8,128)(2,1)S(1)}, u32[]{:S(2)}) copy-start(bf16[32,32,128]{2,1,0:T(8,128)(2,1)S(1)} %collective-permute-done.1.refs_2_) | copy-start | bytes 786436
  39.0 9.0 %collective-permute-start.3 = (bf16[32,32,128]{2,1,0:T(8,128)(2,1)S(1)}, bf16[32,32,128]{2,1,0:T(8,128)(2,1)S(1)}, u32[]{:S(2)}, u32[]{:S(2)}) collective-permute-start(bf16[32,32,128]{2,1,0:T(8,128)(2,1)S(1)} %collective-permute-done.1.refs_2_), channel_id=1, source_target_pairs={{0,14},{2,0},{4,2},{6,4},{8,6},{10,8},{12,10},{14,12},{1,15},{3,1}... | collective-permute-start | bytes 786440 | tf_op jit(solution)/shard_map/ppermute | solution.py:135
  45.4 25.8 %copy-start.4 = (bf16[32,32,128]{2,1,0:T(8,128)(2,1)}, bf16[32,32,128]{2,1,0:T(8,128)(2,1)S(1)}, u32[]{:S(2)}) copy-start(bf16[32,32,128]{2,1,0:T(8,128)(2,1)S(1)} %collective-permute-done.2.refs_3_) | copy-start | bytes 786436
  45.4 8.3 %collective-permute-start.4 = (bf16[32,32,128]{2,1,0:T(8,128)(2,1)S(1)}, bf16[32,32,128]{2,1,0:T(8,128)(2,1)S(1)}, u32[]{:S(2)}, u32[]{:S(2)}) collective-permute-start(bf16[32,32,128]{2,1,0:T(8,128)(2,1)S(1)} %collective-permute-done.2.refs_3_), channel_id=1, source_target_pairs={{0,2},{2,4},{4,6},{6,8},{8,10},{10,12},{12,14},{14,0},{1,3},{3,5},... | collective-permute-start | bytes 786440 | tf_op jit(solution)/shard_map/ppermute | solution.py:135
  48.0 23.3 %copy-start.5 = (bf16[32,32,128]{2,1,0:T(8,128)(2,1)}, bf16[32,32,128]{2,1,0:T(8,128)(2,1)S(1)}, u32[]{:S(2)}) copy-start(bf16[32,32,128]{2,1,0:T(8,128)(2,1)S(1)} %collective-permute-done.3.refs_4_) | copy-start | bytes 786436
  48.0 8.3 %collective-permute-start.5 = (bf16[32,32,128]{2,1,0:T(8,128)(2,1)S(1)}, bf16[32,32,128]{2,1,0:T(8,128)(2,1)S(1)}, u32[]{:S(2)}, u32[]{:S(2)}) collective-permute-start(bf16[32,32,128]{2,1,0:T(8,128)(2,1)S(1)} %collective-permute-done.3.refs_4_), channel_id=1, source_target_pairs={{0,14},{2,0},{4,2},{6,4},{8,6},{10,8},{12,10},{14,12},{1,15},{3,1}... | collective-permute-start | bytes 786440 | tf_op jit(solution)/shard_map/ppermute | solution.py:135
  53.7 17.6 %copy-start.6 = (bf16[32,32,128]{2,1,0:T(8,128)(2,1)}, bf16[32,32,128]{2,1,0:T(8,128)(2,1)S(1)}, u32[]{:S(2)}) copy-start(bf16[32,32,128]{2,1,0:T(8,128)(2,1)S(1)} %collective-permute-done.4.refs_5_) | copy-start | bytes 786436
  53.7 8.3 %collective-permute-start.6 = (bf16[32,32,128]{2,1,0:T(8,128)(2,1)S(1)}, bf16[32,32,128]{2,1,0:T(8,128)(2,1)S(1)}, u32[]{:S(2)}, u32[]{:S(2)}) collective-permute-start(bf16[32,32,128]{2,1,0:T(8,128)(2,1)S(1)} %collective-permute-done.4.refs_5_), channel_id=1, source_target_pairs={{0,2},{2,4},{4,6},{6,8},{8,10},{10,12},{12,14},{14,0},{1,3},{3,5},... | collective-permute-start | bytes 786440 | tf_op jit(solution)/shard_map/ppermute | solution.py:135
  56.3 15.0 %copy-start.7 = (bf16[32,32,128]{2,1,0:T(8,128)(2,1)}, bf16[32,32,128]{2,1,0:T(8,128)(2,1)S(1)}, u32[]{:S(2)}) copy-start(bf16[32,32,128]{2,1,0:T(8,128)(2,1)S(1)} %collective-permute-done.5.refs_6_) | copy-start | bytes 786436
  62.0 13.5 %copy-start.8 = (bf16[32,32,128]{2,1,0:T(8,128)(2,1)}, bf16[32,32,128]{2,1,0:T(8,128)(2,1)S(1)}, u32[]{:S(2)}) copy-start(bf16[32,32,128]{2,1,0:T(8,128)(2,1)S(1)} %collective-permute-done.6.refs_7_) | copy-start | bytes 786436
  62.8 12.7 %collective-permute-start.8 = (bf16[5,32,32,128]{3,2,1,0:T(8,128)(2,1)}, bf16[5,32,32,128]{3,2,1,0:T(8,128)(2,1)}, u32[]{:S(2)}, u32[]{:S(2)}) collective-permute-start(bf16[5,32,32,128]{3,2,1,0:T(8,128)(2,1)} %bitcast_dynamic-update-slice_fusion), channel_id=1, source_target_pairs={{0,1},{1,0},{2,3},{3,2},{4,5},{5,4},{6,7},{7,6},{8,9},{9,8},{10,11... | collective-permute-start | bytes 3932168 | tf_op jit(solution)/shard_map/ppermute | solution.py:139
  71.3 4.2 %collective-permute-start.7 = (bf16[3,32,32,128]{3,2,1,0:T(8,128)(2,1)S(1)}, bf16[3,32,32,128]{3,2,1,0:T(8,128)(2,1)S(1)}, u32[]{:S(2)}, u32[]{:S(2)}) collective-permute-start(bf16[3,32,32,128]{3,2,1,0:T(8,128)(2,1)S(1)} %pad_maximum_fusion), channel_id=1, source_target_pairs={{0,1},{1,0},{2,3},{3,2},{4,5},{5,4},{6,7},{7,6},{8,9},{9,8},{10,11... | collective-permute-start | bytes 2359304 | tf_op jit(solution)/shard_map/ppermute | solution.py:139
  75.5 0.9 copy-start.19
  86.4 4.8 %collective-permute-start.9 = (bf16[8,512,128]{2,1,0:T(8,128)(2,1)}, bf16[8,512,128]{2,1,0:T(8,128)(2,1)S(1)}, u32[]{:S(2)}, u32[]{:S(2)}) collective-permute-start(bf16[8,512,128]{2,1,0:T(8,128)(2,1)} %get-tuple-element.20), channel_id=1, source_target_pairs={{0,1},{1,0},{2,3},{3,2},{4,5},{5,4},{6,7},{7,6},{8,9},{9,8},{10,11... | collective-permute-start | bytes 3145736 | tf_op jit(solution)/shard_map/ppermute | solution.py:139
  92.7 49.9 %copy-start.15 = (bf16[64,128]{1,0:T(8,128)(2,1)S(1)}, bf16[64,128]{1,0:T(8,128)(2,1)}, u32[]{:S(2)}) copy-start(bf16[64,128]{1,0:T(8,128)(2,1)} %param.27) | copy-start | bytes 49156
  128.0 19.6 %copy-start.16 = (f32[31,128]{1,0:T(8,128)S(1)}, f32[31,128]{1,0:T(8,128)}, u32[]{:S(2)}) copy-start(f32[31,128]{1,0:T(8,128)} %param.26) | copy-start | bytes 47620
  128.0 19.6 %copy-start.9 = (bf16[512,192]{1,0:T(8,128)(2,1)S(1)}, bf16[512,192]{1,0:T(8,128)(2,1)}, u32[]{:S(2)}) copy-start(bf16[512,192]{1,0:T(8,128)(2,1)} %get-tuple-element.18) | copy-start | bytes 589828
  128.0 19.6 %copy-start.13 = (bf16[192,128]{1,0:T(8,128)(2,1)S(1)}, bf16[192,128]{1,0:T(8,128)(2,1)}, u32[]{:S(2)}) copy-start(bf16[192,128]{1,0:T(8,128)(2,1)} %cotangent.1) | copy-start | bytes 147460
  143.5 23.1 %copy-start.14 = (bf16[192,128]{1,0:T(8,128)(2,1)S(1)}, bf16[192,128]{1,0:T(8,128)(2,1)}, u32[]{:S(2)}) copy-start(bf16[192,128]{1,0:T(8,128)(2,1)} %param.21) | copy-start | bytes 147460
  143.5 23.1 %copy-start.17 = (f32[192]{0:T(256)S(1)}, f32[192]{0:T(256)}, u32[]{:S(2)}) copy-start(f32[192]{0:T(256)} %param.23) | copy-start | bytes 2308
  143.5 23.1 %copy-start.18 = (f32[192]{0:T(256)S(1)}, f32[192]{0:T(256)}, u32[]{:S(2)}) copy-start(f32[192]{0:T(256)} %param.22) | copy-start | bytes 2308
  143.5 23.1 %copy-start.20 = (f32[128]{0:T(128)S(1)}, f32[128]{0:T(128)}, u32[]{:S(2)}) copy-start(f32[128]{0:T(128)} %param.25) | copy-start | bytes 1540
  143.5 23.1 %copy-start.21 = (f32[128]{0:T(128)S(1)}, f32[128]{0:T(128)}, u32[]{:S(2)}) copy-start(f32[128]{0:T(128)} %param.24) | copy-start | bytes 1540
  143.5 23.1 %all-to-all-start.4 = ((bf16[32,64,128]{2,1,0:T(8,128)(2,1)}), bf16[32,64,128]{2,1,0:T(8,128)(2,1)S(1)}, u32[]{:S(2)}, u32[]{:S(2)}) async-start(bf16[32,64,128]{2,1,0:T(8,128)(2,1)} %broadcast_in_dim.10), calls=%async_computation.4 | async-start | bytes 1048576 | tf_op jit(solution)/shard_map/all_to_all | solution.py:165
  147.9 19.3 %copy-start.12 = (bf16[192,128]{1,0:T(8,128)(2,1)}, bf16[192,128]{1,0:T(8,128)(2,1)S(1)}, u32[]{:S(2)}) copy-start(bf16[192,128]{1,0:T(8,128)(2,1)S(1)} %fusion.3) | copy-start | bytes 147460
  167.2 21.3 %copy-start.3 = (bf16[512,224]{1,0:T(8,128)(2,1)S(1)}, bf16[512,224]{1,0:T(8,128)(2,1)}, u32[]{:S(2)}) copy-start(bf16[512,224]{1,0:T(8,128)(2,1)} %get-tuple-element.16) | copy-start | bytes 688132
  167.8 11.2 %all-to-all-start.5 = ((f32[16,1,384]{2,1,0:T(1,128)}), f32[16,1,384]{2,1,0:T(1,128)S(1)}, u32[]{:S(2)}, u32[]{:S(2)}) async-start(f32[16,1,384]{2,1,0:T(1,128)} %broadcast_in_dim.11), calls=%async_computation.5 | async-start | bytes 49152 | tf_op jit(solution)/shard_map/all_to_all | solution.py:165
  179.0 26.1 %all-to-all-start.3 = ((bf16[32,64,128]{2,1,0:T(8,128)(2,1)}), bf16[32,64,128]{2,1,0:T(8,128)(2,1)S(1)}, u32[]{:S(2)}, u32[]{:S(2)}) async-start(bf16[32,64,128]{2,1,0:T(8,128)(2,1)} %bitcast.15), calls=%async_computation.3 | async-start | bytes 1048576 | tf_op jit(solution)/shard_map/all_to_all | solution.py:212
  188.5 5.0 %copy-start = (bf16[512,2048]{1,0:T(8,128)(2,1)S(1)}, bf16[512,2048]{1,0:T(8,128)(2,1)}, u32[]{:S(2)}) copy-start(bf16[512,2048]{1,0:T(8,128)(2,1)} %get-tuple-element.15) | copy-start | bytes 6291460
  188.5 5.0 %copy-start.2 = (bf16[512,224]{1,0:T(8,128)(2,1)S(1)}, bf16[512,224]{1,0:T(8,128)(2,1)}, u32[]{:S(2)}) copy-start(bf16[512,224]{1,0:T(8,128)(2,1)} %get-tuple-element.14) | copy-start | bytes 688132
  192.2 5.3 %collective-permute-start.10 = (f32[30,128]{1,0:T(8,128)S(1)}, f32[30,128]{1,0:T(8,128)S(1)}, u32[]{:S(2)}, u32[]{:S(2)}) collective-permute-start(f32[30,128]{1,0:T(8,128)S(1)} %slice.256), channel_id=1, source_target_pairs={{16,0},{32,16},{48,32},{64,48},{80,64},{96,80},{112,96},{128,112},... | collective-permute-start | bytes 46088 | tf_op jit(solution)/shard_map/ppermute | solution.py:224

commit v2 on v1

--- a/solution.py
+++ b/solution.py
@@ -8,7 +8,8 @@
 
 
 TP = ("chip", "core")
-EARLY = 1
+BATCHES = (3, 2, 2, 1)
+EARLY = 2
 BF16 = jnp.bfloat16
 F32 = jnp.float32
 
@@ -19,6 +20,10 @@
 
 def silu_slope(pre_value, sigmoid_value):
     return sigmoid_value * (1.0 + pre_value * (1.0 - sigmoid_value))
+
+
+def near(*arrays):
+    return tuple(pltpu.with_memory_space_constraint(a, pltpu.VMEM) for a in arrays)
 
 
 def whole(count, space=pltpu.VMEM):
@@ -64,31 +69,87 @@
     )(routes, weights, rows, cotangent)
 
 
-def expert_body(me, *refs, blocks, slots):
+def columns(chip, core, width):
+    return pl.ds(pl.multiple_of((2 * chip + core) * width, width), width)
+
+
+def put_blocks(me, steps, mine, others, rows, routed, blocks, slots):
     chips = blocks // 2
-    mine, shared = (refs[:chips], refs[chips : chips + 2])
-    gate_weight, up_weight, down_weight = refs[chips + 2 : chips + 5]
-    rows, routed, hidden_out, up_out, kept, given = refs[chips + 5 :]
     width = mine[0].shape[-1]
     count = mine[0].shape[-3] * slots
     my_chip, my_core = (me[0] // 2, lax.rem(me[0], 2))
-
-    def columns(chip, core):
-        return pl.ds(pl.multiple_of((2 * chip + core) * width, width), width)
-
-    def put(cols, part):
-        rows[:, cols] = part[:, :slots, :].reshape(count, width)
-        routed[:, cols] = part[:, slots:, :].reshape(count, width)
-
-    early = 2 * EARLY + 1
-    for n, steps in enumerate(ring_order(chips)):
-        chip = lax.rem(my_chip + steps + chips, chips)
-        put(columns(chip, my_core), mine[n])
-        batch, at = (shared[0], n) if n < early else (shared[1], n - early)
-        put(columns(chip, 1 - my_core), batch[at])
-    gate_pre = dot(rows[...], gate_weight[0], 1, 1)
-    up_pre = dot(rows[...], up_weight[0], 1, 1)
-    hidden_grad = dot(routed[...], down_weight[0], 1, 1)
+    found = []
+    for step, part, (batch, at) in zip(steps, mine, others):
+        chip = lax.rem(my_chip + step + chips, chips)
+        for core, value in ((my_core, part), (1 - my_core, batch.at[at])):
+            cols = columns(chip, core, width)
+            rows[:, cols] = value[:, :slots, :].reshape(count, width)
+            routed[:, cols] = value[:, slots:, :].reshape(count, width)
+        found.append(pl.ds(pl.multiple_of(chip * 2 * width, 2 * width), 2 * width))
+    return found
+
+
+def products(rows, routed, weights, found):
+    sums = [None] * 3
+    for cols in found:
+        for n, (left, weight) in enumerate(zip((rows, rows, routed), weights)):
+            part = dot(left[:, cols], weight[:, cols], 1, 1)
+            sums[n] = part if sums[n] is None else sums[n] + part
+    return sums
+
+
+def first_body(me, *refs, blocks, slots, batches):
+    count = sum(batches)
+    mine, shared = (refs[:count], refs[count : count + len(batches)])
+    weights = refs[count + len(batches) : count + len(batches) + 3]
+    rows, routed, *sums, held0, held1, held2 = refs[count + len(batches) + 3 :]
+    others = [(batch, at) for batch, size in zip(shared, batches) for at in range(size)]
+    held = (held0, held1, held2)
+    for weight, keep in zip(weights, held):
+        keep[...] = weight[0]
+    steps = ring_order(blocks // 2)[:count]
+    found = put_blocks(me, steps, mine, others, rows, routed, blocks, slots)
+    for out, value in zip(sums, products(rows, routed, held, found)):
+        out[...] = value
+
+
+def first_products(me, mine, shared, weights, slots, blocks):
+    batches = [b.shape[0] for b in shared]
+    experts, _, _ = mine[0].shape
+    count, hidden, channels = (experts * slots, weights[0].shape[1], weights[0].shape[2])
+    return pl.pallas_call(
+        functools.partial(first_body, blocks=blocks, slots=slots, batches=batches),
+        in_specs=whole(1, pltpu.SMEM) + whole(len(mine) + len(shared) + 3),
+        out_specs=whole(8),
+        out_shape=(
+            *[pltpu.VMEM((count, channels), BF16)] * 2,
+            *[pltpu.VMEM((count, hidden), F32)] * 3,
+            *[pltpu.VMEM((hidden, channels), BF16)] * 3,
+        ),
+        cost_estimate=pl.CostEstimate(
+            flops=4 * count * hidden * channels, transcendentals=0, bytes_accessed=12 * 1024 * 1024
+        ),
+        compiler_params=pltpu.CompilerParams(vmem_limit_bytes=12 * 1024 * 1024),
+        name="first_products",
+    )(me, *mine, *shared, *weights)
+
+
+def rest_body(me, *refs, blocks, slots, batches):
+    chips = blocks // 2
+    count = sum(batches)
+    mine, shared = (refs[:count], refs[count : count + len(batches)])
+    _, _, gate_sum, up_sum, down_sum, *weights = refs[count + len(batches) : count + len(batches) + 8]
+    rows, routed, hidden_out, up_out, kept, given = refs[count + len(batches) + 8 :]
+    others = [(batch, at) for batch, size in zip(shared, batches) for at in range(size)]
+    steps = ring_order(chips)[-count:]
+    found = put_blocks(me, steps, mine, others, rows, routed, blocks, slots)
+    gate_pre, up_pre, hidden_grad = products(rows, routed, weights, found)
+    gate_pre = gate_pre + gate_sum[...]
+    up_pre = up_pre + up_sum[...]
+    hidden_grad = hidden_grad + down_sum[...]
+    gate_weight, up_weight = weights[:2]
+    width = mine[0].shape[-1]
+    my_core = lax.rem(me[0], 2)
     gate_sigmoid = jax.nn.sigmoid(gate_pre)
     gate_active = gate_pre * gate_sigmoid
     hidden_out[...] = (gate_active * up_pre).astype(BF16)
@@ -98,7 +159,7 @@
     for out, core in ((given, 1 - my_core), (kept, my_core)):
         for j in range(0, chips, 2):
             gate_cols, up_cols = (
-                jnp.concatenate([weight[0, :, columns(j + i, core)] for i in (0, 1)], axis=1)
+                jnp.concatenate([weight[:, columns(j + i, core, width)] for i in (0, 1)], axis=1)
                 for weight in (gate_weight, up_weight)
             )
             both = dot(gate_grad, gate_cols, 1, 0) + dot(up_grad, up_cols, 1, 0)
@@ -106,28 +167,29 @@
                 out[j + i] = both[:, i * width : (i + 1) * width].astype(BF16)
 
 
-def expert_backward(me, parts, gate_weight, up_weight, down_weight, slots, blocks):
-    experts, _, width = parts[0].shape
-    count = experts * slots
-    _, hidden, channels = gate_weight.shape
-    work = 2 * count * hidden * channels
+def rest_products(me, mine, shared, early, slots, blocks):
+    batches = [b.shape[0] for b in shared]
+    count, channels = early[0].shape
+    hidden = early[2].shape[1]
+    first = 1 + len(mine) + len(shared)
     return pl.pallas_call(
-        functools.partial(expert_body, blocks=blocks, slots=slots),
-        in_specs=whole(1, pltpu.SMEM) + whole(len(parts) + 3),
+        functools.partial(rest_body, blocks=blocks, slots=slots, batches=batches),
+        in_specs=whole(1, pltpu.SMEM) + whole(len(mine) + len(shared) + 8),
         out_specs=whole(6),
         out_shape=(
-            jax.ShapeDtypeStruct((count, channels), BF16),
-            jax.ShapeDtypeStruct((count, channels), BF16),
-            jax.ShapeDtypeStruct((count, hidden), BF16),
-            jax.ShapeDtypeStruct((count, hidden), BF16),
-            jax.ShapeDtypeStruct((blocks // 2, count, width), BF16),
-            jax.ShapeDtypeStruct((blocks // 2, count, width), BF16),
-        ),
+            *[pltpu.VMEM((count, channels), BF16)] * 2,
+            *[pltpu.VMEM((count, hidden), BF16)] * 2,
+            *[pltpu.VMEM((blocks // 2, count, channels // blocks), BF16)] * 2,
+        ),
+        input_output_aliases={first: 0, first + 1: 1},
         cost_estimate=pl.CostEstimate(
-            flops=5 * work, transcendentals=count * hidden, bytes_accessed=12 * 1024 * 1024
-        ),
-        name="expert_backward",
-    )(me, *parts, gate_weight, up_weight, down_weight)
+            flops=6 * count * hidden * channels,
+            transcendentals=count * hidden,
+            bytes_accessed=12 * 1024 * 1024,
+        ),
+        compiler_params=pltpu.CompilerParams(vmem_limit_bytes=12 * 1024 * 1024),
+        name="rest_products",
+    )(me, *mine, *shared, *near(*early))
 
 
 def along_chips(value, steps):
@@ -148,10 +210,11 @@
     arrived = [own]
     for n, steps in enumerate(ring_order(chips)[1:]):
         arrived.append(along_chips(arrived[max(0, n - 1)], 1 if steps < 0 else -1))
-    early = 2 * EARLY + 1
-    first = to_other_core(jnp.stack(arrived[:early]))
-    second = to_other_core(jnp.stack(arrived[early:]))
-    return [*arrived, first, second]
+    shared, at = ([], 0)
+    for size in BATCHES:
+        shared.append(to_other_core(jnp.stack(arrived[at : at + size])))
+        at += size
+    return arrived, shared
 
 
 def added_up(kept, given):
@@ -191,9 +254,11 @@
     sent, place = send_rows(routes.T, route_weight.T, moe_in, cotangent, devices, slots)
     own = lax.all_to_all(sent, "sp", split_axis=0, concat_axis=0, tiled=True)
     proj = sent_to_all(w_proj, "sp").reshape(-1, channels)
-    parts = all_blocks(own)
-    rows, routed, hidden, up_grad, kept, given = expert_backward(
-        me, parts, w_gate, w_up, w_down, slots, blocks
+    mine, others = all_blocks(own)
+    done = sum(BATCHES[:EARLY])
+    early = first_products(me, mine[:done], others[:EARLY], (w_gate, w_up, w_down), slots, blocks)
+    rows, routed, hidden, up_grad, kept, given = rest_products(
+        me, mine[done:], others[EARLY:], early, slots, blocks
     )
     shared = added_up(kept, given)
     shared = shared.reshape(devices, slots, channels)
@@ -213,8 +278,8 @@
     act_grad = dot(columns, proj, 1, 0)
     normed_grad = act_grad * silu_slope(pre_act, act_sigmoid) * ln_gain[None, :]
     sums = jnp.concatenate([jnp.sum(normed_grad, axis=1), jnp.sum(normed_grad * normed, axis=1)])
-    sums = sent_to_all(sums[None], TP)
-    sums = jnp.sum(sums, axis=(0, 1))
+    sums = lax.all_gather(sums, TP, axis=0, tiled=False)
+    sums = jnp.sum(sums, axis=0)
     first_sum, second_sum = (sums[:local_tokens], sums[local_tokens:])
     width = channels * blocks
     conv_grad = norm_rstd[:, None] * (

time: 207 us -> 216 us (1.043); the launches traced: 206 us -> 213 us
  starting transfers between devices: 52.8 us -> 58.7 us
  waiting for transfers between devices: 29.4 us -> 23.9 us
  local copies, waits for them, and re-layouts: 6.25 us -> 10.7 us
  Pallas kernels: 12.2 us -> 8.24 us
  other arithmetic: 3.67 us -> 6.96 us
    all_gather x0 -> x1, blocking collectives: none -> 15.9 us  [steps(): sums = lax.all_gather(sums, TP, axis=0, tiled=False)]
    all_to_all x1 -> x0, blocking collectives: 14.4 us -> none  [steps(): lax.all_to_all(shared, 'sp', split_axis=0, concat_axis=0, tiled=True)]
    all_to_all x0 -> x1, waiting for transfers between devices: none -> 9.3 us  [steps(): lax.all_to_all(shared, 'sp', split_axis=0, concat_axis=0, tiled=True)]
    all_to_all x1, waiting for transfers between devices: 6.73 us -> 0.01 us  [steps(): lax.all_to_all(proj_part, 'sp', split_axis=0, concat_axis=0, tiled=True)]
    all_to_all x2 -> x1, waiting for transfers between devices: 5.99 us -> 0.01 us  [sent_to_all(): return lax.all_to_all(copies, axis, split_axis=0, concat_axis=0, tiled=True)]
    unnamed x48 -> x45, local copies, waits for them, and re-layouts: 3.93 us -> 9.77 us
    all_to_all x0 -> x1, starting transfers between devices: none -> 5.24 us  [steps(): lax.all_to_all(shared, 'sp', split_axis=0, concat_axis=0, tiled=True)]
    pallas_call x1 -> x2, Pallas kernels: 10.1 us -> 6.15 us  [the longest x1 4.07 us: rest_products(): pl.pallas_call(functools.partial(rest_body, blocks=blocks, slots=slots, b...]
  transfers between devices with their start and end apart: 14 -> 16, of which waited for: 9 -> 6; matrix products, arithmetic and copies ran while one was open for 5% -> 5% of each run, Pallas kernels for 0% -> 1%
where the time goes in v2:
time: 216 us; the launch traced here: 213 us
  blocking collectives  95.1 us (44%)
  starting transfers between devices  58.7 us (27%)
  waiting for transfers between devices  23.9 us (11%)
  local copies, waits for them, and re-layouts  10.7 us (5%)
  Pallas kernels  8.24 us (4%)
  matrix products  7.93 us (4%)
  other arithmetic  6.96 us (3%)
    all_to_all x1, blocking collectives, added_up(): lax.all_to_all(both.astype(BF16), 'chip', split_axis=0, concat_axis=0, ti...  35.4 us
    all_to_all x1, blocking collectives, steps(): own = lax.all_to_all(sent, 'sp', split_axis=0, concat_axis=0, tiled=True)  25 us
    ppermute x7, starting transfers between devices, along_chips(): lax.ppermute(value, 'chip', [(y, (y + steps) % count) for y in range(coun...  21.9 us
    all_gather x1, blocking collectives, steps(): columns = lax.all_gather(grad_stream, TP, axis=1, tiled=True)  18.7 us
    ppermute x5, starting transfers between devices, to_other_core(): return lax.ppermute(value, 'core', [(0, 1), (1, 0)])  16.1 us
    all_gather x1, blocking collectives, steps(): sums = lax.all_gather(sums, TP, axis=0, tiled=False)  15.9 us
    ppermute x7, waiting for transfers between devices, along_chips(): lax.ppermute(value, 'chip', [(y, (y + steps) % count) for y in range(coun...  10.3 us
    unnamed x45, local copies, waits for them, and re-layouts  9.77 us
  transfers between devices with their start and end apart: 16, of which 6 were waited for; matrix products, arithmetic and copies ran while one was open for 5% of the time, Pallas kernels for 1%

profile of v2, /device:TPU:1, one launch (start us, length us, event | category | flops | bytes accessed | tf_op | source)
XLA Modules:
  0.0 212.6 jit_solution(8546411557115306273)
XLA Ops:
  0.6 2.1 send_rows.1
  2.7 25.0 %all_to_all.25.refs_0_ = bf16[32,32,128]{2,1,0:T(8,128)(2,1)S(1)} all-to-all(bf16[32,32,128]{2,1,0:T(8,128)(2,1)} %get-tuple-element.21), channel_id=1, replica_groups=mesh['sp'=32,'chip'=8,'core'=2] {'sp'}, dimensions={0} | all-to-all | bytes 524288 | tf_op jit(solution)/shard_map/all_to_all | solution.py:255
  27.7 3.2 %collective-permute-start = (bf16[32,32,128]{2,1,0:T(8,128)(2,1)S(1)}, bf16[32,32,128]{2,1,0:T(8,128)(2,1)S(1)}, u32[]{:S(2)}, u32[]{:S(2)}) collective-permute-start(bf16[32,32,128]{2,1,0:T(8,128)(2,1)S(1)} %all_to_all.25.refs_0_), channel_id=1, source_target_pairs={{0,2},{2,4},{4,6},{6,8},{8,10},{10,12},{12,14},{14,0},{1,3},{3,5},... | collective-permute-start | bytes 786440 | tf_op jit(solution)/shard_map/ppermute | solution.py:197
  30.9 3.8 %collective-permute-start.3 = (bf16[32,32,128]{2,1,0:T(8,128)(2,1)S(1)}, bf16[32,32,128]{2,1,0:T(8,128)(2,1)S(1)}, u32[]{:S(2)}, u32[]{:S(2)}) collective-permute-start(bf16[32,32,128]{2,1,0:T(8,128)(2,1)S(1)} %all_to_all.25.refs_0_), channel_id=1, source_target_pairs={{0,14},{2,0},{4,2},{6,4},{8,6},{10,8},{12,10},{14,12},{1,15},{3,1}... | collective-permute-start | bytes 786440 | tf_op jit(solution)/shard_map/ppermute | solution.py:197
  34.8 2.3 %collective-permute-done.refs_1_ = bf16[32,32,128]{2,1,0:T(8,128)(2,1)S(1)} collective-permute-done((bf16[32,32,128]{2,1,0:T(8,128)(2,1)S(1)}, bf16[32,32,128]{2,1,0:T(8,128)(2,1)S(1)}, u32[]{:S(2)}, u32[]{:S(2)}) %collective-permute-start) | collective-permute-done | bytes 262176 | tf_op jit(solution)/shard_map/ppermute | solution.py:197
  37.0 1.9 collective-permute-start.1
  39.0 4.6 %collective-permute-start.4 = (bf16[32,32,128]{2,1,0:T(8,128)(2,1)S(1)}, bf16[32,32,128]{2,1,0:T(8,128)(2,1)S(1)}, u32[]{:S(2)}, u32[]{:S(2)}) collective-permute-start(bf16[32,32,128]{2,1,0:T(8,128)(2,1)S(1)} %collective-permute-done.3.refs_2_), channel_id=1, source_target_pairs={{0,14},{2,0},{4,2},{6,4},{8,6},{10,8},{12,10},{14,12},{1,15},{3,1}... | collective-permute-start | bytes 786440 | tf_op jit(solution)/shard_map/ppermute | solution.py:197
  43.6 1.8 collective-permute-done.1.refs_3_
  45.4 1.9 collective-permute-start.2
  47.3 4.6 %collective-permute-start.5 = (bf16[32,32,128]{2,1,0:T(8,128)(2,1)S(1)}, bf16[32,32,128]{2,1,0:T(8,128)(2,1)S(1)}, u32[]{:S(2)}, u32[]{:S(2)}) collective-permute-start(bf16[32,32,128]{2,1,0:T(8,128)(2,1)S(1)} %collective-permute-done.4.refs_4_), channel_id=1, source_target_pairs={{0,14},{2,0},{4,2},{6,4},{8,6},{10,8},{12,10},{14,12},{1,15},{3,1}... | collective-permute-start | bytes 786440 | tf_op jit(solution)/shard_map/ppermute | solution.py:197
  51.9 1.0 pad_maximum_fusion
  52.9 6.6 %collective-permute-start.9 = (bf16[3,32,32,128]{3,2,1,0:T(8,128)(2,1)}, bf16[3,32,32,128]{3,2,1,0:T(8,128)(2,1)S(1)}, u32[]{:S(2)}, u32[]{:S(2)}) collective-permute-start(bf16[3,32,32,128]{3,2,1,0:T(8,128)(2,1)} %pad_maximum_fusion), channel_id=1, source_target_pairs={{0,1},{1,0},{2,3},{3,2},{4,5},{5,4},{6,7},{7,6},{8,9},{9,8},{10,11... | collective-permute-start | bytes 2359304 | tf_op jit(solution)/shard_map/ppermute | solution.py:201
  59.5 0.9 pad_maximum_fusion.2
  60.3 1.9 collective-permute-start.10
  62.3 0.9 pad_maximum_fusion.1
  63.2 1.9 collective-permute-start.6
  65.1 2.4 %collective-permute-start.7 = (bf16[2,32,32,128]{3,2,1,0:T(8,128)(2,1)}, bf16[2,32,32,128]{3,2,1,0:T(8,128)(2,1)}, u32[]{:S(2)}, u32[]{:S(2)}) collective-permute-start(bf16[2,32,32,128]{3,2,1,0:T(8,128)(2,1)} %pad_maximum_fusion.1), channel_id=1, source_target_pairs={{0,1},{1,0},{2,3},{3,2},{4,5},{5,4},{6,7},{7,6},{8,9},{9,8},{10,11... | collective-permute-start | bytes 1572872 | tf_op jit(solution)/shard_map/ppermute | solution.py:201
  67.5 6.2 %collective-permute-done.6.refs_2_ = bf16[32,32,128]{2,1,0:T(8,128)(2,1)} collective-permute-done((bf16[32,32,128]{2,1,0:T(8,128)(2,1)S(1)}, bf16[32,32,128]{2,1,0:T(8,128)(2,1)}, u32[]{:S(2)}, u32[]{:S(2)}) %collective-permute-start.6) | collective-permute-done | bytes 262176 | tf_op jit(solution)/shard_map/ppermute | solution.py:197
  73.7 3.3 %collective-permute-start.8 = (bf16[1,32,32,128]{3,2,1,0:T(8,128)(2,1)}, bf16[1,32,32,128]{3,2,1,0:T(8,128)(2,1)}, u32[]{:S(2)}, u32[]{:S(2)}) collective-permute-start(bf16[1,32,32,128]{3,2,1,0:T(8,128)(2,1)} %bitcast.5), channel_id=1, source_target_pairs={{0,1},{1,0},{2,3},{3,2},{4,5},{5,4},{6,7},{7,6},{8,9},{9,8},{10,11... | collective-permute-start | bytes 786440 | tf_op jit(solution)/shard_map/ppermute | solution.py:201
  77.0 0.9 copy-done.8
  77.9 0.8 copy-done.10
  78.7 0.9 copy-done.4
  79.7 1.2 copy-done.5
  80.8 1.2 copy-done.6
  82.0 1.2 copy-done.7
  83.2 1.1 copy-done.9
  84.3 1.0 copy-done.11
  85.4 2.1 first_products.1
  87.5 4.1 %rest_products.1 = (bf16[512,2048]{1,0:T(8,128)(2,1)S(1)}, bf16[512,2048]{1,0:T(8,128)(2,1)S(1)}, bf16[512,224]{1,0:T(8,128)(2,1)S(1)}, bf16[512,224]{1,0:T(8,12...) custom-call(s32[1]{0:T(128)} %bitcast.me, ...), custom_call_target="tpu_custom_call", output_to_operand_aliasing={{0}: (6, {}), {1}: (7, {})} | custom-call | flops 1409286144 | bytes 12582912 | tf_op jit(solution)/shard_map/rest_products/pallas_call | solution.py:175
  91.6 1.3 copy-done
  92.9 1.9 collective-permute-start.11
  94.8 2.6 %collective-permute-done.11 = bf16[8,512,128]{2,1,0:T(8,128)(2,1)S(1)} collective-permute-done((bf16[8,512,128]{2,1,0:T(8,128)(2,1)S(1)}, bf16[8,512,128]{2,1,0:T(8,128)(2,1)S(1)}, u32[]{:S(2)}, u32[]{:S(2)}) %collective-permute-start.11) | collective-permute-done | bytes 1048608 | tf_op jit(solution)/shard_map/ppermute | solution.py:201
  97.8 35.4 %all_to_all.26 = bf16[8,512,128]{2,1,0:T(8,128)(2,1)} all-to-all(bf16[8,512,128]{2,1,0:T(8,128)(2,1)S(1)} %add_convert_fusion), channel_id=1, replica_groups=mesh['sp'=32,'chip'=8,'core'=2] {'chip'}, dimensions={0} | all-to-all | bytes 2097152 | tf_op jit(solution)/shard_map/all_to_all | solution.py:222
  133.2 2.1 reduce_sum.48
  135.2 5.2 %all-to-all-start.2 = ((bf16[32,16,128]{2,1,0:T(8,128)(2,1)}), bf16[32,16,128]{2,1,0:T(8,128)(2,1)S(1)}, u32[]{:S(2)}, u32[]{:S(2)}) async-start(bf16[32,16,128]{2,1,0:T(8,128)(2,1)} %bitcast.13), calls=%async_computation.2 | async-start | bytes 262144 | tf_op jit(solution)/shard_map/all_to_all | solution.py:265
  140.5 9.3 %all-to-all-done.2 = bf16[32,16,128]{2,1,0:T(8,128)(2,1)S(1)} async-done(((bf16[32,16,128]{2,1,0:T(8,128)(2,1)}), bf16[32,16,128]{2,1,0:T(8,128)(2,1)S(1)}, u32[]{:S(2)}, u32[]{:S(2)}) %all-to-all-start.2) | async-done | bytes 131104 | tf_op jit(solution)/shard_map/all_to_all | solution.py:265
  149.9 0.9 broadcast_in_dim.8
  150.8 4.8 %all-to-all-start.4 = ((bf16[32,64,128]{2,1,0:T(8,128)(2,1)}), bf16[32,64,128]{2,1,0:T(8,128)(2,1)}, u32[]{:S(2)}, u32[]{:S(2)}) async-start(bf16[32,64,128]{2,1,0:T(8,128)(2,1)} %broadcast_in_dim.8), calls=%async_computation.4 | async-start | bytes 1048576 | tf_op jit(solution)/shard_map/all_to_all | solution.py:228
  155.6 3.2 %fusion.1 = bf16[1,224,2048]{2,1,0:T(8,128)(2,1)} fusion(bf16[512,224]{1,0:T(8,128)(2,1)S(1)} %get-tuple-element.32, bf16[512,2048]{1,0:T(8,128)(2,1)} %copy-done), kind=kOutput, calls=%fused_computation.3 | convolution fusion | flops 470220800 | bytes 3244032 | tf_op jit(solution)/shard_map/dot_general | solution.py:18
  159.1 18.7 %all_gather.9 = bf16[192,2048]{1,0:T(8,128)(2,1)S(1)} all-gather(bf16[192,128]{1,0:T(8,128)(2,1)S(1)} %fusion.3), channel_id=1, replica_groups=mesh['sp'=32,'chip'=8,'core'=2] {'chip','core'}, dimensions={1}, use_global_device_ids=true | all-gather | bytes 835584 | tf_op jit(solution)/shard_map/all_gather | solution.py:271
  177.8 1.3 convolution_convert_fusion.2
  179.2 1.5 fusion.100
  180.7 9.4 %all-to-all-start.3 = ((bf16[32,64,128]{2,1,0:T(8,128)(2,1)}), bf16[32,64,128]{2,1,0:T(8,128)(2,1)S(1)}, u32[]{:S(2)}, u32[]{:S(2)}) async-start(bf16[32,64,128]{2,1,0:T(8,128)(2,1)} %bitcast.97), calls=%async_computation.3 | async-start | bytes 1048576 | tf_op jit(solution)/shard_map/all_to_all | solution.py:277
  190.2 15.9 %all-gather.1 = f32[16,1,384]{2,1,0:T(1,128)S(1)} all-gather(f32[1,1,384]{2,1,0:T(1,128)S(1)} %reshape.39), channel_id=2, replica_groups=mesh['sp'=32,'chip'=8,'core'=2] {'chip','core'}, dimensions={0}, use_global_device_ids=true | all-gather | bytes 26112 | tf_op jit(solution)/shard_map/all_gather | solution.py:281
  206.5 1.3 collective-permute-start.12
  207.8 1.6 fusion
  209.4 1.6 collective-permute-done.12
  211.0 0.9 fusion.8
  (56 shorter events, 1.7 us)
Async XLA Ops:
  27.7 9.3 %collective-permute-start = (bf16[32,32,128]{2,1,0:T(8,128)(2,1)S(1)}, bf16[32,32,128]{2,1,0:T(8,128)(2,1)S(1)}, u32[]{:S(2)}, u32[]{:S(2)}) collective-permute-start(bf16[32,32,128]{2,1,0:T(8,128)(2,1)S(1)} %all_to_all.25.refs_0_), channel_id=1, source_target_pairs={{0,2},{2,4},{4,6},{6,8},{8,10},{10,12},{12,14},{14,0},{1,3},{3,5},... | collective-permute-start | bytes 786440 | tf_op jit(solution)/shard_map/ppermute | solution.py:197
  30.9 8.0 %collective-permute-start.3 = (bf16[32,32,128]{2,1,0:T(8,128)(2,1)S(1)}, bf16[32,32,128]{2,1,0:T(8,128)(2,1)S(1)}, u32[]{:S(2)}, u32[]{:S(2)}) collective-permute-start(bf16[32,32,128]{2,1,0:T(8,128)(2,1)S(1)} %all_to_all.25.refs_0_), channel_id=1, source_target_pairs={{0,14},{2,0},{4,2},{6,4},{8,6},{10,8},{12,10},{14,12},{1,15},{3,1}... | collective-permute-start | bytes 786440 | tf_op jit(solution)/shard_map/ppermute | solution.py:197
  37.0 8.3 %collective-permute-start.1 = (bf16[32,32,128]{2,1,0:T(8,128)(2,1)S(1)}, bf16[32,32,128]{2,1,0:T(8,128)(2,1)S(1)}, u32[]{:S(2)}, u32[]{:S(2)}) collective-permute-start(bf16[32,32,128]{2,1,0:T(8,128)(2,1)S(1)} %collective-permute-done.refs_1_), channel_id=1, source_target_pairs={{0,2},{2,4},{4,6},{6,8},{8,10},{10,12},{12,14},{14,0},{1,3},{3,5},... | collective-permute-start | bytes 786440 | tf_op jit(solution)/shard_map/ppermute | solution.py:197
  39.0 8.3 %collective-permute-start.4 = (bf16[32,32,128]{2,1,0:T(8,128)(2,1)S(1)}, bf16[32,32,128]{2,1,0:T(8,128)(2,1)S(1)}, u32[]{:S(2)}, u32[]{:S(2)}) collective-permute-start(bf16[32,32,128]{2,1,0:T(8,128)(2,1)S(1)} %collective-permute-done.3.refs_2_), channel_id=1, source_target_pairs={{0,14},{2,0},{4,2},{6,4},{8,6},{10,8},{12,10},{14,12},{1,15},{3,1}... | collective-permute-start | bytes 786440 | tf_op jit(solution)/shard_map/ppermute | solution.py:197
  45.4 16.9 %collective-permute-start.2 = (bf16[32,32,128]{2,1,0:T(8,128)(2,1)S(1)}, bf16[32,32,128]{2,1,0:T(8,128)(2,1)S(1)}, u32[]{:S(2)}, u32[]{:S(2)}) collective-permute-start(bf16[32,32,128]{2,1,0:T(8,128)(2,1)S(1)} %collective-permute-done.1.refs_3_), channel_id=1, source_target_pairs={{0,2},{2,4},{4,6},{6,8},{8,10},{10,12},{12,14},{14,0},{1,3},{3,5},... | collective-permute-start | bytes 786440 | tf_op jit(solution)/shard_map/ppermute | solution.py:197
  47.3 26.4 %copy-start.3 = (bf16[32,32,128]{2,1,0:T(8,128)(2,1)}, bf16[32,32,128]{2,1,0:T(8,128)(2,1)S(1)}, u32[]{:S(2)}) copy-start(bf16[32,32,128]{2,1,0:T(8,128)(2,1)S(1)} %collective-permute-done.4.refs_4_) | copy-start | bytes 786436
  47.3 15.0 %collective-permute-start.5 = (bf16[32,32,128]{2,1,0:T(8,128)(2,1)S(1)}, bf16[32,32,128]{2,1,0:T(8,128)(2,1)S(1)}, u32[]{:S(2)}, u32[]{:S(2)}) collective-permute-start(bf16[32,32,128]{2,1,0:T(8,128)(2,1)S(1)} %collective-permute-done.4.refs_4_), channel_id=1, source_target_pairs={{0,14},{2,0},{4,2},{6,4},{8,6},{10,8},{12,10},{14,12},{1,15},{3,1}... | collective-permute-start | bytes 786440 | tf_op jit(solution)/shard_map/ppermute | solution.py:197
  52.9 24.2 %collective-permute-start.9 = (bf16[3,32,32,128]{3,2,1,0:T(8,128)(2,1)}, bf16[3,32,32,128]{3,2,1,0:T(8,128)(2,1)S(1)}, u32[]{:S(2)}, u32[]{:S(2)}) collective-permute-start(bf16[3,32,32,128]{3,2,1,0:T(8,128)(2,1)} %pad_maximum_fusion), channel_id=1, source_target_pairs={{0,1},{1,0},{2,3},{3,2},{4,5},{5,4},{6,7},{7,6},{8,9},{9,8},{10,11... | collective-permute-start | bytes 2359304 | tf_op jit(solution)/shard_map/ppermute | solution.py:201
  60.3 17.6 %collective-permute-start.10 = (bf16[2,32,32,128]{3,2,1,0:T(8,128)(2,1)}, bf16[2,32,32,128]{3,2,1,0:T(8,128)(2,1)S(1)}, u32[]{:S(2)}, u32[]{:S(2)}) collective-permute-start(bf16[2,32,32,128]{3,2,1,0:T(8,128)(2,1)} %pad_maximum_fusion.2), channel_id=1, source_target_pairs={{0,1},{1,0},{2,3},{3,2},{4,5},{5,4},{6,7},{7,6},{8,9},{9,8},{10,11... | collective-permute-start | bytes 1572872 | tf_op jit(solution)/shard_map/ppermute | solution.py:201
  62.3 11.4 %copy-start.1 = (bf16[32,32,128]{2,1,0:T(8,128)(2,1)}, bf16[32,32,128]{2,1,0:T(8,128)(2,1)S(1)}, u32[]{:S(2)}) copy-start(bf16[32,32,128]{2,1,0:T(8,128)(2,1)S(1)} %collective-permute-done.5.refs_1_) | copy-start | bytes 786436
  63.2 10.6 %collective-permute-start.6 = (bf16[32,32,128]{2,1,0:T(8,128)(2,1)S(1)}, bf16[32,32,128]{2,1,0:T(8,128)(2,1)}, u32[]{:S(2)}, u32[]{:S(2)}) collective-permute-start(bf16[32,32,128]{2,1,0:T(8,128)(2,1)S(1)} %collective-permute-done.2.refs_0_), channel_id=1, source_target_pairs={{0,2},{2,4},{4,6},{6,8},{8,10},{10,12},{12,14},{14,0},{1,3},{3,5},... | collective-permute-start | bytes 786440 | tf_op jit(solution)/shard_map/ppermute | solution.py:197
  65.1 22.4 %collective-permute-start.7 = (bf16[2,32,32,128]{3,2,1,0:T(8,128)(2,1)}, bf16[2,32,32,128]{3,2,1,0:T(8,128)(2,1)}, u32[]{:S(2)}, u32[]{:S(2)}) collective-permute-start(bf16[2,32,32,128]{3,2,1,0:T(8,128)(2,1)} %pad_maximum_fusion.1), channel_id=1, source_target_pairs={{0,1},{1,0},{2,3},{3,2},{4,5},{5,4},{6,7},{7,6},{8,9},{9,8},{10,11... | collective-permute-start | bytes 1572872 | tf_op jit(solution)/shard_map/ppermute | solution.py:201
  73.7 13.7 %collective-permute-start.8 = (bf16[1,32,32,128]{3,2,1,0:T(8,128)(2,1)}, bf16[1,32,32,128]{3,2,1,0:T(8,128)(2,1)}, u32[]{:S(2)}, u32[]{:S(2)}) collective-permute-start(bf16[1,32,32,128]{3,2,1,0:T(8,128)(2,1)} %bitcast.5), channel_id=1, source_target_pairs={{0,1},{1,0},{2,3},{3,2},{4,5},{5,4},{6,7},{7,6},{8,9},{9,8},{10,11... | collective-permute-start | bytes 786440 | tf_op jit(solution)/shard_map/ppermute | solution.py:201
  77.0 0.9 copy-start.8
  77.9 0.8 copy-start.10
  78.7 0.9 copy-start.4
  79.7 1.2 copy-start.5
  80.8 1.2 copy-start.6
  82.0 1.2 copy-start.7
  83.2 1.1 copy-start.9
  84.3 1.0 copy-start.11
  85.4 2.1 copy-start.2
  91.6 1.4 copy-start
  92.9 4.5 %collective-permute-start.11 = (bf16[8,512,128]{2,1,0:T(8,128)(2,1)S(1)}, bf16[8,512,128]{2,1,0:T(8,128)(2,1)S(1)}, u32[]{:S(2)}, u32[]{:S(2)}) collective-permute-start(bf16[8,512,128]{2,1,0:T(8,128)(2,1)S(1)} %get-tuple-element.36), channel_id=1, source_target_pairs={{0,1},{1,0},{2,3},{3,2},{4,5},{5,4},{6,7},{7,6},{8,9},{9,8},{10,11... | collective-permute-start | bytes 3145736 | tf_op jit(solution)/shard_map/ppermute | solution.py:201
  97.7 42.8 %copy-start.17 = (f32[31,128]{1,0:T(8,128)S(1)}, f32[31,128]{1,0:T(8,128)}, u32[]{:S(2)}) copy-start(f32[31,128]{1,0:T(8,128)} %param.26) | copy-start | bytes 47620
  97.8 52.1 %copy-start.16 = (bf16[64,128]{1,0:T(8,128)(2,1)S(1)}, bf16[64,128]{1,0:T(8,128)(2,1)}, u32[]{:S(2)}) copy-start(bf16[64,128]{1,0:T(8,128)(2,1)} %param.27) | copy-start | bytes 49156
  135.2 14.6 %all-to-all-start.2 = ((bf16[32,16,128]{2,1,0:T(8,128)(2,1)}), bf16[32,16,128]{2,1,0:T(8,128)(2,1)S(1)}, u32[]{:S(2)}, u32[]{:S(2)}) async-start(bf16[32,16,128]{2,1,0:T(8,128)(2,1)} %bitcast.13), calls=%async_computation.2 | async-start | bytes 262144 | tf_op jit(solution)/shard_map/all_to_all | solution.py:265
  150.8 8.0 %copy-start.12 = (bf16[512,192]{1,0:T(8,128)(2,1)S(1)}, bf16[512,192]{1,0:T(8,128)(2,1)}, u32[]{:S(2)}) copy-start(bf16[512,192]{1,0:T(8,128)(2,1)} %get-tuple-element.34) | copy-start | bytes 589828
  150.8 8.0 %copy-start.14 = (bf16[192,128]{1,0:T(8,128)(2,1)S(1)}, bf16[192,128]{1,0:T(8,128)(2,1)}, u32[]{:S(2)}) copy-start(bf16[192,128]{1,0:T(8,128)(2,1)} %cotangent.1) | copy-start | bytes 147460
  150.8 28.4 %all-to-all-start.4 = ((bf16[32,64,128]{2,1,0:T(8,128)(2,1)}), bf16[32,64,128]{2,1,0:T(8,128)(2,1)}, u32[]{:S(2)}, u32[]{:S(2)}) async-start(bf16[32,64,128]{2,1,0:T(8,128)(2,1)} %broadcast_in_dim.8), calls=%async_computation.4 | async-start | bytes 1048576 | tf_op jit(solution)/shard_map/all_to_all | solution.py:228
  155.5 22.3 %copy-start.15 = (bf16[192,128]{1,0:T(8,128)(2,1)S(1)}, bf16[192,128]{1,0:T(8,128)(2,1)}, u32[]{:S(2)}) copy-start(bf16[192,128]{1,0:T(8,128)(2,1)} %param.21) | copy-start | bytes 147460
  155.5 22.3 %copy-start.18 = (f32[192]{0:T(256)S(1)}, f32[192]{0:T(256)}, u32[]{:S(2)}) copy-start(f32[192]{0:T(256)} %param.23) | copy-start | bytes 2308
  155.6 22.2 %copy-start.19 = (f32[192]{0:T(256)S(1)}, f32[192]{0:T(256)}, u32[]{:S(2)}) copy-start(f32[192]{0:T(256)} %param.22) | copy-start | bytes 2308
  155.6 22.2 %copy-start.20 = (f32[128]{0:T(128)S(1)}, f32[128]{0:T(128)}, u32[]{:S(2)}) copy-start(f32[128]{0:T(128)} %param.25) | copy-start | bytes 1540
  155.6 22.2 %copy-start.21 = (f32[128]{0:T(128)S(1)}, f32[128]{0:T(128)}, u32[]{:S(2)}) copy-start(f32[128]{0:T(128)} %param.24) | copy-start | bytes 1540
  159.1 21.6 %copy-start.13 = (bf16[192,128]{1,0:T(8,128)(2,1)}, bf16[192,128]{1,0:T(8,128)(2,1)S(1)}, u32[]{:S(2)}) copy-start(bf16[192,128]{1,0:T(8,128)(2,1)S(1)} %fusion.3) | copy-start | bytes 147460
  180.7 31.2 %all-to-all-start.3 = ((bf16[32,64,128]{2,1,0:T(8,128)(2,1)}), bf16[32,64,128]{2,1,0:T(8,128)(2,1)S(1)}, u32[]{:S(2)}, u32[]{:S(2)}) async-start(bf16[32,64,128]{2,1,0:T(8,128)(2,1)} %bitcast.97), calls=%async_computation.3 | async-start | bytes 1048576 | tf_op jit(solution)/shard_map/all_to_all | solution.py:277
  206.5 4.5 %collective-permute-start.12 = (f32[30,128]{1,0:T(8,128)S(1)}, f32[30,128]{1,0:T(8,128)S(1)}, u32[]{:S(2)}, u32[]{:S(2)}) collective-permute-start(f32[30,128]{1,0:T(8,128)S(1)} %slice.256), channel_id=1, source_target_pairs={{16,0},{32,16},{48,32},{64,48},{80,64},{96,80},{112,96},{128,112},... | collective-permute-start | bytes 46088 | tf_op jit(solution)/shard_map/ppermute | solution.py:289

commit v3 on v2

--- a/solution.py
+++ b/solution.py
@@ -20,6 +20,10 @@
 
 def silu_slope(pre_value, sigmoid_value):
     return sigmoid_value * (1.0 + pre_value * (1.0 - sigmoid_value))
+
+
+def far(*arrays):
+    return tuple(pltpu.with_memory_space_constraint(a, pltpu.HBM) for a in arrays)
 
 
 def near(*arrays):
@@ -76,15 +80,14 @@
 def put_blocks(me, steps, mine, others, rows, routed, blocks, slots):
     chips = blocks // 2
     width = mine[0].shape[-1]
-    count = mine[0].shape[-3] * slots
     my_chip, my_core = (me[0] // 2, lax.rem(me[0], 2))
     found = []
     for step, part, (batch, at) in zip(steps, mine, others):
         chip = lax.rem(my_chip + step + chips, chips)
         for core, value in ((my_core, part), (1 - my_core, batch.at[at])):
             cols = columns(chip, core, width)
-            rows[:, cols] = value[:, :slots, :].reshape(count, width)
-            routed[:, cols] = value[:, slots:, :].reshape(count, width)
+            rows[:, :, cols] = value[:, :slots, :]
+            routed[:, :, cols] = value[:, slots:, :]
         found.append(pl.ds(pl.multiple_of(chip * 2 * width, 2 * width), 2 * width))
     return found
 
@@ -93,22 +96,39 @@
     sums = [None] * 3
     for cols in found:
         for n, (left, weight) in enumerate(zip((rows, rows, routed), weights)):
-            part = dot(left[:, cols], weight[:, cols], 1, 1)
+            taken = left[..., cols].reshape(-1, cols.size)
+            part = dot(taken, weight[:, cols], 1, 1)
             sums[n] = part if sums[n] is None else sums[n] + part
     return sums
 
 
 def first_body(me, *refs, blocks, slots, batches):
+    chips = blocks // 2
     count = sum(batches)
     mine, shared = (refs[:count], refs[count : count + len(batches)])
     weights = refs[count + len(batches) : count + len(batches) + 3]
-    rows, routed, *sums, held0, held1, held2 = refs[count + len(batches) + 3 :]
+    rows, routed, *sums, held0, held1, held2, sems, weight_sems = refs[count + len(batches) + 3 :]
     others = [(batch, at) for batch, size in zip(shared, batches) for at in range(size)]
     held = (held0, held1, held2)
-    for weight, keep in zip(weights, held):
-        keep[...] = weight[0]
-    steps = ring_order(blocks // 2)[:count]
-    found = put_blocks(me, steps, mine, others, rows, routed, blocks, slots)
+    width = mine[0].shape[-1]
+    my_chip, my_core = (me[0] // 2, lax.rem(me[0], 2))
+    copies = [
+        pltpu.make_async_copy(weight.at[0], keep, weight_sems.at[n])
+        for n, (weight, keep) in enumerate(zip(weights, held))
+    ]
+    found = []
+    for n, (step, (batch, at)) in enumerate(zip(ring_order(chips), others)):
+        chip = lax.rem(my_chip + step + chips, chips)
+        for i, (core, source) in enumerate(((my_core, mine[n]), (1 - my_core, batch.at[at]))):
+            cols = columns(chip, core, width)
+            for k, target in enumerate((rows, routed)):
+                part = source.at[:, pl.ds(k * slots, slots), :]
+                copies.append(pltpu.make_async_copy(part, target.at[:, :, cols], sems.at[n, i, k]))
+        found.append(pl.ds(pl.multiple_of(chip * 2 * width, 2 * width), 2 * width))
+    for copy in copies:
+        copy.start()
+    for copy in copies:
+        copy.wait()
     for out, value in zip(sums, products(rows, routed, held, found)):
         out[...] = value
 
@@ -119,10 +139,15 @@
     count, hidden, channels = (experts * slots, weights[0].shape[1], weights[0].shape[2])
     return pl.pallas_call(
         functools.partial(first_body, blocks=blocks, slots=slots, batches=batches),
-        in_specs=whole(1, pltpu.SMEM) + whole(len(mine) + len(shared) + 3),
+        in_specs=whole(1, pltpu.SMEM)
+        + whole(len(mine) + len(shared) + 3, pltpu.HBM),
         out_specs=whole(8),
+        scratch_shapes=[
+            pltpu.SemaphoreType.DMA((len(mine), 2, 2)),
+            pltpu.SemaphoreType.DMA((3,)),
+        ],
         out_shape=(
-            *[pltpu.VMEM((count, channels), BF16)] * 2,
+            *[pltpu.VMEM((experts, slots, channels), BF16)] * 2,
             *[pltpu.VMEM((count, hidden), F32)] * 3,
             *[pltpu.VMEM((hidden, channels), BF16)] * 3,
         ),
@@ -131,7 +156,7 @@
         ),
         compiler_params=pltpu.CompilerParams(vmem_limit_bytes=12 * 1024 * 1024),
         name="first_products",
-    )(me, *mine, *shared, *weights)
+    )(me, *far(*mine, *shared, *weights))
 
 
 def rest_body(me, *refs, blocks, slots, batches):
@@ -139,10 +164,18 @@
     count = sum(batches)
     mine, shared = (refs[:count], refs[count : count + len(batches)])
     _, _, gate_sum, up_sum, down_sum, *weights = refs[count + len(batches) : count + len(batches) + 8]
-    rows, routed, hidden_out, up_out, kept, given = refs[count + len(batches) + 8 :]
+    outs = refs[count + len(batches) + 8 :]
+    rows, routed, kept, given, *far_outs = outs[:8]
+    hidden_held, up_held, sems = outs[8:]
+    sends = [
+        pltpu.make_async_copy(held, out, sems.at[n])
+        for n, (held, out) in enumerate(zip((rows, routed, hidden_held, up_held), far_outs))
+    ]
     others = [(batch, at) for batch, size in zip(shared, batches) for at in range(size)]
     steps = ring_order(chips)[-count:]
     found = put_blocks(me, steps, mine, others, rows, routed, blocks, slots)
+    sends[0].start()
+    sends[1].start()
     gate_pre, up_pre, hidden_grad = products(rows, routed, weights, found)
     gate_pre = gate_pre + gate_sum[...]
     up_pre = up_pre + up_sum[...]
@@ -152,10 +185,12 @@
     my_core = lax.rem(me[0], 2)
     gate_sigmoid = jax.nn.sigmoid(gate_pre)
     gate_active = gate_pre * gate_sigmoid
-    hidden_out[...] = (gate_active * up_pre).astype(BF16)
+    hidden_held[...] = (gate_active * up_pre).astype(BF16)
     gate_grad = (hidden_grad * up_pre * silu_slope(gate_pre, gate_sigmoid)).astype(BF16)
     up_grad = (hidden_grad * gate_active).astype(BF16)
-    up_out[...] = up_grad
+    up_held[...] = up_grad
+    sends[2].start()
+    sends[3].start()
     for out, core in ((given, 1 - my_core), (kept, my_core)):
         for j in range(0, chips, 2):
             gate_cols, up_cols = (
@@ -165,22 +200,26 @@
             both = dot(gate_grad, gate_cols, 1, 0) + dot(up_grad, up_cols, 1, 0)
             for i in (0, 1):
                 out[j + i] = both[:, i * width : (i + 1) * width].astype(BF16)
+    for send in sends:
+        send.wait()
 
 
 def rest_products(me, mine, shared, early, slots, blocks):
     batches = [b.shape[0] for b in shared]
-    count, channels = early[0].shape
-    hidden = early[2].shape[1]
+    experts, _, channels = early[0].shape
+    count, hidden = early[2].shape
     first = 1 + len(mine) + len(shared)
     return pl.pallas_call(
         functools.partial(rest_body, blocks=blocks, slots=slots, batches=batches),
         in_specs=whole(1, pltpu.SMEM) + whole(len(mine) + len(shared) + 8),
-        out_specs=whole(6),
+        out_specs=whole(4) + whole(4, pl.ANY),
         out_shape=(
-            *[pltpu.VMEM((count, channels), BF16)] * 2,
-            *[pltpu.VMEM((count, hidden), BF16)] * 2,
+            *[pltpu.VMEM((experts, slots, channels), BF16)] * 2,
             *[pltpu.VMEM((blocks // 2, count, channels // blocks), BF16)] * 2,
-        ),
+            *[pltpu.HBM((experts, slots, channels), BF16)] * 2,
+            *[pltpu.HBM((count, hidden), BF16)] * 2,
+        ),
+        scratch_shapes=[pltpu.VMEM((count, hidden), BF16)] * 2 + [pltpu.SemaphoreType.DMA((4,))],
         input_output_aliases={first: 0, first + 1: 1},
         cost_estimate=pl.CostEstimate(
             flops=6 * count * hidden * channels,
@@ -257,14 +296,14 @@
     mine, others = all_blocks(own)
     done = sum(BATCHES[:EARLY])
     early = first_products(me, mine[:done], others[:EARLY], (w_gate, w_up, w_down), slots, blocks)
-    rows, routed, hidden, up_grad, kept, given = rest_products(
+    _, _, kept, given, rows, routed, hidden, up_grad = rest_products(
         me, mine[done:], others[EARLY:], early, slots, blocks
     )
     shared = added_up(kept, given)
     shared = shared.reshape(devices, slots, channels)
     returned = lax.all_to_all(shared, "sp", split_axis=0, concat_axis=0, tiled=True)
-    grad_up = dot(up_grad, rows, 0, 0).astype(BF16)[None]
-    grad_down = dot(hidden, routed, 0, 0).astype(BF16)[None]
+    grad_up = dot(up_grad, rows.reshape(-1, rows.shape[2]), 0, 0).astype(BF16)[None]
+    grad_down = dot(hidden, routed.reshape(-1, routed.shape[2]), 0, 0).astype(BF16)[None]
     grad_stream = (
         cotangent.astype(F32) + dot(place, returned.reshape(devices * slots, channels), 0, 0)
     ).astype(BF16)

time: 216 us -> 205 us (0.949)
  local copies, waits for them, and re-layouts: 10.7 us -> 1.69 us
  Pallas kernels: 8.24 us -> 10.6 us
    unnamed x45 -> x61, local copies, waits for them, and re-layouts: 9.77 us -> 0.15 us
  transfers between devices with their start and end apart: 16 -> 16, of which waited for: 6 -> 6; matrix products, arithmetic and copies ran while one was open for 5% -> 4% of each run, Pallas kernels for 1% -> 2%
where the time goes in v3:
time: 205 us; the launch traced here: 202 us
  blocking collectives  95.1 us (46%)
  starting transfers between devices  58.7 us (29%)
  waiting for transfers between devices  23.2 us (11%)
  Pallas kernels  10.6 us (5%)
  matrix products  6.33 us (3%)
  other arithmetic  4.94 us (2%)
    all_to_all x1, blocking collectives, added_up(): lax.all_to_all(both.astype(BF16), 'chip', split_axis=0, concat_axis=0, ti...  35.5 us
    all_to_all x1, blocking collectives, steps(): own = lax.all_to_all(sent, 'sp', split_axis=0, concat_axis=0, tiled=True)  25 us
    ppermute x7, starting transfers between devices, along_chips(): lax.ppermute(value, 'chip', [(y, (y + steps) % count) for y in range(coun...  21.9 us
    all_gather x1, blocking collectives, steps(): columns = lax.all_gather(grad_stream, TP, axis=1, tiled=True)  18.7 us
    ppermute x5, starting transfers between devices, to_other_core(): return lax.ppermute(value, 'core', [(0, 1), (1, 0)])  16.1 us
    all_gather x1, blocking collectives, steps(): sums = lax.all_gather(sums, TP, axis=0, tiled=False)  15.9 us
    ppermute x7, waiting for transfers between devices, along_chips(): lax.ppermute(value, 'chip', [(y, (y + steps) % count) for y in range(coun...  10.2 us
    all_to_all x1, starting transfers between devices, steps(): lax.all_to_all(proj_part, 'sp', split_axis=0, concat_axis=0, tiled=True)  9.43 us
  transfers between devices with their start and end apart: 16, of which 6 were waited for; matrix products, arithmetic and copies ran while one was open for 4% of the time, Pallas kernels for 2%

profile of v3, /device:TPU:1, one launch (start us, length us, event | category | flops | bytes accessed | tf_op | source)
XLA Modules:
  0.0 201.9 jit_solution(13691090820649309348)
XLA Ops:
  0.6 2.1 %send_rows.1 = (bf16[32,32,128]{2,1,0:T(8,128)(2,1)}, bf16[512,192]{1,0:T(8,128)(2,1)}) custom-call(s32[2,192]{1,0:T(2,128)} %bitcast.103, f32[2,192]{1,0:T(2,128)} %bitcast.104, bf16[192,128]{1,0:T(8,128)(2,1)} %rows.1, bf16[192,128]{1,0:T(8,128)(2,1)} %cotangent.1), custom_call_target="tpu_custom_call" | custom-call | tf_op jit(solution)/shard_map/send_rows/pallas_call | solution.py:64
  2.7 25.0 %all_to_all.25.refs_0_ = bf16[32,32,128]{2,1,0:T(8,128)(2,1)S(1)} all-to-all(bf16[32,32,128]{2,1,0:T(8,128)(2,1)} %get-tuple-element.21), channel_id=1, replica_groups=mesh['sp'=32,'chip'=8,'core'=2] {'sp'}, dimensions={0} | all-to-all | bytes 524288 | tf_op jit(solution)/shard_map/all_to_all | solution.py:294
  27.7 3.2 %collective-permute-start = (bf16[32,32,128]{2,1,0:T(8,128)(2,1)S(1)}, bf16[32,32,128]{2,1,0:T(8,128)(2,1)S(1)}, u32[]{:S(2)}, u32[]{:S(2)}) collective-permute-start(bf16[32,32,128]{2,1,0:T(8,128)(2,1)S(1)} %all_to_all.25.refs_0_), channel_id=1, source_target_pairs={{0,2},{2,4},{4,6},{6,8},{8,10},{10,12},{12,14},{14,0},{1,3},{3,5},... | collective-permute-start | bytes 786440 | tf_op jit(solution)/shard_map/ppermute | solution.py:236
  30.9 3.8 %collective-permute-start.3 = (bf16[32,32,128]{2,1,0:T(8,128)(2,1)S(1)}, bf16[32,32,128]{2,1,0:T(8,128)(2,1)S(1)}, u32[]{:S(2)}, u32[]{:S(2)}) collective-permute-start(bf16[32,32,128]{2,1,0:T(8,128)(2,1)S(1)} %all_to_all.25.refs_0_), channel_id=1, source_target_pairs={{0,14},{2,0},{4,2},{6,4},{8,6},{10,8},{12,10},{14,12},{1,15},{3,1}... | collective-permute-start | bytes 786440 | tf_op jit(solution)/shard_map/ppermute | solution.py:236
  34.8 2.3 %collective-permute-done.refs_1_ = bf16[32,32,128]{2,1,0:T(8,128)(2,1)S(1)} collective-permute-done((bf16[32,32,128]{2,1,0:T(8,128)(2,1)S(1)}, bf16[32,32,128]{2,1,0:T(8,128)(2,1)S(1)}, u32[]{:S(2)}, u32[]{:S(2)}) %collective-permute-start) | collective-permute-done | bytes 262176 | tf_op jit(solution)/shard_map/ppermute | solution.py:236
  37.1 1.9 collective-permute-start.1
  39.0 4.6 %collective-permute-start.4 = (bf16[32,32,128]{2,1,0:T(8,128)(2,1)S(1)}, bf16[32,32,128]{2,1,0:T(8,128)(2,1)S(1)}, u32[]{:S(2)}, u32[]{:S(2)}) collective-permute-start(bf16[32,32,128]{2,1,0:T(8,128)(2,1)S(1)} %collective-permute-done.3.refs_2_), channel_id=1, source_target_pairs={{0,14},{2,0},{4,2},{6,4},{8,6},{10,8},{12,10},{14,12},{1,15},{3,1}... | collective-permute-start | bytes 786440 | tf_op jit(solution)/shard_map/ppermute | solution.py:236
  43.6 1.8 collective-permute-done.1.refs_3_
  45.4 1.9 collective-permute-start.2
  47.3 4.6 %collective-permute-start.5 = (bf16[32,32,128]{2,1,0:T(8,128)(2,1)S(1)}, bf16[32,32,128]{2,1,0:T(8,128)(2,1)S(1)}, u32[]{:S(2)}, u32[]{:S(2)}) collective-permute-start(bf16[32,32,128]{2,1,0:T(8,128)(2,1)S(1)} %collective-permute-done.4.refs_4_), channel_id=1, source_target_pairs={{0,14},{2,0},{4,2},{6,4},{8,6},{10,8},{12,10},{14,12},{1,15},{3,1}... | collective-permute-start | bytes 786440 | tf_op jit(solution)/shard_map/ppermute | solution.py:236
  51.9 1.0 pad_maximum_fusion
  52.9 6.6 %collective-permute-start.9 = (bf16[3,32,32,128]{3,2,1,0:T(8,128)(2,1)}, bf16[3,32,32,128]{3,2,1,0:T(8,128)(2,1)}, u32[]{:S(2)}, u32[]{:S(2)}) collective-permute-start(bf16[3,32,32,128]{3,2,1,0:T(8,128)(2,1)} %pad_maximum_fusion), channel_id=1, source_target_pairs={{0,1},{1,0},{2,3},{3,2},{4,5},{5,4},{6,7},{7,6},{8,9},{9,8},{10,11... | collective-permute-start | bytes 2359304 | tf_op jit(solution)/shard_map/ppermute | solution.py:240
  59.5 0.8 pad_maximum_fusion.2
  60.3 1.9 collective-permute-start.10
  62.3 0.1 pad_maximum_fusion.1
  62.3 1.9 collective-permute-start.6
  64.3 2.4 %collective-permute-start.7 = (bf16[2,32,32,128]{3,2,1,0:T(8,128)(2,1)S(1)}, bf16[2,32,32,128]{3,2,1,0:T(8,128)(2,1)S(1)}, u32[]{:S(2)}, u32[]{:S(2)}) collective-permute-start(bf16[2,32,32,128]{3,2,1,0:T(8,128)(2,1)S(1)} %pad_maximum_fusion.1), channel_id=1, source_target_pairs={{0,1},{1,0},{2,3},{3,2},{4,5},{5,4},{6,7},{7,6},{8,9},{9,8},{10,11... | collective-permute-start | bytes 1572872 | tf_op jit(solution)/shard_map/ppermute | solution.py:240
  66.7 6.1 %collective-permute-done.6.refs_2_ = bf16[32,32,128]{2,1,0:T(8,128)(2,1)S(1)} collective-permute-done((bf16[32,32,128]{2,1,0:T(8,128)(2,1)S(1)}, bf16[32,32,128]{2,1,0:T(8,128)(2,1)S(1)}, u32[]{:S(2)}, u32[]{:S(2)}) %collective-permute-start.6) | collective-permute-done | bytes 262176 | tf_op jit(solution)/shard_map/ppermute | solution.py:236
  72.8 3.3 %collective-permute-start.8 = (bf16[1,32,32,128]{3,2,1,0:T(8,128)(2,1)S(1)}, bf16[1,32,32,128]{3,2,1,0:T(8,128)(2,1)S(1)}, u32[]{:S(2)}, u32[]{:S(2)}) collective-permute-start(bf16[1,32,32,128]{3,2,1,0:T(8,128)(2,1)S(1)} %bitcast.94), channel_id=1, source_target_pairs={{0,1},{1,0},{2,3},{3,2},{4,5},{5,4},{6,7},{7,6},{8,9},{9,8},{10,11... | collective-permute-start | bytes 786440 | tf_op jit(solution)/shard_map/ppermute | solution.py:240
  76.1 3.9 %first_products.1 = (bf16[32,16,2048]{2,1,0:T(8,128)(2,1)S(1)}, bf16[32,16,2048]{2,1,0:T(8,128)(2,1)S(1)}, f32[512,224]{1,0:T(8,128)S(1)}, f32[512,224]{1,0:T(8,...) custom-call(s32[1]{0:T(128)} %bitcast.me, ...), custom_call_target="tpu_custom_call" | custom-call | flops 939524096 | bytes 12582912 | tf_op jit(solution)/shard_map/first_products/pallas_call | solution.py:140
  80.1 4.6 %rest_products.1 = (bf16[32,16,2048]{2,1,0:T(8,128)(2,1)S(1)}, bf16[32,16,2048]{2,1,0:T(8,128)(2,1)S(1)}, bf16[8,512,128]{2,1,0:T(8,128)(2,1)S(1)}, bf16[8,512,1...) custom-call(s32[1]{0:T(128)} %bitcast.me, ...), custom_call_target="tpu_custom_call", output_to_operand_aliasing={{0}: (6, {}), {1}: (7, {})} | custom-call | flops 1409286144 | bytes 12582912 | tf_op jit(solution)/shard_map/rest_products/pallas_call | solution.py:212
  84.7 1.9 collective-permute-start.11
  86.7 2.6 %collective-permute-done.11 = bf16[8,512,128]{2,1,0:T(8,128)(2,1)S(1)} collective-permute-done((bf16[8,512,128]{2,1,0:T(8,128)(2,1)S(1)}, bf16[8,512,128]{2,1,0:T(8,128)(2,1)S(1)}, u32[]{:S(2)}, u32[]{:S(2)}) %collective-permute-start.11) | collective-permute-done | bytes 1048608 | tf_op jit(solution)/shard_map/ppermute | solution.py:240
  89.3 0.3 add_convert_fusion
  89.6 0.0 copy-start.14
  89.6 35.5 %all_to_all.26 = bf16[8,512,128]{2,1,0:T(8,128)(2,1)S(1)} all-to-all(bf16[8,512,128]{2,1,0:T(8,128)(2,1)S(1)} %add_convert_fusion), channel_id=1, replica_groups=mesh['sp'=32,'chip'=8,'core'=2] {'chip'}, dimensions={0} | all-to-all | bytes 2097152 | tf_op jit(solution)/shard_map/all_to_all | solution.py:261
  125.1 0.8 reduce_sum.48
  125.9 5.3 %all-to-all-start.2 = ((bf16[32,16,128]{2,1,0:T(8,128)(2,1)}), bf16[32,16,128]{2,1,0:T(8,128)(2,1)S(1)}, u32[]{:S(2)}, u32[]{:S(2)}) async-start(bf16[32,16,128]{2,1,0:T(8,128)(2,1)} %bitcast.15), calls=%async_computation.2 | async-start | bytes 262144 | tf_op jit(solution)/shard_map/all_to_all | solution.py:304
  131.2 0.6 slice_bitcast_fusion.30
  131.8 8.7 %all-to-all-done.2 = bf16[32,16,128]{2,1,0:T(8,128)(2,1)S(1)} async-done(((bf16[32,16,128]{2,1,0:T(8,128)(2,1)}), bf16[32,16,128]{2,1,0:T(8,128)(2,1)S(1)}, u32[]{:S(2)}, u32[]{:S(2)}) %all-to-all-start.2) | async-done | bytes 131104 | tf_op jit(solution)/shard_map/all_to_all | solution.py:304
  140.5 0.9 broadcast_in_dim.8
  141.4 4.8 %all-to-all-start.4 = ((bf16[32,64,128]{2,1,0:T(8,128)(2,1)}), bf16[32,64,128]{2,1,0:T(8,128)(2,1)}, u32[]{:S(2)}, u32[]{:S(2)}) async-start(bf16[32,64,128]{2,1,0:T(8,128)(2,1)} %broadcast_in_dim.8), calls=%async_computation.4 | async-start | bytes 1048576 | tf_op jit(solution)/shard_map/all_to_all | solution.py:267
  146.2 1.6 fusion.1
  147.9 0.3 fusion.3
  148.1 0.0 copy-start.10
  148.1 18.7 %all_gather.9 = bf16[192,2048]{1,0:T(8,128)(2,1)S(1)} all-gather(bf16[192,128]{1,0:T(8,128)(2,1)S(1)} %fusion.3), channel_id=1, replica_groups=mesh['sp'=32,'chip'=8,'core'=2] {'chip','core'}, dimensions={1}, use_global_device_ids=true | all-gather | bytes 835584 | tf_op jit(solution)/shard_map/all_gather | solution.py:310
  166.9 1.4 convolution_convert_fusion.2
  168.3 1.5 fusion.100
  169.8 9.4 %all-to-all-start.3 = ((bf16[32,64,128]{2,1,0:T(8,128)(2,1)}), bf16[32,64,128]{2,1,0:T(8,128)(2,1)S(1)}, u32[]{:S(2)}, u32[]{:S(2)}) async-start(bf16[32,64,128]{2,1,0:T(8,128)(2,1)} %bitcast.17), calls=%async_computation.3 | async-start | bytes 1048576 | tf_op jit(solution)/shard_map/all_to_all | solution.py:316
  179.4 0.1 pad_maximum_fusion.4
  179.4 15.9 %all-gather.1 = f32[16,1,384]{2,1,0:T(1,128)S(1)} all-gather(f32[1,1,384]{2,1,0:T(1,128)S(1)} %reshape.47), channel_id=2, replica_groups=mesh['sp'=32,'chip'=8,'core'=2] {'chip','core'}, dimensions={0}, use_global_device_ids=true | all-gather | bytes 26112 | tf_op jit(solution)/shard_map/all_gather | solution.py:320
  195.4 0.1 slice_multiply_fusion.1
  195.5 0.2 subtract_multiply_fusion
  195.7 1.3 collective-permute-start.12
  197.0 1.6 fusion
  198.6 1.6 collective-permute-done.12
  200.3 0.9 fusion.8
  201.2 0.7 convert_reduce_fusion
  (72 shorter events, 0.2 us)
Async XLA Ops:
  27.7 48.4 %copy-start = (bf16[32,32,128]{2,1,0:T(8,128)(2,1)}, bf16[32,32,128]{2,1,0:T(8,128)(2,1)S(1)}, u32[]{:S(2)}) copy-start(bf16[32,32,128]{2,1,0:T(8,128)(2,1)S(1)} %all_to_all.25.refs_0_) | copy-start | bytes 786436
  27.7 9.3 %collective-permute-start = (bf16[32,32,128]{2,1,0:T(8,128)(2,1)S(1)}, bf16[32,32,128]{2,1,0:T(8,128)(2,1)S(1)}, u32[]{:S(2)}, u32[]{:S(2)}) collective-permute-start(bf16[32,32,128]{2,1,0:T(8,128)(2,1)S(1)} %all_to_all.25.refs_0_), channel_id=1, source_target_pairs={{0,2},{2,4},{4,6},{6,8},{8,10},{10,12},{12,14},{14,0},{1,3},{3,5},... | collective-permute-start | bytes 786440 | tf_op jit(solution)/shard_map/ppermute | solution.py:236
  30.9 8.0 %collective-permute-start.3 = (bf16[32,32,128]{2,1,0:T(8,128)(2,1)S(1)}, bf16[32,32,128]{2,1,0:T(8,128)(2,1)S(1)}, u32[]{:S(2)}, u32[]{:S(2)}) collective-permute-start(bf16[32,32,128]{2,1,0:T(8,128)(2,1)S(1)} %all_to_all.25.refs_0_), channel_id=1, source_target_pairs={{0,14},{2,0},{4,2},{6,4},{8,6},{10,8},{12,10},{14,12},{1,15},{3,1}... | collective-permute-start | bytes 786440 | tf_op jit(solution)/shard_map/ppermute | solution.py:236
  37.1 39.1 %copy-start.3 = (bf16[32,32,128]{2,1,0:T(8,128)(2,1)}, bf16[32,32,128]{2,1,0:T(8,128)(2,1)S(1)}, u32[]{:S(2)}) copy-start(bf16[32,32,128]{2,1,0:T(8,128)(2,1)S(1)} %collective-permute-done.refs_1_) | copy-start | bytes 786436
  37.1 8.3 %collective-permute-start.1 = (bf16[32,32,128]{2,1,0:T(8,128)(2,1)S(1)}, bf16[32,32,128]{2,1,0:T(8,128)(2,1)S(1)}, u32[]{:S(2)}, u32[]{:S(2)}) collective-permute-start(bf16[32,32,128]{2,1,0:T(8,128)(2,1)S(1)} %collective-permute-done.refs_1_), channel_id=1, source_target_pairs={{0,2},{2,4},{4,6},{6,8},{8,10},{10,12},{12,14},{14,0},{1,3},{3,5},... | collective-permute-start | bytes 786440 | tf_op jit(solution)/shard_map/ppermute | solution.py:236
  39.0 37.1 %copy-start.4 = (bf16[32,32,128]{2,1,0:T(8,128)(2,1)}, bf16[32,32,128]{2,1,0:T(8,128)(2,1)S(1)}, u32[]{:S(2)}) copy-start(bf16[32,32,128]{2,1,0:T(8,128)(2,1)S(1)} %collective-permute-done.3.refs_2_) | copy-start | bytes 786436
  39.0 8.3 %collective-permute-start.4 = (bf16[32,32,128]{2,1,0:T(8,128)(2,1)S(1)}, bf16[32,32,128]{2,1,0:T(8,128)(2,1)S(1)}, u32[]{:S(2)}, u32[]{:S(2)}) collective-permute-start(bf16[32,32,128]{2,1,0:T(8,128)(2,1)S(1)} %collective-permute-done.3.refs_2_), channel_id=1, source_target_pairs={{0,14},{2,0},{4,2},{6,4},{8,6},{10,8},{12,10},{14,12},{1,15},{3,1}... | collective-permute-start | bytes 786440 | tf_op jit(solution)/shard_map/ppermute | solution.py:236
  45.4 30.8 %copy-start.5 = (bf16[32,32,128]{2,1,0:T(8,128)(2,1)}, bf16[32,32,128]{2,1,0:T(8,128)(2,1)S(1)}, u32[]{:S(2)}) copy-start(bf16[32,32,128]{2,1,0:T(8,128)(2,1)S(1)} %collective-permute-done.1.refs_3_) | copy-start | bytes 786436
  45.4 16.9 %collective-permute-start.2 = (bf16[32,32,128]{2,1,0:T(8,128)(2,1)S(1)}, bf16[32,32,128]{2,1,0:T(8,128)(2,1)S(1)}, u32[]{:S(2)}, u32[]{:S(2)}) collective-permute-start(bf16[32,32,128]{2,1,0:T(8,128)(2,1)S(1)} %collective-permute-done.1.refs_3_), channel_id=1, source_target_pairs={{0,2},{2,4},{4,6},{6,8},{8,10},{10,12},{12,14},{14,0},{1,3},{3,5},... | collective-permute-start | bytes 786440 | tf_op jit(solution)/shard_map/ppermute | solution.py:236
  47.3 28.8 %copy-start.6 = (bf16[32,32,128]{2,1,0:T(8,128)(2,1)}, bf16[32,32,128]{2,1,0:T(8,128)(2,1)S(1)}, u32[]{:S(2)}) copy-start(bf16[32,32,128]{2,1,0:T(8,128)(2,1)S(1)} %collective-permute-done.4.refs_4_) | copy-start | bytes 786436
  47.3 15.0 %collective-permute-start.5 = (bf16[32,32,128]{2,1,0:T(8,128)(2,1)S(1)}, bf16[32,32,128]{2,1,0:T(8,128)(2,1)S(1)}, u32[]{:S(2)}, u32[]{:S(2)}) collective-permute-start(bf16[32,32,128]{2,1,0:T(8,128)(2,1)S(1)} %collective-permute-done.4.refs_4_), channel_id=1, source_target_pairs={{0,14},{2,0},{4,2},{6,4},{8,6},{10,8},{12,10},{14,12},{1,15},{3,1}... | collective-permute-start | bytes 786440 | tf_op jit(solution)/shard_map/ppermute | solution.py:236
  52.9 23.2 %collective-permute-start.9 = (bf16[3,32,32,128]{3,2,1,0:T(8,128)(2,1)}, bf16[3,32,32,128]{3,2,1,0:T(8,128)(2,1)}, u32[]{:S(2)}, u32[]{:S(2)}) collective-permute-start(bf16[3,32,32,128]{3,2,1,0:T(8,128)(2,1)} %pad_maximum_fusion), channel_id=1, source_target_pairs={{0,1},{1,0},{2,3},{3,2},{4,5},{5,4},{6,7},{7,6},{8,9},{9,8},{10,11... | collective-permute-start | bytes 2359304 | tf_op jit(solution)/shard_map/ppermute | solution.py:240
  60.3 15.7 %collective-permute-start.10 = (bf16[2,32,32,128]{3,2,1,0:T(8,128)(2,1)}, bf16[2,32,32,128]{3,2,1,0:T(8,128)(2,1)}, u32[]{:S(2)}, u32[]{:S(2)}) collective-permute-start(bf16[2,32,32,128]{3,2,1,0:T(8,128)(2,1)} %pad_maximum_fusion.2), channel_id=1, source_target_pairs={{0,1},{1,0},{2,3},{3,2},{4,5},{5,4},{6,7},{7,6},{8,9},{9,8},{10,11... | collective-permute-start | bytes 1572872 | tf_op jit(solution)/shard_map/ppermute | solution.py:240
  62.3 10.5 %collective-permute-start.6 = (bf16[32,32,128]{2,1,0:T(8,128)(2,1)S(1)}, bf16[32,32,128]{2,1,0:T(8,128)(2,1)S(1)}, u32[]{:S(2)}, u32[]{:S(2)}) collective-permute-start(bf16[32,32,128]{2,1,0:T(8,128)(2,1)S(1)} %collective-permute-done.2.refs_0_), channel_id=1, source_target_pairs={{0,2},{2,4},{4,6},{6,8},{8,10},{10,12},{12,14},{14,0},{1,3},{3,5},... | collective-permute-start | bytes 786440 | tf_op jit(solution)/shard_map/ppermute | solution.py:236
  64.3 15.8 %collective-permute-start.7 = (bf16[2,32,32,128]{3,2,1,0:T(8,128)(2,1)S(1)}, bf16[2,32,32,128]{3,2,1,0:T(8,128)(2,1)S(1)}, u32[]{:S(2)}, u32[]{:S(2)}) collective-permute-start(bf16[2,32,32,128]{3,2,1,0:T(8,128)(2,1)S(1)} %pad_maximum_fusion.1), channel_id=1, source_target_pairs={{0,1},{1,0},{2,3},{3,2},{4,5},{5,4},{6,7},{7,6},{8,9},{9,8},{10,11... | collective-permute-start | bytes 1572872 | tf_op jit(solution)/shard_map/ppermute | solution.py:240
  72.8 7.3 %collective-permute-start.8 = (bf16[1,32,32,128]{3,2,1,0:T(8,128)(2,1)S(1)}, bf16[1,32,32,128]{3,2,1,0:T(8,128)(2,1)S(1)}, u32[]{:S(2)}, u32[]{:S(2)}) collective-permute-start(bf16[1,32,32,128]{3,2,1,0:T(8,128)(2,1)S(1)} %bitcast.94), channel_id=1, source_target_pairs={{0,1},{1,0},{2,3},{3,2},{4,5},{5,4},{6,7},{7,6},{8,9},{9,8},{10,11... | collective-permute-start | bytes 786440 | tf_op jit(solution)/shard_map/ppermute | solution.py:240
  84.7 4.6 %collective-permute-start.11 = (bf16[8,512,128]{2,1,0:T(8,128)(2,1)S(1)}, bf16[8,512,128]{2,1,0:T(8,128)(2,1)S(1)}, u32[]{:S(2)}, u32[]{:S(2)}) collective-permute-start(bf16[8,512,128]{2,1,0:T(8,128)(2,1)S(1)} %get-tuple-element.36), channel_id=1, source_target_pairs={{0,1},{1,0},{2,3},{3,2},{4,5},{5,4},{6,7},{7,6},{8,9},{9,8},{10,11... | collective-permute-start | bytes 3145736 | tf_op jit(solution)/shard_map/ppermute | solution.py:240
  89.6 41.6 %copy-start.14 = (f32[31,128]{1,0:T(8,128)S(1)}, f32[31,128]{1,0:T(8,128)}, u32[]{:S(2)}) copy-start(f32[31,128]{1,0:T(8,128)} %param.26) | copy-start | bytes 47620
  89.6 50.9 %copy-start.13 = (bf16[64,128]{1,0:T(8,128)(2,1)S(1)}, bf16[64,128]{1,0:T(8,128)(2,1)}, u32[]{:S(2)}) copy-start(bf16[64,128]{1,0:T(8,128)(2,1)} %param.27) | copy-start | bytes 49156
  89.6 56.6 %copy-start.2 = (bf16[32,16,2048]{2,1,0:T(8,128)(2,1)S(1)}, bf16[32,16,2048]{2,1,0:T(8,128)(2,1)}, u32[]{:S(2)}) copy-start(bf16[32,16,2048]{2,1,0:T(8,128)(2,1)} %get-tuple-element.33) | copy-start | bytes 6291460
  89.6 56.6 %copy-start.8 = (bf16[512,224]{1,0:T(8,128)(2,1)S(1)}, bf16[512,224]{1,0:T(8,128)(2,1)}, u32[]{:S(2)}) copy-start(bf16[512,224]{1,0:T(8,128)(2,1)} %get-tuple-element.32) | copy-start | bytes 688132
  125.9 14.6 %all-to-all-start.2 = ((bf16[32,16,128]{2,1,0:T(8,128)(2,1)}), bf16[32,16,128]{2,1,0:T(8,128)(2,1)S(1)}, u32[]{:S(2)}, u32[]{:S(2)}) async-start(bf16[32,16,128]{2,1,0:T(8,128)(2,1)} %bitcast.15), calls=%async_computation.2 | async-start | bytes 262144 | tf_op jit(solution)/shard_map/all_to_all | solution.py:304
  141.4 6.4 %copy-start.9 = (bf16[512,192]{1,0:T(8,128)(2,1)S(1)}, bf16[512,192]{1,0:T(8,128)(2,1)}, u32[]{:S(2)}) copy-start(bf16[512,192]{1,0:T(8,128)(2,1)} %get-tuple-element.34) | copy-start | bytes 589828
  141.4 6.5 %copy-start.11 = (bf16[192,128]{1,0:T(8,128)(2,1)S(1)}, bf16[192,128]{1,0:T(8,128)(2,1)}, u32[]{:S(2)}) copy-start(bf16[192,128]{1,0:T(8,128)(2,1)} %cotangent.1) | copy-start | bytes 147460
  141.4 26.9 %all-to-all-start.4 = ((bf16[32,64,128]{2,1,0:T(8,128)(2,1)}), bf16[32,64,128]{2,1,0:T(8,128)(2,1)}, u32[]{:S(2)}, u32[]{:S(2)}) async-start(bf16[32,64,128]{2,1,0:T(8,128)(2,1)} %broadcast_in_dim.8), calls=%async_computation.4 | async-start | bytes 1048576 | tf_op jit(solution)/shard_map/all_to_all | solution.py:267
  146.2 20.7 %copy-start.12 = (bf16[192,128]{1,0:T(8,128)(2,1)S(1)}, bf16[192,128]{1,0:T(8,128)(2,1)}, u32[]{:S(2)}) copy-start(bf16[192,128]{1,0:T(8,128)(2,1)} %param.21) | copy-start | bytes 147460
  146.2 20.7 %copy-start.22 = (f32[192]{0:T(256)S(1)}, f32[192]{0:T(256)}, u32[]{:S(2)}) copy-start(f32[192]{0:T(256)} %param.23) | copy-start | bytes 2308
  146.2 20.7 %copy-start.24 = (f32[192]{0:T(256)S(1)}, f32[192]{0:T(256)}, u32[]{:S(2)}) copy-start(f32[192]{0:T(256)} %param.22) | copy-start | bytes 2308
  146.2 20.6 %copy-start.26 = (f32[128]{0:T(128)S(1)}, f32[128]{0:T(128)}, u32[]{:S(2)}) copy-start(f32[128]{0:T(128)} %param.25) | copy-start | bytes 1540
  146.2 20.6 %copy-start.28 = (f32[128]{0:T(128)S(1)}, f32[128]{0:T(128)}, u32[]{:S(2)}) copy-start(f32[128]{0:T(128)} %param.24) | copy-start | bytes 1540
  147.8 20.4 %copy-start.23 = (f32[192]{0:T(256)S(1)}, f32[192]{0:T(256)}, u32[]{:S(2)}) copy-start(f32[192]{0:T(256)} %param.23) | copy-start | bytes 2308
  147.8 20.4 %copy-start.25 = (f32[192]{0:T(256)S(1)}, f32[192]{0:T(256)}, u32[]{:S(2)}) copy-start(f32[192]{0:T(256)} %param.22) | copy-start | bytes 2308
  147.8 20.4 %copy-start.27 = (f32[128]{0:T(128)S(1)}, f32[128]{0:T(128)}, u32[]{:S(2)}) copy-start(f32[128]{0:T(128)} %param.25) | copy-start | bytes 1540
  147.8 20.4 %copy-start.29 = (f32[128]{0:T(128)S(1)}, f32[128]{0:T(128)}, u32[]{:S(2)}) copy-start(f32[128]{0:T(128)} %param.24) | copy-start | bytes 1540
  148.1 21.7 %copy-start.10 = (bf16[192,128]{1,0:T(8,128)(2,1)}, bf16[192,128]{1,0:T(8,128)(2,1)S(1)}, u32[]{:S(2)}) copy-start(bf16[192,128]{1,0:T(8,128)(2,1)S(1)} %fusion.3) | copy-start | bytes 147460
  166.9 30.1 %copy-start.1 = (bf16[32,16,2048]{2,1,0:T(8,128)(2,1)S(1)}, bf16[32,16,2048]{2,1,0:T(8,128)(2,1)}, u32[]{:S(2)}) copy-start(bf16[32,16,2048]{2,1,0:T(8,128)(2,1)} %get-tuple-element.31) | copy-start | bytes 6291460
  166.9 30.1 %copy-start.7 = (bf16[512,224]{1,0:T(8,128)(2,1)S(1)}, bf16[512,224]{1,0:T(8,128)(2,1)}, u32[]{:S(2)}) copy-start(bf16[512,224]{1,0:T(8,128)(2,1)} %get-tuple-element.30) | copy-start | bytes 688132
  169.8 31.4 %all-to-all-start.3 = ((bf16[32,64,128]{2,1,0:T(8,128)(2,1)}), bf16[32,64,128]{2,1,0:T(8,128)(2,1)S(1)}, u32[]{:S(2)}, u32[]{:S(2)}) async-start(bf16[32,64,128]{2,1,0:T(8,128)(2,1)} %bitcast.17), calls=%async_computation.3 | async-start | bytes 1048576 | tf_op jit(solution)/shard_map/all_to_all | solution.py:316
  179.3 20.9 %copy-start.15 = (f32[128]{0:T(128)S(1)}, f32[128]{0:T(128)}, u32[]{:S(2)}) copy-start(f32[128]{0:T(128)} %get-tuple-element.51) | copy-start | bytes 1540
  179.3 20.9 %copy-start.16 = (f32[128]{0:T(128)S(1)}, f32[128]{0:T(128)}, u32[]{:S(2)}) copy-start(f32[128]{0:T(128)} %get-tuple-element.52) | copy-start | bytes 1540
  179.3 20.9 %copy-start.17 = (f32[128]{0:T(128)S(1)}, f32[128]{0:T(128)}, u32[]{:S(2)}) copy-start(f32[128]{0:T(128)} %get-tuple-element.53) | copy-start | bytes 1540
  179.3 20.9 %copy-start.18 = (f32[128]{0:T(128)S(1)}, f32[128]{0:T(128)}, u32[]{:S(2)}) copy-start(f32[128]{0:T(128)} %get-tuple-element.54) | copy-start | bytes 1540
  179.3 20.9 %copy-start.19 = (f32[128]{0:T(128)S(1)}, f32[128]{0:T(128)}, u32[]{:S(2)}) copy-start(f32[128]{0:T(128)} %get-tuple-element.55) | copy-start | bytes 1540
  179.3 20.9 %copy-start.20 = (f32[128]{0:T(128)S(1)}, f32[128]{0:T(128)}, u32[]{:S(2)}) copy-start(f32[128]{0:T(128)} %get-tuple-element.56) | copy-start | bytes 1540
  179.3 20.9 %copy-start.21 = (f32[128]{0:T(128)S(1)}, f32[128]{0:T(128)}, u32[]{:S(2)}) copy-start(f32[128]{0:T(128)} %get-tuple-element.57) | copy-start | bytes 1540
  195.7 4.5 %collective-permute-start.12 = (f32[30,128]{1,0:T(8,128)S(1)}, f32[30,128]{1,0:T(8,128)S(1)}, u32[]{:S(2)}, u32[]{:S(2)}) collective-permute-start(f32[30,128]{1,0:T(8,128)S(1)} %slice.256), channel_id=1, source_target_pairs={{16,0},{32,16},{48,32},{64,48},{80,64},{96,80},{112,96},{128,112},... | collective-permute-start | bytes 46088 | tf_op jit(solution)/shard_map/ppermute | solution.py:328

commit v4 on v3

--- a/solution.py
+++ b/solution.py
@@ -247,8 +247,12 @@
 def all_blocks(own):
     chips = lax.axis_size("chip")
     arrived = [own]
-    for n, steps in enumerate(ring_order(chips)[1:]):
+    for n, steps in enumerate(ring_order(chips)[1:-1]):
         arrived.append(along_chips(arrived[max(0, n - 1)], 1 if steps < 0 else -1))
+    half = own.shape[0] // 2
+    low = along_chips(arrived[-4][:half], 2)
+    high = along_chips(arrived[-3][half:], -2)
+    arrived.append(jnp.concatenate([low, high], axis=0))
     shared, at = ([], 0)
     for size in BATCHES:
         shared.append(to_other_core(jnp.stack(arrived[at : at + size])))

time: 205 us -> 210 us (1.024)
  starting transfers between devices: 58.7 us -> 63.6 us
    ppermute x7 -> x8, starting transfers between devices: 21.9 us -> 27.6 us  [along_chips(): lax.ppermute(value, 'chip', [(y, (y + steps) % count) for y in range(coun...]
    all_to_all x1, blocking collectives: 35.5 us -> 33.3 us  [added_up(): lax.all_to_all(both.astype(BF16), 'chip', split_axis=0, concat_axis=0, ti...]
    ppermute x7 -> x8, waiting for transfers between devices: 10.2 us -> 12.2 us  [along_chips(): lax.ppermute(value, 'chip', [(y, (y + steps) % count) for y in range(coun...]
  transfers between devices with their start and end apart: 16 -> 17, of which waited for: 6 -> 7; matrix products, arithmetic and copies ran while one was open for 4% -> 4% of each run, Pallas kernels for 2% -> 2%
where the time goes in v4:
time: 210 us; the launch traced here: 207 us
  blocking collectives  93 us (44%)
  starting transfers between devices  63.6 us (30%)
  waiting for transfers between devices  25.1 us (12%)
  Pallas kernels  10.6 us (5%)
  matrix products  6.32 us (3%)
  other arithmetic  4.94 us (2%)
    all_to_all x1, blocking collectives, added_up(): lax.all_to_all(both.astype(BF16), 'chip', split_axis=0, concat_axis=0, ti...  33.3 us
    ppermute x8, starting transfers between devices, along_chips(): lax.ppermute(value, 'chip', [(y, (y + steps) % count) for y in range(coun...  27.6 us
    all_to_all x1, blocking collectives, steps(): own = lax.all_to_all(sent, 'sp', split_axis=0, concat_axis=0, tiled=True)  25 us
    all_gather x1, blocking collectives, steps(): columns = lax.all_gather(grad_stream, TP, axis=1, tiled=True)  18.7 us
    all_gather x1, blocking collectives, steps(): sums = lax.all_gather(sums, TP, axis=0, tiled=False)  15.9 us
    ppermute x5, starting transfers between devices, to_other_core(): return lax.ppermute(value, 'core', [(0, 1), (1, 0)])  15.3 us
    ppermute x8, waiting for transfers between devices, along_chips(): lax.ppermute(value, 'chip', [(y, (y + steps) % count) for y in range(coun...  12.2 us
    all_to_all x1, starting transfers between devices, steps(): lax.all_to_all(proj_part, 'sp', split_axis=0, concat_axis=0, tiled=True)  9.43 us
  transfers between devices with their start and end apart: 17, of which 7 were waited for; matrix products, arithmetic and copies ran while one was open for 4% of the time, Pallas kernels for 2%

profile of v4, /device:TPU:1, one launch (start us, length us, event | category | flops | bytes accessed | tf_op | source)
XLA Modules:
  0.0 206.6 jit_solution(9649079649321875340)
XLA Ops:
  0.6 2.1 %send_rows.1 = (bf16[32,32,128]{2,1,0:T(8,128)(2,1)}, bf16[512,192]{1,0:T(8,128)(2,1)}) custom-call(s32[2,192]{1,0:T(2,128)} %bitcast.103, f32[2,192]{1,0:T(2,128)} %bitcast.104, bf16[192,128]{1,0:T(8,128)(2,1)} %rows.1, bf16[192,128]{1,0:T(8,128)(2,1)} %cotangent.1), custom_call_target="tpu_custom_call" | custom-call | tf_op jit(solution)/shard_map/send_rows/pallas_call | solution.py:64
  2.7 25.0 %all_to_all.25.refs_0_ = bf16[32,32,128]{2,1,0:T(8,128)(2,1)S(1)} all-to-all(bf16[32,32,128]{2,1,0:T(8,128)(2,1)} %get-tuple-element.21), channel_id=1, replica_groups=mesh['sp'=32,'chip'=8,'core'=2] {'sp'}, dimensions={0} | all-to-all | bytes 524288 | tf_op jit(solution)/shard_map/all_to_all | solution.py:298
  27.7 3.2 %collective-permute-start = (bf16[32,32,128]{2,1,0:T(8,128)(2,1)S(1)}, bf16[32,32,128]{2,1,0:T(8,128)(2,1)S(1)}, u32[]{:S(2)}, u32[]{:S(2)}) collective-permute-start(bf16[32,32,128]{2,1,0:T(8,128)(2,1)S(1)} %all_to_all.25.refs_0_), channel_id=1, source_target_pairs={{0,2},{2,4},{4,6},{6,8},{8,10},{10,12},{12,14},{14,0},{1,3},{3,5},... | collective-permute-start | bytes 786440 | tf_op jit(solution)/shard_map/ppermute | solution.py:236
  30.9 3.8 %collective-permute-start.3 = (bf16[32,32,128]{2,1,0:T(8,128)(2,1)S(1)}, bf16[32,32,128]{2,1,0:T(8,128)(2,1)S(1)}, u32[]{:S(2)}, u32[]{:S(2)}) collective-permute-start(bf16[32,32,128]{2,1,0:T(8,128)(2,1)S(1)} %all_to_all.25.refs_0_), channel_id=1, source_target_pairs={{0,14},{2,0},{4,2},{6,4},{8,6},{10,8},{12,10},{14,12},{1,15},{3,1}... | collective-permute-start | bytes 786440 | tf_op jit(solution)/shard_map/ppermute | solution.py:236
  34.8 2.3 %collective-permute-done.refs_1_ = bf16[32,32,128]{2,1,0:T(8,128)(2,1)S(1)} collective-permute-done((bf16[32,32,128]{2,1,0:T(8,128)(2,1)S(1)}, bf16[32,32,128]{2,1,0:T(8,128)(2,1)S(1)}, u32[]{:S(2)}, u32[]{:S(2)}) %collective-permute-start) | collective-permute-done | bytes 262176 | tf_op jit(solution)/shard_map/ppermute | solution.py:236
  37.1 1.9 collective-permute-start.1
  39.0 4.6 %collective-permute-start.4 = (bf16[32,32,128]{2,1,0:T(8,128)(2,1)S(1)}, bf16[32,32,128]{2,1,0:T(8,128)(2,1)S(1)}, u32[]{:S(2)}, u32[]{:S(2)}) collective-permute-start(bf16[32,32,128]{2,1,0:T(8,128)(2,1)S(1)} %collective-permute-done.3.refs_2_), channel_id=1, source_target_pairs={{0,14},{2,0},{4,2},{6,4},{8,6},{10,8},{12,10},{14,12},{1,15},{3,1}... | collective-permute-start | bytes 786440 | tf_op jit(solution)/shard_map/ppermute | solution.py:236
  43.6 1.8 collective-permute-done.1.refs_3_
  45.4 1.9 collective-permute-start.2
  47.3 4.6 %collective-permute-start.5 = (bf16[32,32,128]{2,1,0:T(8,128)(2,1)S(1)}, bf16[32,32,128]{2,1,0:T(8,128)(2,1)S(1)}, u32[]{:S(2)}, u32[]{:S(2)}) collective-permute-start(bf16[32,32,128]{2,1,0:T(8,128)(2,1)S(1)} %collective-permute-done.4.refs_4_), channel_id=1, source_target_pairs={{0,14},{2,0},{4,2},{6,4},{8,6},{10,8},{12,10},{14,12},{1,15},{3,1}... | collective-permute-start | bytes 786440 | tf_op jit(solution)/shard_map/ppermute | solution.py:236
  51.9 1.0 pad_maximum_fusion
  52.9 6.6 %collective-permute-start.10 = (bf16[3,32,32,128]{3,2,1,0:T(8,128)(2,1)}, bf16[3,32,32,128]{3,2,1,0:T(8,128)(2,1)}, u32[]{:S(2)}, u32[]{:S(2)}) collective-permute-start(bf16[3,32,32,128]{3,2,1,0:T(8,128)(2,1)} %pad_maximum_fusion), channel_id=1, source_target_pairs={{0,1},{1,0},{2,3},{3,2},{4,5},{5,4},{6,7},{7,6},{8,9},{9,8},{10,11... | collective-permute-start | bytes 2359304 | tf_op jit(solution)/shard_map/ppermute | solution.py:240
  59.5 0.8 pad_maximum_fusion.2
  60.3 1.9 collective-permute-start.11
  62.3 1.9 collective-permute-start.6
  64.2 0.1 pad_maximum_fusion.1
  64.3 2.5 %collective-permute-start.8 = (bf16[2,32,32,128]{3,2,1,0:T(8,128)(2,1)S(1)}, bf16[2,32,32,128]{3,2,1,0:T(8,128)(2,1)S(1)}, u32[]{:S(2)}, u32[]{:S(2)}) collective-permute-start(bf16[2,32,32,128]{3,2,1,0:T(8,128)(2,1)S(1)} %pad_maximum_fusion.1), channel_id=1, source_target_pairs={{0,1},{1,0},{2,3},{3,2},{4,5},{5,4},{6,7},{7,6},{8,9},{9,8},{10,11... | collective-permute-start | bytes 1572872 | tf_op jit(solution)/shard_map/ppermute | solution.py:240
  66.8 5.7 %collective-permute-start.7 = (bf16[16,32,128]{2,1,0:T(8,128)(2,1)S(1)}, bf16[16,32,128]{2,1,0:T(8,128)(2,1)S(1)}, u32[]{:S(2)}, u32[]{:S(2)}) collective-permute-start(bf16[16,32,128]{2,1,0:T(8,128)(2,1)S(1)} %slice.265), channel_id=1, source_target_pairs={{0,12},{2,14},{4,0},{6,2},{8,4},{10,6},{12,8},{14,10},{1,13},{3,15... | collective-permute-start | bytes 393224 | tf_op jit(solution)/shard_map/ppermute | solution.py:236
  72.5 0.9 collective-permute-done.6
  73.4 7.2 %collective-permute-done.7 = bf16[16,32,128]{2,1,0:T(8,128)(2,1)S(1)} collective-permute-done((bf16[16,32,128]{2,1,0:T(8,128)(2,1)S(1)}, bf16[16,32,128]{2,1,0:T(8,128)(2,1)S(1)}, u32[]{:S(2)}, u32[]{:S(2)}) %collective-permute-start.7) | collective-permute-done | bytes 131104 | tf_op jit(solution)/shard_map/ppermute | solution.py:236
  80.6 2.3 %collective-permute-start.9 = (bf16[1,32,32,128]{3,2,1,0:T(8,128)(2,1)S(1)}, bf16[1,32,32,128]{3,2,1,0:T(8,128)(2,1)S(1)}, u32[]{:S(2)}, u32[]{:S(2)}) collective-permute-start(bf16[1,32,32,128]{3,2,1,0:T(8,128)(2,1)S(1)} %bitcast.94), channel_id=1, source_target_pairs={{0,1},{1,0},{2,3},{3,2},{4,5},{5,4},{6,7},{7,6},{8,9},{9,8},{10,11... | collective-permute-start | bytes 786440 | tf_op jit(solution)/shard_map/ppermute | solution.py:240
  83.0 3.9 %first_products.1 = (bf16[32,16,2048]{2,1,0:T(8,128)(2,1)S(1)}, bf16[32,16,2048]{2,1,0:T(8,128)(2,1)S(1)}, f32[512,224]{1,0:T(8,128)S(1)}, f32[512,224]{1,0:T(8,...) custom-call(s32[1]{0:T(128)} %bitcast.me, ...), custom_call_target="tpu_custom_call" | custom-call | flops 939524096 | bytes 12582912 | tf_op jit(solution)/shard_map/first_products/pallas_call | solution.py:140
  86.9 4.6 %rest_products.1 = (bf16[32,16,2048]{2,1,0:T(8,128)(2,1)S(1)}, bf16[32,16,2048]{2,1,0:T(8,128)(2,1)S(1)}, bf16[8,512,128]{2,1,0:T(8,128)(2,1)S(1)}, bf16[8,512,1...) custom-call(s32[1]{0:T(128)} %bitcast.me, ...), custom_call_target="tpu_custom_call", output_to_operand_aliasing={{0}: (6, {}), {1}: (7, {})} | custom-call | flops 1409286144 | bytes 12582912 | tf_op jit(solution)/shard_map/rest_products/pallas_call | solution.py:212
  91.6 2.0 collective-permute-start.12
  93.6 2.5 %collective-permute-done.12 = bf16[8,512,128]{2,1,0:T(8,128)(2,1)S(1)} collective-permute-done((bf16[8,512,128]{2,1,0:T(8,128)(2,1)S(1)}, bf16[8,512,128]{2,1,0:T(8,128)(2,1)S(1)}, u32[]{:S(2)}, u32[]{:S(2)}) %collective-permute-start.12) | collective-permute-done | bytes 1048608 | tf_op jit(solution)/shard_map/ppermute | solution.py:240
  96.1 0.3 add_convert_fusion
  96.5 33.3 %all_to_all.26 = bf16[8,512,128]{2,1,0:T(8,128)(2,1)S(1)} all-to-all(bf16[8,512,128]{2,1,0:T(8,128)(2,1)S(1)} %add_convert_fusion), channel_id=1, replica_groups=mesh['sp'=32,'chip'=8,'core'=2] {'chip'}, dimensions={0} | all-to-all | bytes 2097152 | tf_op jit(solution)/shard_map/all_to_all | solution.py:265
  129.8 0.8 reduce_sum.48
  130.6 5.2 %all-to-all-start.2 = ((bf16[32,16,128]{2,1,0:T(8,128)(2,1)}), bf16[32,16,128]{2,1,0:T(8,128)(2,1)S(1)}, u32[]{:S(2)}, u32[]{:S(2)}) async-start(bf16[32,16,128]{2,1,0:T(8,128)(2,1)} %bitcast.15), calls=%async_computation.2 | async-start | bytes 262144 | tf_op jit(solution)/shard_map/all_to_all | solution.py:308
  135.9 0.6 slice_bitcast_fusion.30
  136.5 8.7 %all-to-all-done.2 = bf16[32,16,128]{2,1,0:T(8,128)(2,1)S(1)} async-done(((bf16[32,16,128]{2,1,0:T(8,128)(2,1)}), bf16[32,16,128]{2,1,0:T(8,128)(2,1)S(1)}, u32[]{:S(2)}, u32[]{:S(2)}) %all-to-all-start.2) | async-done | bytes 131104 | tf_op jit(solution)/shard_map/all_to_all | solution.py:308
  145.2 0.9 broadcast_in_dim.8
  146.1 4.7 %all-to-all-start.4 = ((bf16[32,64,128]{2,1,0:T(8,128)(2,1)}), bf16[32,64,128]{2,1,0:T(8,128)(2,1)}, u32[]{:S(2)}, u32[]{:S(2)}) async-start(bf16[32,64,128]{2,1,0:T(8,128)(2,1)} %broadcast_in_dim.8), calls=%async_computation.4 | async-start | bytes 1048576 | tf_op jit(solution)/shard_map/all_to_all | solution.py:271
  151.0 1.6 fusion.1
  152.6 0.3 fusion.3
  152.9 18.7 %all_gather.9 = bf16[192,2048]{1,0:T(8,128)(2,1)S(1)} all-gather(bf16[192,128]{1,0:T(8,128)(2,1)S(1)} %fusion.3), channel_id=1, replica_groups=mesh['sp'=32,'chip'=8,'core'=2] {'chip','core'}, dimensions={1}, use_global_device_ids=true | all-gather | bytes 835584 | tf_op jit(solution)/shard_map/all_gather | solution.py:314
  171.6 1.4 convolution_convert_fusion.2
  173.0 1.5 fusion.100
  174.6 9.4 %all-to-all-start.3 = ((bf16[32,64,128]{2,1,0:T(8,128)(2,1)}), bf16[32,64,128]{2,1,0:T(8,128)(2,1)S(1)}, u32[]{:S(2)}, u32[]{:S(2)}) async-start(bf16[32,64,128]{2,1,0:T(8,128)(2,1)} %bitcast.17), calls=%async_computation.3 | async-start | bytes 1048576 | tf_op jit(solution)/shard_map/all_to_all | solution.py:320
  184.1 0.1 pad_maximum_fusion.4
  184.2 15.9 %all-gather.1 = f32[16,1,384]{2,1,0:T(1,128)S(1)} all-gather(f32[1,1,384]{2,1,0:T(1,128)S(1)} %reshape.47), channel_id=2, replica_groups=mesh['sp'=32,'chip'=8,'core'=2] {'chip','core'}, dimensions={0}, use_global_device_ids=true | all-gather | bytes 26112 | tf_op jit(solution)/shard_map/all_gather | solution.py:324
  200.1 0.1 slice_multiply_fusion.1
  200.2 0.2 subtract_multiply_fusion
  200.4 1.3 collective-permute-start.13
  201.7 1.6 fusion
  203.3 1.6 collective-permute-done.13
  205.0 0.9 fusion.8
  205.9 0.7 convert_reduce_fusion
  (78 shorter events, 0.3 us)
Async XLA Ops:
  27.7 39.1 %copy-start = (bf16[32,32,128]{2,1,0:T(8,128)(2,1)}, bf16[32,32,128]{2,1,0:T(8,128)(2,1)S(1)}, u32[]{:S(2)}) copy-start(bf16[32,32,128]{2,1,0:T(8,128)(2,1)S(1)} %all_to_all.25.refs_0_) | copy-start | bytes 786436
  27.7 9.3 %collective-permute-start = (bf16[32,32,128]{2,1,0:T(8,128)(2,1)S(1)}, bf16[32,32,128]{2,1,0:T(8,128)(2,1)S(1)}, u32[]{:S(2)}, u32[]{:S(2)}) collective-permute-start(bf16[32,32,128]{2,1,0:T(8,128)(2,1)S(1)} %all_to_all.25.refs_0_), channel_id=1, source_target_pairs={{0,2},{2,4},{4,6},{6,8},{8,10},{10,12},{12,14},{14,0},{1,3},{3,5},... | collective-permute-start | bytes 786440 | tf_op jit(solution)/shard_map/ppermute | solution.py:236
  30.9 8.0 %collective-permute-start.3 = (bf16[32,32,128]{2,1,0:T(8,128)(2,1)S(1)}, bf16[32,32,128]{2,1,0:T(8,128)(2,1)S(1)}, u32[]{:S(2)}, u32[]{:S(2)}) collective-permute-start(bf16[32,32,128]{2,1,0:T(8,128)(2,1)S(1)} %all_to_all.25.refs_0_), channel_id=1, source_target_pairs={{0,14},{2,0},{4,2},{6,4},{8,6},{10,8},{12,10},{14,12},{1,15},{3,1}... | collective-permute-start | bytes 786440 | tf_op jit(solution)/shard_map/ppermute | solution.py:236
  37.1 29.7 %copy-start.5 = (bf16[32,32,128]{2,1,0:T(8,128)(2,1)}, bf16[32,32,128]{2,1,0:T(8,128)(2,1)S(1)}, u32[]{:S(2)}) copy-start(bf16[32,32,128]{2,1,0:T(8,128)(2,1)S(1)} %collective-permute-done.refs_1_) | copy-start | bytes 786436
  37.1 8.3 %collective-permute-start.1 = (bf16[32,32,128]{2,1,0:T(8,128)(2,1)S(1)}, bf16[32,32,128]{2,1,0:T(8,128)(2,1)S(1)}, u32[]{:S(2)}, u32[]{:S(2)}) collective-permute-start(bf16[32,32,128]{2,1,0:T(8,128)(2,1)S(1)} %collective-permute-done.refs_1_), channel_id=1, source_target_pairs={{0,2},{2,4},{4,6},{6,8},{8,10},{10,12},{12,14},{14,0},{1,3},{3,5},... | collective-permute-start | bytes 786440 | tf_op jit(solution)/shard_map/ppermute | solution.py:236
  39.0 27.8 %copy-start.6 = (bf16[32,32,128]{2,1,0:T(8,128)(2,1)}, bf16[32,32,128]{2,1,0:T(8,128)(2,1)S(1)}, u32[]{:S(2)}) copy-start(bf16[32,32,128]{2,1,0:T(8,128)(2,1)S(1)} %collective-permute-done.3.refs_2_) | copy-start | bytes 786436
  39.0 8.3 %collective-permute-start.4 = (bf16[32,32,128]{2,1,0:T(8,128)(2,1)S(1)}, bf16[32,32,128]{2,1,0:T(8,128)(2,1)S(1)}, u32[]{:S(2)}, u32[]{:S(2)}) collective-permute-start(bf16[32,32,128]{2,1,0:T(8,128)(2,1)S(1)} %collective-permute-done.3.refs_2_), channel_id=1, source_target_pairs={{0,14},{2,0},{4,2},{6,4},{8,6},{10,8},{12,10},{14,12},{1,15},{3,1}... | collective-permute-start | bytes 786440 | tf_op jit(solution)/shard_map/ppermute | solution.py:236
  45.4 21.4 %copy-start.3 = (bf16[32,32,128]{2,1,0:T(8,128)(2,1)}, bf16[32,32,128]{2,1,0:T(8,128)(2,1)S(1)}, u32[]{:S(2)}) copy-start(bf16[32,32,128]{2,1,0:T(8,128)(2,1)S(1)} %collective-permute-done.1.refs_3_) | copy-start | bytes 786436
  45.4 18.8 %collective-permute-start.2 = (bf16[32,32,128]{2,1,0:T(8,128)(2,1)S(1)}, bf16[32,32,128]{2,1,0:T(8,128)(2,1)S(1)}, u32[]{:S(2)}, u32[]{:S(2)}) collective-permute-start(bf16[32,32,128]{2,1,0:T(8,128)(2,1)S(1)} %collective-permute-done.1.refs_3_), channel_id=1, source_target_pairs={{0,2},{2,4},{4,6},{6,8},{8,10},{10,12},{12,14},{14,0},{1,3},{3,5},... | collective-permute-start | bytes 786440 | tf_op jit(solution)/shard_map/ppermute | solution.py:236
  47.3 19.5 %copy-start.4 = (bf16[32,32,128]{2,1,0:T(8,128)(2,1)}, bf16[32,32,128]{2,1,0:T(8,128)(2,1)S(1)}, u32[]{:S(2)}) copy-start(bf16[32,32,128]{2,1,0:T(8,128)(2,1)S(1)} %collective-permute-done.4.refs_4_) | copy-start | bytes 786436
  47.3 16.9 %collective-permute-start.5 = (bf16[32,32,128]{2,1,0:T(8,128)(2,1)S(1)}, bf16[32,32,128]{2,1,0:T(8,128)(2,1)S(1)}, u32[]{:S(2)}, u32[]{:S(2)}) collective-permute-start(bf16[32,32,128]{2,1,0:T(8,128)(2,1)S(1)} %collective-permute-done.4.refs_4_), channel_id=1, source_target_pairs={{0,14},{2,0},{4,2},{6,4},{8,6},{10,8},{12,10},{14,12},{1,15},{3,1}... | collective-permute-start | bytes 786440 | tf_op jit(solution)/shard_map/ppermute | solution.py:236
  52.9 30.1 %collective-permute-start.10 = (bf16[3,32,32,128]{3,2,1,0:T(8,128)(2,1)}, bf16[3,32,32,128]{3,2,1,0:T(8,128)(2,1)}, u32[]{:S(2)}, u32[]{:S(2)}) collective-permute-start(bf16[3,32,32,128]{3,2,1,0:T(8,128)(2,1)} %pad_maximum_fusion), channel_id=1, source_target_pairs={{0,1},{1,0},{2,3},{3,2},{4,5},{5,4},{6,7},{7,6},{8,9},{9,8},{10,11... | collective-permute-start | bytes 2359304 | tf_op jit(solution)/shard_map/ppermute | solution.py:240
  60.3 22.6 %collective-permute-start.11 = (bf16[2,32,32,128]{3,2,1,0:T(8,128)(2,1)}, bf16[2,32,32,128]{3,2,1,0:T(8,128)(2,1)}, u32[]{:S(2)}, u32[]{:S(2)}) collective-permute-start(bf16[2,32,32,128]{3,2,1,0:T(8,128)(2,1)} %pad_maximum_fusion.2), channel_id=1, source_target_pairs={{0,1},{1,0},{2,3},{3,2},{4,5},{5,4},{6,7},{7,6},{8,9},{9,8},{10,11... | collective-permute-start | bytes 1572872 | tf_op jit(solution)/shard_map/ppermute | solution.py:240
  62.3 11.1 %collective-permute-start.6 = (bf16[16,32,128]{2,1,0:T(8,128)(2,1)S(1)}, bf16[16,32,128]{2,1,0:T(8,128)(2,1)S(1)}, u32[]{:S(2)}, u32[]{:S(2)}) collective-permute-start(bf16[16,32,128]{2,1,0:T(8,128)(2,1)S(1)} %slice.264), channel_id=1, source_target_pairs={{0,4},{2,6},{4,8},{6,10},{8,12},{10,14},{12,0},{14,2},{1,5},{3,7},... | collective-permute-start | bytes 393224 | tf_op jit(solution)/shard_map/ppermute | solution.py:236
  64.3 22.6 %collective-permute-start.8 = (bf16[2,32,32,128]{3,2,1,0:T(8,128)(2,1)S(1)}, bf16[2,32,32,128]{3,2,1,0:T(8,128)(2,1)S(1)}, u32[]{:S(2)}, u32[]{:S(2)}) collective-permute-start(bf16[2,32,32,128]{3,2,1,0:T(8,128)(2,1)S(1)} %pad_maximum_fusion.1), channel_id=1, source_target_pairs={{0,1},{1,0},{2,3},{3,2},{4,5},{5,4},{6,7},{7,6},{8,9},{9,8},{10,11... | collective-permute-start | bytes 1572872 | tf_op jit(solution)/shard_map/ppermute | solution.py:240
  66.8 13.8 %collective-permute-start.7 = (bf16[16,32,128]{2,1,0:T(8,128)(2,1)S(1)}, bf16[16,32,128]{2,1,0:T(8,128)(2,1)S(1)}, u32[]{:S(2)}, u32[]{:S(2)}) collective-permute-start(bf16[16,32,128]{2,1,0:T(8,128)(2,1)S(1)} %slice.265), channel_id=1, source_target_pairs={{0,12},{2,14},{4,0},{6,2},{8,4},{10,6},{12,8},{14,10},{1,13},{3,15... | collective-permute-start | bytes 393224 | tf_op jit(solution)/shard_map/ppermute | solution.py:236
  80.6 6.3 %collective-permute-start.9 = (bf16[1,32,32,128]{3,2,1,0:T(8,128)(2,1)S(1)}, bf16[1,32,32,128]{3,2,1,0:T(8,128)(2,1)S(1)}, u32[]{:S(2)}, u32[]{:S(2)}) collective-permute-start(bf16[1,32,32,128]{3,2,1,0:T(8,128)(2,1)S(1)} %bitcast.94), channel_id=1, source_target_pairs={{0,1},{1,0},{2,3},{3,2},{4,5},{5,4},{6,7},{7,6},{8,9},{9,8},{10,11... | collective-permute-start | bytes 786440 | tf_op jit(solution)/shard_map/ppermute | solution.py:240
  91.6 4.6 %collective-permute-start.12 = (bf16[8,512,128]{2,1,0:T(8,128)(2,1)S(1)}, bf16[8,512,128]{2,1,0:T(8,128)(2,1)S(1)}, u32[]{:S(2)}, u32[]{:S(2)}) collective-permute-start(bf16[8,512,128]{2,1,0:T(8,128)(2,1)S(1)} %get-tuple-element.36), channel_id=1, source_target_pairs={{0,1},{1,0},{2,3},{3,2},{4,5},{5,4},{6,7},{7,6},{8,9},{9,8},{10,11... | collective-permute-start | bytes 3145736 | tf_op jit(solution)/shard_map/ppermute | solution.py:240
  96.4 39.5 %copy-start.14 = (f32[31,128]{1,0:T(8,128)S(1)}, f32[31,128]{1,0:T(8,128)}, u32[]{:S(2)}) copy-start(f32[31,128]{1,0:T(8,128)} %param.26) | copy-start | bytes 47620
  96.4 48.8 %copy-start.13 = (bf16[64,128]{1,0:T(8,128)(2,1)S(1)}, bf16[64,128]{1,0:T(8,128)(2,1)}, u32[]{:S(2)}) copy-start(bf16[64,128]{1,0:T(8,128)(2,1)} %param.27) | copy-start | bytes 49156
  96.4 54.5 %copy-start.2 = (bf16[32,16,2048]{2,1,0:T(8,128)(2,1)S(1)}, bf16[32,16,2048]{2,1,0:T(8,128)(2,1)}, u32[]{:S(2)}) copy-start(bf16[32,16,2048]{2,1,0:T(8,128)(2,1)} %get-tuple-element.33) | copy-start | bytes 6291460
  96.4 54.5 %copy-start.8 = (bf16[512,224]{1,0:T(8,128)(2,1)S(1)}, bf16[512,224]{1,0:T(8,128)(2,1)}, u32[]{:S(2)}) copy-start(bf16[512,224]{1,0:T(8,128)(2,1)} %get-tuple-element.32) | copy-start | bytes 688132
  130.6 14.6 %all-to-all-start.2 = ((bf16[32,16,128]{2,1,0:T(8,128)(2,1)}), bf16[32,16,128]{2,1,0:T(8,128)(2,1)S(1)}, u32[]{:S(2)}, u32[]{:S(2)}) async-start(bf16[32,16,128]{2,1,0:T(8,128)(2,1)} %bitcast.15), calls=%async_computation.2 | async-start | bytes 262144 | tf_op jit(solution)/shard_map/all_to_all | solution.py:308
  146.1 6.4 %copy-start.9 = (bf16[512,192]{1,0:T(8,128)(2,1)S(1)}, bf16[512,192]{1,0:T(8,128)(2,1)}, u32[]{:S(2)}) copy-start(bf16[512,192]{1,0:T(8,128)(2,1)} %get-tuple-element.34) | copy-start | bytes 589828
  146.1 6.4 %copy-start.11 = (bf16[192,128]{1,0:T(8,128)(2,1)S(1)}, bf16[192,128]{1,0:T(8,128)(2,1)}, u32[]{:S(2)}) copy-start(bf16[192,128]{1,0:T(8,128)(2,1)} %cotangent.1) | copy-start | bytes 147460
  146.1 26.9 %all-to-all-start.4 = ((bf16[32,64,128]{2,1,0:T(8,128)(2,1)}), bf16[32,64,128]{2,1,0:T(8,128)(2,1)}, u32[]{:S(2)}, u32[]{:S(2)}) async-start(bf16[32,64,128]{2,1,0:T(8,128)(2,1)} %broadcast_in_dim.8), calls=%async_computation.4 | async-start | bytes 1048576 | tf_op jit(solution)/shard_map/all_to_all | solution.py:271
  150.9 20.7 %copy-start.12 = (bf16[192,128]{1,0:T(8,128)(2,1)S(1)}, bf16[192,128]{1,0:T(8,128)(2,1)}, u32[]{:S(2)}) copy-start(bf16[192,128]{1,0:T(8,128)(2,1)} %param.21) | copy-start | bytes 147460
  150.9 20.7 %copy-start.22 = (f32[192]{0:T(256)S(1)}, f32[192]{0:T(256)}, u32[]{:S(2)}) copy-start(f32[192]{0:T(256)} %param.23) | copy-start | bytes 2308
  150.9 20.7 %copy-start.24 = (f32[192]{0:T(256)S(1)}, f32[192]{0:T(256)}, u32[]{:S(2)}) copy-start(f32[192]{0:T(256)} %param.22) | copy-start | bytes 2308
  150.9 20.6 %copy-start.26 = (f32[128]{0:T(128)S(1)}, f32[128]{0:T(128)}, u32[]{:S(2)}) copy-start(f32[128]{0:T(128)} %param.25) | copy-start | bytes 1540
  151.0 20.6 %copy-start.28 = (f32[128]{0:T(128)S(1)}, f32[128]{0:T(128)}, u32[]{:S(2)}) copy-start(f32[128]{0:T(128)} %param.24) | copy-start | bytes 1540
  152.6 20.4 %copy-start.23 = (f32[192]{0:T(256)S(1)}, f32[192]{0:T(256)}, u32[]{:S(2)}) copy-start(f32[192]{0:T(256)} %param.23) | copy-start | bytes 2308
  152.6 20.4 %copy-start.25 = (f32[192]{0:T(256)S(1)}, f32[192]{0:T(256)}, u32[]{:S(2)}) copy-start(f32[192]{0:T(256)} %param.22) | copy-start | bytes 2308
  152.6 20.4 %copy-start.27 = (f32[128]{0:T(128)S(1)}, f32[128]{0:T(128)}, u32[]{:S(2)}) copy-start(f32[128]{0:T(128)} %param.25) | copy-start | bytes 1540
  152.6 20.4 %copy-start.29 = (f32[128]{0:T(128)S(1)}, f32[128]{0:T(128)}, u32[]{:S(2)}) copy-start(f32[128]{0:T(128)} %param.24) | copy-start | bytes 1540
  152.8 21.7 %copy-start.10 = (bf16[192,128]{1,0:T(8,128)(2,1)}, bf16[192,128]{1,0:T(8,128)(2,1)S(1)}, u32[]{:S(2)}) copy-start(bf16[192,128]{1,0:T(8,128)(2,1)S(1)} %fusion.3) | copy-start | bytes 147460
  171.6 30.1 %copy-start.1 = (bf16[32,16,2048]{2,1,0:T(8,128)(2,1)S(1)}, bf16[32,16,2048]{2,1,0:T(8,128)(2,1)}, u32[]{:S(2)}) copy-start(bf16[32,16,2048]{2,1,0:T(8,128)(2,1)} %get-tuple-element.31) | copy-start | bytes 6291460
  171.6 30.1 %copy-start.7 = (bf16[512,224]{1,0:T(8,128)(2,1)S(1)}, bf16[512,224]{1,0:T(8,128)(2,1)}, u32[]{:S(2)}) copy-start(bf16[512,224]{1,0:T(8,128)(2,1)} %get-tuple-element.30) | copy-start | bytes 688132
  174.6 31.4 %all-to-all-start.3 = ((bf16[32,64,128]{2,1,0:T(8,128)(2,1)}), bf16[32,64,128]{2,1,0:T(8,128)(2,1)S(1)}, u32[]{:S(2)}, u32[]{:S(2)}) async-start(bf16[32,64,128]{2,1,0:T(8,128)(2,1)} %bitcast.17), calls=%async_computation.3 | async-start | bytes 1048576 | tf_op jit(solution)/shard_map/all_to_all | solution.py:320
  184.0 20.9 %copy-start.15 = (f32[128]{0:T(128)S(1)}, f32[128]{0:T(128)}, u32[]{:S(2)}) copy-start(f32[128]{0:T(128)} %get-tuple-element.51) | copy-start | bytes 1540
  184.0 20.9 %copy-start.16 = (f32[128]{0:T(128)S(1)}, f32[128]{0:T(128)}, u32[]{:S(2)}) copy-start(f32[128]{0:T(128)} %get-tuple-element.52) | copy-start | bytes 1540
  184.0 20.9 %copy-start.17 = (f32[128]{0:T(128)S(1)}, f32[128]{0:T(128)}, u32[]{:S(2)}) copy-start(f32[128]{0:T(128)} %get-tuple-element.53) | copy-start | bytes 1540
  184.0 20.9 %copy-start.18 = (f32[128]{0:T(128)S(1)}, f32[128]{0:T(128)}, u32[]{:S(2)}) copy-start(f32[128]{0:T(128)} %get-tuple-element.54) | copy-start | bytes 1540
  184.0 20.9 %copy-start.19 = (f32[128]{0:T(128)S(1)}, f32[128]{0:T(128)}, u32[]{:S(2)}) copy-start(f32[128]{0:T(128)} %get-tuple-element.55) | copy-start | bytes 1540
  184.0 20.9 %copy-start.20 = (f32[128]{0:T(128)S(1)}, f32[128]{0:T(128)}, u32[]{:S(2)}) copy-start(f32[128]{0:T(128)} %get-tuple-element.56) | copy-start | bytes 1540
  184.1 20.9 %copy-start.21 = (f32[128]{0:T(128)S(1)}, f32[128]{0:T(128)}, u32[]{:S(2)}) copy-start(f32[128]{0:T(128)} %get-tuple-element.57) | copy-start | bytes 1540
  200.4 4.5 %collective-permute-start.13 = (f32[30,128]{1,0:T(8,128)S(1)}, f32[30,128]{1,0:T(8,128)S(1)}, u32[]{:S(2)}, u32[]{:S(2)}) collective-permute-start(f32[30,128]{1,0:T(8,128)S(1)} %slice.266), channel_id=1, source_target_pairs={{16,0},{32,16},{48,32},{64,48},{80,64},{96,80},{112,96},{128,112},... | collective-permute-start | bytes 46088 | tf_op jit(solution)/shard_map/ppermute | solution.py:332

commit v5 on v3

--- a/solution.py
+++ b/solution.py
@@ -34,7 +34,7 @@
     return [pl.BlockSpec(memory_space=space)] * count
 
 
-def send_body(routes, weights, rows, cotangent, sent, place_out, *, experts, slots):
+def places(routes, weights, experts, slots):
     top, tokens = routes.shape
     expert = lax.broadcasted_iota(jnp.int32, (experts, tokens), 0)
     named = [(expert == routes[k : k + 1, :]).astype(F32) for k in range(top)]
@@ -50,7 +50,13 @@
         slot = jnp.sum(earlier * named[k], axis=0, keepdims=True).astype(jnp.int32)
         hit = (position == routes[k : k + 1, :] * slots + slot).astype(F32)
         place = place + hit
-        weight = weight + jnp.sum(hit * weights[k : k + 1, :], axis=1, keepdims=True)
+        if weights is not None:
+            weight = weight + jnp.sum(hit * weights[k : k + 1, :], axis=1, keepdims=True)
+    return place, weight
+
+
+def send_body(routes, weights, rows, cotangent, sent, place_out, *, experts, slots):
+    place, weight = places(routes, weights, experts, slots)
     place = place.astype(BF16)
     place_out[...] = place
     channels = rows.shape[1]
@@ -71,6 +77,64 @@
         ),
         name="send_rows",
     )(routes, weights, rows, cotangent)
+
+
+def rim_body(routes, place_out, *, experts, slots):
+    place, _ = places(routes, None, experts, slots)
+    place_out[...] = place.astype(BF16)
+
+
+def rim_places(routes, experts, slots):
+    return pl.pallas_call(
+        functools.partial(rim_body, experts=experts, slots=slots),
+        in_specs=whole(1),
+        out_specs=whole(1)[0],
+        out_shape=jax.ShapeDtypeStruct((experts * slots, routes.shape[1]), BF16),
+        name="rim_places",
+    )(routes)
+
+
+def summed_body(arrived, out):
+    experts, both, width = out.shape
+    total = functools.reduce(jnp.add, [part[...].astype(F32) for part in [arrived.at[k] for k in range(arrived.shape[0])]])
+    total = total.astype(BF16).reshape(experts, both // 2, width)
+    out[:, : both // 2, :] = total
+    out[: experts - 1, both // 2 :, :] = total[1:]
+    out[experts - 1 :, both // 2 :, :] = total[:1]
+
+
+def summed(arrived, experts):
+    _, count, width = arrived.shape
+    return pl.pallas_call(
+        summed_body,
+        in_specs=whole(1),
+        out_specs=whole(1)[0],
+        out_shape=pltpu.VMEM((experts, 2 * count // experts, width), BF16),
+        compiler_params=pltpu.CompilerParams(vmem_limit_bytes=12 * 1024 * 1024),
+        name="summed",
+    )(arrived)
+
+
+def combined_body(returned, place, rim_place, cotangent, rim_cotangent, out):
+    _, both, width = returned.shape
+    tokens = cotangent.shape[0]
+    mine = returned[:, : both // 2, :].reshape(-1, width)
+    after = returned[:, both // 2 :, :].reshape(-1, width)
+    out[:tokens, :] = (cotangent[...].astype(F32) + dot(place[...], mine, 0, 0)).astype(BF16)
+    rim = rim_cotangent[...].astype(F32) + dot(rim_place[...], after, 0, 0)
+    out[tokens:, :] = rim.astype(BF16)
+
+
+def combined(returned, place, rim_place, cotangent, rim_cotangent):
+    tokens = cotangent.shape[0] + rim_cotangent.shape[0]
+    return pl.pallas_call(
+        combined_body,
+        in_specs=whole(5),
+        out_specs=whole(1)[0],
+        out_shape=pltpu.VMEM((tokens, cotangent.shape[1]), BF16),
+        compiler_params=pltpu.CompilerParams(vmem_limit_bytes=12 * 1024 * 1024),
+        name="combined",
+    )(returned, place, rim_place, cotangent, rim_cotangent)
 
 
 def columns(chip, core, width):
@@ -236,6 +300,11 @@
     return lax.ppermute(value, "chip", [(y, (y + steps) % count) for y in range(count)])
 
 
+def from_after(value):
+    count = lax.axis_size("sp")
+    return lax.ppermute(value, "sp", [(source, source - 1) for source in range(1, count)])
+
+
 def to_other_core(value):
     return lax.ppermute(value, "core", [(0, 1), (1, 0)])
 
@@ -259,7 +328,12 @@
 def added_up(kept, given):
     both = kept.astype(F32) + to_other_core(given).astype(F32)
     arrived = lax.all_to_all(both.astype(BF16), "chip", split_axis=0, concat_axis=0, tiled=True)
-    return jnp.sum(arrived.astype(F32), axis=0).astype(BF16)
+    return arrived
+
+
+def affine(value, mean, rstd, gain, shift):
+    normed = (value.astype(F32) - mean[:, None]) * rstd[:, None]
+    return normed, normed * gain[None, :] + shift[None, :]
 
 
 def sent_to_all(value, axis):
@@ -299,36 +373,41 @@
     _, _, kept, given, rows, routed, hidden, up_grad = rest_products(
         me, mine[done:], others[EARLY:], early, slots, blocks
     )
-    shared = added_up(kept, given)
-    shared = shared.reshape(devices, slots, channels)
+    rim = 8 * (-(-(taps.shape[0] - 1) // 8))
+    rim_cotangent, rim_pre = from_after(jnp.stack([cotangent[:rim], conv_pre[:rim]]))
+    facts = [routes[:rim, 0].astype(F32), routes[:rim, 1].astype(F32)]
+    facts = from_after(jnp.stack([*facts, norm_mean[:rim], norm_rstd[:rim]]))
+    rim_place = rim_places(facts[:2].astype(jnp.int32), devices, slots)
+    shared = summed(added_up(kept, given), devices)
     returned = lax.all_to_all(shared, "sp", split_axis=0, concat_axis=0, tiled=True)
     grad_up = dot(up_grad, rows.reshape(-1, rows.shape[2]), 0, 0).astype(BF16)[None]
     grad_down = dot(hidden, routed.reshape(-1, routed.shape[2]), 0, 0).astype(BF16)[None]
-    grad_stream = (
-        cotangent.astype(F32) + dot(place, returned.reshape(devices * slots, channels), 0, 0)
-    ).astype(BF16)
-    columns = lax.all_gather(grad_stream, TP, axis=1, tiled=True)
-    normed = (conv_pre.astype(F32) - norm_mean[:, None]) * norm_rstd[:, None]
-    pre_act = normed * ln_gain[None, :] + ln_shift[None, :]
+    stream = combined(returned, place, rim_place, cotangent, rim_cotangent)
+    grad_stream = stream[:local_tokens]
+    columns = lax.all_gather(stream, TP, axis=1, tiled=True)
+    own_act = affine(conv_pre, norm_mean, norm_rstd, ln_gain, ln_shift)[1]
+    activated = (own_act * jax.nn.sigmoid(own_act)).astype(BF16)
+    proj_part = dot(columns[:local_tokens], activated, 0, 0).astype(BF16)
+    proj_part = proj_part.reshape(devices, -1, channels)
+    proj_parts = lax.all_to_all(proj_part, "sp", split_axis=0, concat_axis=0, tiled=True)
+    mean = jnp.concatenate([norm_mean, facts[2]])
+    rstd = jnp.concatenate([norm_rstd, facts[3]])
+    wide_pre = jnp.concatenate([conv_pre, rim_pre], axis=0)
+    normed, pre_act = affine(wide_pre, mean, rstd, ln_gain, ln_shift)
     act_sigmoid = jax.nn.sigmoid(pre_act)
-    activated = (pre_act * act_sigmoid).astype(BF16)
-    proj_part = dot(columns, activated, 0, 0).astype(BF16).reshape(devices, -1, channels)
-    proj_parts = lax.all_to_all(proj_part, "sp", split_axis=0, concat_axis=0, tiled=True)
     act_grad = dot(columns, proj, 1, 0)
     normed_grad = act_grad * silu_slope(pre_act, act_sigmoid) * ln_gain[None, :]
-    sums = jnp.concatenate([jnp.sum(normed_grad, axis=1), jnp.sum(normed_grad * normed, axis=1)])
+    sums = jnp.stack([jnp.sum(normed_grad, axis=1), jnp.sum(normed_grad * normed, axis=1)])
+    spare = -sums.shape[1] % 128
+    sums = jnp.pad(sums, ((0, 0), (0, spare))).reshape(-1)
     sums = lax.all_gather(sums, TP, axis=0, tiled=False)
     sums = jnp.sum(sums, axis=0)
-    first_sum, second_sum = (sums[:local_tokens], sums[local_tokens:])
+    first_sum, second_sum = sums.reshape(2, -1)[:, : local_tokens + rim]
     width = channels * blocks
-    conv_grad = norm_rstd[:, None] * (
+    extended = rstd[:, None] * (
         normed_grad - first_sum[:, None] / width - normed * (second_sum[:, None] / width)
     )
     lag_count = taps.shape[0]
-    rim_rows = lax.ppermute(
-        conv_grad[: lag_count - 1], "sp", [(source, source - 1) for source in range(1, devices)]
-    )
-    extended = jnp.concatenate([conv_grad, rim_rows], axis=0)
     grad_conv = jnp.zeros((local_tokens, channels), F32)
     for lag in range(lag_count):
         grad_conv = grad_conv + taps[lag][None, :] * extended[lag : lag + local_tokens]

time: 205 us -> 205 us (level)
  blocking collectives: 95.1 us -> 59.6 us
  waiting for transfers between devices: 23.2 us -> 47.4 us
  starting transfers between devices: 58.7 us -> 66.5 us
  Pallas kernels: 10.6 us -> 13.3 us
    all_to_all x1 -> x0, blocking collectives: 35.5 us -> none  [added_up(): lax.all_to_all(both.astype(BF16), 'chip', split_axis=0, concat_axis=0, ti...]
    all_to_all x0 -> x1, waiting for transfers between devices: none -> 24.5 us  [added_up(): lax.all_to_all(both.astype(BF16), 'chip', split_axis=0, concat_axis=0, ti...]
    all_to_all x0 -> x1, starting transfers between devices: none -> 6.53 us  [added_up(): lax.all_to_all(both.astype(BF16), 'chip', split_axis=0, concat_axis=0, ti...]
    pallas_call x0 -> x3, Pallas kernels: none -> 2.68 us  [the longest x1 1.58 us: rim_places(): pl.pallas_call(functools.partial(rim_body, experts=experts, slots=slots),...]
    dot_general x5 -> x4, matrix products: 6.33 us -> 6.67 us  [dot(): lax.dot_general(a, b, (((a_dim,), (b_dim,)), ((), ())), preferred_element...]
  transfers between devices with their start and end apart: 16 -> 18, of which waited for: 6 -> 7; matrix products, arithmetic and copies ran while one was open for 4% -> 6% of each run, Pallas kernels for 2% -> 3%
where the time goes in v5:
time: 205 us; the launch traced here: 204 us
  starting transfers between devices  66.5 us (32%)
  blocking collectives  59.6 us (29%)
  waiting for transfers between devices  47.4 us (23%)
  Pallas kernels  13.3 us (6%)
  matrix products  6.67 us (3%)
  other arithmetic  5.74 us (3%)
  local copies, waits for them, and re-layouts  3.08 us (2%)
    all_to_all x1, blocking collectives, steps(): own = lax.all_to_all(sent, 'sp', split_axis=0, concat_axis=0, tiled=True)  25 us
    all_to_all x1, waiting for transfers between devices, added_up(): lax.all_to_all(both.astype(BF16), 'chip', split_axis=0, concat_axis=0, ti...  24.5 us
    ppermute x7, starting transfers between devices, along_chips(): lax.ppermute(value, 'chip', [(y, (y + steps) % count) for y in range(coun...  21.9 us
    all_gather x1, blocking collectives, steps(): columns = lax.all_gather(stream, TP, axis=1, tiled=True)  18.5 us
    ppermute x5, starting transfers between devices, to_other_core(): return lax.ppermute(value, 'core', [(0, 1), (1, 0)])  16.1 us
    all_gather x1, blocking collectives, steps(): sums = lax.all_gather(sums, TP, axis=0, tiled=False)  16.1 us
    ppermute x7, waiting for transfers between devices, along_chips(): lax.ppermute(value, 'chip', [(y, (y + steps) % count) for y in range(coun...  10.2 us
    all_to_all x1, starting transfers between devices, steps(): lax.all_to_all(proj_part, 'sp', split_axis=0, concat_axis=0, tiled=True)  9.51 us
  transfers between devices with their start and end apart: 18, of which 7 were waited for; matrix products, arithmetic and copies ran while one was open for 6% of the time, Pallas kernels for 3%

profile of v5, /device:TPU:1, one launch (start us, length us, event | category | flops | bytes accessed | tf_op | source)
XLA Modules:
  0.0 203.8 jit_solution(16741500049999763036)
XLA Ops:
  0.6 2.1 %send_rows.1 = (bf16[32,32,128]{2,1,0:T(8,128)(2,1)}, bf16[512,192]{1,0:T(8,128)(2,1)}) custom-call(s32[2,192]{1,0:T(2,128)} %bitcast.122, f32[2,192]{1,0:T(2,128)} %bitcast.125, bf16[192,128]{1,0:T(8,128)(2,1)} %rows.1, bf16[192,128]{1,0:T(8,128)(2,1)} %cotangent.3), custom_call_target="tpu_custom_call" | custom-call | tf_op jit(solution)/shard_map/send_rows/pallas_call | solution.py:70
  2.7 25.0 %all_to_all.25.refs_0_ = bf16[32,32,128]{2,1,0:T(8,128)(2,1)S(1)} all-to-all(bf16[32,32,128]{2,1,0:T(8,128)(2,1)} %get-tuple-element.21), channel_id=1, replica_groups=mesh['sp'=32,'chip'=8,'core'=2] {'sp'}, dimensions={0} | all-to-all | bytes 524288 | tf_op jit(solution)/shard_map/all_to_all | solution.py:368
  27.7 3.2 %collective-permute-start = (bf16[32,32,128]{2,1,0:T(8,128)(2,1)S(1)}, bf16[32,32,128]{2,1,0:T(8,128)(2,1)S(1)}, u32[]{:S(2)}, u32[]{:S(2)}) collective-permute-start(bf16[32,32,128]{2,1,0:T(8,128)(2,1)S(1)} %all_to_all.25.refs_0_), channel_id=1, source_target_pairs={{0,2},{2,4},{4,6},{6,8},{8,10},{10,12},{12,14},{14,0},{1,3},{3,5},... | collective-permute-start | bytes 786440 | tf_op jit(solution)/shard_map/ppermute | solution.py:300
  30.9 3.8 %collective-permute-start.3 = (bf16[32,32,128]{2,1,0:T(8,128)(2,1)S(1)}, bf16[32,32,128]{2,1,0:T(8,128)(2,1)S(1)}, u32[]{:S(2)}, u32[]{:S(2)}) collective-permute-start(bf16[32,32,128]{2,1,0:T(8,128)(2,1)S(1)} %all_to_all.25.refs_0_), channel_id=1, source_target_pairs={{0,14},{2,0},{4,2},{6,4},{8,6},{10,8},{12,10},{14,12},{1,15},{3,1}... | collective-permute-start | bytes 786440 | tf_op jit(solution)/shard_map/ppermute | solution.py:300
  34.8 2.3 %collective-permute-done.refs_1_ = bf16[32,32,128]{2,1,0:T(8,128)(2,1)S(1)} collective-permute-done((bf16[32,32,128]{2,1,0:T(8,128)(2,1)S(1)}, bf16[32,32,128]{2,1,0:T(8,128)(2,1)S(1)}, u32[]{:S(2)}, u32[]{:S(2)}) %collective-permute-start) | collective-permute-done | bytes 262176 | tf_op jit(solution)/shard_map/ppermute | solution.py:300
  37.1 1.9 collective-permute-start.1
  39.0 4.6 %collective-permute-start.4 = (bf16[32,32,128]{2,1,0:T(8,128)(2,1)S(1)}, bf16[32,32,128]{2,1,0:T(8,128)(2,1)S(1)}, u32[]{:S(2)}, u32[]{:S(2)}) collective-permute-start(bf16[32,32,128]{2,1,0:T(8,128)(2,1)S(1)} %collective-permute-done.3.refs_2_), channel_id=1, source_target_pairs={{0,14},{2,0},{4,2},{6,4},{8,6},{10,8},{12,10},{14,12},{1,15},{3,1}... | collective-permute-start | bytes 786440 | tf_op jit(solution)/shard_map/ppermute | solution.py:300
  43.6 1.8 collective-permute-done.1.refs_3_
  45.4 1.9 collective-permute-start.2
  47.3 4.6 %collective-permute-start.5 = (bf16[32,32,128]{2,1,0:T(8,128)(2,1)S(1)}, bf16[32,32,128]{2,1,0:T(8,128)(2,1)S(1)}, u32[]{:S(2)}, u32[]{:S(2)}) collective-permute-start(bf16[32,32,128]{2,1,0:T(8,128)(2,1)S(1)} %collective-permute-done.4.refs_4_), channel_id=1, source_target_pairs={{0,14},{2,0},{4,2},{6,4},{8,6},{10,8},{12,10},{14,12},{1,15},{3,1}... | collective-permute-start | bytes 786440 | tf_op jit(solution)/shard_map/ppermute | solution.py:300
  51.9 1.0 pad_maximum_fusion
  52.9 6.6 %collective-permute-start.9 = (bf16[3,32,32,128]{3,2,1,0:T(8,128)(2,1)}, bf16[3,32,32,128]{3,2,1,0:T(8,128)(2,1)}, u32[]{:S(2)}, u32[]{:S(2)}) collective-permute-start(bf16[3,32,32,128]{3,2,1,0:T(8,128)(2,1)} %pad_maximum_fusion), channel_id=1, source_target_pairs={{0,1},{1,0},{2,3},{3,2},{4,5},{5,4},{6,7},{7,6},{8,9},{9,8},{10,11... | collective-permute-start | bytes 2359304 | tf_op jit(solution)/shard_map/ppermute | solution.py:309
  59.5 0.8 pad_maximum_fusion.2
  60.3 1.9 collective-permute-start.10
  62.3 1.9 collective-permute-start.6
  64.3 2.4 %collective-permute-start.7 = (bf16[2,32,32,128]{3,2,1,0:T(8,128)(2,1)S(1)}, bf16[2,32,32,128]{3,2,1,0:T(8,128)(2,1)S(1)}, u32[]{:S(2)}, u32[]{:S(2)}) collective-permute-start(bf16[2,32,32,128]{3,2,1,0:T(8,128)(2,1)S(1)} %pad_maximum_fusion.1), channel_id=1, source_target_pairs={{0,1},{1,0},{2,3},{3,2},{4,5},{5,4},{6,7},{7,6},{8,9},{9,8},{10,11... | collective-permute-start | bytes 1572872 | tf_op jit(solution)/shard_map/ppermute | solution.py:309
  66.7 6.1 %collective-permute-done.6.refs_2_ = bf16[32,32,128]{2,1,0:T(8,128)(2,1)S(1)} collective-permute-done((bf16[32,32,128]{2,1,0:T(8,128)(2,1)S(1)}, bf16[32,32,128]{2,1,0:T(8,128)(2,1)S(1)}, u32[]{:S(2)}, u32[]{:S(2)}) %collective-permute-start.6) | collective-permute-done | bytes 262176 | tf_op jit(solution)/shard_map/ppermute | solution.py:300
  72.8 3.3 %collective-permute-start.8 = (bf16[1,32,32,128]{3,2,1,0:T(8,128)(2,1)S(1)}, bf16[1,32,32,128]{3,2,1,0:T(8,128)(2,1)S(1)}, u32[]{:S(2)}, u32[]{:S(2)}) collective-permute-start(bf16[1,32,32,128]{3,2,1,0:T(8,128)(2,1)S(1)} %bitcast.113), channel_id=1, source_target_pairs={{0,1},{1,0},{2,3},{3,2},{4,5},{5,4},{6,7},{7,6},{8,9},{9,8},{10,11... | collective-permute-start | bytes 786440 | tf_op jit(solution)/shard_map/ppermute | solution.py:309
  76.1 3.9 %first_products.1 = (bf16[32,16,2048]{2,1,0:T(8,128)(2,1)S(1)}, bf16[32,16,2048]{2,1,0:T(8,128)(2,1)S(1)}, f32[512,224]{1,0:T(8,128)S(1)}, f32[512,224]{1,0:T(8,...) custom-call(s32[1]{0:T(128)} %bitcast.me, ...), custom_call_target="tpu_custom_call" | custom-call | flops 939524096 | bytes 12582912 | tf_op jit(solution)/shard_map/first_products/pallas_call | solution.py:204
  80.1 4.6 %rest_products.1 = (bf16[32,16,2048]{2,1,0:T(8,128)(2,1)S(1)}, bf16[32,16,2048]{2,1,0:T(8,128)(2,1)S(1)}, bf16[8,512,128]{2,1,0:T(8,128)(2,1)S(1)}, bf16[8,512,1...) custom-call(s32[1]{0:T(128)} %bitcast.me, ...), custom_call_target="tpu_custom_call", output_to_operand_aliasing={{0}: (6, {}), {1}: (7, {})} | custom-call | flops 1409286144 | bytes 12582912 | tf_op jit(solution)/shard_map/rest_products/pallas_call | solution.py:276
  84.7 1.9 collective-permute-start.11
  86.6 2.6 %collective-permute-done.11 = bf16[8,512,128]{2,1,0:T(8,128)(2,1)S(1)} collective-permute-done((bf16[8,512,128]{2,1,0:T(8,128)(2,1)S(1)}, bf16[8,512,128]{2,1,0:T(8,128)(2,1)S(1)}, u32[]{:S(2)}, u32[]{:S(2)}) %collective-permute-start.11) | collective-permute-done | bytes 1048608 | tf_op jit(solution)/shard_map/ppermute | solution.py:309
  89.3 1.3 add_convert_fusion
  90.5 6.5 %all-to-all-start.1 = ((bf16[8,512,128]{2,1,0:T(8,128)(2,1)}), bf16[8,512,128]{2,1,0:T(8,128)(2,1)S(1)}, u32[]{:S(2)}, u32[]{:S(2)}) async-start(bf16[8,512,128]{2,1,0:T(8,128)(2,1)} %add_convert_fusion), calls=%async_computation.1 | async-start | bytes 2097152 | tf_op jit(solution)/shard_map/all_to_all | solution.py:330
  97.2 1.3 collective-permute-start.12
  98.5 1.3 collective-permute-start.13
  99.8 0.6 slice_bitcast_fusion.36
  100.5 0.6 slice_bitcast_fusion.33
  101.1 0.7 collective-permute-done.12
  101.9 24.5 %all-to-all-done.1.arrived = bf16[8,512,128]{2,1,0:T(8,128)(2,1)S(1)} async-done(((bf16[8,512,128]{2,1,0:T(8,128)(2,1)}), bf16[8,512,128]{2,1,0:T(8,128)(2,1)S(1)}, u32[]{:S(2)}, u32[]{:S(2)}) %all-to-all-start.1) | async-done | bytes 1048608 | tf_op jit(solution)/shard_map/all_to_all | solution.py:330
  126.3 0.8 summed.1
  127.2 5.3 %all-to-all-start.2 = ((bf16[32,32,128]{2,1,0:T(8,128)(2,1)}), bf16[32,32,128]{2,1,0:T(8,128)(2,1)S(1)}, u32[]{:S(2)}, u32[]{:S(2)}) async-start(bf16[32,32,128]{2,1,0:T(8,128)(2,1)} %summed.1), calls=%async_computation.2 | async-start | bytes 524288 | tf_op jit(solution)/shard_map/all_to_all | solution.py:382
  132.4 0.6 slice_convert_fusion.routes
  133.1 1.6 rim_places.1.rim_place
  134.6 9.4 %all-to-all-done.2.returned = bf16[32,32,128]{2,1,0:T(8,128)(2,1)S(1)} async-done(((bf16[32,32,128]{2,1,0:T(8,128)(2,1)}), bf16[32,32,128]{2,1,0:T(8,128)(2,1)S(1)}, u32[]{:S(2)}, u32[]{:S(2)}) %all-to-all-start.2) | async-done | bytes 262176 | tf_op jit(solution)/shard_map/all_to_all | solution.py:382
  144.0 0.9 broadcast_in_dim.8
  145.0 4.6 %all-to-all-start.4 = ((bf16[32,64,128]{2,1,0:T(8,128)(2,1)}), bf16[32,64,128]{2,1,0:T(8,128)(2,1)S(1)}, u32[]{:S(2)}, u32[]{:S(2)}) async-start(bf16[32,64,128]{2,1,0:T(8,128)(2,1)} %broadcast_in_dim.8), calls=%async_computation.4 | async-start | bytes 1048576 | tf_op jit(solution)/shard_map/all_to_all | solution.py:341
  149.6 3.2 %fusion.1 = bf16[1,224,2048]{2,1,0:T(8,128)(2,1)} fusion(bf16[512,224]{1,0:T(8,128)(2,1)S(1)} %copy-done.10, bf16[512,2048]{1,0:T(8,128)(2,1)} %bitcast.116), kind=kOutput, calls=%fused_computation.3 | convolution fusion | flops 470220800 | bytes 3244032 | tf_op jit(solution)/shard_map/dot_general | solution.py:18
  152.8 1.6 fusion
  154.4 0.3 combined.1
  154.7 0.6 slice.295
  155.3 18.5 %all_gather.6 = bf16[224,2048]{1,0:T(8,128)(2,1)S(1)} all-gather(bf16[224,128]{1,0:T(8,128)(2,1)S(1)} %combined.1), channel_id=1, replica_groups=mesh['sp'=32,'chip'=8,'core'=2] {'chip','core'}, dimensions={1}, use_global_device_ids=true | all-gather | bytes 974848 | tf_op jit(solution)/shard_map/all_gather | solution.py:387
  173.9 1.4 convolution_convert_fusion.2
  175.5 9.5 %all-to-all-start.3 = ((bf16[32,64,128]{2,1,0:T(8,128)(2,1)}), bf16[32,64,128]{2,1,0:T(8,128)(2,1)S(1)}, u32[]{:S(2)}, u32[]{:S(2)}) async-start(bf16[32,64,128]{2,1,0:T(8,128)(2,1)} %bitcast.22), calls=%async_computation.3 | async-start | bytes 1048576 | tf_op jit(solution)/shard_map/all_to_all | solution.py:392
  185.0 0.5 fusion.41
  185.6 16.1 %all-gather = f32[16,1,512]{2,1,0:T(1,128)S(1)} all-gather(f32[1,1,512]{2,1,0:T(1,128)S(1)} %reshape.80), channel_id=1, replica_groups=mesh['sp'=32,'chip'=8,'core'=2] {'chip','core'}, dimensions={0}, use_global_device_ids=true | all-gather | bytes 34816 | tf_op jit(solution)/shard_map/all_gather | solution.py:403
  202.1 0.9 fusion.5
  203.1 0.7 convert_reduce_fusion
  (120 shorter events, 0.8 us)
Async XLA Ops:
  27.7 48.4 %copy-start.3 = (bf16[32,32,128]{2,1,0:T(8,128)(2,1)}, bf16[32,32,128]{2,1,0:T(8,128)(2,1)S(1)}, u32[]{:S(2)}) copy-start(bf16[32,32,128]{2,1,0:T(8,128)(2,1)S(1)} %all_to_all.25.refs_0_) | copy-start | bytes 786436
  27.7 9.3 %collective-permute-start = (bf16[32,32,128]{2,1,0:T(8,128)(2,1)S(1)}, bf16[32,32,128]{2,1,0:T(8,128)(2,1)S(1)}, u32[]{:S(2)}, u32[]{:S(2)}) collective-permute-start(bf16[32,32,128]{2,1,0:T(8,128)(2,1)S(1)} %all_to_all.25.refs_0_), channel_id=1, source_target_pairs={{0,2},{2,4},{4,6},{6,8},{8,10},{10,12},{12,14},{14,0},{1,3},{3,5},... | collective-permute-start | bytes 786440 | tf_op jit(solution)/shard_map/ppermute | solution.py:300
  30.9 8.0 %collective-permute-start.3 = (bf16[32,32,128]{2,1,0:T(8,128)(2,1)S(1)}, bf16[32,32,128]{2,1,0:T(8,128)(2,1)S(1)}, u32[]{:S(2)}, u32[]{:S(2)}) collective-permute-start(bf16[32,32,128]{2,1,0:T(8,128)(2,1)S(1)} %all_to_all.25.refs_0_), channel_id=1, source_target_pairs={{0,14},{2,0},{4,2},{6,4},{8,6},{10,8},{12,10},{14,12},{1,15},{3,1}... | collective-permute-start | bytes 786440 | tf_op jit(solution)/shard_map/ppermute | solution.py:300
  37.1 39.1 %copy-start.5 = (bf16[32,32,128]{2,1,0:T(8,128)(2,1)}, bf16[32,32,128]{2,1,0:T(8,128)(2,1)S(1)}, u32[]{:S(2)}) copy-start(bf16[32,32,128]{2,1,0:T(8,128)(2,1)S(1)} %collective-permute-done.refs_1_) | copy-start | bytes 786436
  37.1 8.3 %collective-permute-start.1 = (bf16[32,32,128]{2,1,0:T(8,128)(2,1)S(1)}, bf16[32,32,128]{2,1,0:T(8,128)(2,1)S(1)}, u32[]{:S(2)}, u32[]{:S(2)}) collective-permute-start(bf16[32,32,128]{2,1,0:T(8,128)(2,1)S(1)} %collective-permute-done.refs_1_), channel_id=1, source_target_pairs={{0,2},{2,4},{4,6},{6,8},{8,10},{10,12},{12,14},{14,0},{1,3},{3,5},... | collective-permute-start | bytes 786440 | tf_op jit(solution)/shard_map/ppermute | solution.py:300
  39.0 37.1 %copy-start.6 = (bf16[32,32,128]{2,1,0:T(8,128)(2,1)}, bf16[32,32,128]{2,1,0:T(8,128)(2,1)S(1)}, u32[]{:S(2)}) copy-start(bf16[32,32,128]{2,1,0:T(8,128)(2,1)S(1)} %collective-permute-done.3.refs_2_) | copy-start | bytes 786436
  39.0 8.3 %collective-permute-start.4 = (bf16[32,32,128]{2,1,0:T(8,128)(2,1)S(1)}, bf16[32,32,128]{2,1,0:T(8,128)(2,1)S(1)}, u32[]{:S(2)}, u32[]{:S(2)}) collective-permute-start(bf16[32,32,128]{2,1,0:T(8,128)(2,1)S(1)} %collective-permute-done.3.refs_2_), channel_id=1, source_target_pairs={{0,14},{2,0},{4,2},{6,4},{8,6},{10,8},{12,10},{14,12},{1,15},{3,1}... | collective-permute-start | bytes 786440 | tf_op jit(solution)/shard_map/ppermute | solution.py:300
  45.4 30.8 %copy-start.7 = (bf16[32,32,128]{2,1,0:T(8,128)(2,1)}, bf16[32,32,128]{2,1,0:T(8,128)(2,1)S(1)}, u32[]{:S(2)}) copy-start(bf16[32,32,128]{2,1,0:T(8,128)(2,1)S(1)} %collective-permute-done.1.refs_3_) | copy-start | bytes 786436
  45.4 16.9 %collective-permute-start.2 = (bf16[32,32,128]{2,1,0:T(8,128)(2,1)S(1)}, bf16[32,32,128]{2,1,0:T(8,128)(2,1)S(1)}, u32[]{:S(2)}, u32[]{:S(2)}) collective-permute-start(bf16[32,32,128]{2,1,0:T(8,128)(2,1)S(1)} %collective-permute-done.1.refs_3_), channel_id=1, source_target_pairs={{0,2},{2,4},{4,6},{6,8},{8,10},{10,12},{12,14},{14,0},{1,3},{3,5},... | collective-permute-start | bytes 786440 | tf_op jit(solution)/shard_map/ppermute | solution.py:300
  47.3 28.8 %copy-start.8 = (bf16[32,32,128]{2,1,0:T(8,128)(2,1)}, bf16[32,32,128]{2,1,0:T(8,128)(2,1)S(1)}, u32[]{:S(2)}) copy-start(bf16[32,32,128]{2,1,0:T(8,128)(2,1)S(1)} %collective-permute-done.4.refs_4_) | copy-start | bytes 786436
  47.3 15.0 %collective-permute-start.5 = (bf16[32,32,128]{2,1,0:T(8,128)(2,1)S(1)}, bf16[32,32,128]{2,1,0:T(8,128)(2,1)S(1)}, u32[]{:S(2)}, u32[]{:S(2)}) collective-permute-start(bf16[32,32,128]{2,1,0:T(8,128)(2,1)S(1)} %collective-permute-done.4.refs_4_), channel_id=1, source_target_pairs={{0,14},{2,0},{4,2},{6,4},{8,6},{10,8},{12,10},{14,12},{1,15},{3,1}... | collective-permute-start | bytes 786440 | tf_op jit(solution)/shard_map/ppermute | solution.py:300
  52.9 23.2 %collective-permute-start.9 = (bf16[3,32,32,128]{3,2,1,0:T(8,128)(2,1)}, bf16[3,32,32,128]{3,2,1,0:T(8,128)(2,1)}, u32[]{:S(2)}, u32[]{:S(2)}) collective-permute-start(bf16[3,32,32,128]{3,2,1,0:T(8,128)(2,1)} %pad_maximum_fusion), channel_id=1, source_target_pairs={{0,1},{1,0},{2,3},{3,2},{4,5},{5,4},{6,7},{7,6},{8,9},{9,8},{10,11... | collective-permute-start | bytes 2359304 | tf_op jit(solution)/shard_map/ppermute | solution.py:309
  60.3 15.7 %collective-permute-start.10 = (bf16[2,32,32,128]{3,2,1,0:T(8,128)(2,1)}, bf16[2,32,32,128]{3,2,1,0:T(8,128)(2,1)}, u32[]{:S(2)}, u32[]{:S(2)}) collective-permute-start(bf16[2,32,32,128]{3,2,1,0:T(8,128)(2,1)} %pad_maximum_fusion.2), channel_id=1, source_target_pairs={{0,1},{1,0},{2,3},{3,2},{4,5},{5,4},{6,7},{7,6},{8,9},{9,8},{10,11... | collective-permute-start | bytes 1572872 | tf_op jit(solution)/shard_map/ppermute | solution.py:309
  62.3 10.5 %collective-permute-start.6 = (bf16[32,32,128]{2,1,0:T(8,128)(2,1)S(1)}, bf16[32,32,128]{2,1,0:T(8,128)(2,1)S(1)}, u32[]{:S(2)}, u32[]{:S(2)}) collective-permute-start(bf16[32,32,128]{2,1,0:T(8,128)(2,1)S(1)} %collective-permute-done.2.refs_0_), channel_id=1, source_target_pairs={{0,2},{2,4},{4,6},{6,8},{8,10},{10,12},{12,14},{14,0},{1,3},{3,5},... | collective-permute-start | bytes 786440 | tf_op jit(solution)/shard_map/ppermute | solution.py:300
  64.3 15.8 %collective-permute-start.7 = (bf16[2,32,32,128]{3,2,1,0:T(8,128)(2,1)S(1)}, bf16[2,32,32,128]{3,2,1,0:T(8,128)(2,1)S(1)}, u32[]{:S(2)}, u32[]{:S(2)}) collective-permute-start(bf16[2,32,32,128]{3,2,1,0:T(8,128)(2,1)S(1)} %pad_maximum_fusion.1), channel_id=1, source_target_pairs={{0,1},{1,0},{2,3},{3,2},{4,5},{5,4},{6,7},{7,6},{8,9},{9,8},{10,11... | collective-permute-start | bytes 1572872 | tf_op jit(solution)/shard_map/ppermute | solution.py:309
  72.8 7.3 %collective-permute-start.8 = (bf16[1,32,32,128]{3,2,1,0:T(8,128)(2,1)S(1)}, bf16[1,32,32,128]{3,2,1,0:T(8,128)(2,1)S(1)}, u32[]{:S(2)}, u32[]{:S(2)}) collective-permute-start(bf16[1,32,32,128]{3,2,1,0:T(8,128)(2,1)S(1)} %bitcast.113), channel_id=1, source_target_pairs={{0,1},{1,0},{2,3},{3,2},{4,5},{5,4},{6,7},{7,6},{8,9},{9,8},{10,11... | collective-permute-start | bytes 786440 | tf_op jit(solution)/shard_map/ppermute | solution.py:309
  84.7 4.6 %collective-permute-start.11 = (bf16[8,512,128]{2,1,0:T(8,128)(2,1)S(1)}, bf16[8,512,128]{2,1,0:T(8,128)(2,1)S(1)}, u32[]{:S(2)}, u32[]{:S(2)}) collective-permute-start(bf16[8,512,128]{2,1,0:T(8,128)(2,1)S(1)} %get-tuple-element.35), channel_id=1, source_target_pairs={{0,1},{1,0},{2,3},{3,2},{4,5},{5,4},{6,7},{7,6},{8,9},{9,8},{10,11... | collective-permute-start | bytes 3145736 | tf_op jit(solution)/shard_map/ppermute | solution.py:309
  90.5 53.5 %copy-start.12 = (bf16[64,128]{1,0:T(8,128)(2,1)S(1)}, bf16[64,128]{1,0:T(8,128)(2,1)}, u32[]{:S(2)}) copy-start(bf16[64,128]{1,0:T(8,128)(2,1)} %param.27) | copy-start | bytes 49156
  90.5 35.8 %all-to-all-start.1 = ((bf16[8,512,128]{2,1,0:T(8,128)(2,1)}), bf16[8,512,128]{2,1,0:T(8,128)(2,1)S(1)}, u32[]{:S(2)}, u32[]{:S(2)}) async-start(bf16[8,512,128]{2,1,0:T(8,128)(2,1)} %add_convert_fusion), calls=%async_computation.1 | async-start | bytes 2097152 | tf_op jit(solution)/shard_map/all_to_all | solution.py:330
  97.1 52.5 %copy-start.10 = (bf16[512,224]{1,0:T(8,128)(2,1)S(1)}, bf16[512,224]{1,0:T(8,128)(2,1)}, u32[]{:S(2)}) copy-start(bf16[512,224]{1,0:T(8,128)(2,1)} %get-tuple-element.32) | copy-start | bytes 688132
  97.2 4.6 %collective-permute-start.12 = (f32[4,32]{1,0:T(4,128)S(1)}, f32[4,32]{1,0:T(4,128)S(1)}, u32[]{:S(2)}, u32[]{:S(2)}) collective-permute-start(f32[4,32]{1,0:T(4,128)S(1)} %pad_maximum_fusion.5), channel_id=1, source_target_pairs={{16,0},{32,16},{48,32},{64,48},{80,64},{96,80},{112,96},{128,112},... | collective-permute-start | bytes 1544 | tf_op jit(solution)/shard_map/ppermute | solution.py:305
  98.5 36.1 %collective-permute-start.13 = (bf16[2,32,128]{2,1,0:T(8,128)(2,1)S(1)}, bf16[2,32,128]{2,1,0:T(8,128)(2,1)S(1)}, u32[]{:S(2)}, u32[]{:S(2)}) collective-permute-start(bf16[2,32,128]{2,1,0:T(8,128)(2,1)S(1)} %pad_maximum_fusion.4), channel_id=1, source_target_pairs={{16,0},{32,16},{48,32},{64,48},{80,64},{96,80},{112,96},{128,112},... | collective-permute-start | bytes 49160 | tf_op jit(solution)/shard_map/ppermute | solution.py:305
  127.2 16.9 %all-to-all-start.2 = ((bf16[32,32,128]{2,1,0:T(8,128)(2,1)}), bf16[32,32,128]{2,1,0:T(8,128)(2,1)S(1)}, u32[]{:S(2)}, u32[]{:S(2)}) async-start(bf16[32,32,128]{2,1,0:T(8,128)(2,1)} %summed.1), calls=%async_computation.2 | async-start | bytes 524288 | tf_op jit(solution)/shard_map/all_to_all | solution.py:382
  145.0 30.5 %all-to-all-start.4 = ((bf16[32,64,128]{2,1,0:T(8,128)(2,1)}), bf16[32,64,128]{2,1,0:T(8,128)(2,1)S(1)}, u32[]{:S(2)}, u32[]{:S(2)}) async-start(bf16[32,64,128]{2,1,0:T(8,128)(2,1)} %broadcast_in_dim.8), calls=%async_computation.4 | async-start | bytes 1048576 | tf_op jit(solution)/shard_map/all_to_all | solution.py:341
  175.2 26.7 %copy-start.21 = (f32[128]{0:T(128)S(1)}, f32[128]{0:T(128)}, u32[]{:S(2)}) copy-start(f32[128]{0:T(128)} %get-tuple-element.47) | copy-start | bytes 1540
  175.2 26.7 %copy-start.22 = (f32[128]{0:T(128)S(1)}, f32[128]{0:T(128)}, u32[]{:S(2)}) copy-start(f32[128]{0:T(128)} %get-tuple-element.48) | copy-start | bytes 1540
  175.3 26.7 %copy-start.23 = (f32[128]{0:T(128)S(1)}, f32[128]{0:T(128)}, u32[]{:S(2)}) copy-start(f32[128]{0:T(128)} %get-tuple-element.49) | copy-start | bytes 1540
  175.3 26.7 %copy-start.24 = (f32[128]{0:T(128)S(1)}, f32[128]{0:T(128)}, u32[]{:S(2)}) copy-start(f32[128]{0:T(128)} %get-tuple-element.50) | copy-start | bytes 1540
  175.3 26.7 %copy-start.25 = (f32[128]{0:T(128)S(1)}, f32[128]{0:T(128)}, u32[]{:S(2)}) copy-start(f32[128]{0:T(128)} %get-tuple-element.51) | copy-start | bytes 1540
  175.3 26.7 %copy-start.26 = (f32[128]{0:T(128)S(1)}, f32[128]{0:T(128)}, u32[]{:S(2)}) copy-start(f32[128]{0:T(128)} %get-tuple-element.52) | copy-start | bytes 1540
  175.3 26.7 %copy-start.27 = (f32[128]{0:T(128)S(1)}, f32[128]{0:T(128)}, u32[]{:S(2)}) copy-start(f32[128]{0:T(128)} %get-tuple-element.53) | copy-start | bytes 1540
  175.3 26.7 %copy-start.28 = (f32[128]{0:T(128)S(1)}, f32[128]{0:T(128)}, u32[]{:S(2)}) copy-start(f32[128]{0:T(128)} %get-tuple-element.54) | copy-start | bytes 1540
  175.3 26.7 %copy-start.29 = (f32[128]{0:T(128)S(1)}, f32[128]{0:T(128)}, u32[]{:S(2)}) copy-start(f32[128]{0:T(128)} %get-tuple-element.55) | copy-start | bytes 1540
  175.3 26.7 %copy-start.30 = (f32[128]{0:T(128)S(1)}, f32[128]{0:T(128)}, u32[]{:S(2)}) copy-start(f32[128]{0:T(128)} %get-tuple-element.56) | copy-start | bytes 1540
  175.3 26.7 %copy-start.31 = (f32[128]{0:T(128)S(1)}, f32[128]{0:T(128)}, u32[]{:S(2)}) copy-start(f32[128]{0:T(128)} %get-tuple-element.57) | copy-start | bytes 1540
  175.3 26.7 %copy-start.32 = (f32[128]{0:T(128)S(1)}, f32[128]{0:T(128)}, u32[]{:S(2)}) copy-start(f32[128]{0:T(128)} %get-tuple-element.58) | copy-start | bytes 1540
  175.4 26.7 %copy-start.33 = (f32[128]{0:T(128)S(1)}, f32[128]{0:T(128)}, u32[]{:S(2)}) copy-start(f32[128]{0:T(128)} %get-tuple-element.59) | copy-start | bytes 1540
  175.4 26.7 %copy-start.34 = (f32[128]{0:T(128)S(1)}, f32[128]{0:T(128)}, u32[]{:S(2)}) copy-start(f32[128]{0:T(128)} %get-tuple-element.60) | copy-start | bytes 1540
  175.4 26.7 %copy-start.35 = (f32[128]{0:T(128)S(1)}, f32[128]{0:T(128)}, u32[]{:S(2)}) copy-start(f32[128]{0:T(128)} %get-tuple-element.61) | copy-start | bytes 1540
  175.4 26.7 %copy-start.36 = (f32[128]{0:T(128)S(1)}, f32[128]{0:T(128)}, u32[]{:S(2)}) copy-start(f32[128]{0:T(128)} %get-tuple-element.62) | copy-start | bytes 1540
  175.4 26.7 %copy-start.37 = (f32[128]{0:T(128)S(1)}, f32[128]{0:T(128)}, u32[]{:S(2)}) copy-start(f32[128]{0:T(128)} %get-tuple-element.63) | copy-start | bytes 1540
  175.4 26.7 %copy-start.38 = (f32[128]{0:T(128)S(1)}, f32[128]{0:T(128)}, u32[]{:S(2)}) copy-start(f32[128]{0:T(128)} %get-tuple-element.64) | copy-start | bytes 1540
  175.4 26.7 %copy-start.39 = (f32[128]{0:T(128)S(1)}, f32[128]{0:T(128)}, u32[]{:S(2)}) copy-start(f32[128]{0:T(128)} %get-tuple-element.65) | copy-start | bytes 1540
  175.4 26.7 %copy-start.40 = (f32[128]{0:T(128)S(1)}, f32[128]{0:T(128)}, u32[]{:S(2)}) copy-start(f32[128]{0:T(128)} %get-tuple-element.66) | copy-start | bytes 1540
  175.4 26.7 %copy-start.41 = (f32[128]{0:T(128)S(1)}, f32[128]{0:T(128)}, u32[]{:S(2)}) copy-start(f32[128]{0:T(128)} %get-tuple-element.67) | copy-start | bytes 1540
  175.5 26.7 %copy-start.42 = (f32[128]{0:T(128)S(1)}, f32[128]{0:T(128)}, u32[]{:S(2)}) copy-start(f32[128]{0:T(128)} %get-tuple-element.68) | copy-start | bytes 1540
  175.5 26.7 %copy-start.43 = (f32[128]{0:T(128)S(1)}, f32[128]{0:T(128)}, u32[]{:S(2)}) copy-start(f32[128]{0:T(128)} %get-tuple-element.69) | copy-start | bytes 1540
  175.5 27.6 %all-to-all-start.3 = ((bf16[32,64,128]{2,1,0:T(8,128)(2,1)}), bf16[32,64,128]{2,1,0:T(8,128)(2,1)S(1)}, u32[]{:S(2)}, u32[]{:S(2)}) async-start(bf16[32,64,128]{2,1,0:T(8,128)(2,1)} %bitcast.22), calls=%async_computation.3 | async-start | bytes 1048576 | tf_op jit(solution)/shard_map/all_to_all | solution.py:392
  (16 other events, 220.3 us)

commit v6 on v5

--- a/solution.py
+++ b/solution.py
@@ -89,7 +89,8 @@
         functools.partial(rim_body, experts=experts, slots=slots),
         in_specs=whole(1),
         out_specs=whole(1)[0],
-        out_shape=jax.ShapeDtypeStruct((experts * slots, routes.shape[1]), BF16),
+        out_shape=pltpu.VMEM((experts * slots, routes.shape[1]), BF16),
+        compiler_params=pltpu.CompilerParams(vmem_limit_bytes=12 * 1024 * 1024),
         name="rim_places",
     )(routes)
 
@@ -115,12 +116,14 @@
     )(arrived)
 
 
-def combined_body(returned, place, rim_place, cotangent, rim_cotangent, out):
+def combined_body(returned, place, rim_place, cotangent, rim_cotangent, out, own_out):
     _, both, width = returned.shape
     tokens = cotangent.shape[0]
     mine = returned[:, : both // 2, :].reshape(-1, width)
     after = returned[:, both // 2 :, :].reshape(-1, width)
-    out[:tokens, :] = (cotangent[...].astype(F32) + dot(place[...], mine, 0, 0)).astype(BF16)
+    own = (cotangent[...].astype(F32) + dot(place[...], mine, 0, 0)).astype(BF16)
+    out[:tokens, :] = own
+    own_out[...] = own
     rim = rim_cotangent[...].astype(F32) + dot(rim_place[...], after, 0, 0)
     out[tokens:, :] = rim.astype(BF16)
 
@@ -130,8 +133,11 @@
     return pl.pallas_call(
         combined_body,
         in_specs=whole(5),
-        out_specs=whole(1)[0],
-        out_shape=pltpu.VMEM((tokens, cotangent.shape[1]), BF16),
+        out_specs=whole(2),
+        out_shape=(
+            pltpu.VMEM((tokens, cotangent.shape[1]), BF16),
+            pltpu.VMEM(cotangent.shape, BF16),
+        ),
         compiler_params=pltpu.CompilerParams(vmem_limit_bytes=12 * 1024 * 1024),
         name="combined",
     )(returned, place, rim_place, cotangent, rim_cotangent)
@@ -316,8 +322,12 @@
 def all_blocks(own):
     chips = lax.axis_size("chip")
     arrived = [own]
-    for n, steps in enumerate(ring_order(chips)[1:]):
+    for n, steps in enumerate(ring_order(chips)[1:-1]):
         arrived.append(along_chips(arrived[max(0, n - 1)], 1 if steps < 0 else -1))
+    half = own.shape[0] // 2
+    low = along_chips(arrived[-4][:half], 2)
+    high = along_chips(arrived[-3][half:], -2)
+    arrived.append(jnp.concatenate([low, high], axis=0))
     shared, at = ([], 0)
     for size in BATCHES:
         shared.append(to_other_core(jnp.stack(arrived[at : at + size])))
@@ -382,8 +392,7 @@
     returned = lax.all_to_all(shared, "sp", split_axis=0, concat_axis=0, tiled=True)
     grad_up = dot(up_grad, rows.reshape(-1, rows.shape[2]), 0, 0).astype(BF16)[None]
     grad_down = dot(hidden, routed.reshape(-1, routed.shape[2]), 0, 0).astype(BF16)[None]
-    stream = combined(returned, place, rim_place, cotangent, rim_cotangent)
-    grad_stream = stream[:local_tokens]
+    stream, grad_stream = combined(returned, place, rim_place, cotangent, rim_cotangent)
     columns = lax.all_gather(stream, TP, axis=1, tiled=True)
     own_act = affine(conv_pre, norm_mean, norm_rstd, ln_gain, ln_shift)[1]
     activated = (own_act * jax.nn.sigmoid(own_act)).astype(BF16)

time: 205 us -> 209 us (1.020)
  waiting for transfers between devices: 47.4 us -> 51.2 us
  starting transfers between devices: 66.5 us -> 69.3 us
    ppermute x7 -> x8, starting transfers between devices: 21.9 us -> 27.6 us  [along_chips(): lax.ppermute(value, 'chip', [(y, (y + steps) % count) for y in range(coun...]
    all_to_all x1, starting transfers between devices: 6.53 us -> 4.41 us  [added_up(): lax.all_to_all(both.astype(BF16), 'chip', split_axis=0, concat_axis=0, ti...]
    ppermute x7 -> x8, waiting for transfers between devices: 10.2 us -> 12.2 us  [along_chips(): lax.ppermute(value, 'chip', [(y, (y + steps) % count) for y in range(coun...]
  transfers between devices with their start and end apart: 18 -> 19, of which waited for: 7 -> 8; matrix products, arithmetic and copies ran while one was open for 6% -> 6% of each run, Pallas kernels for 3% -> 3%
where the time goes in v6:
time: 209 us; the launch traced here: 208 us
  starting transfers between devices  69.3 us (33%)
  blocking collectives  59.6 us (29%)
  waiting for transfers between devices  51.2 us (24%)
  Pallas kernels  11.9 us (6%)
  matrix products  6.74 us (3%)
  other arithmetic  5.08 us (2%)
  local copies, waits for them, and re-layouts  2.98 us (1%)
    ppermute x8, starting transfers between devices, along_chips(): lax.ppermute(value, 'chip', [(y, (y + steps) % count) for y in range(coun...  27.6 us
    all_to_all x1, blocking collectives, steps(): own = lax.all_to_all(sent, 'sp', split_axis=0, concat_axis=0, tiled=True)  25 us
    all_to_all x1, waiting for transfers between devices, added_up(): lax.all_to_all(both.astype(BF16), 'chip', split_axis=0, concat_axis=0, ti...  24.5 us
    all_gather x1, blocking collectives, steps(): columns = lax.all_gather(stream, TP, axis=1, tiled=True)  18.5 us
    all_gather x1, blocking collectives, steps(): sums = lax.all_gather(sums, TP, axis=0, tiled=False)  16.1 us
    ppermute x5, starting transfers between devices, to_other_core(): return lax.ppermute(value, 'core', [(0, 1), (1, 0)])  15.3 us
    ppermute x8, waiting for transfers between devices, along_chips(): lax.ppermute(value, 'chip', [(y, (y + steps) % count) for y in range(coun...  12.2 us
    all_to_all x1, waiting for transfers between devices, steps(): lax.all_to_all(shared, 'sp', split_axis=0, concat_axis=0, tiled=True)  11.2 us
  transfers between devices with their start and end apart: 19, of which 8 were waited for; matrix products, arithmetic and copies ran while one was open for 6% of the time, Pallas kernels for 3%

profile of v6, /device:TPU:1, one launch (start us, length us, event | category | flops | bytes accessed | tf_op | source)
XLA Modules:
  0.0 208.2 jit_solution(206598174767863828)
XLA Ops:
  0.6 2.1 %send_rows.1 = (bf16[32,32,128]{2,1,0:T(8,128)(2,1)}, bf16[512,192]{1,0:T(8,128)(2,1)}) custom-call(s32[2,192]{1,0:T(2,128)} %bitcast.122, f32[2,192]{1,0:T(2,128)} %bitcast.125, bf16[192,128]{1,0:T(8,128)(2,1)} %rows.1, bf16[192,128]{1,0:T(8,128)(2,1)} %cotangent.3), custom_call_target="tpu_custom_call" | custom-call | tf_op jit(solution)/shard_map/send_rows/pallas_call | solution.py:70
  2.7 25.0 %all_to_all.25.refs_0_ = bf16[32,32,128]{2,1,0:T(8,128)(2,1)S(1)} all-to-all(bf16[32,32,128]{2,1,0:T(8,128)(2,1)} %get-tuple-element.23), channel_id=1, replica_groups=mesh['sp'=32,'chip'=8,'core'=2] {'sp'}, dimensions={0} | all-to-all | bytes 524288 | tf_op jit(solution)/shard_map/all_to_all | solution.py:378
  27.7 3.2 %collective-permute-start = (bf16[32,32,128]{2,1,0:T(8,128)(2,1)S(1)}, bf16[32,32,128]{2,1,0:T(8,128)(2,1)S(1)}, u32[]{:S(2)}, u32[]{:S(2)}) collective-permute-start(bf16[32,32,128]{2,1,0:T(8,128)(2,1)S(1)} %all_to_all.25.refs_0_), channel_id=1, source_target_pairs={{0,2},{2,4},{4,6},{6,8},{8,10},{10,12},{12,14},{14,0},{1,3},{3,5},... | collective-permute-start | bytes 786440 | tf_op jit(solution)/shard_map/ppermute | solution.py:306
  30.9 3.8 %collective-permute-start.3 = (bf16[32,32,128]{2,1,0:T(8,128)(2,1)S(1)}, bf16[32,32,128]{2,1,0:T(8,128)(2,1)S(1)}, u32[]{:S(2)}, u32[]{:S(2)}) collective-permute-start(bf16[32,32,128]{2,1,0:T(8,128)(2,1)S(1)} %all_to_all.25.refs_0_), channel_id=1, source_target_pairs={{0,14},{2,0},{4,2},{6,4},{8,6},{10,8},{12,10},{14,12},{1,15},{3,1}... | collective-permute-start | bytes 786440 | tf_op jit(solution)/shard_map/ppermute | solution.py:306
  34.8 2.3 %collective-permute-done.refs_1_ = bf16[32,32,128]{2,1,0:T(8,128)(2,1)S(1)} collective-permute-done((bf16[32,32,128]{2,1,0:T(8,128)(2,1)S(1)}, bf16[32,32,128]{2,1,0:T(8,128)(2,1)S(1)}, u32[]{:S(2)}, u32[]{:S(2)}) %collective-permute-start) | collective-permute-done | bytes 262176 | tf_op jit(solution)/shard_map/ppermute | solution.py:306
  37.1 1.9 collective-permute-start.1
  39.0 4.6 %collective-permute-start.4 = (bf16[32,32,128]{2,1,0:T(8,128)(2,1)S(1)}, bf16[32,32,128]{2,1,0:T(8,128)(2,1)S(1)}, u32[]{:S(2)}, u32[]{:S(2)}) collective-permute-start(bf16[32,32,128]{2,1,0:T(8,128)(2,1)S(1)} %collective-permute-done.3.refs_2_), channel_id=1, source_target_pairs={{0,14},{2,0},{4,2},{6,4},{8,6},{10,8},{12,10},{14,12},{1,15},{3,1}... | collective-permute-start | bytes 786440 | tf_op jit(solution)/shard_map/ppermute | solution.py:306
  43.6 1.8 collective-permute-done.1.refs_3_
  45.4 1.9 collective-permute-start.2
  47.3 4.6 %collective-permute-start.5 = (bf16[32,32,128]{2,1,0:T(8,128)(2,1)S(1)}, bf16[32,32,128]{2,1,0:T(8,128)(2,1)S(1)}, u32[]{:S(2)}, u32[]{:S(2)}) collective-permute-start(bf16[32,32,128]{2,1,0:T(8,128)(2,1)S(1)} %collective-permute-done.4.refs_4_), channel_id=1, source_target_pairs={{0,14},{2,0},{4,2},{6,4},{8,6},{10,8},{12,10},{14,12},{1,15},{3,1}... | collective-permute-start | bytes 786440 | tf_op jit(solution)/shard_map/ppermute | solution.py:306
  52.0 6.6 %collective-permute-start.10 = (bf16[3,32,32,128]{3,2,1,0:T(8,128)(2,1)S(1)}, bf16[3,32,32,128]{3,2,1,0:T(8,128)(2,1)}, u32[]{:S(2)}, u32[]{:S(2)}) collective-permute-start(bf16[3,32,32,128]{3,2,1,0:T(8,128)(2,1)S(1)} %pad_maximum_fusion), channel_id=1, source_target_pairs={{0,1},{1,0},{2,3},{3,2},{4,5},{5,4},{6,7},{7,6},{8,9},{9,8},{10,11... | collective-permute-start | bytes 2359304 | tf_op jit(solution)/shard_map/ppermute | solution.py:315
  58.6 0.8 pad_maximum_fusion.2
  59.5 1.9 collective-permute-start.11
  61.4 1.9 collective-permute-start.6
  63.4 0.8 pad_maximum_fusion.1
  64.2 2.5 %collective-permute-start.8 = (bf16[2,32,32,128]{3,2,1,0:T(8,128)(2,1)}, bf16[2,32,32,128]{3,2,1,0:T(8,128)(2,1)S(1)}, u32[]{:S(2)}, u32[]{:S(2)}) collective-permute-start(bf16[2,32,32,128]{3,2,1,0:T(8,128)(2,1)} %pad_maximum_fusion.1), channel_id=1, source_target_pairs={{0,1},{1,0},{2,3},{3,2},{4,5},{5,4},{6,7},{7,6},{8,9},{9,8},{10,11... | collective-permute-start | bytes 1572872 | tf_op jit(solution)/shard_map/ppermute | solution.py:315
  66.7 5.7 %collective-permute-start.7 = (bf16[16,32,128]{2,1,0:T(8,128)(2,1)S(1)}, bf16[16,32,128]{2,1,0:T(8,128)(2,1)S(1)}, u32[]{:S(2)}, u32[]{:S(2)}) collective-permute-start(bf16[16,32,128]{2,1,0:T(8,128)(2,1)S(1)} %slice.300), channel_id=1, source_target_pairs={{0,12},{2,14},{4,0},{6,2},{8,4},{10,6},{12,8},{14,10},{1,13},{3,15... | collective-permute-start | bytes 393224 | tf_op jit(solution)/shard_map/ppermute | solution.py:306
  72.6 7.9 %collective-permute-done.7 = bf16[16,32,128]{2,1,0:T(8,128)(2,1)S(1)} collective-permute-done((bf16[16,32,128]{2,1,0:T(8,128)(2,1)S(1)}, bf16[16,32,128]{2,1,0:T(8,128)(2,1)S(1)}, u32[]{:S(2)}, u32[]{:S(2)}) %collective-permute-start.7) | collective-permute-done | bytes 131104 | tf_op jit(solution)/shard_map/ppermute | solution.py:306
  80.5 2.3 %collective-permute-start.9 = (bf16[1,32,32,128]{3,2,1,0:T(8,128)(2,1)S(1)}, bf16[1,32,32,128]{3,2,1,0:T(8,128)(2,1)S(1)}, u32[]{:S(2)}, u32[]{:S(2)}) collective-permute-start(bf16[1,32,32,128]{3,2,1,0:T(8,128)(2,1)S(1)} %bitcast.113), channel_id=1, source_target_pairs={{0,1},{1,0},{2,3},{3,2},{4,5},{5,4},{6,7},{7,6},{8,9},{9,8},{10,11... | collective-permute-start | bytes 786440 | tf_op jit(solution)/shard_map/ppermute | solution.py:315
  82.9 3.9 %first_products.1 = (bf16[32,16,2048]{2,1,0:T(8,128)(2,1)S(1)}, bf16[32,16,2048]{2,1,0:T(8,128)(2,1)S(1)}, f32[512,224]{1,0:T(8,128)S(1)}, f32[512,224]{1,0:T(8,...) custom-call(s32[1]{0:T(128)} %bitcast.me, ...), custom_call_target="tpu_custom_call" | custom-call | flops 939524096 | bytes 12582912 | tf_op jit(solution)/shard_map/first_products/pallas_call | solution.py:210
  86.8 4.5 %rest_products.1 = (bf16[32,16,2048]{2,1,0:T(8,128)(2,1)S(1)}, bf16[32,16,2048]{2,1,0:T(8,128)(2,1)S(1)}, bf16[8,512,128]{2,1,0:T(8,128)(2,1)S(1)}, bf16[8,512,1...) custom-call(s32[1]{0:T(128)} %bitcast.me, ...), custom_call_target="tpu_custom_call", output_to_operand_aliasing={{0}: (6, {}), {1}: (7, {})} | custom-call | flops 1409286144 | bytes 12582912 | tf_op jit(solution)/shard_map/rest_products/pallas_call | solution.py:282
  91.4 2.0 collective-permute-start.12
  93.4 2.5 %collective-permute-done.12 = bf16[8,512,128]{2,1,0:T(8,128)(2,1)S(1)} collective-permute-done((bf16[8,512,128]{2,1,0:T(8,128)(2,1)S(1)}, bf16[8,512,128]{2,1,0:T(8,128)(2,1)S(1)}, u32[]{:S(2)}, u32[]{:S(2)}) %collective-permute-start.12) | collective-permute-done | bytes 1048608 | tf_op jit(solution)/shard_map/ppermute | solution.py:315
  96.0 1.3 add_convert_fusion
  97.3 4.4 %all-to-all-start.1 = ((bf16[8,512,128]{2,1,0:T(8,128)(2,1)}), bf16[8,512,128]{2,1,0:T(8,128)(2,1)S(1)}, u32[]{:S(2)}, u32[]{:S(2)}) async-start(bf16[8,512,128]{2,1,0:T(8,128)(2,1)} %add_convert_fusion), calls=%async_computation.1 | async-start | bytes 2097152 | tf_op jit(solution)/shard_map/all_to_all | solution.py:340
  101.7 1.3 collective-permute-start.13
  103.1 1.3 collective-permute-start.14
  104.4 0.6 slice_bitcast_fusion.36
  105.0 0.6 slice_bitcast_fusion.33
  105.6 0.7 collective-permute-done.13
  106.4 24.5 %all-to-all-done.1.arrived = bf16[8,512,128]{2,1,0:T(8,128)(2,1)S(1)} async-done(((bf16[8,512,128]{2,1,0:T(8,128)(2,1)}), bf16[8,512,128]{2,1,0:T(8,128)(2,1)S(1)}, u32[]{:S(2)}, u32[]{:S(2)}) %all-to-all-start.1) | async-done | bytes 1048608 | tf_op jit(solution)/shard_map/all_to_all | solution.py:340
  130.9 0.8 summed.1
  131.8 5.2 %all-to-all-start.2 = ((bf16[32,32,128]{2,1,0:T(8,128)(2,1)}), bf16[32,32,128]{2,1,0:T(8,128)(2,1)S(1)}, u32[]{:S(2)}, u32[]{:S(2)}) async-start(bf16[32,32,128]{2,1,0:T(8,128)(2,1)} %summed.1), calls=%async_computation.2 | async-start | bytes 524288 | tf_op jit(solution)/shard_map/all_to_all | solution.py:392
  137.1 0.2 rim_places.1.rim_place
  137.4 11.2 %all-to-all-done.2.returned = bf16[32,32,128]{2,1,0:T(8,128)(2,1)S(1)} async-done(((bf16[32,32,128]{2,1,0:T(8,128)(2,1)}), bf16[32,32,128]{2,1,0:T(8,128)(2,1)S(1)}, u32[]{:S(2)}, u32[]{:S(2)}) %all-to-all-start.2) | async-done | bytes 262176 | tf_op jit(solution)/shard_map/all_to_all | solution.py:392
  148.6 0.9 broadcast_in_dim.8
  149.5 4.6 %all-to-all-start.4 = ((bf16[32,64,128]{2,1,0:T(8,128)(2,1)}), bf16[32,64,128]{2,1,0:T(8,128)(2,1)S(1)}, u32[]{:S(2)}, u32[]{:S(2)}) async-start(bf16[32,64,128]{2,1,0:T(8,128)(2,1)} %broadcast_in_dim.8), calls=%async_computation.4 | async-start | bytes 1048576 | tf_op jit(solution)/shard_map/all_to_all | solution.py:351
  154.2 3.3 %fusion.1 = bf16[1,224,2048]{2,1,0:T(8,128)(2,1)} fusion(bf16[512,224]{1,0:T(8,128)(2,1)} %get-tuple-element.34, bf16[512,2048]{1,0:T(8,128)(2,1)} %bitcast.116), kind=kOutput, calls=%fused_computation.3 | convolution fusion | flops 470220800 | bytes 3244032 | tf_op jit(solution)/shard_map/dot_general | solution.py:18
  157.5 1.6 fusion
  159.1 0.3 combined.1
  159.4 18.5 %all_gather.6 = bf16[224,2048]{1,0:T(8,128)(2,1)S(1)} all-gather(bf16[224,128]{1,0:T(8,128)(2,1)S(1)} %get-tuple-element.40), channel_id=1, replica_groups=mesh['sp'=32,'chip'=8,'core'=2] {'chip','core'}, dimensions={1}, use_global_device_ids=true | all-gather | bytes 974848 | tf_op jit(solution)/shard_map/all_gather | solution.py:396
  177.9 1.4 convolution_convert_fusion.2
  179.4 9.5 %all-to-all-start.3 = ((bf16[32,64,128]{2,1,0:T(8,128)(2,1)}), bf16[32,64,128]{2,1,0:T(8,128)(2,1)S(1)}, u32[]{:S(2)}, u32[]{:S(2)}) async-start(bf16[32,64,128]{2,1,0:T(8,128)(2,1)} %bitcast.22), calls=%async_computation.3 | async-start | bytes 1048576 | tf_op jit(solution)/shard_map/all_to_all | solution.py:401
  188.9 0.5 fusion.41
  189.5 16.1 %all-gather = f32[16,1,512]{2,1,0:T(1,128)S(1)} all-gather(f32[1,1,512]{2,1,0:T(1,128)S(1)} %reshape.80), channel_id=1, replica_groups=mesh['sp'=32,'chip'=8,'core'=2] {'chip','core'}, dimensions={0}, use_global_device_ids=true | all-gather | bytes 34816 | tf_op jit(solution)/shard_map/all_gather | solution.py:412
  205.6 0.6 copy.24
  206.5 0.9 fusion.5
  207.5 0.7 convert_reduce_fusion
  (98 shorter events, 0.9 us)
Async XLA Ops:
  27.7 39.0 %copy-start.2 = (bf16[32,32,128]{2,1,0:T(8,128)(2,1)}, bf16[32,32,128]{2,1,0:T(8,128)(2,1)S(1)}, u32[]{:S(2)}) copy-start(bf16[32,32,128]{2,1,0:T(8,128)(2,1)S(1)} %all_to_all.25.refs_0_) | copy-start | bytes 786436
  27.7 9.3 %collective-permute-start = (bf16[32,32,128]{2,1,0:T(8,128)(2,1)S(1)}, bf16[32,32,128]{2,1,0:T(8,128)(2,1)S(1)}, u32[]{:S(2)}, u32[]{:S(2)}) collective-permute-start(bf16[32,32,128]{2,1,0:T(8,128)(2,1)S(1)} %all_to_all.25.refs_0_), channel_id=1, source_target_pairs={{0,2},{2,4},{4,6},{6,8},{8,10},{10,12},{12,14},{14,0},{1,3},{3,5},... | collective-permute-start | bytes 786440 | tf_op jit(solution)/shard_map/ppermute | solution.py:306
  30.9 8.0 %collective-permute-start.3 = (bf16[32,32,128]{2,1,0:T(8,128)(2,1)S(1)}, bf16[32,32,128]{2,1,0:T(8,128)(2,1)S(1)}, u32[]{:S(2)}, u32[]{:S(2)}) collective-permute-start(bf16[32,32,128]{2,1,0:T(8,128)(2,1)S(1)} %all_to_all.25.refs_0_), channel_id=1, source_target_pairs={{0,14},{2,0},{4,2},{6,4},{8,6},{10,8},{12,10},{14,12},{1,15},{3,1}... | collective-permute-start | bytes 786440 | tf_op jit(solution)/shard_map/ppermute | solution.py:306
  37.1 29.7 %copy-start.6 = (bf16[32,32,128]{2,1,0:T(8,128)(2,1)}, bf16[32,32,128]{2,1,0:T(8,128)(2,1)S(1)}, u32[]{:S(2)}) copy-start(bf16[32,32,128]{2,1,0:T(8,128)(2,1)S(1)} %collective-permute-done.refs_1_) | copy-start | bytes 786436
  37.1 8.3 %collective-permute-start.1 = (bf16[32,32,128]{2,1,0:T(8,128)(2,1)S(1)}, bf16[32,32,128]{2,1,0:T(8,128)(2,1)S(1)}, u32[]{:S(2)}, u32[]{:S(2)}) collective-permute-start(bf16[32,32,128]{2,1,0:T(8,128)(2,1)S(1)} %collective-permute-done.refs_1_), channel_id=1, source_target_pairs={{0,2},{2,4},{4,6},{6,8},{8,10},{10,12},{12,14},{14,0},{1,3},{3,5},... | collective-permute-start | bytes 786440 | tf_op jit(solution)/shard_map/ppermute | solution.py:306
  39.0 27.7 %copy-start.7 = (bf16[32,32,128]{2,1,0:T(8,128)(2,1)}, bf16[32,32,128]{2,1,0:T(8,128)(2,1)S(1)}, u32[]{:S(2)}) copy-start(bf16[32,32,128]{2,1,0:T(8,128)(2,1)S(1)} %collective-permute-done.3.refs_2_) | copy-start | bytes 786436
  39.0 8.3 %collective-permute-start.4 = (bf16[32,32,128]{2,1,0:T(8,128)(2,1)S(1)}, bf16[32,32,128]{2,1,0:T(8,128)(2,1)S(1)}, u32[]{:S(2)}, u32[]{:S(2)}) collective-permute-start(bf16[32,32,128]{2,1,0:T(8,128)(2,1)S(1)} %collective-permute-done.3.refs_2_), channel_id=1, source_target_pairs={{0,14},{2,0},{4,2},{6,4},{8,6},{10,8},{12,10},{14,12},{1,15},{3,1}... | collective-permute-start | bytes 786440 | tf_op jit(solution)/shard_map/ppermute | solution.py:306
  45.4 21.4 %copy-start.4 = (bf16[32,32,128]{2,1,0:T(8,128)(2,1)}, bf16[32,32,128]{2,1,0:T(8,128)(2,1)S(1)}, u32[]{:S(2)}) copy-start(bf16[32,32,128]{2,1,0:T(8,128)(2,1)S(1)} %collective-permute-done.1.refs_3_) | copy-start | bytes 786436
  45.4 18.0 %collective-permute-start.2 = (bf16[32,32,128]{2,1,0:T(8,128)(2,1)S(1)}, bf16[32,32,128]{2,1,0:T(8,128)(2,1)S(1)}, u32[]{:S(2)}, u32[]{:S(2)}) collective-permute-start(bf16[32,32,128]{2,1,0:T(8,128)(2,1)S(1)} %collective-permute-done.1.refs_3_), channel_id=1, source_target_pairs={{0,2},{2,4},{4,6},{6,8},{8,10},{10,12},{12,14},{14,0},{1,3},{3,5},... | collective-permute-start | bytes 786440 | tf_op jit(solution)/shard_map/ppermute | solution.py:306
  47.3 19.4 %copy-start.5 = (bf16[32,32,128]{2,1,0:T(8,128)(2,1)}, bf16[32,32,128]{2,1,0:T(8,128)(2,1)S(1)}, u32[]{:S(2)}) copy-start(bf16[32,32,128]{2,1,0:T(8,128)(2,1)S(1)} %collective-permute-done.4.refs_4_) | copy-start | bytes 786436
  47.3 16.1 %collective-permute-start.5 = (bf16[32,32,128]{2,1,0:T(8,128)(2,1)S(1)}, bf16[32,32,128]{2,1,0:T(8,128)(2,1)S(1)}, u32[]{:S(2)}, u32[]{:S(2)}) collective-permute-start(bf16[32,32,128]{2,1,0:T(8,128)(2,1)S(1)} %collective-permute-done.4.refs_4_), channel_id=1, source_target_pairs={{0,14},{2,0},{4,2},{6,4},{8,6},{10,8},{12,10},{14,12},{1,15},{3,1}... | collective-permute-start | bytes 786440 | tf_op jit(solution)/shard_map/ppermute | solution.py:306
  52.0 30.9 %collective-permute-start.10 = (bf16[3,32,32,128]{3,2,1,0:T(8,128)(2,1)S(1)}, bf16[3,32,32,128]{3,2,1,0:T(8,128)(2,1)}, u32[]{:S(2)}, u32[]{:S(2)}) collective-permute-start(bf16[3,32,32,128]{3,2,1,0:T(8,128)(2,1)S(1)} %pad_maximum_fusion), channel_id=1, source_target_pairs={{0,1},{1,0},{2,3},{3,2},{4,5},{5,4},{6,7},{7,6},{8,9},{9,8},{10,11... | collective-permute-start | bytes 2359304 | tf_op jit(solution)/shard_map/ppermute | solution.py:315
  59.5 23.4 %collective-permute-start.11 = (bf16[2,32,32,128]{3,2,1,0:T(8,128)(2,1)}, bf16[2,32,32,128]{3,2,1,0:T(8,128)(2,1)}, u32[]{:S(2)}, u32[]{:S(2)}) collective-permute-start(bf16[2,32,32,128]{3,2,1,0:T(8,128)(2,1)} %pad_maximum_fusion.2), channel_id=1, source_target_pairs={{0,1},{1,0},{2,3},{3,2},{4,5},{5,4},{6,7},{7,6},{8,9},{9,8},{10,11... | collective-permute-start | bytes 1572872 | tf_op jit(solution)/shard_map/ppermute | solution.py:315
  61.4 11.1 %collective-permute-start.6 = (bf16[16,32,128]{2,1,0:T(8,128)(2,1)S(1)}, bf16[16,32,128]{2,1,0:T(8,128)(2,1)S(1)}, u32[]{:S(2)}, u32[]{:S(2)}) collective-permute-start(bf16[16,32,128]{2,1,0:T(8,128)(2,1)S(1)} %slice.299), channel_id=1, source_target_pairs={{0,4},{2,6},{4,8},{6,10},{8,12},{10,14},{12,0},{14,2},{1,5},{3,7},... | collective-permute-start | bytes 393224 | tf_op jit(solution)/shard_map/ppermute | solution.py:306
  64.2 22.6 %collective-permute-start.8 = (bf16[2,32,32,128]{3,2,1,0:T(8,128)(2,1)}, bf16[2,32,32,128]{3,2,1,0:T(8,128)(2,1)S(1)}, u32[]{:S(2)}, u32[]{:S(2)}) collective-permute-start(bf16[2,32,32,128]{3,2,1,0:T(8,128)(2,1)} %pad_maximum_fusion.1), channel_id=1, source_target_pairs={{0,1},{1,0},{2,3},{3,2},{4,5},{5,4},{6,7},{7,6},{8,9},{9,8},{10,11... | collective-permute-start | bytes 1572872 | tf_op jit(solution)/shard_map/ppermute | solution.py:315
  66.7 13.8 %collective-permute-start.7 = (bf16[16,32,128]{2,1,0:T(8,128)(2,1)S(1)}, bf16[16,32,128]{2,1,0:T(8,128)(2,1)S(1)}, u32[]{:S(2)}, u32[]{:S(2)}) collective-permute-start(bf16[16,32,128]{2,1,0:T(8,128)(2,1)S(1)} %slice.300), channel_id=1, source_target_pairs={{0,12},{2,14},{4,0},{6,2},{8,4},{10,6},{12,8},{14,10},{1,13},{3,15... | collective-permute-start | bytes 393224 | tf_op jit(solution)/shard_map/ppermute | solution.py:306
  80.5 6.3 %collective-permute-start.9 = (bf16[1,32,32,128]{3,2,1,0:T(8,128)(2,1)S(1)}, bf16[1,32,32,128]{3,2,1,0:T(8,128)(2,1)S(1)}, u32[]{:S(2)}, u32[]{:S(2)}) collective-permute-start(bf16[1,32,32,128]{3,2,1,0:T(8,128)(2,1)S(1)} %bitcast.113), channel_id=1, source_target_pairs={{0,1},{1,0},{2,3},{3,2},{4,5},{5,4},{6,7},{7,6},{8,9},{9,8},{10,11... | collective-permute-start | bytes 786440 | tf_op jit(solution)/shard_map/ppermute | solution.py:315
  91.4 4.6 %collective-permute-start.12 = (bf16[8,512,128]{2,1,0:T(8,128)(2,1)S(1)}, bf16[8,512,128]{2,1,0:T(8,128)(2,1)S(1)}, u32[]{:S(2)}, u32[]{:S(2)}) collective-permute-start(bf16[8,512,128]{2,1,0:T(8,128)(2,1)S(1)} %get-tuple-element.37), channel_id=1, source_target_pairs={{0,1},{1,0},{2,3},{3,2},{4,5},{5,4},{6,7},{7,6},{8,9},{9,8},{10,11... | collective-permute-start | bytes 3145736 | tf_op jit(solution)/shard_map/ppermute | solution.py:315
  96.0 5.7 %copy-start.14 = (f32[192]{0:T(256)S(1)}, f32[192]{0:T(256)}, u32[]{:S(2)}) copy-start(f32[192]{0:T(256)} %param.22) | copy-start | bytes 2308
  96.0 7.1 %copy-start.1 = (bf16[192,128]{1,0:T(8,128)(2,1)S(1)}, bf16[192,128]{1,0:T(8,128)(2,1)}, u32[]{:S(2)}) copy-start(bf16[192,128]{1,0:T(8,128)(2,1)} %cotangent.3) | copy-start | bytes 147460
  96.0 7.1 %copy-start.9 = (bf16[192,128]{1,0:T(8,128)(2,1)S(1)}, bf16[192,128]{1,0:T(8,128)(2,1)}, u32[]{:S(2)}) copy-start(bf16[192,128]{1,0:T(8,128)(2,1)} %param.21) | copy-start | bytes 147460
  96.0 8.4 %copy-start.11 = (f32[31,128]{1,0:T(8,128)S(1)}, f32[31,128]{1,0:T(8,128)}, u32[]{:S(2)}) copy-start(f32[31,128]{1,0:T(8,128)} %param.26) | copy-start | bytes 47620
  97.3 51.4 %copy-start.10 = (bf16[64,128]{1,0:T(8,128)(2,1)S(1)}, bf16[64,128]{1,0:T(8,128)(2,1)}, u32[]{:S(2)}) copy-start(bf16[64,128]{1,0:T(8,128)(2,1)} %param.27) | copy-start | bytes 49156
  97.3 33.7 %all-to-all-start.1 = ((bf16[8,512,128]{2,1,0:T(8,128)(2,1)}), bf16[8,512,128]{2,1,0:T(8,128)(2,1)S(1)}, u32[]{:S(2)}, u32[]{:S(2)}) async-start(bf16[8,512,128]{2,1,0:T(8,128)(2,1)} %add_convert_fusion), calls=%async_computation.1 | async-start | bytes 2097152 | tf_op jit(solution)/shard_map/all_to_all | solution.py:340
  101.7 4.6 %collective-permute-start.13 = (f32[4,32]{1,0:T(4,128)S(1)}, f32[4,32]{1,0:T(4,128)S(1)}, u32[]{:S(2)}, u32[]{:S(2)}) collective-permute-start(f32[4,32]{1,0:T(4,128)S(1)} %pad_maximum_fusion.5), channel_id=1, source_target_pairs={{16,0},{32,16},{48,32},{64,48},{80,64},{96,80},{112,96},{128,112},... | collective-permute-start | bytes 1544 | tf_op jit(solution)/shard_map/ppermute | solution.py:311
  103.1 34.3 %collective-permute-start.14 = (bf16[2,32,128]{2,1,0:T(8,128)(2,1)S(1)}, bf16[2,32,128]{2,1,0:T(8,128)(2,1)S(1)}, u32[]{:S(2)}, u32[]{:S(2)}) collective-permute-start(bf16[2,32,128]{2,1,0:T(8,128)(2,1)S(1)} %pad_maximum_fusion.4), channel_id=1, source_target_pairs={{16,0},{32,16},{48,32},{64,48},{80,64},{96,80},{112,96},{128,112},... | collective-permute-start | bytes 49160 | tf_op jit(solution)/shard_map/ppermute | solution.py:311
  131.8 16.8 %all-to-all-start.2 = ((bf16[32,32,128]{2,1,0:T(8,128)(2,1)}), bf16[32,32,128]{2,1,0:T(8,128)(2,1)S(1)}, u32[]{:S(2)}, u32[]{:S(2)}) async-start(bf16[32,32,128]{2,1,0:T(8,128)(2,1)} %summed.1), calls=%async_computation.2 | async-start | bytes 524288 | tf_op jit(solution)/shard_map/all_to_all | solution.py:392
  149.5 7.9 %copy-start.3 = (bf16[32,16,2048]{2,1,0:T(8,128)(2,1)S(1)}, bf16[32,16,2048]{2,1,0:T(8,128)(2,1)}, u32[]{:S(2)}) copy-start(bf16[32,16,2048]{2,1,0:T(8,128)(2,1)} %get-tuple-element.33) | copy-start | bytes 6291460
  149.5 7.9 %copy-start.8 = (bf16[512,224]{1,0:T(8,128)(2,1)S(1)}, bf16[512,224]{1,0:T(8,128)(2,1)}, u32[]{:S(2)}) copy-start(bf16[512,224]{1,0:T(8,128)(2,1)} %get-tuple-element.32) | copy-start | bytes 688132
  149.5 29.9 %all-to-all-start.4 = ((bf16[32,64,128]{2,1,0:T(8,128)(2,1)}), bf16[32,64,128]{2,1,0:T(8,128)(2,1)S(1)}, u32[]{:S(2)}, u32[]{:S(2)}) async-start(bf16[32,64,128]{2,1,0:T(8,128)(2,1)} %broadcast_in_dim.8), calls=%async_computation.4 | async-start | bytes 1048576 | tf_op jit(solution)/shard_map/all_to_all | solution.py:351
  157.5 20.5 %copy-start.28 = (f32[128]{0:T(128)S(1)}, f32[128]{0:T(128)}, u32[]{:S(2)}) copy-start(f32[128]{0:T(128)} %param.25) | copy-start | bytes 1540
  157.5 20.4 %copy-start.30 = (f32[128]{0:T(128)S(1)}, f32[128]{0:T(128)}, u32[]{:S(2)}) copy-start(f32[128]{0:T(128)} %param.24) | copy-start | bytes 1540
  159.3 29.6 %copy-start.29 = (f32[128]{0:T(128)S(1)}, f32[128]{0:T(128)}, u32[]{:S(2)}) copy-start(f32[128]{0:T(128)} %param.25) | copy-start | bytes 1540
  159.4 29.6 %copy-start.31 = (f32[128]{0:T(128)S(1)}, f32[128]{0:T(128)}, u32[]{:S(2)}) copy-start(f32[128]{0:T(128)} %param.24) | copy-start | bytes 1540
  179.3 27.1 %copy-start.15 = (f32[128]{0:T(128)S(1)}, f32[128]{0:T(128)}, u32[]{:S(2)}) copy-start(f32[128]{0:T(128)} %get-tuple-element.61) | copy-start | bytes 1540
  179.3 27.1 %copy-start.16 = (f32[128]{0:T(128)S(1)}, f32[128]{0:T(128)}, u32[]{:S(2)}) copy-start(f32[128]{0:T(128)} %get-tuple-element.62) | copy-start | bytes 1540
  179.3 27.1 %copy-start.17 = (f32[128]{0:T(128)S(1)}, f32[128]{0:T(128)}, u32[]{:S(2)}) copy-start(f32[128]{0:T(128)} %get-tuple-element.63) | copy-start | bytes 1540
  179.3 27.2 %copy-start.18 = (f32[128]{0:T(128)S(1)}, f32[128]{0:T(128)}, u32[]{:S(2)}) copy-start(f32[128]{0:T(128)} %get-tuple-element.64) | copy-start | bytes 1540
  179.3 27.2 %copy-start.19 = (f32[128]{0:T(128)S(1)}, f32[128]{0:T(128)}, u32[]{:S(2)}) copy-start(f32[128]{0:T(128)} %get-tuple-element.65) | copy-start | bytes 1540
  179.3 27.2 %copy-start.20 = (f32[128]{0:T(128)S(1)}, f32[128]{0:T(128)}, u32[]{:S(2)}) copy-start(f32[128]{0:T(128)} %get-tuple-element.66) | copy-start | bytes 1540
  179.3 27.2 %copy-start.21 = (f32[128]{0:T(128)S(1)}, f32[128]{0:T(128)}, u32[]{:S(2)}) copy-start(f32[128]{0:T(128)} %get-tuple-element.67) | copy-start | bytes 1540
  179.3 27.2 %copy-start.22 = (f32[128]{0:T(128)S(1)}, f32[128]{0:T(128)}, u32[]{:S(2)}) copy-start(f32[128]{0:T(128)} %get-tuple-element.68) | copy-start | bytes 1540
  179.3 27.2 %copy-start.23 = (f32[128]{0:T(128)S(1)}, f32[128]{0:T(128)}, u32[]{:S(2)}) copy-start(f32[128]{0:T(128)} %get-tuple-element.69) | copy-start | bytes 1540
  179.3 27.2 %copy-start.24 = (f32[128]{0:T(128)S(1)}, f32[128]{0:T(128)}, u32[]{:S(2)}) copy-start(f32[128]{0:T(128)} %get-tuple-element.70) | copy-start | bytes 1540
  179.3 27.2 %copy-start.25 = (f32[128]{0:T(128)S(1)}, f32[128]{0:T(128)}, u32[]{:S(2)}) copy-start(f32[128]{0:T(128)} %get-tuple-element.71) | copy-start | bytes 1540
  179.4 27.2 %copy-start.26 = (f32[128]{0:T(128)S(1)}, f32[128]{0:T(128)}, u32[]{:S(2)}) copy-start(f32[128]{0:T(128)} %get-tuple-element.72) | copy-start | bytes 1540
  179.4 27.2 %copy-start.27 = (f32[128]{0:T(128)S(1)}, f32[128]{0:T(128)}, u32[]{:S(2)}) copy-start(f32[128]{0:T(128)} %get-tuple-element.73) | copy-start | bytes 1540
  179.4 28.1 %all-to-all-start.3 = ((bf16[32,64,128]{2,1,0:T(8,128)(2,1)}), bf16[32,64,128]{2,1,0:T(8,128)(2,1)S(1)}, u32[]{:S(2)}, u32[]{:S(2)}) async-start(bf16[32,64,128]{2,1,0:T(8,128)(2,1)} %bitcast.22), calls=%async_computation.3 | async-start | bytes 1048576 | tf_op jit(solution)/shard_map/all_to_all | solution.py:401
  (3 other events, 13.1 us)

commit v7 on v6

--- a/solution.py
+++ b/solution.py
@@ -136,7 +136,7 @@
         out_specs=whole(2),
         out_shape=(
             pltpu.VMEM((tokens, cotangent.shape[1]), BF16),
-            pltpu.VMEM(cotangent.shape, BF16),
+            jax.ShapeDtypeStruct(cotangent.shape, BF16),
         ),
         compiler_params=pltpu.CompilerParams(vmem_limit_bytes=12 * 1024 * 1024),
         name="combined",
@@ -229,14 +229,47 @@
     )(me, *far(*mine, *shared, *weights))
 
 
+def partial_rows(out, gate_grad, up_grad, gate_weight, up_weight, core):
+    chips, _, width = out.shape
+    for j in range(0, chips, 2):
+        gate_cols, up_cols = (
+            jnp.concatenate([weight[:, columns(j + i, core, width)] for i in (0, 1)], axis=1)
+            for weight in (gate_weight, up_weight)
+        )
+        both = dot(gate_grad, gate_cols, 1, 0) + dot(up_grad, up_cols, 1, 0)
+        for i in (0, 1):
+            out[j + i] = both[:, i * width : (i + 1) * width].astype(BF16)
+
+
+def kept_body(me, gate_grad, up_grad, gate_weight, up_weight, out):
+    core = lax.rem(me[0], 2)
+    partial_rows(out, gate_grad[...], up_grad[...], gate_weight, up_weight, core)
+
+
+def kept_products(me, gate_grad, up_grad, gate_weight, up_weight, blocks):
+    count, hidden = gate_grad.shape
+    channels = gate_weight.shape[1]
+    return pl.pallas_call(
+        kept_body,
+        in_specs=whole(1, pltpu.SMEM) + whole(4),
+        out_specs=whole(1)[0],
+        out_shape=pltpu.VMEM((blocks // 2, count, channels // blocks), BF16),
+        cost_estimate=pl.CostEstimate(
+            flops=2 * count * hidden * channels, transcendentals=0, bytes_accessed=4 * 1024 * 1024
+        ),
+        compiler_params=pltpu.CompilerParams(vmem_limit_bytes=12 * 1024 * 1024),
+        name="kept_products",
+    )(me, *near(gate_grad, up_grad, gate_weight, up_weight))
+
+
 def rest_body(me, *refs, blocks, slots, batches):
     chips = blocks // 2
     count = sum(batches)
     mine, shared = (refs[:count], refs[count : count + len(batches)])
     _, _, gate_sum, up_sum, down_sum, *weights = refs[count + len(batches) : count + len(batches) + 8]
     outs = refs[count + len(batches) + 8 :]
-    rows, routed, kept, given, *far_outs = outs[:8]
-    hidden_held, up_held, sems = outs[8:]
+    rows, routed, given, gate_out, up_out, *far_outs = outs[:9]
+    hidden_held, up_held, sems = outs[9:]
     sends = [
         pltpu.make_async_copy(held, out, sems.at[n])
         for n, (held, out) in enumerate(zip((rows, routed, hidden_held, up_held), far_outs))
@@ -251,7 +284,6 @@
     up_pre = up_pre + up_sum[...]
     hidden_grad = hidden_grad + down_sum[...]
     gate_weight, up_weight = weights[:2]
-    width = mine[0].shape[-1]
     my_core = lax.rem(me[0], 2)
     gate_sigmoid = jax.nn.sigmoid(gate_pre)
     gate_active = gate_pre * gate_sigmoid
@@ -261,15 +293,9 @@
     up_held[...] = up_grad
     sends[2].start()
     sends[3].start()
-    for out, core in ((given, 1 - my_core), (kept, my_core)):
-        for j in range(0, chips, 2):
-            gate_cols, up_cols = (
-                jnp.concatenate([weight[:, columns(j + i, core, width)] for i in (0, 1)], axis=1)
-                for weight in (gate_weight, up_weight)
-            )
-            both = dot(gate_grad, gate_cols, 1, 0) + dot(up_grad, up_cols, 1, 0)
-            for i in (0, 1):
-                out[j + i] = both[:, i * width : (i + 1) * width].astype(BF16)
+    partial_rows(given, gate_grad, up_grad, gate_weight, up_weight, 1 - my_core)
+    gate_out[...] = gate_grad
+    up_out[...] = up_grad
     for send in sends:
         send.wait()
 
@@ -282,10 +308,11 @@
     return pl.pallas_call(
         functools.partial(rest_body, blocks=blocks, slots=slots, batches=batches),
         in_specs=whole(1, pltpu.SMEM) + whole(len(mine) + len(shared) + 8),
-        out_specs=whole(4) + whole(4, pl.ANY),
+        out_specs=whole(5) + whole(4, pl.ANY),
         out_shape=(
             *[pltpu.VMEM((experts, slots, channels), BF16)] * 2,
-            *[pltpu.VMEM((blocks // 2, count, channels // blocks), BF16)] * 2,
+            pltpu.VMEM((blocks // 2, count, channels // blocks), BF16),
+            *[pltpu.VMEM((count, hidden), BF16)] * 2,
             *[pltpu.HBM((experts, slots, channels), BF16)] * 2,
             *[pltpu.HBM((count, hidden), BF16)] * 2,
         ),
@@ -322,21 +349,20 @@
 def all_blocks(own):
     chips = lax.axis_size("chip")
     arrived = [own]
-    for n, steps in enumerate(ring_order(chips)[1:-1]):
+    for n, steps in enumerate(ring_order(chips)[1:]):
         arrived.append(along_chips(arrived[max(0, n - 1)], 1 if steps < 0 else -1))
-    half = own.shape[0] // 2
-    low = along_chips(arrived[-4][:half], 2)
-    high = along_chips(arrived[-3][half:], -2)
-    arrived.append(jnp.concatenate([low, high], axis=0))
     shared, at = ([], 0)
-    for size in BATCHES:
+    for size in BATCHES[:-1]:
         shared.append(to_other_core(jnp.stack(arrived[at : at + size])))
         at += size
+    count = lax.axis_size(TP)
+    across = [(t, ((t - 2) % count) ^ 1) for t in range(count)]
+    shared.append(lax.ppermute(arrived[-2], TP, across)[None])
     return arrived, shared
 
 
-def added_up(kept, given):
-    both = kept.astype(F32) + to_other_core(given).astype(F32)
+def added_up(kept, other):
+    both = kept.astype(F32) + other.astype(F32)
     arrived = lax.all_to_all(both.astype(BF16), "chip", split_axis=0, concat_axis=0, tiled=True)
     return arrived
 
@@ -380,7 +406,7 @@
     mine, others = all_blocks(own)
     done = sum(BATCHES[:EARLY])
     early = first_products(me, mine[:done], others[:EARLY], (w_gate, w_up, w_down), slots, blocks)
-    _, _, kept, given, rows, routed, hidden, up_grad = rest_products(
+    _, _, given, gate_rows, up_rows, rows, routed, hidden, up_grad = rest_products(
         me, mine[done:], others[EARLY:], early, slots, blocks
     )
     rim = 8 * (-(-(taps.shape[0] - 1) // 8))
@@ -388,7 +414,9 @@
     facts = [routes[:rim, 0].astype(F32), routes[:rim, 1].astype(F32)]
     facts = from_after(jnp.stack([*facts, norm_mean[:rim], norm_rstd[:rim]]))
     rim_place = rim_places(facts[:2].astype(jnp.int32), devices, slots)
-    shared = summed(added_up(kept, given), devices)
+    other = to_other_core(given)
+    kept = kept_products(me, gate_rows, up_rows, early[5], early[6], blocks)
+    shared = summed(added_up(kept, other), devices)
     returned = lax.all_to_all(shared, "sp", split_axis=0, concat_axis=0, tiled=True)
     grad_up = dot(up_grad, rows.reshape(-1, rows.shape[2]), 0, 0).astype(BF16)[None]
     grad_down = dot(hidden, routed.reshape(-1, routed.shape[2]), 0, 0).astype(BF16)[None]

time: 209 us -> 202 us (0.967)
  waiting for transfers between devices: 51.2 us -> 46.2 us
    ppermute x8 -> x7, starting transfers between devices: 27.6 us -> 22.2 us  [along_chips(): lax.ppermute(value, 'chip', [(y, (y + steps) % count) for y in range(coun...]
    ppermute x8 -> x7, waiting for transfers between devices: 12.2 us -> 7.39 us  [along_chips(): lax.ppermute(value, 'chip', [(y, (y + steps) % count) for y in range(coun...]
    ppermute x0 -> x1, starting transfers between devices: none -> 2.93 us  [all_blocks(): shared.append(lax.ppermute(arrived[-2], TP, across)[None])]
    all_to_all x1, starting transfers between devices: 4.41 us -> 6.53 us  [added_up(): lax.all_to_all(both.astype(BF16), 'chip', split_axis=0, concat_axis=0, ti...]
    ppermute x5 -> x4, starting transfers between devices: 15.3 us -> 14.2 us  [to_other_core(): return lax.ppermute(value, 'core', [(0, 1), (1, 0)])]
  transfers between devices with their start and end apart: 19 -> 18, of which waited for: 8 -> 8; matrix products, arithmetic and copies ran while one was open for 6% -> 6% of each run, Pallas kernels for 3% -> 3%
where the time goes in v7:
time: 202 us; the launch traced here: 201 us
  starting transfers between devices  67.9 us (34%)
  blocking collectives  59.7 us (30%)
  waiting for transfers between devices  46.2 us (23%)
  Pallas kernels  11.9 us (6%)
  matrix products  6.75 us (3%)
  other arithmetic  5.18 us (3%)
  local copies, waits for them, and re-layouts  2.27 us (1%)
    all_to_all x1, blocking collectives, steps(): own = lax.all_to_all(sent, 'sp', split_axis=0, concat_axis=0, tiled=True)  25 us
    all_to_all x1, waiting for transfers between devices, added_up(): lax.all_to_all(both.astype(BF16), 'chip', split_axis=0, concat_axis=0, ti...  24.5 us
    ppermute x7, starting transfers between devices, along_chips(): lax.ppermute(value, 'chip', [(y, (y + steps) % count) for y in range(coun...  22.2 us
    all_gather x1, blocking collectives, steps(): columns = lax.all_gather(stream, TP, axis=1, tiled=True)  18.7 us
    all_gather x1, blocking collectives, steps(): sums = lax.all_gather(sums, TP, axis=0, tiled=False)  16.1 us
    ppermute x4, starting transfers between devices, to_other_core(): return lax.ppermute(value, 'core', [(0, 1), (1, 0)])  14.2 us
    all_to_all x1, waiting for transfers between devices, steps(): lax.all_to_all(shared, 'sp', split_axis=0, concat_axis=0, tiled=True)  11.2 us
    all_to_all x1, starting transfers between devices, steps(): lax.all_to_all(proj_part, 'sp', split_axis=0, concat_axis=0, tiled=True)  9.51 us
  transfers between devices with their start and end apart: 18, of which 8 were waited for; matrix products, arithmetic and copies ran while one was open for 6% of the time, Pallas kernels for 3%

profile of v7, /device:TPU:1, one launch (start us, length us, event | category | flops | bytes accessed | tf_op | source)
XLA Modules:
  0.0 201.2 jit_solution(18003297305353956897)
XLA Ops:
  0.6 2.1 %send_rows.1 = (bf16[32,32,128]{2,1,0:T(8,128)(2,1)}, bf16[512,192]{1,0:T(8,128)(2,1)}) custom-call(s32[2,192]{1,0:T(2,128)} %bitcast.122, f32[2,192]{1,0:T(2,128)} %bitcast.125, bf16[192,128]{1,0:T(8,128)(2,1)} %rows.1, bf16[192,128]{1,0:T(8,128)(2,1)} %cotangent.3), custom_call_target="tpu_custom_call" | custom-call | tf_op jit(solution)/shard_map/send_rows/pallas_call | solution.py:70
  2.7 25.0 %all_to_all.25.refs_0_ = bf16[32,32,128]{2,1,0:T(8,128)(2,1)S(1)} all-to-all(bf16[32,32,128]{2,1,0:T(8,128)(2,1)} %get-tuple-element.24), channel_id=1, replica_groups=mesh['sp'=32,'chip'=8,'core'=2] {'sp'}, dimensions={0} | all-to-all | bytes 524288 | tf_op jit(solution)/shard_map/all_to_all | solution.py:404
  27.7 3.2 %collective-permute-start = (bf16[32,32,128]{2,1,0:T(8,128)(2,1)S(1)}, bf16[32,32,128]{2,1,0:T(8,128)(2,1)S(1)}, u32[]{:S(2)}, u32[]{:S(2)}) collective-permute-start(bf16[32,32,128]{2,1,0:T(8,128)(2,1)S(1)} %all_to_all.25.refs_0_), channel_id=1, source_target_pairs={{0,2},{2,4},{4,6},{6,8},{8,10},{10,12},{12,14},{14,0},{1,3},{3,5},... | collective-permute-start | bytes 786440 | tf_op jit(solution)/shard_map/ppermute | solution.py:333
  30.9 3.8 %collective-permute-start.3 = (bf16[32,32,128]{2,1,0:T(8,128)(2,1)S(1)}, bf16[32,32,128]{2,1,0:T(8,128)(2,1)S(1)}, u32[]{:S(2)}, u32[]{:S(2)}) collective-permute-start(bf16[32,32,128]{2,1,0:T(8,128)(2,1)S(1)} %all_to_all.25.refs_0_), channel_id=1, source_target_pairs={{0,14},{2,0},{4,2},{6,4},{8,6},{10,8},{12,10},{14,12},{1,15},{3,1}... | collective-permute-start | bytes 786440 | tf_op jit(solution)/shard_map/ppermute | solution.py:333
  34.8 2.3 %collective-permute-done.refs_1_ = bf16[32,32,128]{2,1,0:T(8,128)(2,1)S(1)} collective-permute-done((bf16[32,32,128]{2,1,0:T(8,128)(2,1)S(1)}, bf16[32,32,128]{2,1,0:T(8,128)(2,1)S(1)}, u32[]{:S(2)}, u32[]{:S(2)}) %collective-permute-start) | collective-permute-done | bytes 262176 | tf_op jit(solution)/shard_map/ppermute | solution.py:333
  37.1 1.9 collective-permute-start.1
  39.0 4.6 %collective-permute-start.4 = (bf16[32,32,128]{2,1,0:T(8,128)(2,1)S(1)}, bf16[32,32,128]{2,1,0:T(8,128)(2,1)S(1)}, u32[]{:S(2)}, u32[]{:S(2)}) collective-permute-start(bf16[32,32,128]{2,1,0:T(8,128)(2,1)S(1)} %collective-permute-done.3.refs_2_), channel_id=1, source_target_pairs={{0,14},{2,0},{4,2},{6,4},{8,6},{10,8},{12,10},{14,12},{1,15},{3,1}... | collective-permute-start | bytes 786440 | tf_op jit(solution)/shard_map/ppermute | solution.py:333
  43.6 1.8 collective-permute-done.1.refs_3_
  45.4 1.9 collective-permute-start.2
  47.3 4.6 %collective-permute-start.5 = (bf16[32,32,128]{2,1,0:T(8,128)(2,1)S(1)}, bf16[32,32,128]{2,1,0:T(8,128)(2,1)S(1)}, u32[]{:S(2)}, u32[]{:S(2)}) collective-permute-start(bf16[32,32,128]{2,1,0:T(8,128)(2,1)S(1)} %collective-permute-done.4.refs_4_), channel_id=1, source_target_pairs={{0,14},{2,0},{4,2},{6,4},{8,6},{10,8},{12,10},{14,12},{1,15},{3,1}... | collective-permute-start | bytes 786440 | tf_op jit(solution)/shard_map/ppermute | solution.py:333
  51.9 1.0 pad_maximum_fusion
  52.9 6.6 %collective-permute-start.9 = (bf16[3,32,32,128]{3,2,1,0:T(8,128)(2,1)}, bf16[3,32,32,128]{3,2,1,0:T(8,128)(2,1)}, u32[]{:S(2)}, u32[]{:S(2)}) collective-permute-start(bf16[3,32,32,128]{3,2,1,0:T(8,128)(2,1)} %pad_maximum_fusion), channel_id=1, source_target_pairs={{0,1},{1,0},{2,3},{3,2},{4,5},{5,4},{6,7},{7,6},{8,9},{9,8},{10,11... | collective-permute-start | bytes 2359304 | tf_op jit(solution)/shard_map/ppermute | solution.py:342
  59.5 0.8 pad_maximum_fusion.2
  60.3 1.9 collective-permute-start.10
  62.3 2.4 %collective-permute-start.7 = (bf16[2,32,32,128]{3,2,1,0:T(8,128)(2,1)S(1)}, bf16[2,32,32,128]{3,2,1,0:T(8,128)(2,1)S(1)}, u32[]{:S(2)}, u32[]{:S(2)}) collective-permute-start(bf16[2,32,32,128]{3,2,1,0:T(8,128)(2,1)S(1)} %pad_maximum_fusion.1), channel_id=1, source_target_pairs={{0,1},{1,0},{2,3},{3,2},{4,5},{5,4},{6,7},{7,6},{8,9},{9,8},{10,11... | collective-permute-start | bytes 1572872 | tf_op jit(solution)/shard_map/ppermute | solution.py:342
  64.8 2.9 %collective-permute-start.8 = (bf16[32,32,128]{2,1,0:T(8,128)(2,1)S(1)}, bf16[32,32,128]{2,1,0:T(8,128)(2,1)S(1)}, u32[]{:S(2)}, u32[]{:S(2)}) collective-permute-start(bf16[32,32,128]{2,1,0:T(8,128)(2,1)S(1)} %collective-permute-done.5.refs_1_), channel_id=1, source_target_pairs={{0,15},{1,14},{2,1},{3,0},{4,3},{5,2},{6,5},{7,4},{8,7},{9,6},{10,... | collective-permute-start | bytes 786440 | tf_op jit(solution)/shard_map/ppermute | solution.py:360
  67.7 2.3 %collective-permute-start.6 = (bf16[32,32,128]{2,1,0:T(8,128)(2,1)S(1)}, bf16[32,32,128]{2,1,0:T(8,128)(2,1)S(1)}, u32[]{:S(2)}, u32[]{:S(2)}) collective-permute-start(bf16[32,32,128]{2,1,0:T(8,128)(2,1)S(1)} %collective-permute-done.2.refs_0_), channel_id=1, source_target_pairs={{0,2},{2,4},{4,6},{6,8},{8,10},{10,12},{12,14},{14,0},{1,3},{3,5},... | collective-permute-start | bytes 786440 | tf_op jit(solution)/shard_map/ppermute | solution.py:333
  70.0 3.9 %first_products.1 = (bf16[32,16,2048]{2,1,0:T(8,128)(2,1)S(1)}, bf16[32,16,2048]{2,1,0:T(8,128)(2,1)S(1)}, f32[512,224]{1,0:T(8,128)S(1)}, f32[512,224]{1,0:T(8,...) custom-call(s32[1]{0:T(128)} %bitcast.me, ...), custom_call_target="tpu_custom_call" | custom-call | flops 939524096 | bytes 12582912 | tf_op jit(solution)/shard_map/first_products/pallas_call | solution.py:210
  74.0 0.9 collective-permute-done.8
  74.9 3.3 %collective-permute-done.6.refs_2_ = bf16[32,32,128]{2,1,0:T(8,128)(2,1)S(1)} collective-permute-done((bf16[32,32,128]{2,1,0:T(8,128)(2,1)S(1)}, bf16[32,32,128]{2,1,0:T(8,128)(2,1)S(1)}, u32[]{:S(2)}, u32[]{:S(2)}) %collective-permute-start.6) | collective-permute-done | bytes 262176 | tf_op jit(solution)/shard_map/ppermute | solution.py:333
  78.2 3.2 %rest_products.1 = (bf16[32,16,2048]{2,1,0:T(8,128)(2,1)S(1)}, bf16[32,16,2048]{2,1,0:T(8,128)(2,1)S(1)}, bf16[8,512,128]{2,1,0:T(8,128)(2,1)S(1)}, bf16[512,224...) custom-call(s32[1]{0:T(128)} %bitcast.me, ...), custom_call_target="tpu_custom_call", output_to_operand_aliasing={{0}: (6, {}), {1}: (7, {})} | custom-call | flops 1409286144 | bytes 12582912 | tf_op jit(solution)/shard_map/rest_products/pallas_call | solution.py:308
  81.3 3.3 %collective-permute-start.11 = (bf16[8,512,128]{2,1,0:T(8,128)(2,1)S(1)}, bf16[8,512,128]{2,1,0:T(8,128)(2,1)S(1)}, u32[]{:S(2)}, u32[]{:S(2)}) collective-permute-start(bf16[8,512,128]{2,1,0:T(8,128)(2,1)S(1)} %get-tuple-element.39), channel_id=1, source_target_pairs={{0,1},{1,0},{2,3},{3,2},{4,5},{5,4},{6,7},{7,6},{8,9},{9,8},{10,11... | collective-permute-start | bytes 3145736 | tf_op jit(solution)/shard_map/ppermute | solution.py:342
  84.6 0.8 kept_products.1
  85.5 1.4 collective-permute-done.11
  86.9 1.3 add_convert_fusion
  88.1 6.5 %all-to-all-start.1 = ((bf16[8,512,128]{2,1,0:T(8,128)(2,1)}), bf16[8,512,128]{2,1,0:T(8,128)(2,1)S(1)}, u32[]{:S(2)}, u32[]{:S(2)}) async-start(bf16[8,512,128]{2,1,0:T(8,128)(2,1)} %add_convert_fusion), calls=%async_computation.1 | async-start | bytes 2097152 | tf_op jit(solution)/shard_map/all_to_all | solution.py:366
  94.7 1.3 collective-permute-start.12
  96.1 1.3 collective-permute-start.13
  97.4 0.5 slice_bitcast_fusion.36
  97.9 0.6 slice_bitcast_fusion.33
  98.6 0.8 collective-permute-done.12
  99.4 24.5 %all-to-all-done.1.arrived = bf16[8,512,128]{2,1,0:T(8,128)(2,1)S(1)} async-done(((bf16[8,512,128]{2,1,0:T(8,128)(2,1)}), bf16[8,512,128]{2,1,0:T(8,128)(2,1)S(1)}, u32[]{:S(2)}, u32[]{:S(2)}) %all-to-all-start.1) | async-done | bytes 1048608 | tf_op jit(solution)/shard_map/all_to_all | solution.py:366
  123.9 0.8 summed.1
  124.7 5.3 %all-to-all-start.2 = ((bf16[32,32,128]{2,1,0:T(8,128)(2,1)}), bf16[32,32,128]{2,1,0:T(8,128)(2,1)S(1)}, u32[]{:S(2)}, u32[]{:S(2)}) async-start(bf16[32,32,128]{2,1,0:T(8,128)(2,1)} %summed.1), calls=%async_computation.2 | async-start | bytes 524288 | tf_op jit(solution)/shard_map/all_to_all | solution.py:420
  130.1 0.2 rim_places.1.rim_place
  130.4 11.2 %all-to-all-done.2.returned = bf16[32,32,128]{2,1,0:T(8,128)(2,1)S(1)} async-done(((bf16[32,32,128]{2,1,0:T(8,128)(2,1)}), bf16[32,32,128]{2,1,0:T(8,128)(2,1)S(1)}, u32[]{:S(2)}, u32[]{:S(2)}) %all-to-all-start.2) | async-done | bytes 262176 | tf_op jit(solution)/shard_map/all_to_all | solution.py:420
  141.6 0.9 broadcast_in_dim.11
  142.5 4.6 %all-to-all-start.4 = ((bf16[32,64,128]{2,1,0:T(8,128)(2,1)}), bf16[32,64,128]{2,1,0:T(8,128)(2,1)S(1)}, u32[]{:S(2)}, u32[]{:S(2)}) async-start(bf16[32,64,128]{2,1,0:T(8,128)(2,1)} %broadcast_in_dim.11), calls=%async_computation.4 | async-start | bytes 1048576 | tf_op jit(solution)/shard_map/all_to_all | solution.py:377
  147.1 3.3 %fusion.1 = bf16[1,224,2048]{2,1,0:T(8,128)(2,1)} fusion(bf16[512,224]{1,0:T(8,128)(2,1)} %get-tuple-element.35, bf16[512,2048]{1,0:T(8,128)(2,1)} %bitcast.116), kind=kOutput, calls=%fused_computation.3 | convolution fusion | flops 470220800 | bytes 3244032 | tf_op jit(solution)/shard_map/dot_general | solution.py:18
  150.5 1.6 fusion
  152.1 0.9 combined.1
  152.9 18.7 %all_gather.6 = bf16[224,2048]{1,0:T(8,128)(2,1)S(1)} all-gather(bf16[224,128]{1,0:T(8,128)(2,1)S(1)} %get-tuple-element.42), channel_id=1, replica_groups=mesh['sp'=32,'chip'=8,'core'=2] {'chip','core'}, dimensions={1}, use_global_device_ids=true | all-gather | bytes 974848 | tf_op jit(solution)/shard_map/all_gather | solution.py:424
  171.6 1.4 convolution_convert_fusion.2
  173.1 9.5 %all-to-all-start.3 = ((bf16[32,64,128]{2,1,0:T(8,128)(2,1)}), bf16[32,64,128]{2,1,0:T(8,128)(2,1)S(1)}, u32[]{:S(2)}, u32[]{:S(2)}) async-start(bf16[32,64,128]{2,1,0:T(8,128)(2,1)} %bitcast.22), calls=%async_computation.3 | async-start | bytes 1048576 | tf_op jit(solution)/shard_map/all_to_all | solution.py:429
  182.6 0.5 fusion.41
  183.2 16.1 %all-gather = f32[16,1,512]{2,1,0:T(1,128)S(1)} all-gather(f32[1,1,512]{2,1,0:T(1,128)S(1)} %reshape.80), channel_id=1, replica_groups=mesh['sp'=32,'chip'=8,'core'=2] {'chip','core'}, dimensions={0}, use_global_device_ids=true | all-gather | bytes 34816 | tf_op jit(solution)/shard_map/all_gather | solution.py:440
  199.6 0.9 fusion.5
  200.5 0.7 convert_reduce_fusion
  (92 shorter events, 0.7 us)
Async XLA Ops:
  27.7 42.2 %copy-start.2 = (bf16[32,32,128]{2,1,0:T(8,128)(2,1)}, bf16[32,32,128]{2,1,0:T(8,128)(2,1)S(1)}, u32[]{:S(2)}) copy-start(bf16[32,32,128]{2,1,0:T(8,128)(2,1)S(1)} %all_to_all.25.refs_0_) | copy-start | bytes 786436
  27.7 9.3 %collective-permute-start = (bf16[32,32,128]{2,1,0:T(8,128)(2,1)S(1)}, bf16[32,32,128]{2,1,0:T(8,128)(2,1)S(1)}, u32[]{:S(2)}, u32[]{:S(2)}) collective-permute-start(bf16[32,32,128]{2,1,0:T(8,128)(2,1)S(1)} %all_to_all.25.refs_0_), channel_id=1, source_target_pairs={{0,2},{2,4},{4,6},{6,8},{8,10},{10,12},{12,14},{14,0},{1,3},{3,5},... | collective-permute-start | bytes 786440 | tf_op jit(solution)/shard_map/ppermute | solution.py:333
  30.9 8.0 %collective-permute-start.3 = (bf16[32,32,128]{2,1,0:T(8,128)(2,1)S(1)}, bf16[32,32,128]{2,1,0:T(8,128)(2,1)S(1)}, u32[]{:S(2)}, u32[]{:S(2)}) collective-permute-start(bf16[32,32,128]{2,1,0:T(8,128)(2,1)S(1)} %all_to_all.25.refs_0_), channel_id=1, source_target_pairs={{0,14},{2,0},{4,2},{6,4},{8,6},{10,8},{12,10},{14,12},{1,15},{3,1}... | collective-permute-start | bytes 786440 | tf_op jit(solution)/shard_map/ppermute | solution.py:333
  37.1 32.9 %copy-start.4 = (bf16[32,32,128]{2,1,0:T(8,128)(2,1)}, bf16[32,32,128]{2,1,0:T(8,128)(2,1)S(1)}, u32[]{:S(2)}) copy-start(bf16[32,32,128]{2,1,0:T(8,128)(2,1)S(1)} %collective-permute-done.refs_1_) | copy-start | bytes 786436
  37.1 8.3 %collective-permute-start.1 = (bf16[32,32,128]{2,1,0:T(8,128)(2,1)S(1)}, bf16[32,32,128]{2,1,0:T(8,128)(2,1)S(1)}, u32[]{:S(2)}, u32[]{:S(2)}) collective-permute-start(bf16[32,32,128]{2,1,0:T(8,128)(2,1)S(1)} %collective-permute-done.refs_1_), channel_id=1, source_target_pairs={{0,2},{2,4},{4,6},{6,8},{8,10},{10,12},{12,14},{14,0},{1,3},{3,5},... | collective-permute-start | bytes 786440 | tf_op jit(solution)/shard_map/ppermute | solution.py:333
  39.0 31.0 %copy-start.5 = (bf16[32,32,128]{2,1,0:T(8,128)(2,1)}, bf16[32,32,128]{2,1,0:T(8,128)(2,1)S(1)}, u32[]{:S(2)}) copy-start(bf16[32,32,128]{2,1,0:T(8,128)(2,1)S(1)} %collective-permute-done.3.refs_2_) | copy-start | bytes 786436
  39.0 8.3 %collective-permute-start.4 = (bf16[32,32,128]{2,1,0:T(8,128)(2,1)S(1)}, bf16[32,32,128]{2,1,0:T(8,128)(2,1)S(1)}, u32[]{:S(2)}, u32[]{:S(2)}) collective-permute-start(bf16[32,32,128]{2,1,0:T(8,128)(2,1)S(1)} %collective-permute-done.3.refs_2_), channel_id=1, source_target_pairs={{0,14},{2,0},{4,2},{6,4},{8,6},{10,8},{12,10},{14,12},{1,15},{3,1}... | collective-permute-start | bytes 786440 | tf_op jit(solution)/shard_map/ppermute | solution.py:333
  45.4 24.6 %copy-start.6 = (bf16[32,32,128]{2,1,0:T(8,128)(2,1)}, bf16[32,32,128]{2,1,0:T(8,128)(2,1)S(1)}, u32[]{:S(2)}) copy-start(bf16[32,32,128]{2,1,0:T(8,128)(2,1)S(1)} %collective-permute-done.1.refs_3_) | copy-start | bytes 786436
  45.4 16.9 %collective-permute-start.2 = (bf16[32,32,128]{2,1,0:T(8,128)(2,1)S(1)}, bf16[32,32,128]{2,1,0:T(8,128)(2,1)S(1)}, u32[]{:S(2)}, u32[]{:S(2)}) collective-permute-start(bf16[32,32,128]{2,1,0:T(8,128)(2,1)S(1)} %collective-permute-done.1.refs_3_), channel_id=1, source_target_pairs={{0,2},{2,4},{4,6},{6,8},{8,10},{10,12},{12,14},{14,0},{1,3},{3,5},... | collective-permute-start | bytes 786440 | tf_op jit(solution)/shard_map/ppermute | solution.py:333
  47.3 22.7 %copy-start.7 = (bf16[32,32,128]{2,1,0:T(8,128)(2,1)}, bf16[32,32,128]{2,1,0:T(8,128)(2,1)S(1)}, u32[]{:S(2)}) copy-start(bf16[32,32,128]{2,1,0:T(8,128)(2,1)S(1)} %collective-permute-done.4.refs_4_) | copy-start | bytes 786436
  47.3 15.0 %collective-permute-start.5 = (bf16[32,32,128]{2,1,0:T(8,128)(2,1)S(1)}, bf16[32,32,128]{2,1,0:T(8,128)(2,1)S(1)}, u32[]{:S(2)}, u32[]{:S(2)}) collective-permute-start(bf16[32,32,128]{2,1,0:T(8,128)(2,1)S(1)} %collective-permute-done.4.refs_4_), channel_id=1, source_target_pairs={{0,14},{2,0},{4,2},{6,4},{8,6},{10,8},{12,10},{14,12},{1,15},{3,1}... | collective-permute-start | bytes 786440 | tf_op jit(solution)/shard_map/ppermute | solution.py:333
  52.9 17.1 %collective-permute-start.9 = (bf16[3,32,32,128]{3,2,1,0:T(8,128)(2,1)}, bf16[3,32,32,128]{3,2,1,0:T(8,128)(2,1)}, u32[]{:S(2)}, u32[]{:S(2)}) collective-permute-start(bf16[3,32,32,128]{3,2,1,0:T(8,128)(2,1)} %pad_maximum_fusion), channel_id=1, source_target_pairs={{0,1},{1,0},{2,3},{3,2},{4,5},{5,4},{6,7},{7,6},{8,9},{9,8},{10,11... | collective-permute-start | bytes 2359304 | tf_op jit(solution)/shard_map/ppermute | solution.py:342
  60.3 9.6 %collective-permute-start.10 = (bf16[2,32,32,128]{3,2,1,0:T(8,128)(2,1)}, bf16[2,32,32,128]{3,2,1,0:T(8,128)(2,1)}, u32[]{:S(2)}, u32[]{:S(2)}) collective-permute-start(bf16[2,32,32,128]{3,2,1,0:T(8,128)(2,1)} %pad_maximum_fusion.2), channel_id=1, source_target_pairs={{0,1},{1,0},{2,3},{3,2},{4,5},{5,4},{6,7},{7,6},{8,9},{9,8},{10,11... | collective-permute-start | bytes 1572872 | tf_op jit(solution)/shard_map/ppermute | solution.py:342
  62.3 15.8 %collective-permute-start.7 = (bf16[2,32,32,128]{3,2,1,0:T(8,128)(2,1)S(1)}, bf16[2,32,32,128]{3,2,1,0:T(8,128)(2,1)S(1)}, u32[]{:S(2)}, u32[]{:S(2)}) collective-permute-start(bf16[2,32,32,128]{3,2,1,0:T(8,128)(2,1)S(1)} %pad_maximum_fusion.1), channel_id=1, source_target_pairs={{0,1},{1,0},{2,3},{3,2},{4,5},{5,4},{6,7},{7,6},{8,9},{9,8},{10,11... | collective-permute-start | bytes 1572872 | tf_op jit(solution)/shard_map/ppermute | solution.py:342
  64.8 10.1 %collective-permute-start.8 = (bf16[32,32,128]{2,1,0:T(8,128)(2,1)S(1)}, bf16[32,32,128]{2,1,0:T(8,128)(2,1)S(1)}, u32[]{:S(2)}, u32[]{:S(2)}) collective-permute-start(bf16[32,32,128]{2,1,0:T(8,128)(2,1)S(1)} %collective-permute-done.5.refs_1_), channel_id=1, source_target_pairs={{0,15},{1,14},{2,1},{3,0},{4,3},{5,2},{6,5},{7,4},{8,7},{9,6},{10,... | collective-permute-start | bytes 786440 | tf_op jit(solution)/shard_map/ppermute | solution.py:360
  67.7 10.5 %collective-permute-start.6 = (bf16[32,32,128]{2,1,0:T(8,128)(2,1)S(1)}, bf16[32,32,128]{2,1,0:T(8,128)(2,1)S(1)}, u32[]{:S(2)}, u32[]{:S(2)}) collective-permute-start(bf16[32,32,128]{2,1,0:T(8,128)(2,1)S(1)} %collective-permute-done.2.refs_0_), channel_id=1, source_target_pairs={{0,2},{2,4},{4,6},{6,8},{8,10},{10,12},{12,14},{14,0},{1,3},{3,5},... | collective-permute-start | bytes 786440 | tf_op jit(solution)/shard_map/ppermute | solution.py:333
  81.3 5.5 %collective-permute-start.11 = (bf16[8,512,128]{2,1,0:T(8,128)(2,1)S(1)}, bf16[8,512,128]{2,1,0:T(8,128)(2,1)S(1)}, u32[]{:S(2)}, u32[]{:S(2)}) collective-permute-start(bf16[8,512,128]{2,1,0:T(8,128)(2,1)S(1)} %get-tuple-element.39), channel_id=1, source_target_pairs={{0,1},{1,0},{2,3},{3,2},{4,5},{5,4},{6,7},{7,6},{8,9},{9,8},{10,11... | collective-permute-start | bytes 3145736 | tf_op jit(solution)/shard_map/ppermute | solution.py:342
  85.4 9.3 %copy-start.12 = (s32[192,2]{0,1:T(2,128)S(1)}, s32[192,2]{0,1:T(2,128)}, u32[]{:S(2)}) copy-start(s32[192,2]{0,1:T(2,128)} %param.16) | copy-start | bytes 4612
  85.4 9.3 %copy-start.13 = (f32[192]{0:T(256)S(1)}, f32[192]{0:T(256)}, u32[]{:S(2)}) copy-start(f32[192]{0:T(256)} %param.23) | copy-start | bytes 2308
  85.4 9.3 %copy-start.14 = (f32[192]{0:T(256)S(1)}, f32[192]{0:T(256)}, u32[]{:S(2)}) copy-start(f32[192]{0:T(256)} %param.22) | copy-start | bytes 2308
  85.4 10.6 %copy-start.1 = (bf16[192,128]{1,0:T(8,128)(2,1)S(1)}, bf16[192,128]{1,0:T(8,128)(2,1)}, u32[]{:S(2)}) copy-start(bf16[192,128]{1,0:T(8,128)(2,1)} %cotangent.3) | copy-start | bytes 147460
  85.5 10.6 %copy-start.9 = (bf16[192,128]{1,0:T(8,128)(2,1)S(1)}, bf16[192,128]{1,0:T(8,128)(2,1)}, u32[]{:S(2)}) copy-start(bf16[192,128]{1,0:T(8,128)(2,1)} %param.21) | copy-start | bytes 147460
  85.5 11.9 %copy-start.11 = (f32[31,128]{1,0:T(8,128)S(1)}, f32[31,128]{1,0:T(8,128)}, u32[]{:S(2)}) copy-start(f32[31,128]{1,0:T(8,128)} %param.26) | copy-start | bytes 47620
  88.1 53.4 %copy-start.10 = (bf16[64,128]{1,0:T(8,128)(2,1)S(1)}, bf16[64,128]{1,0:T(8,128)(2,1)}, u32[]{:S(2)}) copy-start(bf16[64,128]{1,0:T(8,128)(2,1)} %param.27) | copy-start | bytes 49156
  88.1 35.8 %all-to-all-start.1 = ((bf16[8,512,128]{2,1,0:T(8,128)(2,1)}), bf16[8,512,128]{2,1,0:T(8,128)(2,1)S(1)}, u32[]{:S(2)}, u32[]{:S(2)}) async-start(bf16[8,512,128]{2,1,0:T(8,128)(2,1)} %add_convert_fusion), calls=%async_computation.1 | async-start | bytes 2097152 | tf_op jit(solution)/shard_map/all_to_all | solution.py:366
  94.7 4.6 %collective-permute-start.12 = (f32[4,32]{1,0:T(4,128)S(1)}, f32[4,32]{1,0:T(4,128)S(1)}, u32[]{:S(2)}, u32[]{:S(2)}) collective-permute-start(f32[4,32]{1,0:T(4,128)S(1)} %pad_maximum_fusion.5), channel_id=1, source_target_pairs={{16,0},{32,16},{48,32},{64,48},{80,64},{96,80},{112,96},{128,112},... | collective-permute-start | bytes 1544 | tf_op jit(solution)/shard_map/ppermute | solution.py:338
  96.1 34.3 %collective-permute-start.13 = (bf16[2,32,128]{2,1,0:T(8,128)(2,1)S(1)}, bf16[2,32,128]{2,1,0:T(8,128)(2,1)S(1)}, u32[]{:S(2)}, u32[]{:S(2)}) collective-permute-start(bf16[2,32,128]{2,1,0:T(8,128)(2,1)S(1)} %pad_maximum_fusion.4), channel_id=1, source_target_pairs={{16,0},{32,16},{48,32},{64,48},{80,64},{96,80},{112,96},{128,112},... | collective-permute-start | bytes 49160 | tf_op jit(solution)/shard_map/ppermute | solution.py:338
  124.7 16.8 %all-to-all-start.2 = ((bf16[32,32,128]{2,1,0:T(8,128)(2,1)}), bf16[32,32,128]{2,1,0:T(8,128)(2,1)S(1)}, u32[]{:S(2)}, u32[]{:S(2)}) async-start(bf16[32,32,128]{2,1,0:T(8,128)(2,1)} %summed.1), calls=%async_computation.2 | async-start | bytes 524288 | tf_op jit(solution)/shard_map/all_to_all | solution.py:420
  142.5 7.9 %copy-start.8 = (bf16[512,224]{1,0:T(8,128)(2,1)S(1)}, bf16[512,224]{1,0:T(8,128)(2,1)}, u32[]{:S(2)}) copy-start(bf16[512,224]{1,0:T(8,128)(2,1)} %get-tuple-element.33) | copy-start | bytes 688132
  142.5 30.6 %all-to-all-start.4 = ((bf16[32,64,128]{2,1,0:T(8,128)(2,1)}), bf16[32,64,128]{2,1,0:T(8,128)(2,1)S(1)}, u32[]{:S(2)}, u32[]{:S(2)}) async-start(bf16[32,64,128]{2,1,0:T(8,128)(2,1)} %broadcast_in_dim.11), calls=%async_computation.4 | async-start | bytes 1048576 | tf_op jit(solution)/shard_map/all_to_all | solution.py:377
  150.4 21.2 %copy-start.28 = (f32[128]{0:T(128)S(1)}, f32[128]{0:T(128)}, u32[]{:S(2)}) copy-start(f32[128]{0:T(128)} %param.25) | copy-start | bytes 1540
  150.4 21.2 %copy-start.30 = (f32[128]{0:T(128)S(1)}, f32[128]{0:T(128)}, u32[]{:S(2)}) copy-start(f32[128]{0:T(128)} %param.24) | copy-start | bytes 1540
  152.9 29.7 %copy-start.29 = (f32[128]{0:T(128)S(1)}, f32[128]{0:T(128)}, u32[]{:S(2)}) copy-start(f32[128]{0:T(128)} %param.25) | copy-start | bytes 1540
  152.9 29.7 %copy-start.31 = (f32[128]{0:T(128)S(1)}, f32[128]{0:T(128)}, u32[]{:S(2)}) copy-start(f32[128]{0:T(128)} %param.24) | copy-start | bytes 1540
  173.0 26.5 %copy-start.15 = (f32[128]{0:T(128)S(1)}, f32[128]{0:T(128)}, u32[]{:S(2)}) copy-start(f32[128]{0:T(128)} %get-tuple-element.63) | copy-start | bytes 1540
  173.0 26.5 %copy-start.16 = (f32[128]{0:T(128)S(1)}, f32[128]{0:T(128)}, u32[]{:S(2)}) copy-start(f32[128]{0:T(128)} %get-tuple-element.64) | copy-start | bytes 1540
  173.0 26.5 %copy-start.17 = (f32[128]{0:T(128)S(1)}, f32[128]{0:T(128)}, u32[]{:S(2)}) copy-start(f32[128]{0:T(128)} %get-tuple-element.65) | copy-start | bytes 1540
  173.0 26.5 %copy-start.18 = (f32[128]{0:T(128)S(1)}, f32[128]{0:T(128)}, u32[]{:S(2)}) copy-start(f32[128]{0:T(128)} %get-tuple-element.66) | copy-start | bytes 1540
  173.0 26.5 %copy-start.19 = (f32[128]{0:T(128)S(1)}, f32[128]{0:T(128)}, u32[]{:S(2)}) copy-start(f32[128]{0:T(128)} %get-tuple-element.67) | copy-start | bytes 1540
  173.0 26.5 %copy-start.20 = (f32[128]{0:T(128)S(1)}, f32[128]{0:T(128)}, u32[]{:S(2)}) copy-start(f32[128]{0:T(128)} %get-tuple-element.68) | copy-start | bytes 1540
  173.0 26.5 %copy-start.21 = (f32[128]{0:T(128)S(1)}, f32[128]{0:T(128)}, u32[]{:S(2)}) copy-start(f32[128]{0:T(128)} %get-tuple-element.69) | copy-start | bytes 1540
  173.0 26.5 %copy-start.22 = (f32[128]{0:T(128)S(1)}, f32[128]{0:T(128)}, u32[]{:S(2)}) copy-start(f32[128]{0:T(128)} %get-tuple-element.70) | copy-start | bytes 1540
  173.0 26.5 %copy-start.23 = (f32[128]{0:T(128)S(1)}, f32[128]{0:T(128)}, u32[]{:S(2)}) copy-start(f32[128]{0:T(128)} %get-tuple-element.71) | copy-start | bytes 1540
  173.0 26.5 %copy-start.24 = (f32[128]{0:T(128)S(1)}, f32[128]{0:T(128)}, u32[]{:S(2)}) copy-start(f32[128]{0:T(128)} %get-tuple-element.72) | copy-start | bytes 1540
  173.0 26.5 %copy-start.25 = (f32[128]{0:T(128)S(1)}, f32[128]{0:T(128)}, u32[]{:S(2)}) copy-start(f32[128]{0:T(128)} %get-tuple-element.73) | copy-start | bytes 1540
  173.0 26.5 %copy-start.26 = (f32[128]{0:T(128)S(1)}, f32[128]{0:T(128)}, u32[]{:S(2)}) copy-start(f32[128]{0:T(128)} %get-tuple-element.74) | copy-start | bytes 1540
  173.1 26.5 %copy-start.27 = (f32[128]{0:T(128)S(1)}, f32[128]{0:T(128)}, u32[]{:S(2)}) copy-start(f32[128]{0:T(128)} %get-tuple-element.75) | copy-start | bytes 1540
  173.1 27.5 %all-to-all-start.3 = ((bf16[32,64,128]{2,1,0:T(8,128)(2,1)}), bf16[32,64,128]{2,1,0:T(8,128)(2,1)S(1)}, u32[]{:S(2)}, u32[]{:S(2)}) async-start(bf16[32,64,128]{2,1,0:T(8,128)(2,1)} %bitcast.22), calls=%async_computation.3 | async-start | bytes 1048576 | tf_op jit(solution)/shard_map/all_to_all | solution.py:429
  (2 other events, 9.6 us)

commit v8 on v7

--- a/solution.py
+++ b/solution.py
@@ -8,8 +8,8 @@
 
 
 TP = ("chip", "core")
-BATCHES = (3, 2, 2, 1)
-EARLY = 2
+BATCHES = (5, 2, 1)
+EARLY = 1
 BF16 = jnp.bfloat16
 F32 = jnp.float32
 
@@ -172,61 +172,81 @@
     return sums
 
 
+def held_body(*refs):
+    count = len(refs) // 2
+    copies = [
+        pltpu.make_async_copy(refs[n].at[0], refs[count + n], refs[-1].at[n]) for n in range(count)
+    ]
+    for copy in copies:
+        copy.start()
+    for copy in copies:
+        copy.wait()
+
+
+def held_weights(weights):
+    return pl.pallas_call(
+        held_body,
+        in_specs=whole(len(weights), pltpu.HBM),
+        out_specs=whole(len(weights)),
+        out_shape=[pltpu.VMEM(w.shape[1:], w.dtype) for w in weights],
+        scratch_shapes=[pltpu.SemaphoreType.DMA((len(weights),))],
+        compiler_params=pltpu.CompilerParams(vmem_limit_bytes=12 * 1024 * 1024),
+        name="held_weights",
+    )(*far(*weights))
+
+
 def first_body(me, *refs, blocks, slots, batches):
     chips = blocks // 2
     count = sum(batches)
     mine, shared = (refs[:count], refs[count : count + len(batches)])
-    weights = refs[count + len(batches) : count + len(batches) + 3]
-    rows, routed, *sums, held0, held1, held2, sems, weight_sems = refs[count + len(batches) + 3 :]
+    held = refs[count + len(batches) : count + len(batches) + 3]
+    rows, routed, *sums, sems = refs[count + len(batches) + 3 :]
     others = [(batch, at) for batch, size in zip(shared, batches) for at in range(size)]
-    held = (held0, held1, held2)
     width = mine[0].shape[-1]
     my_chip, my_core = (me[0] // 2, lax.rem(me[0], 2))
-    copies = [
-        pltpu.make_async_copy(weight.at[0], keep, weight_sems.at[n])
-        for n, (weight, keep) in enumerate(zip(weights, held))
-    ]
-    found = []
+    copies, found = ([], [])
     for n, (step, (batch, at)) in enumerate(zip(ring_order(chips), others)):
         chip = lax.rem(my_chip + step + chips, chips)
+        copies.append([])
         for i, (core, source) in enumerate(((my_core, mine[n]), (1 - my_core, batch.at[at]))):
             cols = columns(chip, core, width)
             for k, target in enumerate((rows, routed)):
                 part = source.at[:, pl.ds(k * slots, slots), :]
-                copies.append(pltpu.make_async_copy(part, target.at[:, :, cols], sems.at[n, i, k]))
+                copies[n].append(
+                    pltpu.make_async_copy(part, target.at[:, :, cols], sems.at[n, i, k])
+                )
         found.append(pl.ds(pl.multiple_of(chip * 2 * width, 2 * width), 2 * width))
-    for copy in copies:
-        copy.start()
-    for copy in copies:
-        copy.wait()
-    for out, value in zip(sums, products(rows, routed, held, found)):
+        for copy in copies[n]:
+            copy.start()
+    totals = [None] * 3
+    for n in range(count):
+        for copy in copies[n]:
+            copy.wait()
+        parts = products(rows, routed, held, found[n : n + 1])
+        totals = [p if t is None else t + p for t, p in zip(totals, parts)]
+    for out, value in zip(sums, totals):
         out[...] = value
 
 
-def first_products(me, mine, shared, weights, slots, blocks):
+def first_products(me, mine, shared, held, slots, blocks):
     batches = [b.shape[0] for b in shared]
     experts, _, _ = mine[0].shape
-    count, hidden, channels = (experts * slots, weights[0].shape[1], weights[0].shape[2])
+    count, (hidden, channels) = (experts * slots, held[0].shape)
     return pl.pallas_call(
         functools.partial(first_body, blocks=blocks, slots=slots, batches=batches),
-        in_specs=whole(1, pltpu.SMEM)
-        + whole(len(mine) + len(shared) + 3, pltpu.HBM),
-        out_specs=whole(8),
-        scratch_shapes=[
-            pltpu.SemaphoreType.DMA((len(mine), 2, 2)),
-            pltpu.SemaphoreType.DMA((3,)),
-        ],
+        in_specs=whole(1, pltpu.SMEM) + whole(len(mine) + len(shared), pltpu.HBM) + whole(3),
+        out_specs=whole(5),
+        scratch_shapes=[pltpu.SemaphoreType.DMA((len(mine), 2, 2))],
         out_shape=(
             *[pltpu.VMEM((experts, slots, channels), BF16)] * 2,
             *[pltpu.VMEM((count, hidden), F32)] * 3,
-            *[pltpu.VMEM((hidden, channels), BF16)] * 3,
         ),
         cost_estimate=pl.CostEstimate(
-            flops=4 * count * hidden * channels, transcendentals=0, bytes_accessed=12 * 1024 * 1024
+            flops=4 * count * hidden * channels, transcendentals=0, bytes_accessed=6 * 1024 * 1024
         ),
         compiler_params=pltpu.CompilerParams(vmem_limit_bytes=12 * 1024 * 1024),
         name="first_products",
-    )(me, *far(*mine, *shared, *weights))
+    )(me, *far(*mine, *shared), *near(*held))
 
 
 def partial_rows(out, gate_grad, up_grad, gate_weight, up_weight, core):
@@ -403,11 +423,14 @@
     sent, place = send_rows(routes.T, route_weight.T, moe_in, cotangent, devices, slots)
     own = lax.all_to_all(sent, "sp", split_axis=0, concat_axis=0, tiled=True)
     proj = sent_to_all(w_proj, "sp").reshape(-1, channels)
+    held = held_weights((w_gate, w_up, w_down))
     mine, others = all_blocks(own)
     done = sum(BATCHES[:EARLY])
-    early = first_products(me, mine[:done], others[:EARLY], (w_gate, w_up, w_down), slots, blocks)
+    early = first_products(
+        me, mine[:done], others[:EARLY], held, slots, blocks
+    )
     _, _, given, gate_rows, up_rows, rows, routed, hidden, up_grad = rest_products(
-        me, mine[done:], others[EARLY:], early, slots, blocks
+        me, mine[done:], others[EARLY:], (*early, *held), slots, blocks
     )
     rim = 8 * (-(-(taps.shape[0] - 1) // 8))
     rim_cotangent, rim_pre = from_after(jnp.stack([cotangent[:rim], conv_pre[:rim]]))
@@ -415,7 +438,7 @@
     facts = from_after(jnp.stack([*facts, norm_mean[:rim], norm_rstd[:rim]]))
     rim_place = rim_places(facts[:2].astype(jnp.int32), devices, slots)
     other = to_other_core(given)
-    kept = kept_products(me, gate_rows, up_rows, early[5], early[6], blocks)
+    kept = kept_products(me, gate_rows, up_rows, held[0], held[1], blocks)
     shared = summed(added_up(kept, other), devices)
     returned = lax.all_to_all(shared, "sp", split_axis=0, concat_axis=0, tiled=True)
     grad_up = dot(up_grad, rows.reshape(-1, rows.shape[2]), 0, 0).astype(BF16)[None]

time: 202 us -> 211 us (1.045)
  local copies, waits for them, and re-layouts: 2.27 us -> 9.74 us
    ppermute x7, waiting for transfers between devices: 7.39 us -> 11.7 us  [along_chips(): lax.ppermute(value, 'chip', [(y, (y + steps) % count) for y in range(coun...]
    unnamed x65 -> x109, local copies, waits for them, and re-layouts: 0.16 us -> 4.28 us
    all_to_all x1, waiting for transfers between devices: 24.5 us -> 21.9 us  [added_up(): lax.all_to_all(both.astype(BF16), 'chip', split_axis=0, concat_axis=0, ti...]
    ppermute x4 -> x3, starting transfers between devices: 14.2 us -> 12.1 us  [to_other_core(): return lax.ppermute(value, 'core', [(0, 1), (1, 0)])]
  transfers between devices with their start and end apart: 18 -> 17, of which waited for: 8 -> 9; matrix products, arithmetic and copies ran while one was open for 6% -> 8% of each run, Pallas kernels for 3% -> 4%
where the time goes in v8:
time: 211 us; the launch traced here: 210 us
  starting transfers between devices  67.9 us (32%)
  blocking collectives  60.2 us (29%)
  waiting for transfers between devices  45.6 us (22%)
  Pallas kernels  13.1 us (6%)
  local copies, waits for them, and re-layouts  9.74 us (5%)
  matrix products  6.13 us (3%)
  other arithmetic  5.47 us (3%)
    all_to_all x1, blocking collectives, steps(): own = lax.all_to_all(sent, 'sp', split_axis=0, concat_axis=0, tiled=True)  25 us
    ppermute x7, starting transfers between devices, along_chips(): lax.ppermute(value, 'chip', [(y, (y + steps) % count) for y in range(coun...  23.4 us
    all_to_all x1, waiting for transfers between devices, added_up(): lax.all_to_all(both.astype(BF16), 'chip', split_axis=0, concat_axis=0, ti...  21.9 us
    all_gather x1, blocking collectives, steps(): columns = lax.all_gather(stream, TP, axis=1, tiled=True)  19.1 us
    all_gather x1, blocking collectives, steps(): sums = lax.all_gather(sums, TP, axis=0, tiled=False)  16.1 us
    ppermute x3, starting transfers between devices, to_other_core(): return lax.ppermute(value, 'core', [(0, 1), (1, 0)])  12.1 us
    ppermute x7, waiting for transfers between devices, along_chips(): lax.ppermute(value, 'chip', [(y, (y + steps) % count) for y in range(coun...  11.7 us
    all_to_all x1, waiting for transfers between devices, steps(): lax.all_to_all(shared, 'sp', split_axis=0, concat_axis=0, tiled=True)  10.5 us
  transfers between devices with their start and end apart: 17, of which 9 were waited for; matrix products, arithmetic and copies ran while one was open for 8% of the time, Pallas kernels for 4%

profile of v8, /device:TPU:1, one launch (start us, length us, event | category | flops | bytes accessed | tf_op | source)
XLA Modules:
  0.0 209.6 jit_solution(4429264071655550130)
XLA Ops:
  0.6 2.1 send_rows.1
  2.7 25.0 %all_to_all.25.refs_0_ = bf16[32,32,128]{2,1,0:T(8,128)(2,1)S(1)} all-to-all(bf16[32,32,128]{2,1,0:T(8,128)(2,1)} %get-tuple-element.24), channel_id=1, replica_groups=mesh['sp'=32,'chip'=8,'core'=2] {'sp'}, dimensions={0} | all-to-all | bytes 524288 | tf_op jit(solution)/shard_map/all_to_all | solution.py:424
  27.7 3.2 %collective-permute-start = (bf16[32,32,128]{2,1,0:T(8,128)(2,1)S(1)}, bf16[32,32,128]{2,1,0:T(8,128)(2,1)S(1)}, u32[]{:S(2)}, u32[]{:S(2)}) collective-permute-start(bf16[32,32,128]{2,1,0:T(8,128)(2,1)S(1)} %all_to_all.25.refs_0_), channel_id=1, source_target_pairs={{0,2},{2,4},{4,6},{6,8},{8,10},{10,12},{12,14},{14,0},{1,3},{3,5},... | collective-permute-start | bytes 786440 | tf_op jit(solution)/shard_map/ppermute | solution.py:353
  30.9 3.8 %collective-permute-start.3 = (bf16[32,32,128]{2,1,0:T(8,128)(2,1)S(1)}, bf16[32,32,128]{2,1,0:T(8,128)(2,1)S(1)}, u32[]{:S(2)}, u32[]{:S(2)}) collective-permute-start(bf16[32,32,128]{2,1,0:T(8,128)(2,1)S(1)} %all_to_all.25.refs_0_), channel_id=1, source_target_pairs={{0,14},{2,0},{4,2},{6,4},{8,6},{10,8},{12,10},{14,12},{1,15},{3,1}... | collective-permute-start | bytes 786440 | tf_op jit(solution)/shard_map/ppermute | solution.py:353
  35.5 1.6 collective-permute-done.refs_1_
  37.1 1.9 collective-permute-start.1
  39.7 4.6 %collective-permute-start.4 = (bf16[32,32,128]{2,1,0:T(8,128)(2,1)S(1)}, bf16[32,32,128]{2,1,0:T(8,128)(2,1)S(1)}, u32[]{:S(2)}, u32[]{:S(2)}) collective-permute-start(bf16[32,32,128]{2,1,0:T(8,128)(2,1)S(1)} %collective-permute-done.3.refs_2_), channel_id=1, source_target_pairs={{0,14},{2,0},{4,2},{6,4},{8,6},{10,8},{12,10},{14,12},{1,15},{3,1}... | collective-permute-start | bytes 786440 | tf_op jit(solution)/shard_map/ppermute | solution.py:353
  45.4 0.8 bitcast_dynamic-update-slice_fusion.1
  46.2 1.4 collective-permute-done.4.refs_4_
  48.3 6.1 %collective-permute-start.9 = (bf16[5,32,32,128]{3,2,1,0:T(8,128)(2,1)}, bf16[5,32,32,128]{3,2,1,0:T(8,128)(2,1)S(1)}, u32[]{:S(2)}, u32[]{:S(2)}) collective-permute-start(bf16[5,32,32,128]{3,2,1,0:T(8,128)(2,1)} %bitcast_dynamic-update-slice_fusion), channel_id=1, source_target_pairs={{0,1},{1,0},{2,3},{3,2},{4,5},{5,4},{6,7},{7,6},{8,9},{9,8},{10,11... | collective-permute-start | bytes 3932168 | tf_op jit(solution)/shard_map/ppermute | solution.py:362
  54.4 2.4 %collective-permute-start.2 = (bf16[32,32,128]{2,1,0:T(8,128)(2,1)S(1)}, bf16[32,32,128]{2,1,0:T(8,128)(2,1)S(1)}, u32[]{:S(2)}, u32[]{:S(2)}) collective-permute-start(bf16[32,32,128]{2,1,0:T(8,128)(2,1)S(1)} %collective-permute-done.1.refs_3_), channel_id=1, source_target_pairs={{0,2},{2,4},{4,6},{6,8},{8,10},{10,12},{12,14},{14,0},{1,3},{3,5},... | collective-permute-start | bytes 786440 | tf_op jit(solution)/shard_map/ppermute | solution.py:353
  56.8 4.8 %collective-permute-start.5 = (bf16[32,32,128]{2,1,0:T(8,128)(2,1)S(1)}, bf16[32,32,128]{2,1,0:T(8,128)(2,1)S(1)}, u32[]{:S(2)}, u32[]{:S(2)}) collective-permute-start(bf16[32,32,128]{2,1,0:T(8,128)(2,1)S(1)} %collective-permute-done.4.refs_4_), channel_id=1, source_target_pairs={{0,14},{2,0},{4,2},{6,4},{8,6},{10,8},{12,10},{14,12},{1,15},{3,1}... | collective-permute-start | bytes 786440 | tf_op jit(solution)/shard_map/ppermute | solution.py:353
  61.7 4.7 %collective-permute-done.2.refs_0_ = bf16[32,32,128]{2,1,0:T(8,128)(2,1)S(1)} collective-permute-done((bf16[32,32,128]{2,1,0:T(8,128)(2,1)S(1)}, bf16[32,32,128]{2,1,0:T(8,128)(2,1)S(1)}, u32[]{:S(2)}, u32[]{:S(2)}) %collective-permute-start.2) | collective-permute-done | bytes 262176 | tf_op jit(solution)/shard_map/ppermute | solution.py:353
  66.4 2.0 collective-permute-done.5.refs_1_
  68.4 0.8 pad_maximum_fusion
  69.2 2.8 %collective-permute-start.7 = (bf16[2,32,32,128]{3,2,1,0:T(8,128)(2,1)}, bf16[2,32,32,128]{3,2,1,0:T(8,128)(2,1)S(1)}, u32[]{:S(2)}, u32[]{:S(2)}) collective-permute-start(bf16[2,32,32,128]{3,2,1,0:T(8,128)(2,1)} %pad_maximum_fusion), channel_id=1, source_target_pairs={{0,1},{1,0},{2,3},{3,2},{4,5},{5,4},{6,7},{7,6},{8,9},{9,8},{10,11... | collective-permute-start | bytes 1572872 | tf_op jit(solution)/shard_map/ppermute | solution.py:362
  72.0 4.1 %collective-permute-start.8 = (bf16[32,32,128]{2,1,0:T(8,128)(2,1)S(1)}, bf16[32,32,128]{2,1,0:T(8,128)(2,1)S(1)}, u32[]{:S(2)}, u32[]{:S(2)}) collective-permute-start(bf16[32,32,128]{2,1,0:T(8,128)(2,1)S(1)} %collective-permute-done.5.refs_1_), channel_id=1, source_target_pairs={{0,15},{1,14},{2,1},{3,0},{4,3},{5,2},{6,5},{7,4},{8,7},{9,6},{10,... | collective-permute-start | bytes 786440 | tf_op jit(solution)/shard_map/ppermute | solution.py:380
  76.1 2.6 %collective-permute-start.6 = (bf16[32,32,128]{2,1,0:T(8,128)(2,1)S(1)}, bf16[32,32,128]{2,1,0:T(8,128)(2,1)S(1)}, u32[]{:S(2)}, u32[]{:S(2)}) collective-permute-start(bf16[32,32,128]{2,1,0:T(8,128)(2,1)S(1)} %collective-permute-done.2.refs_0_), channel_id=1, source_target_pairs={{0,2},{2,4},{4,6},{6,8},{8,10},{10,12},{12,14},{14,0},{1,3},{3,5},... | collective-permute-start | bytes 786440 | tf_op jit(solution)/shard_map/ppermute | solution.py:353
  78.8 1.8 held_weights.1
  80.6 1.1 copy-done.5
  81.7 3.3 %first_products.1 = (bf16[32,16,2048]{2,1,0:T(8,128)(2,1)S(1)}, bf16[32,16,2048]{2,1,0:T(8,128)(2,1)S(1)}, f32[512,224]{1,0:T(8,128)S(1)}, f32[512,224]{1,0:T(8,128)S(1)}, f32[512,224]{1,0:T(8,128)S(1)}) custom-call(s32[1]{0:T(128)} %bitcast.me, bf16[32,32,128]{2,1,0:T(8,128)(2,1)} %copy-done.2, bf16[32,32,128]{2,1,0:T(8,128)(2,1)} %copy-done.6, ...), custom_call_target="tpu_custom_call" | custom-call | flops 939524096 | bytes 6291456 | tf_op jit(solution)/shard_map/first_products/pallas_call | solution.py:235
  85.0 1.6 collective-permute-done.6.refs_2_
  86.6 3.2 %rest_products.1 = (bf16[32,16,2048]{2,1,0:T(8,128)(2,1)S(1)}, bf16[32,16,2048]{2,1,0:T(8,128)(2,1)S(1)}, bf16[8,512,128]{2,1,0:T(8,128)(2,1)S(1)}, bf16[512,224...) custom-call(s32[1]{0:T(128)} %bitcast.me, ...), custom_call_target="tpu_custom_call", output_to_operand_aliasing={{0}: (6, {}), {1}: (7, {})} | custom-call | flops 1409286144 | bytes 12582912 | tf_op jit(solution)/shard_map/rest_products/pallas_call | solution.py:328
  89.8 3.3 %collective-permute-start.10 = (bf16[8,512,128]{2,1,0:T(8,128)(2,1)S(1)}, bf16[8,512,128]{2,1,0:T(8,128)(2,1)S(1)}, u32[]{:S(2)}, u32[]{:S(2)}) collective-permute-start(bf16[8,512,128]{2,1,0:T(8,128)(2,1)S(1)} %get-tuple-element.39), channel_id=1, source_target_pairs={{0,1},{1,0},{2,3},{3,2},{4,5},{5,4},{6,7},{7,6},{8,9},{9,8},{10,11... | collective-permute-start | bytes 3145736 | tf_op jit(solution)/shard_map/ppermute | solution.py:362
  93.1 0.8 kept_products.1
  93.9 1.5 collective-permute-done.10
  95.3 1.3 add_convert_fusion
  96.6 6.5 %all-to-all-start.1 = ((bf16[8,512,128]{2,1,0:T(8,128)(2,1)}), bf16[8,512,128]{2,1,0:T(8,128)(2,1)S(1)}, u32[]{:S(2)}, u32[]{:S(2)}) async-start(bf16[8,512,128]{2,1,0:T(8,128)(2,1)} %add_convert_fusion), calls=%async_computation.1 | async-start | bytes 2097152 | tf_op jit(solution)/shard_map/all_to_all | solution.py:386
  103.2 1.3 collective-permute-start.11
  105.2 1.4 collective-permute-start.12
  106.6 1.7 slice_bitcast_fusion.36
  108.3 1.6 slice_bitcast_fusion.33
  110.5 21.9 %all-to-all-done.1.arrived = bf16[8,512,128]{2,1,0:T(8,128)(2,1)S(1)} async-done(((bf16[8,512,128]{2,1,0:T(8,128)(2,1)}), bf16[8,512,128]{2,1,0:T(8,128)(2,1)S(1)}, u32[]{:S(2)}, u32[]{:S(2)}) %all-to-all-start.1) | async-done | bytes 1048608 | tf_op jit(solution)/shard_map/all_to_all | solution.py:386
  132.4 0.9 summed.1
  133.3 5.0 %all-to-all-start.2 = ((bf16[32,32,128]{2,1,0:T(8,128)(2,1)}), bf16[32,32,128]{2,1,0:T(8,128)(2,1)S(1)}, u32[]{:S(2)}, u32[]{:S(2)}) async-start(bf16[32,32,128]{2,1,0:T(8,128)(2,1)} %summed.1), calls=%async_computation.2 | async-start | bytes 524288 | tf_op jit(solution)/shard_map/all_to_all | solution.py:443
  138.3 0.8 pad_maximum_fusion.5
  139.3 10.5 %all-to-all-done.2.returned = bf16[32,32,128]{2,1,0:T(8,128)(2,1)S(1)} async-done(((bf16[32,32,128]{2,1,0:T(8,128)(2,1)}), bf16[32,32,128]{2,1,0:T(8,128)(2,1)S(1)}, u32[]{:S(2)}, u32[]{:S(2)}) %all-to-all-start.2) | async-done | bytes 262176 | tf_op jit(solution)/shard_map/all_to_all | solution.py:443
  149.8 0.9 broadcast_in_dim.11
  150.7 4.6 %all-to-all-start.4 = ((bf16[32,64,128]{2,1,0:T(8,128)(2,1)}), bf16[32,64,128]{2,1,0:T(8,128)(2,1)}, u32[]{:S(2)}, u32[]{:S(2)}) async-start(bf16[32,64,128]{2,1,0:T(8,128)(2,1)} %broadcast_in_dim.11), calls=%async_computation.4 | async-start | bytes 1048576 | tf_op jit(solution)/shard_map/all_to_all | solution.py:397
  155.4 1.6 fusion.1
  157.1 1.6 fusion
  158.7 0.9 combined.1
  159.5 19.1 %all_gather.6 = bf16[224,2048]{1,0:T(8,128)(2,1)S(1)} all-gather(bf16[224,128]{1,0:T(8,128)(2,1)S(1)} %get-tuple-element.42), channel_id=1, replica_groups=mesh['sp'=32,'chip'=8,'core'=2] {'chip','core'}, dimensions={1}, use_global_device_ids=true | all-gather | bytes 974848 | tf_op jit(solution)/shard_map/all_gather | solution.py:447
  178.7 1.4 convolution_convert_fusion.2
  180.4 9.4 %all-to-all-start.3 = ((bf16[32,64,128]{2,1,0:T(8,128)(2,1)}), bf16[32,64,128]{2,1,0:T(8,128)(2,1)S(1)}, u32[]{:S(2)}, u32[]{:S(2)}) async-start(bf16[32,64,128]{2,1,0:T(8,128)(2,1)} %bitcast.22), calls=%async_computation.3 | async-start | bytes 1048576 | tf_op jit(solution)/shard_map/all_to_all | solution.py:452
  189.8 1.6 fusion.41
  191.4 16.1 %all-gather = f32[16,1,512]{2,1,0:T(1,128)S(1)} all-gather(f32[1,1,512]{2,1,0:T(1,128)S(1)} %reshape.80), channel_id=1, replica_groups=mesh['sp'=32,'chip'=8,'core'=2] {'chip','core'}, dimensions={0}, use_global_device_ids=true | all-gather | bytes 34816 | tf_op jit(solution)/shard_map/all_gather | solution.py:463
  208.0 0.9 fusion.5
  (134 shorter events, 6.0 us)
Async XLA Ops:
  27.7 41.5 %copy-start.2 = (bf16[32,32,128]{2,1,0:T(8,128)(2,1)}, bf16[32,32,128]{2,1,0:T(8,128)(2,1)S(1)}, u32[]{:S(2)}) copy-start(bf16[32,32,128]{2,1,0:T(8,128)(2,1)S(1)} %all_to_all.25.refs_0_) | copy-start | bytes 786436
  27.7 9.3 %collective-permute-start = (bf16[32,32,128]{2,1,0:T(8,128)(2,1)S(1)}, bf16[32,32,128]{2,1,0:T(8,128)(2,1)S(1)}, u32[]{:S(2)}, u32[]{:S(2)}) collective-permute-start(bf16[32,32,128]{2,1,0:T(8,128)(2,1)S(1)} %all_to_all.25.refs_0_), channel_id=1, source_target_pairs={{0,2},{2,4},{4,6},{6,8},{8,10},{10,12},{12,14},{14,0},{1,3},{3,5},... | collective-permute-start | bytes 786440 | tf_op jit(solution)/shard_map/ppermute | solution.py:353
  30.9 8.8 %collective-permute-start.3 = (bf16[32,32,128]{2,1,0:T(8,128)(2,1)S(1)}, bf16[32,32,128]{2,1,0:T(8,128)(2,1)S(1)}, u32[]{:S(2)}, u32[]{:S(2)}) collective-permute-start(bf16[32,32,128]{2,1,0:T(8,128)(2,1)S(1)} %all_to_all.25.refs_0_), channel_id=1, source_target_pairs={{0,14},{2,0},{4,2},{6,4},{8,6},{10,8},{12,10},{14,12},{1,15},{3,1}... | collective-permute-start | bytes 786440 | tf_op jit(solution)/shard_map/ppermute | solution.py:353
  37.1 43.5 %copy-start.6 = (bf16[32,32,128]{2,1,0:T(8,128)(2,1)}, bf16[32,32,128]{2,1,0:T(8,128)(2,1)S(1)}, u32[]{:S(2)}) copy-start(bf16[32,32,128]{2,1,0:T(8,128)(2,1)S(1)} %collective-permute-done.refs_1_) | copy-start | bytes 786436
  37.1 8.3 %collective-permute-start.1 = (bf16[32,32,128]{2,1,0:T(8,128)(2,1)S(1)}, bf16[32,32,128]{2,1,0:T(8,128)(2,1)S(1)}, u32[]{:S(2)}, u32[]{:S(2)}) collective-permute-start(bf16[32,32,128]{2,1,0:T(8,128)(2,1)S(1)} %collective-permute-done.refs_1_), channel_id=1, source_target_pairs={{0,2},{2,4},{4,6},{6,8},{8,10},{10,12},{12,14},{14,0},{1,3},{3,5},... | collective-permute-start | bytes 786440 | tf_op jit(solution)/shard_map/ppermute | solution.py:353
  39.7 7.9 %collective-permute-start.4 = (bf16[32,32,128]{2,1,0:T(8,128)(2,1)S(1)}, bf16[32,32,128]{2,1,0:T(8,128)(2,1)S(1)}, u32[]{:S(2)}, u32[]{:S(2)}) collective-permute-start(bf16[32,32,128]{2,1,0:T(8,128)(2,1)S(1)} %collective-permute-done.3.refs_2_), channel_id=1, source_target_pairs={{0,14},{2,0},{4,2},{6,4},{8,6},{10,8},{12,10},{14,12},{1,15},{3,1}... | collective-permute-start | bytes 786440 | tf_op jit(solution)/shard_map/ppermute | solution.py:353
  48.3 32.2 %collective-permute-start.9 = (bf16[5,32,32,128]{3,2,1,0:T(8,128)(2,1)}, bf16[5,32,32,128]{3,2,1,0:T(8,128)(2,1)S(1)}, u32[]{:S(2)}, u32[]{:S(2)}) collective-permute-start(bf16[5,32,32,128]{3,2,1,0:T(8,128)(2,1)} %bitcast_dynamic-update-slice_fusion), channel_id=1, source_target_pairs={{0,1},{1,0},{2,3},{3,2},{4,5},{5,4},{6,7},{7,6},{8,9},{9,8},{10,11... | collective-permute-start | bytes 3932168 | tf_op jit(solution)/shard_map/ppermute | solution.py:362
  54.4 12.0 %collective-permute-start.2 = (bf16[32,32,128]{2,1,0:T(8,128)(2,1)S(1)}, bf16[32,32,128]{2,1,0:T(8,128)(2,1)S(1)}, u32[]{:S(2)}, u32[]{:S(2)}) collective-permute-start(bf16[32,32,128]{2,1,0:T(8,128)(2,1)S(1)} %collective-permute-done.1.refs_3_), channel_id=1, source_target_pairs={{0,2},{2,4},{4,6},{6,8},{8,10},{10,12},{12,14},{14,0},{1,3},{3,5},... | collective-permute-start | bytes 786440 | tf_op jit(solution)/shard_map/ppermute | solution.py:353
  56.8 11.6 %collective-permute-start.5 = (bf16[32,32,128]{2,1,0:T(8,128)(2,1)S(1)}, bf16[32,32,128]{2,1,0:T(8,128)(2,1)S(1)}, u32[]{:S(2)}, u32[]{:S(2)}) collective-permute-start(bf16[32,32,128]{2,1,0:T(8,128)(2,1)S(1)} %collective-permute-done.4.refs_4_), channel_id=1, source_target_pairs={{0,14},{2,0},{4,2},{6,4},{8,6},{10,8},{12,10},{14,12},{1,15},{3,1}... | collective-permute-start | bytes 786440 | tf_op jit(solution)/shard_map/ppermute | solution.py:353
  69.2 17.4 %collective-permute-start.7 = (bf16[2,32,32,128]{3,2,1,0:T(8,128)(2,1)}, bf16[2,32,32,128]{3,2,1,0:T(8,128)(2,1)S(1)}, u32[]{:S(2)}, u32[]{:S(2)}) collective-permute-start(bf16[2,32,32,128]{3,2,1,0:T(8,128)(2,1)} %pad_maximum_fusion), channel_id=1, source_target_pairs={{0,1},{1,0},{2,3},{3,2},{4,5},{5,4},{6,7},{7,6},{8,9},{9,8},{10,11... | collective-permute-start | bytes 1572872 | tf_op jit(solution)/shard_map/ppermute | solution.py:362
  72.0 13.0 %collective-permute-start.8 = (bf16[32,32,128]{2,1,0:T(8,128)(2,1)S(1)}, bf16[32,32,128]{2,1,0:T(8,128)(2,1)S(1)}, u32[]{:S(2)}, u32[]{:S(2)}) collective-permute-start(bf16[32,32,128]{2,1,0:T(8,128)(2,1)S(1)} %collective-permute-done.5.refs_1_), channel_id=1, source_target_pairs={{0,15},{1,14},{2,1},{3,0},{4,3},{5,2},{6,5},{7,4},{8,7},{9,6},{10,... | collective-permute-start | bytes 786440 | tf_op jit(solution)/shard_map/ppermute | solution.py:380
  76.1 10.5 %collective-permute-start.6 = (bf16[32,32,128]{2,1,0:T(8,128)(2,1)S(1)}, bf16[32,32,128]{2,1,0:T(8,128)(2,1)S(1)}, u32[]{:S(2)}, u32[]{:S(2)}) collective-permute-start(bf16[32,32,128]{2,1,0:T(8,128)(2,1)S(1)} %collective-permute-done.2.refs_0_), channel_id=1, source_target_pairs={{0,2},{2,4},{4,6},{6,8},{8,10},{10,12},{12,14},{14,0},{1,3},{3,5},... | collective-permute-start | bytes 786440 | tf_op jit(solution)/shard_map/ppermute | solution.py:353
  89.8 5.5 %collective-permute-start.10 = (bf16[8,512,128]{2,1,0:T(8,128)(2,1)S(1)}, bf16[8,512,128]{2,1,0:T(8,128)(2,1)S(1)}, u32[]{:S(2)}, u32[]{:S(2)}) collective-permute-start(bf16[8,512,128]{2,1,0:T(8,128)(2,1)S(1)} %get-tuple-element.39), channel_id=1, source_target_pairs={{0,1},{1,0},{2,3},{3,2},{4,5},{5,4},{6,7},{7,6},{8,9},{9,8},{10,11... | collective-permute-start | bytes 3145736 | tf_op jit(solution)/shard_map/ppermute | solution.py:362
  96.6 53.2 %copy-start.13 = (bf16[64,128]{1,0:T(8,128)(2,1)S(1)}, bf16[64,128]{1,0:T(8,128)(2,1)}, u32[]{:S(2)}) copy-start(bf16[64,128]{1,0:T(8,128)(2,1)} %param.27) | copy-start | bytes 49156
  96.6 35.8 %all-to-all-start.1 = ((bf16[8,512,128]{2,1,0:T(8,128)(2,1)}), bf16[8,512,128]{2,1,0:T(8,128)(2,1)S(1)}, u32[]{:S(2)}, u32[]{:S(2)}) async-start(bf16[8,512,128]{2,1,0:T(8,128)(2,1)} %add_convert_fusion), calls=%async_computation.1 | async-start | bytes 2097152 | tf_op jit(solution)/shard_map/all_to_all | solution.py:386
  103.2 6.6 %collective-permute-start.11 = (f32[4,32]{1,0:T(4,128)S(1)}, f32[4,32]{1,0:T(4,128)S(1)}, u32[]{:S(2)}, u32[]{:S(2)}) collective-permute-start(f32[4,32]{1,0:T(4,128)S(1)} %pad_maximum_fusion.3), channel_id=1, source_target_pairs={{16,0},{32,16},{48,32},{64,48},{80,64},{96,80},{112,96},{128,112},... | collective-permute-start | bytes 1544 | tf_op jit(solution)/shard_map/ppermute | solution.py:358
  104.6 50.8 %copy-start.4 = (bf16[32,16,2048]{2,1,0:T(8,128)(2,1)S(1)}, bf16[32,16,2048]{2,1,0:T(8,128)(2,1)}, u32[]{:S(2)}) copy-start(bf16[32,16,2048]{2,1,0:T(8,128)(2,1)} %get-tuple-element.36) | copy-start | bytes 6291460
  104.6 50.8 %copy-start.11 = (bf16[512,224]{1,0:T(8,128)(2,1)S(1)}, bf16[512,224]{1,0:T(8,128)(2,1)}, u32[]{:S(2)}) copy-start(bf16[512,224]{1,0:T(8,128)(2,1)} %get-tuple-element.35) | copy-start | bytes 688132
  105.2 34.1 %collective-permute-start.12 = (bf16[2,32,128]{2,1,0:T(8,128)(2,1)}, bf16[2,32,128]{2,1,0:T(8,128)(2,1)S(1)}, u32[]{:S(2)}, u32[]{:S(2)}) collective-permute-start(bf16[2,32,128]{2,1,0:T(8,128)(2,1)} %pad_maximum_fusion.2), channel_id=1, source_target_pairs={{16,0},{32,16},{48,32},{64,48},{80,64},{96,80},{112,96},{128,112},... | collective-permute-start | bytes 49160 | tf_op jit(solution)/shard_map/ppermute | solution.py:358
  133.3 16.6 %all-to-all-start.2 = ((bf16[32,32,128]{2,1,0:T(8,128)(2,1)}), bf16[32,32,128]{2,1,0:T(8,128)(2,1)S(1)}, u32[]{:S(2)}, u32[]{:S(2)}) async-start(bf16[32,32,128]{2,1,0:T(8,128)(2,1)} %summed.1), calls=%async_computation.2 | async-start | bytes 524288 | tf_op jit(solution)/shard_map/all_to_all | solution.py:443
  150.7 29.3 %all-to-all-start.4 = ((bf16[32,64,128]{2,1,0:T(8,128)(2,1)}), bf16[32,64,128]{2,1,0:T(8,128)(2,1)}, u32[]{:S(2)}, u32[]{:S(2)}) async-start(bf16[32,64,128]{2,1,0:T(8,128)(2,1)} %broadcast_in_dim.11), calls=%async_computation.4 | async-start | bytes 1048576 | tf_op jit(solution)/shard_map/all_to_all | solution.py:397
  180.1 27.6 %copy-start.22 = (f32[128]{0:T(128)S(1)}, f32[128]{0:T(128)}, u32[]{:S(2)}) copy-start(f32[128]{0:T(128)} %get-tuple-element.48) | copy-start | bytes 1540
  180.1 27.6 %copy-start.23 = (f32[128]{0:T(128)S(1)}, f32[128]{0:T(128)}, u32[]{:S(2)}) copy-start(f32[128]{0:T(128)} %get-tuple-element.49) | copy-start | bytes 1540
  180.1 27.6 %copy-start.24 = (f32[128]{0:T(128)S(1)}, f32[128]{0:T(128)}, u32[]{:S(2)}) copy-start(f32[128]{0:T(128)} %get-tuple-element.50) | copy-start | bytes 1540
  180.1 27.6 %copy-start.25 = (f32[128]{0:T(128)S(1)}, f32[128]{0:T(128)}, u32[]{:S(2)}) copy-start(f32[128]{0:T(128)} %get-tuple-element.51) | copy-start | bytes 1540
  180.1 27.6 %copy-start.26 = (f32[128]{0:T(128)S(1)}, f32[128]{0:T(128)}, u32[]{:S(2)}) copy-start(f32[128]{0:T(128)} %get-tuple-element.52) | copy-start | bytes 1540
  180.1 27.6 %copy-start.27 = (f32[128]{0:T(128)S(1)}, f32[128]{0:T(128)}, u32[]{:S(2)}) copy-start(f32[128]{0:T(128)} %get-tuple-element.53) | copy-start | bytes 1540
  180.1 27.6 %copy-start.28 = (f32[128]{0:T(128)S(1)}, f32[128]{0:T(128)}, u32[]{:S(2)}) copy-start(f32[128]{0:T(128)} %get-tuple-element.54) | copy-start | bytes 1540
  180.2 27.6 %copy-start.29 = (f32[128]{0:T(128)S(1)}, f32[128]{0:T(128)}, u32[]{:S(2)}) copy-start(f32[128]{0:T(128)} %get-tuple-element.55) | copy-start | bytes 1540
  180.2 27.6 %copy-start.30 = (f32[128]{0:T(128)S(1)}, f32[128]{0:T(128)}, u32[]{:S(2)}) copy-start(f32[128]{0:T(128)} %get-tuple-element.56) | copy-start | bytes 1540
  180.2 27.6 %copy-start.31 = (f32[128]{0:T(128)S(1)}, f32[128]{0:T(128)}, u32[]{:S(2)}) copy-start(f32[128]{0:T(128)} %get-tuple-element.57) | copy-start | bytes 1540
  180.2 27.6 %copy-start.32 = (f32[128]{0:T(128)S(1)}, f32[128]{0:T(128)}, u32[]{:S(2)}) copy-start(f32[128]{0:T(128)} %get-tuple-element.58) | copy-start | bytes 1540
  180.2 27.6 %copy-start.33 = (f32[128]{0:T(128)S(1)}, f32[128]{0:T(128)}, u32[]{:S(2)}) copy-start(f32[128]{0:T(128)} %get-tuple-element.59) | copy-start | bytes 1540
  180.2 27.6 %copy-start.34 = (f32[128]{0:T(128)S(1)}, f32[128]{0:T(128)}, u32[]{:S(2)}) copy-start(f32[128]{0:T(128)} %get-tuple-element.60) | copy-start | bytes 1540
  180.2 27.6 %copy-start.35 = (f32[128]{0:T(128)S(1)}, f32[128]{0:T(128)}, u32[]{:S(2)}) copy-start(f32[128]{0:T(128)} %get-tuple-element.61) | copy-start | bytes 1540
  180.2 27.6 %copy-start.36 = (f32[128]{0:T(128)S(1)}, f32[128]{0:T(128)}, u32[]{:S(2)}) copy-start(f32[128]{0:T(128)} %get-tuple-element.62) | copy-start | bytes 1540
  180.2 27.6 %copy-start.37 = (f32[128]{0:T(128)S(1)}, f32[128]{0:T(128)}, u32[]{:S(2)}) copy-start(f32[128]{0:T(128)} %get-tuple-element.63) | copy-start | bytes 1540
  180.2 27.6 %copy-start.38 = (f32[128]{0:T(128)S(1)}, f32[128]{0:T(128)}, u32[]{:S(2)}) copy-start(f32[128]{0:T(128)} %get-tuple-element.64) | copy-start | bytes 1540
  180.3 27.6 %copy-start.39 = (f32[128]{0:T(128)S(1)}, f32[128]{0:T(128)}, u32[]{:S(2)}) copy-start(f32[128]{0:T(128)} %get-tuple-element.65) | copy-start | bytes 1540
  180.3 27.6 %copy-start.40 = (f32[128]{0:T(128)S(1)}, f32[128]{0:T(128)}, u32[]{:S(2)}) copy-start(f32[128]{0:T(128)} %get-tuple-element.66) | copy-start | bytes 1540
  180.3 27.6 %copy-start.41 = (f32[128]{0:T(128)S(1)}, f32[128]{0:T(128)}, u32[]{:S(2)}) copy-start(f32[128]{0:T(128)} %get-tuple-element.67) | copy-start | bytes 1540
  180.3 27.6 %copy-start.42 = (f32[128]{0:T(128)S(1)}, f32[128]{0:T(128)}, u32[]{:S(2)}) copy-start(f32[128]{0:T(128)} %get-tuple-element.68) | copy-start | bytes 1540
  180.3 27.6 %copy-start.43 = (f32[128]{0:T(128)S(1)}, f32[128]{0:T(128)}, u32[]{:S(2)}) copy-start(f32[128]{0:T(128)} %get-tuple-element.69) | copy-start | bytes 1540
  180.3 27.6 %copy-start.44 = (f32[128]{0:T(128)S(1)}, f32[128]{0:T(128)}, u32[]{:S(2)}) copy-start(f32[128]{0:T(128)} %get-tuple-element.70) | copy-start | bytes 1540
  180.3 27.6 %copy-start.45 = (f32[128]{0:T(128)S(1)}, f32[128]{0:T(128)}, u32[]{:S(2)}) copy-start(f32[128]{0:T(128)} %get-tuple-element.71) | copy-start | bytes 1540
  180.3 27.6 %copy-start.46 = (f32[128]{0:T(128)S(1)}, f32[128]{0:T(128)}, u32[]{:S(2)}) copy-start(f32[128]{0:T(128)} %get-tuple-element.72) | copy-start | bytes 1540
  180.3 27.6 %copy-start.47 = (f32[128]{0:T(128)S(1)}, f32[128]{0:T(128)}, u32[]{:S(2)}) copy-start(f32[128]{0:T(128)} %get-tuple-element.73) | copy-start | bytes 1540
  180.4 28.6 %all-to-all-start.3 = ((bf16[32,64,128]{2,1,0:T(8,128)(2,1)}), bf16[32,64,128]{2,1,0:T(8,128)(2,1)S(1)}, u32[]{:S(2)}, u32[]{:S(2)}) async-start(bf16[32,64,128]{2,1,0:T(8,128)(2,1)} %bitcast.22), calls=%async_computation.3 | async-start | bytes 1048576 | tf_op jit(solution)/shard_map/all_to_all | solution.py:452
  (21 other events, 318.0 us)

commit v9 on v7

--- a/solution.py
+++ b/solution.py
@@ -98,7 +98,8 @@
 def summed_body(arrived, out):
     experts, both, width = out.shape
     total = functools.reduce(jnp.add, [part[...].astype(F32) for part in [arrived.at[k] for k in range(arrived.shape[0])]])
-    total = total.astype(BF16).reshape(experts, both // 2, width)
+    spread = used_slots(experts, both // 2, 1)
+    total = dot(spread, total.astype(BF16), 1, 0).astype(BF16).reshape(experts, both // 2, width)
     out[:, : both // 2, :] = total
     out[: experts - 1, both // 2 :, :] = total[1:]
     out[experts - 1 :, both // 2 :, :] = total[:1]
@@ -110,7 +111,7 @@
         summed_body,
         in_specs=whole(1),
         out_specs=whole(1)[0],
-        out_shape=pltpu.VMEM((experts, 2 * count // experts, width), BF16),
+        out_shape=pltpu.VMEM((experts, 2 * (count // experts + 1), width), BF16),
         compiler_params=pltpu.CompilerParams(vmem_limit_bytes=12 * 1024 * 1024),
         name="summed",
     )(arrived)
@@ -197,9 +198,15 @@
         found.append(pl.ds(pl.multiple_of(chip * 2 * width, 2 * width), 2 * width))
     for copy in copies:
         copy.start()
-    for copy in copies:
+    for copy in copies[:3]:
         copy.wait()
-    for out, value in zip(sums, products(rows, routed, held, found)):
+    totals = [None] * 3
+    for n in range(count):
+        for copy in copies[3 + 4 * n : 7 + 4 * n]:
+            copy.wait()
+        parts = products(rows, routed, held, found[n : n + 1])
+        totals = [p if t is None else t + p for t, p in zip(totals, parts)]
+    for out, value in zip(sums, totals):
         out[...] = value
 
 
@@ -227,6 +234,16 @@
         compiler_params=pltpu.CompilerParams(vmem_limit_bytes=12 * 1024 * 1024),
         name="first_products",
     )(me, *far(*mine, *shared, *weights))
+
+
+def used_slots(experts, slots, row_dim):
+    shape = [experts * slots] * 2
+    shape[row_dim] = experts * (slots - 1)
+    row = lax.broadcasted_iota(jnp.int32, shape, row_dim)
+    place = lax.broadcasted_iota(jnp.int32, shape, 1 - row_dim)
+    expert = place // slots
+    used = (place - expert == row) & (place - expert * slots < slots - 1)
+    return used.astype(F32).astype(BF16)
 
 
 def partial_rows(out, gate_grad, up_grad, gate_weight, up_weight, core):
@@ -293,9 +310,12 @@
     up_held[...] = up_grad
     sends[2].start()
     sends[3].start()
-    partial_rows(given, gate_grad, up_grad, gate_weight, up_weight, 1 - my_core)
-    gate_out[...] = gate_grad
-    up_out[...] = up_grad
+    used = used_slots(rows.shape[0], slots, 0)
+    gate_rows = dot(used, gate_grad, 1, 0).astype(BF16)
+    up_rows = dot(used, up_grad, 1, 0).astype(BF16)
+    partial_rows(given, gate_rows, up_rows, gate_weight, up_weight, 1 - my_core)
+    gate_out[...] = gate_rows
+    up_out[...] = up_rows
     for send in sends:
         send.wait()
 
@@ -311,8 +331,8 @@
         out_specs=whole(5) + whole(4, pl.ANY),
         out_shape=(
             *[pltpu.VMEM((experts, slots, channels), BF16)] * 2,
-            pltpu.VMEM((blocks // 2, count, channels // blocks), BF16),
-            *[pltpu.VMEM((count, hidden), BF16)] * 2,
+            pltpu.VMEM((blocks // 2, count - experts, channels // blocks), BF16),
+            *[pltpu.VMEM((count - experts, hidden), BF16)] * 2,
             *[pltpu.HBM((experts, slots, channels), BF16)] * 2,
             *[pltpu.HBM((count, hidden), BF16)] * 2,
         ),

time: 202 us -> 202 us (level)
  no operation moved by 1% of the time
where the time goes in v9:
time: 202 us; the launch traced here: 201 us
  starting transfers between devices  67.9 us (34%)
  blocking collectives  59.7 us (30%)
  waiting for transfers between devices  44.5 us (22%)
  Pallas kernels  13.4 us (7%)
  matrix products  6.75 us (3%)
  other arithmetic  5.14 us (3%)
  local copies, waits for them, and re-layouts  2.32 us (1%)
    all_to_all x1, blocking collectives, steps(): own = lax.all_to_all(sent, 'sp', split_axis=0, concat_axis=0, tiled=True)  25 us
    all_to_all x1, waiting for transfers between devices, added_up(): lax.all_to_all(both.astype(BF16), 'chip', split_axis=0, concat_axis=0, ti...  23 us
    ppermute x7, starting transfers between devices, along_chips(): lax.ppermute(value, 'chip', [(y, (y + steps) % count) for y in range(coun...  22.2 us
    all_gather x1, blocking collectives, steps(): columns = lax.all_gather(stream, TP, axis=1, tiled=True)  18.7 us
    all_gather x1, blocking collectives, steps(): sums = lax.all_gather(sums, TP, axis=0, tiled=False)  16.1 us
    ppermute x4, starting transfers between devices, to_other_core(): return lax.ppermute(value, 'core', [(0, 1), (1, 0)])  14.2 us
    all_to_all x1, waiting for transfers between devices, steps(): lax.all_to_all(shared, 'sp', split_axis=0, concat_axis=0, tiled=True)  11.2 us
    all_to_all x1, starting transfers between devices, steps(): lax.all_to_all(proj_part, 'sp', split_axis=0, concat_axis=0, tiled=True)  9.51 us
  transfers between devices with their start and end apart: 18, of which 8 were waited for; matrix products, arithmetic and copies ran while one was open for 6% of the time, Pallas kernels for 3%

profile of v9, /device:TPU:1, one launch (start us, length us, event | category | flops | bytes accessed | tf_op | source)
XLA Modules:
  0.0 201.0 jit_solution(16407329697598477299)
XLA Ops:
  0.6 2.1 %send_rows.1 = (bf16[32,32,128]{2,1,0:T(8,128)(2,1)}, bf16[512,192]{1,0:T(8,128)(2,1)}) custom-call(s32[2,192]{1,0:T(2,128)} %bitcast.122, f32[2,192]{1,0:T(2,128)} %bitcast.125, bf16[192,128]{1,0:T(8,128)(2,1)} %rows.1, bf16[192,128]{1,0:T(8,128)(2,1)} %cotangent.3), custom_call_target="tpu_custom_call" | custom-call | tf_op jit(solution)/shard_map/send_rows/pallas_call | solution.py:70
  2.7 25.0 %all_to_all.25.refs_0_ = bf16[32,32,128]{2,1,0:T(8,128)(2,1)S(1)} all-to-all(bf16[32,32,128]{2,1,0:T(8,128)(2,1)} %get-tuple-element.24), channel_id=1, replica_groups=mesh['sp'=32,'chip'=8,'core'=2] {'sp'}, dimensions={0} | all-to-all | bytes 524288 | tf_op jit(solution)/shard_map/all_to_all | solution.py:424
  27.7 3.2 %collective-permute-start = (bf16[32,32,128]{2,1,0:T(8,128)(2,1)S(1)}, bf16[32,32,128]{2,1,0:T(8,128)(2,1)S(1)}, u32[]{:S(2)}, u32[]{:S(2)}) collective-permute-start(bf16[32,32,128]{2,1,0:T(8,128)(2,1)S(1)} %all_to_all.25.refs_0_), channel_id=1, source_target_pairs={{0,2},{2,4},{4,6},{6,8},{8,10},{10,12},{12,14},{14,0},{1,3},{3,5},... | collective-permute-start | bytes 786440 | tf_op jit(solution)/shard_map/ppermute | solution.py:353
  30.9 3.8 %collective-permute-start.3 = (bf16[32,32,128]{2,1,0:T(8,128)(2,1)S(1)}, bf16[32,32,128]{2,1,0:T(8,128)(2,1)S(1)}, u32[]{:S(2)}, u32[]{:S(2)}) collective-permute-start(bf16[32,32,128]{2,1,0:T(8,128)(2,1)S(1)} %all_to_all.25.refs_0_), channel_id=1, source_target_pairs={{0,14},{2,0},{4,2},{6,4},{8,6},{10,8},{12,10},{14,12},{1,15},{3,1}... | collective-permute-start | bytes 786440 | tf_op jit(solution)/shard_map/ppermute | solution.py:353
  34.8 2.3 %collective-permute-done.refs_1_ = bf16[32,32,128]{2,1,0:T(8,128)(2,1)S(1)} collective-permute-done((bf16[32,32,128]{2,1,0:T(8,128)(2,1)S(1)}, bf16[32,32,128]{2,1,0:T(8,128)(2,1)S(1)}, u32[]{:S(2)}, u32[]{:S(2)}) %collective-permute-start) | collective-permute-done | bytes 262176 | tf_op jit(solution)/shard_map/ppermute | solution.py:353
  37.1 1.9 collective-permute-start.1
  39.0 4.6 %collective-permute-start.4 = (bf16[32,32,128]{2,1,0:T(8,128)(2,1)S(1)}, bf16[32,32,128]{2,1,0:T(8,128)(2,1)S(1)}, u32[]{:S(2)}, u32[]{:S(2)}) collective-permute-start(bf16[32,32,128]{2,1,0:T(8,128)(2,1)S(1)} %collective-permute-done.3.refs_2_), channel_id=1, source_target_pairs={{0,14},{2,0},{4,2},{6,4},{8,6},{10,8},{12,10},{14,12},{1,15},{3,1}... | collective-permute-start | bytes 786440 | tf_op jit(solution)/shard_map/ppermute | solution.py:353
  43.6 1.8 collective-permute-done.1.refs_3_
  45.4 1.9 collective-permute-start.2
  47.3 4.6 %collective-permute-start.5 = (bf16[32,32,128]{2,1,0:T(8,128)(2,1)S(1)}, bf16[32,32,128]{2,1,0:T(8,128)(2,1)S(1)}, u32[]{:S(2)}, u32[]{:S(2)}) collective-permute-start(bf16[32,32,128]{2,1,0:T(8,128)(2,1)S(1)} %collective-permute-done.4.refs_4_), channel_id=1, source_target_pairs={{0,14},{2,0},{4,2},{6,4},{8,6},{10,8},{12,10},{14,12},{1,15},{3,1}... | collective-permute-start | bytes 786440 | tf_op jit(solution)/shard_map/ppermute | solution.py:353
  51.9 1.0 pad_maximum_fusion
  52.9 6.6 %collective-permute-start.9 = (bf16[3,32,32,128]{3,2,1,0:T(8,128)(2,1)}, bf16[3,32,32,128]{3,2,1,0:T(8,128)(2,1)}, u32[]{:S(2)}, u32[]{:S(2)}) collective-permute-start(bf16[3,32,32,128]{3,2,1,0:T(8,128)(2,1)} %pad_maximum_fusion), channel_id=1, source_target_pairs={{0,1},{1,0},{2,3},{3,2},{4,5},{5,4},{6,7},{7,6},{8,9},{9,8},{10,11... | collective-permute-start | bytes 2359304 | tf_op jit(solution)/shard_map/ppermute | solution.py:362
  59.5 0.8 pad_maximum_fusion.2
  60.3 1.9 collective-permute-start.10
  62.3 2.4 %collective-permute-start.7 = (bf16[2,32,32,128]{3,2,1,0:T(8,128)(2,1)S(1)}, bf16[2,32,32,128]{3,2,1,0:T(8,128)(2,1)S(1)}, u32[]{:S(2)}, u32[]{:S(2)}) collective-permute-start(bf16[2,32,32,128]{3,2,1,0:T(8,128)(2,1)S(1)} %pad_maximum_fusion.1), channel_id=1, source_target_pairs={{0,1},{1,0},{2,3},{3,2},{4,5},{5,4},{6,7},{7,6},{8,9},{9,8},{10,11... | collective-permute-start | bytes 1572872 | tf_op jit(solution)/shard_map/ppermute | solution.py:362
  64.8 2.9 %collective-permute-start.8 = (bf16[32,32,128]{2,1,0:T(8,128)(2,1)S(1)}, bf16[32,32,128]{2,1,0:T(8,128)(2,1)S(1)}, u32[]{:S(2)}, u32[]{:S(2)}) collective-permute-start(bf16[32,32,128]{2,1,0:T(8,128)(2,1)S(1)} %collective-permute-done.5.refs_1_), channel_id=1, source_target_pairs={{0,15},{1,14},{2,1},{3,0},{4,3},{5,2},{6,5},{7,4},{8,7},{9,6},{10,... | collective-permute-start | bytes 786440 | tf_op jit(solution)/shard_map/ppermute | solution.py:380
  67.7 2.3 %collective-permute-start.6 = (bf16[32,32,128]{2,1,0:T(8,128)(2,1)S(1)}, bf16[32,32,128]{2,1,0:T(8,128)(2,1)S(1)}, u32[]{:S(2)}, u32[]{:S(2)}) collective-permute-start(bf16[32,32,128]{2,1,0:T(8,128)(2,1)S(1)} %collective-permute-done.2.refs_0_), channel_id=1, source_target_pairs={{0,2},{2,4},{4,6},{6,8},{8,10},{10,12},{12,14},{14,0},{1,3},{3,5},... | collective-permute-start | bytes 786440 | tf_op jit(solution)/shard_map/ppermute | solution.py:353
  70.0 4.0 %first_products.1 = (bf16[32,16,2048]{2,1,0:T(8,128)(2,1)S(1)}, bf16[32,16,2048]{2,1,0:T(8,128)(2,1)S(1)}, f32[512,224]{1,0:T(8,128)S(1)}, f32[512,224]{1,0:T(8,...) custom-call(s32[1]{0:T(128)} %bitcast.me, ...), custom_call_target="tpu_custom_call" | custom-call | flops 939524096 | bytes 12582912 | tf_op jit(solution)/shard_map/first_products/pallas_call | solution.py:217
  74.1 0.8 collective-permute-done.8
  74.9 3.3 %collective-permute-done.6.refs_2_ = bf16[32,32,128]{2,1,0:T(8,128)(2,1)S(1)} collective-permute-done((bf16[32,32,128]{2,1,0:T(8,128)(2,1)S(1)}, bf16[32,32,128]{2,1,0:T(8,128)(2,1)S(1)}, u32[]{:S(2)}, u32[]{:S(2)}) %collective-permute-start.6) | collective-permute-done | bytes 262176 | tf_op jit(solution)/shard_map/ppermute | solution.py:353
  78.2 4.2 %rest_products.1 = (bf16[32,16,2048]{2,1,0:T(8,128)(2,1)S(1)}, bf16[32,16,2048]{2,1,0:T(8,128)(2,1)S(1)}, bf16[8,480,128]{2,1,0:T(8,128)(2,1)S(1)}, bf16[480,224...) custom-call(s32[1]{0:T(128)} %bitcast.me, ...), custom_call_target="tpu_custom_call", output_to_operand_aliasing={{0}: (6, {}), {1}: (7, {})} | custom-call | flops 1409286144 | bytes 12582912 | tf_op jit(solution)/shard_map/rest_products/pallas_call | solution.py:328
  82.4 3.3 %collective-permute-start.11 = (bf16[8,480,128]{2,1,0:T(8,128)(2,1)S(1)}, bf16[8,480,128]{2,1,0:T(8,128)(2,1)S(1)}, u32[]{:S(2)}, u32[]{:S(2)}) collective-permute-start(bf16[8,480,128]{2,1,0:T(8,128)(2,1)S(1)} %get-tuple-element.39), channel_id=1, source_target_pairs={{0,1},{1,0},{2,3},{3,2},{4,5},{5,4},{6,7},{7,6},{8,9},{9,8},{10,11... | collective-permute-start | bytes 2949128 | tf_op jit(solution)/shard_map/ppermute | solution.py:362
  85.7 0.8 kept_products.1
  86.5 1.3 collective-permute-done.11
  87.8 1.2 add_convert_fusion
  89.1 6.5 %all-to-all-start.1 = ((bf16[8,480,128]{2,1,0:T(8,128)(2,1)}), bf16[8,480,128]{2,1,0:T(8,128)(2,1)S(1)}, u32[]{:S(2)}, u32[]{:S(2)}) async-start(bf16[8,480,128]{2,1,0:T(8,128)(2,1)} %add_convert_fusion), calls=%async_computation.1 | async-start | bytes 1966080 | tf_op jit(solution)/shard_map/all_to_all | solution.py:386
  95.7 1.3 collective-permute-start.12
  97.0 1.3 collective-permute-start.13
  98.3 0.6 slice_bitcast_fusion.36
  98.9 0.6 slice_bitcast_fusion.33
  99.6 0.7 collective-permute-done.12
  100.4 23.0 %all-to-all-done.1.arrived = bf16[8,480,128]{2,1,0:T(8,128)(2,1)S(1)} async-done(((bf16[8,480,128]{2,1,0:T(8,128)(2,1)}), bf16[8,480,128]{2,1,0:T(8,128)(2,1)S(1)}, u32[]{:S(2)}, u32[]{:S(2)}) %all-to-all-start.1) | async-done | bytes 983072 | tf_op jit(solution)/shard_map/all_to_all | solution.py:386
  123.4 1.1 summed.1
  124.5 5.3 %all-to-all-start.2 = ((bf16[32,32,128]{2,1,0:T(8,128)(2,1)}), bf16[32,32,128]{2,1,0:T(8,128)(2,1)S(1)}, u32[]{:S(2)}, u32[]{:S(2)}) async-start(bf16[32,32,128]{2,1,0:T(8,128)(2,1)} %summed.1), calls=%async_computation.2 | async-start | bytes 524288 | tf_op jit(solution)/shard_map/all_to_all | solution.py:440
  129.8 0.2 rim_places.1.rim_place
  130.1 11.2 %all-to-all-done.2.returned = bf16[32,32,128]{2,1,0:T(8,128)(2,1)S(1)} async-done(((bf16[32,32,128]{2,1,0:T(8,128)(2,1)}), bf16[32,32,128]{2,1,0:T(8,128)(2,1)S(1)}, u32[]{:S(2)}, u32[]{:S(2)}) %all-to-all-start.2) | async-done | bytes 262176 | tf_op jit(solution)/shard_map/all_to_all | solution.py:440
  141.3 0.9 broadcast_in_dim.11
  142.3 4.6 %all-to-all-start.4 = ((bf16[32,64,128]{2,1,0:T(8,128)(2,1)}), bf16[32,64,128]{2,1,0:T(8,128)(2,1)S(1)}, u32[]{:S(2)}, u32[]{:S(2)}) async-start(bf16[32,64,128]{2,1,0:T(8,128)(2,1)} %broadcast_in_dim.11), calls=%async_computation.4 | async-start | bytes 1048576 | tf_op jit(solution)/shard_map/all_to_all | solution.py:397
  146.9 3.3 %fusion.1 = bf16[1,224,2048]{2,1,0:T(8,128)(2,1)} fusion(bf16[512,224]{1,0:T(8,128)(2,1)} %get-tuple-element.35, bf16[512,2048]{1,0:T(8,128)(2,1)} %bitcast.116), kind=kOutput, calls=%fused_computation.3 | convolution fusion | flops 470220800 | bytes 3244032 | tf_op jit(solution)/shard_map/dot_general | solution.py:18
  150.2 1.6 fusion
  151.8 0.9 combined.1
  152.7 18.7 %all_gather.6 = bf16[224,2048]{1,0:T(8,128)(2,1)S(1)} all-gather(bf16[224,128]{1,0:T(8,128)(2,1)S(1)} %get-tuple-element.42), channel_id=1, replica_groups=mesh['sp'=32,'chip'=8,'core'=2] {'chip','core'}, dimensions={1}, use_global_device_ids=true | all-gather | bytes 974848 | tf_op jit(solution)/shard_map/all_gather | solution.py:444
  171.4 1.4 convolution_convert_fusion.2
  172.8 9.5 %all-to-all-start.3 = ((bf16[32,64,128]{2,1,0:T(8,128)(2,1)}), bf16[32,64,128]{2,1,0:T(8,128)(2,1)S(1)}, u32[]{:S(2)}, u32[]{:S(2)}) async-start(bf16[32,64,128]{2,1,0:T(8,128)(2,1)} %bitcast.22), calls=%async_computation.3 | async-start | bytes 1048576 | tf_op jit(solution)/shard_map/all_to_all | solution.py:449
  182.4 0.5 fusion.41
  182.9 16.1 %all-gather = f32[16,1,512]{2,1,0:T(1,128)S(1)} all-gather(f32[1,1,512]{2,1,0:T(1,128)S(1)} %reshape.80), channel_id=1, replica_groups=mesh['sp'=32,'chip'=8,'core'=2] {'chip','core'}, dimensions={0}, use_global_device_ids=true | all-gather | bytes 34816 | tf_op jit(solution)/shard_map/all_gather | solution.py:460
  199.4 0.9 fusion.5
  200.3 0.7 convert_reduce_fusion
  (92 shorter events, 0.7 us)
Async XLA Ops:
  27.7 42.2 %copy-start.2 = (bf16[32,32,128]{2,1,0:T(8,128)(2,1)}, bf16[32,32,128]{2,1,0:T(8,128)(2,1)S(1)}, u32[]{:S(2)}) copy-start(bf16[32,32,128]{2,1,0:T(8,128)(2,1)S(1)} %all_to_all.25.refs_0_) | copy-start | bytes 786436
  27.7 9.3 %collective-permute-start = (bf16[32,32,128]{2,1,0:T(8,128)(2,1)S(1)}, bf16[32,32,128]{2,1,0:T(8,128)(2,1)S(1)}, u32[]{:S(2)}, u32[]{:S(2)}) collective-permute-start(bf16[32,32,128]{2,1,0:T(8,128)(2,1)S(1)} %all_to_all.25.refs_0_), channel_id=1, source_target_pairs={{0,2},{2,4},{4,6},{6,8},{8,10},{10,12},{12,14},{14,0},{1,3},{3,5},... | collective-permute-start | bytes 786440 | tf_op jit(solution)/shard_map/ppermute | solution.py:353
  30.9 8.0 %collective-permute-start.3 = (bf16[32,32,128]{2,1,0:T(8,128)(2,1)S(1)}, bf16[32,32,128]{2,1,0:T(8,128)(2,1)S(1)}, u32[]{:S(2)}, u32[]{:S(2)}) collective-permute-start(bf16[32,32,128]{2,1,0:T(8,128)(2,1)S(1)} %all_to_all.25.refs_0_), channel_id=1, source_target_pairs={{0,14},{2,0},{4,2},{6,4},{8,6},{10,8},{12,10},{14,12},{1,15},{3,1}... | collective-permute-start | bytes 786440 | tf_op jit(solution)/shard_map/ppermute | solution.py:353
  37.1 32.9 %copy-start.4 = (bf16[32,32,128]{2,1,0:T(8,128)(2,1)}, bf16[32,32,128]{2,1,0:T(8,128)(2,1)S(1)}, u32[]{:S(2)}) copy-start(bf16[32,32,128]{2,1,0:T(8,128)(2,1)S(1)} %collective-permute-done.refs_1_) | copy-start | bytes 786436
  37.1 8.3 %collective-permute-start.1 = (bf16[32,32,128]{2,1,0:T(8,128)(2,1)S(1)}, bf16[32,32,128]{2,1,0:T(8,128)(2,1)S(1)}, u32[]{:S(2)}, u32[]{:S(2)}) collective-permute-start(bf16[32,32,128]{2,1,0:T(8,128)(2,1)S(1)} %collective-permute-done.refs_1_), channel_id=1, source_target_pairs={{0,2},{2,4},{4,6},{6,8},{8,10},{10,12},{12,14},{14,0},{1,3},{3,5},... | collective-permute-start | bytes 786440 | tf_op jit(solution)/shard_map/ppermute | solution.py:353
  39.0 31.0 %copy-start.5 = (bf16[32,32,128]{2,1,0:T(8,128)(2,1)}, bf16[32,32,128]{2,1,0:T(8,128)(2,1)S(1)}, u32[]{:S(2)}) copy-start(bf16[32,32,128]{2,1,0:T(8,128)(2,1)S(1)} %collective-permute-done.3.refs_2_) | copy-start | bytes 786436
  39.0 8.3 %collective-permute-start.4 = (bf16[32,32,128]{2,1,0:T(8,128)(2,1)S(1)}, bf16[32,32,128]{2,1,0:T(8,128)(2,1)S(1)}, u32[]{:S(2)}, u32[]{:S(2)}) collective-permute-start(bf16[32,32,128]{2,1,0:T(8,128)(2,1)S(1)} %collective-permute-done.3.refs_2_), channel_id=1, source_target_pairs={{0,14},{2,0},{4,2},{6,4},{8,6},{10,8},{12,10},{14,12},{1,15},{3,1}... | collective-permute-start | bytes 786440 | tf_op jit(solution)/shard_map/ppermute | solution.py:353
  45.4 24.6 %copy-start.6 = (bf16[32,32,128]{2,1,0:T(8,128)(2,1)}, bf16[32,32,128]{2,1,0:T(8,128)(2,1)S(1)}, u32[]{:S(2)}) copy-start(bf16[32,32,128]{2,1,0:T(8,128)(2,1)S(1)} %collective-permute-done.1.refs_3_) | copy-start | bytes 786436
  45.4 16.9 %collective-permute-start.2 = (bf16[32,32,128]{2,1,0:T(8,128)(2,1)S(1)}, bf16[32,32,128]{2,1,0:T(8,128)(2,1)S(1)}, u32[]{:S(2)}, u32[]{:S(2)}) collective-permute-start(bf16[32,32,128]{2,1,0:T(8,128)(2,1)S(1)} %collective-permute-done.1.refs_3_), channel_id=1, source_target_pairs={{0,2},{2,4},{4,6},{6,8},{8,10},{10,12},{12,14},{14,0},{1,3},{3,5},... | collective-permute-start | bytes 786440 | tf_op jit(solution)/shard_map/ppermute | solution.py:353
  47.3 22.7 %copy-start.7 = (bf16[32,32,128]{2,1,0:T(8,128)(2,1)}, bf16[32,32,128]{2,1,0:T(8,128)(2,1)S(1)}, u32[]{:S(2)}) copy-start(bf16[32,32,128]{2,1,0:T(8,128)(2,1)S(1)} %collective-permute-done.4.refs_4_) | copy-start | bytes 786436
  47.3 15.0 %collective-permute-start.5 = (bf16[32,32,128]{2,1,0:T(8,128)(2,1)S(1)}, bf16[32,32,128]{2,1,0:T(8,128)(2,1)S(1)}, u32[]{:S(2)}, u32[]{:S(2)}) collective-permute-start(bf16[32,32,128]{2,1,0:T(8,128)(2,1)S(1)} %collective-permute-done.4.refs_4_), channel_id=1, source_target_pairs={{0,14},{2,0},{4,2},{6,4},{8,6},{10,8},{12,10},{14,12},{1,15},{3,1}... | collective-permute-start | bytes 786440 | tf_op jit(solution)/shard_map/ppermute | solution.py:353
  52.9 17.1 %collective-permute-start.9 = (bf16[3,32,32,128]{3,2,1,0:T(8,128)(2,1)}, bf16[3,32,32,128]{3,2,1,0:T(8,128)(2,1)}, u32[]{:S(2)}, u32[]{:S(2)}) collective-permute-start(bf16[3,32,32,128]{3,2,1,0:T(8,128)(2,1)} %pad_maximum_fusion), channel_id=1, source_target_pairs={{0,1},{1,0},{2,3},{3,2},{4,5},{5,4},{6,7},{7,6},{8,9},{9,8},{10,11... | collective-permute-start | bytes 2359304 | tf_op jit(solution)/shard_map/ppermute | solution.py:362
  60.3 9.6 %collective-permute-start.10 = (bf16[2,32,32,128]{3,2,1,0:T(8,128)(2,1)}, bf16[2,32,32,128]{3,2,1,0:T(8,128)(2,1)}, u32[]{:S(2)}, u32[]{:S(2)}) collective-permute-start(bf16[2,32,32,128]{3,2,1,0:T(8,128)(2,1)} %pad_maximum_fusion.2), channel_id=1, source_target_pairs={{0,1},{1,0},{2,3},{3,2},{4,5},{5,4},{6,7},{7,6},{8,9},{9,8},{10,11... | collective-permute-start | bytes 1572872 | tf_op jit(solution)/shard_map/ppermute | solution.py:362
  62.3 15.8 %collective-permute-start.7 = (bf16[2,32,32,128]{3,2,1,0:T(8,128)(2,1)S(1)}, bf16[2,32,32,128]{3,2,1,0:T(8,128)(2,1)S(1)}, u32[]{:S(2)}, u32[]{:S(2)}) collective-permute-start(bf16[2,32,32,128]{3,2,1,0:T(8,128)(2,1)S(1)} %pad_maximum_fusion.1), channel_id=1, source_target_pairs={{0,1},{1,0},{2,3},{3,2},{4,5},{5,4},{6,7},{7,6},{8,9},{9,8},{10,11... | collective-permute-start | bytes 1572872 | tf_op jit(solution)/shard_map/ppermute | solution.py:362
  64.8 10.1 %collective-permute-start.8 = (bf16[32,32,128]{2,1,0:T(8,128)(2,1)S(1)}, bf16[32,32,128]{2,1,0:T(8,128)(2,1)S(1)}, u32[]{:S(2)}, u32[]{:S(2)}) collective-permute-start(bf16[32,32,128]{2,1,0:T(8,128)(2,1)S(1)} %collective-permute-done.5.refs_1_), channel_id=1, source_target_pairs={{0,15},{1,14},{2,1},{3,0},{4,3},{5,2},{6,5},{7,4},{8,7},{9,6},{10,... | collective-permute-start | bytes 786440 | tf_op jit(solution)/shard_map/ppermute | solution.py:380
  67.7 10.5 %collective-permute-start.6 = (bf16[32,32,128]{2,1,0:T(8,128)(2,1)S(1)}, bf16[32,32,128]{2,1,0:T(8,128)(2,1)S(1)}, u32[]{:S(2)}, u32[]{:S(2)}) collective-permute-start(bf16[32,32,128]{2,1,0:T(8,128)(2,1)S(1)} %collective-permute-done.2.refs_0_), channel_id=1, source_target_pairs={{0,2},{2,4},{4,6},{6,8},{8,10},{10,12},{12,14},{14,0},{1,3},{3,5},... | collective-permute-start | bytes 786440 | tf_op jit(solution)/shard_map/ppermute | solution.py:353
  82.4 5.4 %collective-permute-start.11 = (bf16[8,480,128]{2,1,0:T(8,128)(2,1)S(1)}, bf16[8,480,128]{2,1,0:T(8,128)(2,1)S(1)}, u32[]{:S(2)}, u32[]{:S(2)}) collective-permute-start(bf16[8,480,128]{2,1,0:T(8,128)(2,1)S(1)} %get-tuple-element.39), channel_id=1, source_target_pairs={{0,1},{1,0},{2,3},{3,2},{4,5},{5,4},{6,7},{7,6},{8,9},{9,8},{10,11... | collective-permute-start | bytes 2949128 | tf_op jit(solution)/shard_map/ppermute | solution.py:362
  86.4 9.2 %copy-start.12 = (s32[192,2]{0,1:T(2,128)S(1)}, s32[192,2]{0,1:T(2,128)}, u32[]{:S(2)}) copy-start(s32[192,2]{0,1:T(2,128)} %param.16) | copy-start | bytes 4612
  86.5 9.2 %copy-start.13 = (f32[192]{0:T(256)S(1)}, f32[192]{0:T(256)}, u32[]{:S(2)}) copy-start(f32[192]{0:T(256)} %param.23) | copy-start | bytes 2308
  86.5 9.2 %copy-start.14 = (f32[192]{0:T(256)S(1)}, f32[192]{0:T(256)}, u32[]{:S(2)}) copy-start(f32[192]{0:T(256)} %param.22) | copy-start | bytes 2308
  86.5 10.5 %copy-start.1 = (bf16[192,128]{1,0:T(8,128)(2,1)S(1)}, bf16[192,128]{1,0:T(8,128)(2,1)}, u32[]{:S(2)}) copy-start(bf16[192,128]{1,0:T(8,128)(2,1)} %cotangent.3) | copy-start | bytes 147460
  86.5 10.5 %copy-start.9 = (bf16[192,128]{1,0:T(8,128)(2,1)S(1)}, bf16[192,128]{1,0:T(8,128)(2,1)}, u32[]{:S(2)}) copy-start(bf16[192,128]{1,0:T(8,128)(2,1)} %param.21) | copy-start | bytes 147460
  86.5 11.8 %copy-start.11 = (f32[31,128]{1,0:T(8,128)S(1)}, f32[31,128]{1,0:T(8,128)}, u32[]{:S(2)}) copy-start(f32[31,128]{1,0:T(8,128)} %param.26) | copy-start | bytes 47620
  89.1 52.3 %copy-start.10 = (bf16[64,128]{1,0:T(8,128)(2,1)S(1)}, bf16[64,128]{1,0:T(8,128)(2,1)}, u32[]{:S(2)}) copy-start(bf16[64,128]{1,0:T(8,128)(2,1)} %param.27) | copy-start | bytes 49156
  89.1 34.3 %all-to-all-start.1 = ((bf16[8,480,128]{2,1,0:T(8,128)(2,1)}), bf16[8,480,128]{2,1,0:T(8,128)(2,1)S(1)}, u32[]{:S(2)}, u32[]{:S(2)}) async-start(bf16[8,480,128]{2,1,0:T(8,128)(2,1)} %add_convert_fusion), calls=%async_computation.1 | async-start | bytes 1966080 | tf_op jit(solution)/shard_map/all_to_all | solution.py:386
  95.7 4.6 %collective-permute-start.12 = (f32[4,32]{1,0:T(4,128)S(1)}, f32[4,32]{1,0:T(4,128)S(1)}, u32[]{:S(2)}, u32[]{:S(2)}) collective-permute-start(f32[4,32]{1,0:T(4,128)S(1)} %pad_maximum_fusion.5), channel_id=1, source_target_pairs={{16,0},{32,16},{48,32},{64,48},{80,64},{96,80},{112,96},{128,112},... | collective-permute-start | bytes 1544 | tf_op jit(solution)/shard_map/ppermute | solution.py:358
  97.0 33.1 %collective-permute-start.13 = (bf16[2,32,128]{2,1,0:T(8,128)(2,1)S(1)}, bf16[2,32,128]{2,1,0:T(8,128)(2,1)S(1)}, u32[]{:S(2)}, u32[]{:S(2)}) collective-permute-start(bf16[2,32,128]{2,1,0:T(8,128)(2,1)S(1)} %pad_maximum_fusion.4), channel_id=1, source_target_pairs={{16,0},{32,16},{48,32},{64,48},{80,64},{96,80},{112,96},{128,112},... | collective-permute-start | bytes 49160 | tf_op jit(solution)/shard_map/ppermute | solution.py:358
  124.5 16.8 %all-to-all-start.2 = ((bf16[32,32,128]{2,1,0:T(8,128)(2,1)}), bf16[32,32,128]{2,1,0:T(8,128)(2,1)S(1)}, u32[]{:S(2)}, u32[]{:S(2)}) async-start(bf16[32,32,128]{2,1,0:T(8,128)(2,1)} %summed.1), calls=%async_computation.2 | async-start | bytes 524288 | tf_op jit(solution)/shard_map/all_to_all | solution.py:440
  142.3 7.9 %copy-start.8 = (bf16[512,224]{1,0:T(8,128)(2,1)S(1)}, bf16[512,224]{1,0:T(8,128)(2,1)}, u32[]{:S(2)}) copy-start(bf16[512,224]{1,0:T(8,128)(2,1)} %get-tuple-element.33) | copy-start | bytes 688132
  142.3 30.6 %all-to-all-start.4 = ((bf16[32,64,128]{2,1,0:T(8,128)(2,1)}), bf16[32,64,128]{2,1,0:T(8,128)(2,1)S(1)}, u32[]{:S(2)}, u32[]{:S(2)}) async-start(bf16[32,64,128]{2,1,0:T(8,128)(2,1)} %broadcast_in_dim.11), calls=%async_computation.4 | async-start | bytes 1048576 | tf_op jit(solution)/shard_map/all_to_all | solution.py:397
  150.2 21.2 %copy-start.28 = (f32[128]{0:T(128)S(1)}, f32[128]{0:T(128)}, u32[]{:S(2)}) copy-start(f32[128]{0:T(128)} %param.25) | copy-start | bytes 1540
  150.2 21.2 %copy-start.30 = (f32[128]{0:T(128)S(1)}, f32[128]{0:T(128)}, u32[]{:S(2)}) copy-start(f32[128]{0:T(128)} %param.24) | copy-start | bytes 1540
  152.7 29.7 %copy-start.29 = (f32[128]{0:T(128)S(1)}, f32[128]{0:T(128)}, u32[]{:S(2)}) copy-start(f32[128]{0:T(128)} %param.25) | copy-start | bytes 1540
  152.7 29.7 %copy-start.31 = (f32[128]{0:T(128)S(1)}, f32[128]{0:T(128)}, u32[]{:S(2)}) copy-start(f32[128]{0:T(128)} %param.24) | copy-start | bytes 1540
  172.7 26.5 %copy-start.15 = (f32[128]{0:T(128)S(1)}, f32[128]{0:T(128)}, u32[]{:S(2)}) copy-start(f32[128]{0:T(128)} %get-tuple-element.63) | copy-start | bytes 1540
  172.7 26.5 %copy-start.16 = (f32[128]{0:T(128)S(1)}, f32[128]{0:T(128)}, u32[]{:S(2)}) copy-start(f32[128]{0:T(128)} %get-tuple-element.64) | copy-start | bytes 1540
  172.7 26.5 %copy-start.17 = (f32[128]{0:T(128)S(1)}, f32[128]{0:T(128)}, u32[]{:S(2)}) copy-start(f32[128]{0:T(128)} %get-tuple-element.65) | copy-start | bytes 1540
  172.7 26.5 %copy-start.18 = (f32[128]{0:T(128)S(1)}, f32[128]{0:T(128)}, u32[]{:S(2)}) copy-start(f32[128]{0:T(128)} %get-tuple-element.66) | copy-start | bytes 1540
  172.7 26.5 %copy-start.19 = (f32[128]{0:T(128)S(1)}, f32[128]{0:T(128)}, u32[]{:S(2)}) copy-start(f32[128]{0:T(128)} %get-tuple-element.67) | copy-start | bytes 1540
  172.8 26.5 %copy-start.20 = (f32[128]{0:T(128)S(1)}, f32[128]{0:T(128)}, u32[]{:S(2)}) copy-start(f32[128]{0:T(128)} %get-tuple-element.68) | copy-start | bytes 1540
  172.8 26.5 %copy-start.21 = (f32[128]{0:T(128)S(1)}, f32[128]{0:T(128)}, u32[]{:S(2)}) copy-start(f32[128]{0:T(128)} %get-tuple-element.69) | copy-start | bytes 1540
  172.8 26.5 %copy-start.22 = (f32[128]{0:T(128)S(1)}, f32[128]{0:T(128)}, u32[]{:S(2)}) copy-start(f32[128]{0:T(128)} %get-tuple-element.70) | copy-start | bytes 1540
  172.8 26.5 %copy-start.23 = (f32[128]{0:T(128)S(1)}, f32[128]{0:T(128)}, u32[]{:S(2)}) copy-start(f32[128]{0:T(128)} %get-tuple-element.71) | copy-start | bytes 1540
  172.8 26.5 %copy-start.24 = (f32[128]{0:T(128)S(1)}, f32[128]{0:T(128)}, u32[]{:S(2)}) copy-start(f32[128]{0:T(128)} %get-tuple-element.72) | copy-start | bytes 1540
  172.8 26.5 %copy-start.25 = (f32[128]{0:T(128)S(1)}, f32[128]{0:T(128)}, u32[]{:S(2)}) copy-start(f32[128]{0:T(128)} %get-tuple-element.73) | copy-start | bytes 1540
  172.8 26.5 %copy-start.26 = (f32[128]{0:T(128)S(1)}, f32[128]{0:T(128)}, u32[]{:S(2)}) copy-start(f32[128]{0:T(128)} %get-tuple-element.74) | copy-start | bytes 1540
  172.8 26.5 %copy-start.27 = (f32[128]{0:T(128)S(1)}, f32[128]{0:T(128)}, u32[]{:S(2)}) copy-start(f32[128]{0:T(128)} %get-tuple-element.75) | copy-start | bytes 1540
  172.8 27.5 %all-to-all-start.3 = ((bf16[32,64,128]{2,1,0:T(8,128)(2,1)}), bf16[32,64,128]{2,1,0:T(8,128)(2,1)S(1)}, u32[]{:S(2)}, u32[]{:S(2)}) async-start(bf16[32,64,128]{2,1,0:T(8,128)(2,1)} %bitcast.22), calls=%async_computation.3 | async-start | bytes 1048576 | tf_op jit(solution)/shard_map/all_to_all | solution.py:449
  (2 other events, 9.6 us)
